TPU v7x, 128 devices: a whole 4x4x4 slice. The times are simulated.
128 devices in a mesh: sp: 32 (over z, y, core), tp: 4 (over x).
Axes of the slice: x: 4, y: 4, z: 4, core: 2. Of those that a mesh axis runs over, the one named last changes fastest.
Arguments:
- tokens: bfloat16 [4096, 6, 2048], P(('sp', 'tp')), may hold values from -6 to 6
- norm_gain: float32 [2048], replicated, may hold values from 0.1 to 1.9
- w_query: bfloat16 [3, 2048, 1024], P(None, 'sp', 'tp'), may hold values from -0.125 to 0.125
- w_key: bfloat16 [3, 2048, 1024], P(None, 'sp', 'tp'), may hold values from -0.125 to 0.125
- w_value: bfloat16 [3, 2048, 1024], P(None, 'sp', 'tp'), may hold values from -0.125 to 0.125
- w_out: bfloat16 [1024, 2048], P('tp', 'sp'), may hold values from -0.1875 to 0.1875
Outputs:
- mixed: bfloat16 [4096, 6, 2048], P(('sp', 'tp'))
- log_weight: float32 [4096, 6, 8], P('sp', None, 'tp')
All inputs are finite; a program needn't handle non-finite values.
Results may differ from a plain program's by a relative error of at most 0.015.
Values may be sent and summed in bfloat16 or wider, within the bound.
No kernel may reach another device: no remote copies, remote signals or barrier semaphores. Data moves between devices by JAX's collectives and lax.ppermute only.
A program may use at most 128 MiB of HBM per device.

v0:
```python
import math

import jax
import jax.numpy as jnp
from jax import lax
from jax.experimental import pallas as pl
from jax.experimental.pallas import tpu as pltpu
from jax.sharding import PartitionSpec as P


GROUPS = 3
ORDER = (2, 0, 1)
STEPS = 24
DILATIONS = (1, 4, 16)
HALOS = (32, 96, 384)
RING = 4
BATCHES = 3
PIECE = 32
SPAN = 256
HEAD_WIDTH = 128
COLS = 256
ROWS = 64
WIDTH = 2048
BLOCK = 128

epsilon = 1e-06


def chip(z, y, core):
    return (z % RING) * 8 + (y % RING) * 2 + core


def chips():
    return [(z, y, core) for z in range(RING) for y in range(RING) for core in range(2)]


def first_leg(shift):
    return [(chip(z, y, k), chip(z + shift * k, y + shift * (1 - k), k)) for z, y, k in chips()]


def second_leg(shift):
    return [(chip(z, y, k), chip(z + shift * (1 - k), y + shift * k, k)) for z, y, k in chips()]


SWAP = [(i, i ^ 1) for i in range(32)]


def swapped(a):
    return lax.ppermute(a, "sp", SWAP)


def turned(a, shift):
    return lax.ppermute(a, "tp", [(i, (i + shift) % RING) for i in range(RING)])


def from_behind(a, blocks):
    return lax.ppermute(a, "sp", [(i, i + 2 * blocks) for i in range(32 - 2 * blocks)])


def place_of(core, first, second):
    s = lax.axis_index("sp")
    z, y = s // 8, (s // 2) % RING
    up = jnp.where(core == 0, second, first)
    along = jnp.where(core == 0, first, second)
    return ((z + RING - up) % RING) * 8 + ((y + RING - along) % RING) * 2 + core


ANY = pl.BlockSpec(memory_space=pl.ANY)
VMEM = pl.BlockSpec(memory_space=pltpu.VMEM)
PARAMS = pltpu.CompilerParams(vmem_limit_bytes=56 * 1024 * 1024)


def bf(*dims):
    return jax.ShapeDtypeStruct(dims, jnp.bfloat16)


def prepare_body(tokens, gain, w_query, w_key, w_value, keep, send, pairs, queries):
    core = lax.axis_index("sp") % 2
    widened_gain = gain[...]
    for b in range(2 * BATCHES):
        v = tokens[b].astype(jnp.float32)
        v = v * lax.rsqrt(jnp.mean(v * v, axis=-1, keepdims=True) + epsilon)
        n = (v * widened_gain).astype(jnp.bfloat16)

        @pl.when(core == b // BATCHES)
        def _():
            keep[b % BATCHES] = n

        @pl.when(core != b // BATCHES)
        def _():
            send[b % BATCHES] = n

    for place, g in enumerate(ORDER):
        pairs[2 * place] = w_key[g]
        pairs[2 * place + 1] = w_value[g]
    queries[...] = w_query[...]


def prepare(tokens, gain, w_query, w_key, w_value):
    shape = bf(BATCHES, PIECE, WIDTH)
    return pl.pallas_call(
        prepare_body, out_shape=(shape, shape, bf(2 * GROUPS, ROWS, COLS), bf(GROUPS, ROWS, COLS)),
        in_specs=[VMEM] * 5, out_specs=(VMEM,) * 4, compiler_params=PARAMS, name="prepare",
    )(jnp.transpose(tokens, (1, 0, 2)), gain.reshape(1, WIDTH), w_query, w_key, w_value)


def fetch(pieces, lines, x_all, x_sems, wanted):
    s, t = lax.axis_index("sp"), lax.axis_index("tp")
    core = s % 2
    copies = []
    for n, piece in enumerate(pieces):
        whose = core if n < RING else 1 - core
        at = whose * (RING * PIECE) + ((t + RING - n % RING) % RING) * PIECE
        at = pl.multiple_of(at, PIECE)
        copies.append(pltpu.make_async_copy(piece, x_all.at[:, pl.ds(at, PIECE), :], x_sems.at[n]))
    for n, line in enumerate(lines):
        whose = core if n < RING else 1 - core
        for j in range(RING):
            at = pl.multiple_of(place_of(whose, j, n % RING) * ROWS, ROWS)
            for first, count, w_all, w_sems in wanted:
                copies.append(
                    pltpu.make_async_copy(
                        line.at[j, pl.ds(first, count)], w_all.at[:, pl.ds(at, ROWS), :], w_sems.at[n * RING + j]
                    )
                )
    for c in copies:
        c.start()
    for c in copies:
        c.wait()


def wide_pair_body(*refs):
    pieces, lines = refs[:8], refs[8:16]
    wide, wide_tail, x_all, w_all, x_sems, w_sems = refs[16:]
    fetch(pieces, lines, x_all, x_sems, ((0, 2, w_all, w_sems),))
    for role in range(2):
        for b in range(BATCHES):
            y = jnp.dot(x_all[b], w_all[role], preferred_element_type=jnp.float32).astype(jnp.bfloat16)
            wide[role, b] = y
            wide_tail[role, b] = y[SPAN // 2 :]


def project_wide(pieces, lines):
    return pl.pallas_call(
        wide_pair_body,
        out_shape=(bf(2, BATCHES, SPAN, COLS), bf(2, BATCHES, SPAN // 2, COLS)),
        in_specs=[ANY] * 16, out_specs=(VMEM,) * 2,
        scratch_shapes=[
            pltpu.VMEM((BATCHES, SPAN, WIDTH), jnp.bfloat16), pltpu.VMEM((2, WIDTH, COLS), jnp.bfloat16),
            pltpu.SemaphoreType.DMA((8,)), pltpu.SemaphoreType.DMA((32,)),
        ],
        compiler_params=PARAMS, name="project_wide",
    )(*pieces, *lines)


def near_pair_body(*refs):
    pieces, lines = refs[:8], refs[8:16]
    near, near_tail, x_all, w_all, x_sems, w_sems = refs[16:]
    fetch(pieces, lines, x_all, x_sems, ((2, 4, w_all, w_sems),))
    for g in range(2):
        for role in range(2):
            for b in range(BATCHES):
                y = jnp.dot(x_all[b], w_all[2 * g + role], preferred_element_type=jnp.float32).astype(jnp.bfloat16)
                near[g, role, b] = y
                if g == 0:
                    near_tail[role, b, : HALOS[0]] = y[SPAN - HALOS[0] :]
                else:
                    near_tail[role, b, HALOS[0] :] = y[SPAN - HALOS[1] :]


def project_near(pieces, lines):
    return pl.pallas_call(
        near_pair_body,
        out_shape=(bf(2, 2, BATCHES, SPAN, COLS), bf(2, BATCHES, HALOS[0] + HALOS[1], COLS)),
        in_specs=[ANY] * 16, out_specs=(VMEM,) * 2,
        scratch_shapes=[
            pltpu.VMEM((BATCHES, SPAN, WIDTH), jnp.bfloat16), pltpu.VMEM((4, WIDTH, COLS), jnp.bfloat16),
            pltpu.SemaphoreType.DMA((8,)), pltpu.SemaphoreType.DMA((32,)),
        ],
        compiler_params=PARAMS, name="project_near",
    )(*pieces, *lines)


def query_body(*refs):
    pieces, lines = refs[:8], refs[8:16]
    out, laid, x_all, w_all, x_sems, w_sems, o_sems = refs[16:]
    fetch(pieces, lines, x_all, x_sems, ((0, GROUPS, w_all, w_sems), (GROUPS, RING, laid, o_sems)))
    for g in range(GROUPS):
        for b in range(BATCHES):
            y = jnp.dot(x_all[b], w_all[g], preferred_element_type=jnp.float32)
            out[g, b] = y.astype(jnp.bfloat16)


def project_queries(pieces, lines):
    return pl.pallas_call(
        query_body,
        out_shape=(bf(GROUPS, BATCHES, SPAN, COLS), bf(RING, WIDTH, COLS)),
        in_specs=[ANY] * 16, out_specs=(VMEM,) * 2,
        scratch_shapes=[
            pltpu.VMEM((BATCHES, SPAN, WIDTH), jnp.bfloat16), pltpu.VMEM((GROUPS, WIDTH, COLS), jnp.bfloat16),
            pltpu.SemaphoreType.DMA((8,)), pltpu.SemaphoreType.DMA((32,)), pltpu.SemaphoreType.DMA((32,)),
        ],
        compiler_params=PARAMS, name="project_queries",
    )(*pieces, *lines)


def bias_of(group, block):
    halo, dilation = HALOS[group], DILATIONS[group]
    dims = (BLOCK, BLOCK + halo)
    q = lax.broadcasted_iota(jnp.int32, dims, 0)
    k = lax.broadcasted_iota(jnp.int32, dims, 1)
    lag = q + halo - k
    start = (lax.axis_index("sp") // 2) * SPAN + block * BLOCK - halo
    seen = (lag >= 0) & (lag <= STEPS * dilation) & ((lag & (dilation - 1)) == 0) & (k + start >= 0)
    return jnp.where(seen, 0.0, -1e30).astype(jnp.float32)


def attend(q, k, v, bias):
    s = lax.dot_general(q, k, (((1,), (1,)), ((), ())), preferred_element_type=jnp.float32)
    s = s * (1.0 / math.sqrt(HEAD_WIDTH)) + bias
    peak = jnp.max(s, axis=-1, keepdims=True)
    lifted = jnp.exp(s - peak)
    total = jnp.sum(lifted, axis=-1, keepdims=True)
    o = jnp.dot(lifted.astype(jnp.bfloat16), v, preferred_element_type=jnp.float32)
    return o / total, peak + jnp.log(total)


def joined(o1, l1, o2, l2):
    top = jnp.maximum(l1, l2)
    a, c = jnp.exp(l1 - top), jnp.exp(l2 - top)
    total = a + c
    return (a * o1 + c * o2) / total, top + jnp.log(total)


def near_body(q, near, tail, out, logs, k0, k1, sems):
    copies = [
        pltpu.make_async_copy(tail.at[:, :, pl.ds(0, HALOS[0])], k0.at[:, :, pl.ds(0, HALOS[0])], sems.at[0]),
        pltpu.make_async_copy(tail.at[:, :, pl.ds(HALOS[0], HALOS[1])], k1.at[:, :, pl.ds(0, HALOS[1])], sems.at[1]),
        pltpu.make_async_copy(near.at[0], k0.at[:, :, pl.ds(HALOS[0], SPAN)], sems.at[2]),
        pltpu.make_async_copy(near.at[1], k1.at[:, :, pl.ds(HALOS[1], SPAN)], sems.at[3]),
    ]
    for c in copies:
        c.start()
    for c in copies:
        c.wait()
    for i in range(SPAN // BLOCK):
        rows = slice(i * BLOCK, (i + 1) * BLOCK)
        biases = [bias_of(g, i) for g in range(2)]
        for b in range(BATCHES):
            for h in range(COLS // HEAD_WIDTH):
                cols = slice(h * HEAD_WIDTH, (h + 1) * HEAD_WIDTH)
                parts = []
                for g, held in enumerate((k0, k1)):
                    keys = slice(i * BLOCK, (i + 1) * BLOCK + HALOS[g])
                    parts.append(attend(q[g, b, rows, cols], held[0, b, keys, cols], held[1, b, keys, cols], biases[g]))
                o, l = joined(*parts[0], *parts[1])
                out[b, rows, cols] = o
                logs[b, rows, cols] = jnp.broadcast_to(l, (BLOCK, HEAD_WIDTH))


def attend_near(q, near, tail):
    shape = jax.ShapeDtypeStruct((BATCHES, SPAN, COLS), jnp.float32)
    return pl.pallas_call(
        near_body, out_shape=(shape, shape), in_specs=[VMEM, ANY, ANY], out_specs=(VMEM, VMEM),
        scratch_shapes=[
            pltpu.VMEM((2, BATCHES, HALOS[0] + SPAN, COLS), jnp.bfloat16),
            pltpu.VMEM((2, BATCHES, HALOS[1] + SPAN, COLS), jnp.bfloat16),
            pltpu.SemaphoreType.DMA((4,)),
        ],
        compiler_params=PARAMS, name="attend_near",
    )(q, near, tail)


def wide_body(q, wide, back, tail, other, logs, c0, c1, c2, c3, kept, sent, held, mixed, sems):
    copies = [
        pltpu.make_async_copy(tail, held.at[:, :, pl.ds(0, SPAN // 2)], sems.at[0]),
        pltpu.make_async_copy(back, held.at[:, :, pl.ds(SPAN // 2, SPAN)], sems.at[1]),
        pltpu.make_async_copy(wide, held.at[:, :, pl.ds(HALOS[2], SPAN)], sems.at[2]),
    ]
    for c in copies:
        c.start()
    for c in copies:
        c.wait()
    core, t = lax.axis_index("sp") % 2, lax.axis_index("tp")
    for i in range(SPAN // BLOCK):
        rows = slice(i * BLOCK, (i + 1) * BLOCK)
        bias = bias_of(2, i)
        for b in range(BATCHES):
            for h in range(COLS // HEAD_WIDTH):
                cols = slice(h * HEAD_WIDTH, (h + 1) * HEAD_WIDTH)
                keys = slice(i * BLOCK, (i + 1) * BLOCK + HALOS[2])
                o, l = attend(q[2, b, rows, cols], held[0, b, keys, cols], held[1, b, keys, cols], bias)
                o, l = joined(other[b, rows, cols], logs[b, rows, cols], o, l)
                mixed[b, rows, cols] = o.astype(jnp.bfloat16)
                line = jnp.transpose(l)[0:1]

                @pl.when(core == i)
                def _():
                    kept[b * 2 + h : b * 2 + h + 1, :] = line

                @pl.when(core != i)
                def _():
                    sent[b * 2 + h : b * 2 + h + 1, :] = line

    for d, out in enumerate((c0, c1, c2, c3)):
        for far in range(2):
            whose = core if far == 0 else 1 - core
            at = pl.multiple_of(whose * (RING * PIECE) + ((t + d) % RING) * PIECE, PIECE)
            out[far] = mixed[:, pl.ds(at, PIECE), :]


def attend_wide(q, wide, back, tail, other, logs):
    piece = jax.ShapeDtypeStruct((2, BATCHES, PIECE, COLS), jnp.bfloat16)
    line = jax.ShapeDtypeStruct((2 * BATCHES, BLOCK), jnp.float32)
    return pl.pallas_call(
        wide_body, out_shape=(piece,) * 4 + (line,) * 2, in_specs=[VMEM, ANY, ANY, ANY, VMEM, VMEM],
        out_specs=(VMEM,) * 6,
        scratch_shapes=[
            pltpu.VMEM((2, BATCHES, HALOS[2] + SPAN, COLS), jnp.bfloat16),
            pltpu.VMEM((BATCHES, SPAN, COLS), jnp.bfloat16),
            pltpu.SemaphoreType.DMA((3,)),
        ],
        compiler_params=PARAMS, name="attend_wide",
    )(q, wide, back, tail, other, logs)


def final_body(r0, r1, r2, r3, s0, s1, s2, s3, w, out, held):
    core = lax.axis_index("sp") % 2
    for d, (r, s) in enumerate(((r0, s0), (r1, s1), (r2, s2), (r3, s3))):
        held[d, core] = r[0].reshape(BATCHES * PIECE, COLS)
        held[d, 1 - core] = s[...].reshape(BATCHES * PIECE, COLS)
    for n in range(4):
        cols = slice(n * 512, (n + 1) * 512)
        acc = None
        for d in range(RING):
            a = held[d].reshape(2 * BATCHES * PIECE, COLS)
            y = lax.dot_general(a, w[d, cols], (((1,), (1,)), ((), ())), preferred_element_type=jnp.float32)
            acc = y if acc is None else acc + y
        acc = acc.astype(jnp.bfloat16)
        for b in range(2 * BATCHES):
            out[b, :, cols] = acc[b * PIECE : (b + 1) * PIECE]


def finish(received, crossed, w):
    mixed = pl.pallas_call(
        final_body, out_shape=bf(2 * BATCHES, PIECE, WIDTH),
        in_specs=[VMEM] * 9, out_specs=VMEM,
        scratch_shapes=[pltpu.VMEM((RING, 2, BATCHES * PIECE, COLS), jnp.bfloat16)],
        compiler_params=PARAMS, name="finish",
    )(*received, *crossed, w)
    return jnp.transpose(mixed, (1, 0, 2))


def ring_of(a):
    came = {d: turned(a, d) for d in (1, 3, 2)}
    return [a, came[1], came[2], came[3]]


def spread(own):
    near = {d: lax.ppermute(own, "sp", first_leg(d)) for d in (1, 3, 2)}
    line = jnp.stack((own, near[1], near[2], near[3]))
    far = {d: lax.ppermute(line, "sp", second_leg(d)) for d in (1, 3, 2)}
    lines = [line, far[1], far[2], far[3]]
    return lines + [swapped(a) for a in lines]


def layer(tokens, norm_gain, w_query, w_key, w_value, w_out):
    core = lax.axis_index("sp") % 2
    keep, send, pair_own, query_own = prepare(tokens, norm_gain, w_query, w_key, w_value)
    crossing = swapped(send)
    pieces = ring_of(keep) + ring_of(crossing)
    pair_lines = spread(pair_own)
    outs = ring_of(jnp.transpose(w_out))
    rest = spread(jnp.concatenate((query_own, jnp.stack(outs)), 0))

    wide, wide_tail = project_wide(pieces, pair_lines)
    back = from_behind(wide, 1)
    wide_tail = from_behind(wide_tail, 2)
    near, near_tail = project_near(pieces, pair_lines)
    near_tail = from_behind(near_tail, 1)
    queries, laid = project_queries(pieces, rest)
    other, logs = attend_near(queries, near, near_tail)
    *combined, kept, sent = attend_wide(queries, wide, back, wide_tail, other, logs)

    received = [combined[0]] + [turned(combined[d], d) for d in (1, 2, 3)]
    crossed = [swapped(a[1]) for a in received]
    mixed = finish(received, crossed, laid)

    came = swapped(sent)
    low = jnp.where(core == 0, kept, came)
    high = jnp.where(core == 0, came, kept)
    log_weight = jnp.concatenate((low, high), 0).reshape(2 * BATCHES, 2, BLOCK)
    return (mixed, jnp.transpose(log_weight, (2, 0, 1)))


def solution(mesh):
    in_specs = (
        P(("sp", "tp"), None, None),
        P(),
        P(None, "sp", "tp"),
        P(None, "sp", "tp"),
        P(None, "sp", "tp"),
        P("tp", "sp"),
    )
    out_specs = (P(("sp", "tp"), None, None), P("sp", None, "tp"))
    return jax.shard_map(layer, mesh=mesh, in_specs=in_specs, out_specs=out_specs, check_vma=False)
```

profile of v0, /device:TPU:97, one launch (start us, length us, event | category | flops | bytes accessed | tf_op | source)
XLA Modules:
  0.0 175.0 jit_solution(12535637903015410096)
XLA Ops:
  1.9 2.5 %collective-permute-start.8 = (bf16[64,256]{1,0:T(8,128)(2,1)}, bf16[64,256]{1,0:T(8,128)(2,1)S(1)}, u32[]{:S(2)}, u32[]{:S(2)}) collective-permute-start(bf16[64,256]{1,0:T(8,128)(2,1)} %bitcast.41), channel_id=1, source_target_pairs={{0,2},{1,3},{2,0},{3,1},{4,6},{5,7},{6,4},{7,5},{8,10},{9,11},{10,... | collective-permute-start | bytes 98312 | tf_op jit(solution)/shard_map/ppermute | solution.py:53
  5.5 3.0 %prepare.1 = (bf16[3,32,2048]{2,1,0:T(8,128)(2,1)}, bf16[3,32,2048]{2,1,0:T(8,128)(2,1)}, bf16[6,64,256]{2,1,0:T(8,128)(2,1)}, bf16[3,64,256]{2,1,0:T(8,128)(2,1)}) custom-call(bf16[6,32,2048]{2,1,0:T(8,128)(2,1)} %bitcast.30, f32[1,2048]{1,0:T(1,128)} %bitcast.43, bf16[3,64,256]{2,1,0:T(8,128)(2,1)} %w_query.1, bf16[3,64,256]{2,1,0:T(8,128)(2,1)} %w_key.1, ...), custom_call_target="tpu_custom_call" | custom-call | tf_op jit(solution)/shard_map/prepare/pallas_call | solution.py:101
  10.4 3.7 %collective-permute-start.21 = (bf16[6,64,256]{2,1,0:T(8,128)(2,1)}, bf16[6,64,256]{2,1,0:T(8,128)(2,1)S(1)}, u32[]{:S(2)}, u32[]{:S(2)}) collective-permute-start(bf16[6,64,256]{2,1,0:T(8,128)(2,1)} %get-tuple-element.24), channel_id=1, source_target_pairs={{0,16},{4,68},{8,24},{12,76},{16,0},{20,84},{24,8},{28,92},{32,48}... | collective-permute-start | bytes 589832 | tf_op jit(solution)/shard_map/ppermute | solution.py:360
  14.2 2.7 %collective-permute-start.3 = (bf16[3,32,2048]{2,1,0:T(8,128)(2,1)}, bf16[3,32,2048]{2,1,0:T(8,128)(2,1)S(1)}, u32[]{:S(2)}, u32[]{:S(2)}) collective-permute-start(bf16[3,32,2048]{2,1,0:T(8,128)(2,1)} %get-tuple-element.21), channel_id=1, source_target_pairs={{0,4},{4,0},{8,12},{12,8},{16,20},{20,16},{24,28},{28,24},{32,36},... | collective-permute-start | bytes 1179656 | tf_op jit(solution)/shard_map/ppermute | solution.py:49
  17.2 2.5 %collective-permute-done.21 = bf16[6,64,256]{2,1,0:T(8,128)(2,1)S(1)} collective-permute-done((bf16[6,64,256]{2,1,0:T(8,128)(2,1)}, bf16[6,64,256]{2,1,0:T(8,128)(2,1)S(1)}, u32[]{:S(2)}, u32[]{:S(2)}) %collective-permute-start.21) | collective-permute-done | bytes 196640 | tf_op jit(solution)/shard_map/ppermute | solution.py:360
  22.0 1.3 collective-permute-done.11
  24.7 1.3 collective-permute-done.10
  26.0 2.1 %collective-permute-start.5 = (bf16[3,32,2048]{2,1,0:T(8,128)(2,1)S(1)}, bf16[3,32,2048]{2,1,0:T(8,128)(2,1)S(1)}, u32[]{:S(2)}, u32[]{:S(2)}) collective-permute-start(bf16[3,32,2048]{2,1,0:T(8,128)(2,1)S(1)} %collective-permute-done.3.refs_4_), channel_id=1, source_target_pairs={{0,2},{1,3},{2,0},{3,1},{4,6},{5,7},{6,4},{7,5},{8,10},{9,11},{10,... | collective-permute-start | bytes 1179656 | tf_op jit(solution)/shard_map/ppermute | solution.py:53
  31.3 4.4 %collective-permute-done.1.refs_2_ = bf16[3,32,2048]{2,1,0:T(8,128)(2,1)S(1)} collective-permute-done((bf16[3,32,2048]{2,1,0:T(8,128)(2,1)}, bf16[3,32,2048]{2,1,0:T(8,128)(2,1)S(1)}, u32[]{:S(2)}, u32[]{:S(2)}) %collective-permute-start.1) | collective-permute-done | bytes 393248 | tf_op jit(solution)/shard_map/ppermute | solution.py:53
  35.6 6.8 %collective-permute-start.24 = (bf16[4,6,64,256]{3,2,1,0:T(8,128)(2,1)S(1)}, bf16[4,6,64,256]{3,2,1,0:T(8,128)(2,1)S(1)}, u32[]{:S(2)}, u32[]{:S(2)}) collective-permute-start(bf16[4,6,64,256]{3,2,1,0:T(8,128)(2,1)S(1)} %pad_maximum_fusion.1.refs_8_), channel_id=1, source_target_pairs={{0,64},{4,20},{8,72},{12,28},{16,80},{20,4},{24,88},{28,12},{32,96... | collective-permute-start | bytes 2359304 | tf_op jit(solution)/shard_map/ppermute | solution.py:362
  42.5 3.5 %collective-permute-start.6 = (bf16[3,32,2048]{2,1,0:T(8,128)(2,1)S(1)}, bf16[3,32,2048]{2,1,0:T(8,128)(2,1)S(1)}, u32[]{:S(2)}, u32[]{:S(2)}) collective-permute-start(bf16[3,32,2048]{2,1,0:T(8,128)(2,1)S(1)} %collective-permute-done.3.refs_4_), channel_id=1, source_target_pairs={{0,3},{1,0},{2,1},{3,2},{4,7},{5,4},{6,5},{7,6},{8,11},{9,8},{10,9... | collective-permute-start | bytes 1179656 | tf_op jit(solution)/shard_map/ppermute | solution.py:53
  46.9 2.1 %collective-permute-start.25 = (bf16[4,6,64,256]{3,2,1,0:T(8,128)(2,1)S(1)}, bf16[4,6,64,256]{3,2,1,0:T(8,128)(2,1)S(1)}, u32[]{:S(2)}, u32[]{:S(2)}) collective-permute-start(bf16[4,6,64,256]{3,2,1,0:T(8,128)(2,1)S(1)} %pad_maximum_fusion.1.refs_8_), channel_id=1, source_target_pairs={{0,96},{4,28},{8,104},{12,4},{16,112},{20,12},{24,120},{28,20},{32... | collective-permute-start | bytes 2359304 | tf_op jit(solution)/shard_map/ppermute | solution.py:362
  49.0 3.6 %collective-permute-done.5.refs_6_ = bf16[3,32,2048]{2,1,0:T(8,128)(2,1)S(1)} collective-permute-done((bf16[3,32,2048]{2,1,0:T(8,128)(2,1)S(1)}, bf16[3,32,2048]{2,1,0:T(8,128)(2,1)S(1)}, u32[]{:S(2)}, u32[]{:S(2)}) %collective-permute-start.5) | collective-permute-done | bytes 393248 | tf_op jit(solution)/shard_map/ppermute | solution.py:53
  52.5 5.5 %collective-permute-start.26 = (bf16[4,6,64,256]{3,2,1,0:T(8,128)(2,1)S(1)}, bf16[4,6,64,256]{3,2,1,0:T(8,128)(2,1)S(1)}, u32[]{:S(2)}, u32[]{:S(2)}) collective-permute-start(bf16[4,6,64,256]{3,2,1,0:T(8,128)(2,1)S(1)} %pad_maximum_fusion.1.refs_8_), channel_id=1, source_target_pairs={{0,4},{4,0},{8,12},{12,8},{16,20},{20,16},{24,28},{28,24},{32,36},... | collective-permute-start | bytes 2359304 | tf_op jit(solution)/shard_map/ppermute | solution.py:49
  58.2 1.4 collective-permute-start.13
  59.5 2.6 %collective-permute-start.14 = (bf16[4,7,64,256]{3,2,1,0:T(8,128)(2,1)S(1)}, bf16[4,7,64,256]{3,2,1,0:T(8,128)(2,1)}, u32[]{:S(2)}, u32[]{:S(2)}) collective-permute-start(bf16[4,7,64,256]{3,2,1,0:T(8,128)(2,1)S(1)} %pad_maximum_fusion.refs_8_), channel_id=1, source_target_pairs={{0,64},{4,20},{8,72},{12,28},{16,80},{20,4},{24,88},{28,12},{32,96... | collective-permute-start | bytes 2752520 | tf_op jit(solution)/shard_map/ppermute | solution.py:362
  63.2 17.7 %collective-permute-start.27 = (bf16[4,6,64,256]{3,2,1,0:T(8,128)(2,1)S(1)}, bf16[4,6,64,256]{3,2,1,0:T(8,128)(2,1)S(1)}, u32[]{:S(2)}, u32[]{:S(2)}) collective-permute-start(bf16[4,6,64,256]{3,2,1,0:T(8,128)(2,1)S(1)} %collective-permute-done.23.refs_9_), channel_id=1, source_target_pairs={{0,4},{4,0},{8,12},{12,8},{16,20},{20,16},{24,28},{28,24},{32,36},... | collective-permute-start | bytes 2359304 | tf_op jit(solution)/shard_map/ppermute | solution.py:49
  81.5 1.4 collective-permute-done.14.refs_10_
  82.9 8.0 %collective-permute-start.17 = (bf16[4,7,64,256]{3,2,1,0:T(8,128)(2,1)}, bf16[4,7,64,256]{3,2,1,0:T(8,128)(2,1)}, u32[]{:S(2)}, u32[]{:S(2)}) collective-permute-start(bf16[4,7,64,256]{3,2,1,0:T(8,128)(2,1)} %collective-permute-done.13.refs_9_), channel_id=1, source_target_pairs={{0,4},{4,0},{8,12},{12,8},{16,20},{20,16},{24,28},{28,24},{32,36},... | collective-permute-start | bytes 2752520 | tf_op jit(solution)/shard_map/ppermute | solution.py:49
  92.8 5.9 %project_wide.1 = (bf16[2,3,256,256]{3,2,1,0:T(8,128)(2,1)}, bf16[2,3,128,256]{3,2,1,0:T(8,128)(2,1)}) custom-call(bf16[3,32,2048]{2,1,0:T(8,128)(2,1)} %get-tuple-element.20.refs_0_, bf16[3,32,2048]{2,1,0:T(8,128)(2,1)} %copy-done.3, bf16[3,32,2048]{2,1,0:T(8,128)(2,1)} %copy-done.4, bf16[3,32,2048]{2,1,0:T(8,128)(2,1)} %copy-done.5, ...), custom_call_target="tpu_custom_call" | custom-call | tf_op jit(solution)/shard_map/project_wide/pallas_call | solution.py:144
  98.7 3.3 %collective-permute-start.30 = (bf16[2,3,256,256]{3,2,1,0:T(8,128)(2,1)}, bf16[2,3,256,256]{3,2,1,0:T(8,128)(2,1)S(1)}, u32[]{:S(2)}, u32[]{:S(2)}) collective-permute-start(bf16[2,3,256,256]{3,2,1,0:T(8,128)(2,1)} %get-tuple-element.25.wide), channel_id=1, source_target_pairs={{0,8},{4,12},{8,16},{12,20},{16,24},{20,28},{24,32},{28,36},{32,40... | collective-permute-start | bytes 2359304 | tf_op jit(solution)/shard_map/ppermute | solution.py:57
  102.0 8.4 %project_near.1 = (bf16[2,2,3,256,256]{4,3,2,1,0:T(8,128)(2,1)}, bf16[2,3,128,256]{3,2,1,0:T(8,128)(2,1)}) custom-call(bf16[3,32,2048]{2,1,0:T(8,128)(2,1)} %get-tuple-element.20.refs_0_, bf16[3,32,2048]{2,1,0:T(8,128)(2,1)} %copy-done.3, bf16[3,32,2048]{2,1,0:T(8,128)(2,1)} %copy-done.4, bf16[3,32,2048]{2,1,0:T(8,128)(2,1)} %copy-done.5, ...), custom_call_target="tpu_custom_call" | custom-call | tf_op jit(solution)/shard_map/project_near/pallas_call | solution.py:172
  110.5 3.2 %collective-permute-start.32 = (bf16[2,3,128,256]{3,2,1,0:T(8,128)(2,1)}, bf16[2,3,128,256]{3,2,1,0:T(8,128)(2,1)S(1)}, u32[]{:S(2)}, u32[]{:S(2)}) collective-permute-start(bf16[2,3,128,256]{3,2,1,0:T(8,128)(2,1)} %get-tuple-element.28), channel_id=1, source_target_pairs={{0,8},{4,12},{8,16},{12,20},{16,24},{20,28},{24,32},{28,36},{32,40... | collective-permute-start | bytes 1179656 | tf_op jit(solution)/shard_map/ppermute | solution.py:57
  113.7 3.2 %collective-permute-start.31 = (bf16[2,3,128,256]{3,2,1,0:T(8,128)(2,1)S(1)}, bf16[2,3,128,256]{3,2,1,0:T(8,128)(2,1)S(1)}, u32[]{:S(2)}, u32[]{:S(2)}) collective-permute-start(bf16[2,3,128,256]{3,2,1,0:T(8,128)(2,1)S(1)} %copy-done.25), channel_id=1, source_target_pairs={{0,16},{4,20},{8,24},{12,28},{16,32},{20,36},{24,40},{28,44},{32,4... | collective-permute-start | bytes 1179656 | tf_op jit(solution)/shard_map/ppermute | solution.py:57
  117.0 8.5 %project_queries.1 = (bf16[3,3,256,256]{3,2,1,0:T(8,128)(2,1)}, bf16[4,2048,256]{2,1,0:T(8,128)(2,1)}) custom-call(bf16[3,32,2048]{2,1,0:T(8,128)(2,1)} %get-tuple-element.20.refs_0_, bf16[3,32,2048]{2,1,0:T(8,128)(2,1)} %copy-done.3, bf16[3,32,2048]{2,1,0:T(8,128)(2,1)} %copy-done.4, bf16[3,32,2048]{2,1,0:T(8,128)(2,1)} %copy-done.5, ...), custom_call_target="tpu_custom_call" | custom-call | tf_op jit(solution)/shard_map/project_queries/pallas_call | solution.py:195
  125.5 13.5 %collective-permute-done.32.tail = bf16[2,3,128,256]{3,2,1,0:T(8,128)(2,1)S(1)} collective-permute-done((bf16[2,3,128,256]{3,2,1,0:T(8,128)(2,1)}, bf16[2,3,128,256]{3,2,1,0:T(8,128)(2,1)S(1)}, u32[]{:S(2)}, u32[]{:S(2)}) %collective-permute-start.32) | collective-permute-done | bytes 393248 | tf_op jit(solution)/shard_map/ppermute | solution.py:57
  139.7 8.7 %attend_near.1 = (f32[3,256,256]{2,1,0:T(8,128)}, f32[3,256,256]{2,1,0:T(8,128)}) custom-call(bf16[3,3,256,256]{3,2,1,0:T(8,128)(2,1)} %get-tuple-element.23.q, bf16[2,2,3,256,256]{4,3,2,1,0:T(8,128)(2,1)} %get-tuple-element.27.near, bf16[2,3,128,256]{3,2,1,0:T(8,128)(2,1)} %copy-done.17), custom_call_target="tpu_custom_call" | custom-call | tf_op jit(solution)/shard_map/attend_near/pallas_call | solution.py:263
  149.5 9.7 %attend_wide.1 = (bf16[2,3,32,256]{3,2,1,0:T(8,128)(2,1)}, bf16[2,3,32,256]{3,2,1,0:T(8,128)(2,1)}, bf16[2,3,32,256]{3,2,1,0:T(8,128)(2,1)}, bf16[2,3,32,256]{3,...) custom-call(bf16[3,3,256,256]{3,2,1,0:T(8,128)(2,1)} %get-tuple-element.23.q, ...), custom_call_target="tpu_custom_call" | custom-call | tf_op jit(solution)/shard_map/attend_wide/pallas_call | solution.py:315
  159.7 2.2 %collective-permute-start.35 = (bf16[2,3,32,256]{3,2,1,0:T(8,128)(2,1)}, bf16[2,3,32,256]{3,2,1,0:T(8,128)(2,1)S(1)}, u32[]{:S(2)}, u32[]{:S(2)}) collective-permute-start(bf16[2,3,32,256]{3,2,1,0:T(8,128)(2,1)} %get-tuple-element.34), channel_id=1, source_target_pairs={{0,3},{1,0},{2,1},{3,2},{4,7},{5,4},{6,5},{7,6},{8,11},{9,8},{10,9... | collective-permute-start | bytes 294920 | tf_op jit(solution)/shard_map/ppermute | solution.py:53
  161.9 1.4 collective-permute-start.40
  165.0 2.0 %collective-permute-done.33.r1 = bf16[2,3,32,256]{3,2,1,0:T(8,128)(2,1)S(1)} collective-permute-done((bf16[2,3,32,256]{3,2,1,0:T(8,128)(2,1)}, bf16[2,3,32,256]{3,2,1,0:T(8,128)(2,1)S(1)}, u32[]{:S(2)}, u32[]{:S(2)}) %collective-permute-start.33) | collective-permute-done | bytes 98336 | tf_op jit(solution)/shard_map/ppermute | solution.py:53
  170.2 4.9 %finish.1 = bf16[6,32,2048]{2,1,0:T(8,128)(2,1)} custom-call(bf16[2,3,32,256]{3,2,1,0:T(8,128)(2,1)} %get-tuple-element.31.r0, bf16[2,3,32,256]{3,2,1,0:T(8,128)(2,1)} %copy-done.18, bf16[2,3,32,256]{3,2,1,0:T(8,128)(2,1)} %copy-done.19, bf16[2,3,32,256]{3,2,1,0:T(8,128)(2,1)} %copy-done.20, bf16[3,32,256]{2,1,0:T(8,128)(2,1)} %copy-done.21, ...), custom_call_target="tpu_custom_call" | custom-call | tf_op jit(solution)/shard_map/finish/pallas_call | solution.py:345
  (123 shorter events, 22.9 us)
Async XLA Ops:
  0.6 9.7 %collective-permute-start.7 = (bf16[64,256]{1,0:T(8,128)(2,1)}, bf16[64,256]{1,0:T(8,128)(2,1)S(1)}, u32[]{:S(2)}, u32[]{:S(2)}) collective-permute-start(bf16[64,256]{1,0:T(8,128)(2,1)} %bitcast.40), channel_id=1, source_target_pairs={{0,1},{1,2},{2,3},{3,0},{4,5},{5,6},{6,7},{7,4},{8,9},{9,10},{10,1... | collective-permute-start | bytes 98312 | tf_op jit(solution)/shard_map/ppermute | solution.py:53
  1.9 8.4 %collective-permute-start.8 = (bf16[64,256]{1,0:T(8,128)(2,1)}, bf16[64,256]{1,0:T(8,128)(2,1)S(1)}, u32[]{:S(2)}, u32[]{:S(2)}) collective-permute-start(bf16[64,256]{1,0:T(8,128)(2,1)} %bitcast.41), channel_id=1, source_target_pairs={{0,2},{1,3},{2,0},{3,1},{4,6},{5,7},{6,4},{7,5},{8,10},{9,11},{10,... | collective-permute-start | bytes 98312 | tf_op jit(solution)/shard_map/ppermute | solution.py:53
  8.5 8.4 %collective-permute-start.22 = (bf16[6,64,256]{2,1,0:T(8,128)(2,1)}, bf16[6,64,256]{2,1,0:T(8,128)(2,1)S(1)}, u32[]{:S(2)}, u32[]{:S(2)}) collective-permute-start(bf16[6,64,256]{2,1,0:T(8,128)(2,1)} %get-tuple-element.24), channel_id=1, source_target_pairs={{0,24},{4,100},{8,0},{12,108},{16,8},{20,116},{24,16},{28,124},{32... | collective-permute-start | bytes 589832 | tf_op jit(solution)/shard_map/ppermute | solution.py:360
  10.4 10.5 %collective-permute-start.12 = (bf16[7,64,256]{2,1,0:T(8,128)(2,1)S(1)}, bf16[7,64,256]{2,1,0:T(8,128)(2,1)S(1)}, u32[]{:S(2)}, u32[]{:S(2)}) collective-permute-start(bf16[7,64,256]{2,1,0:T(8,128)(2,1)S(1)} %bitcast_dynamic-update-slice_fusion.1), channel_id=1, source_target_pairs={{0,24},{4,100},{8,0},{12,108},{16,8},{20,116},{24,16},{28,124},{32... | collective-permute-start | bytes 688136 | tf_op jit(solution)/shard_map/ppermute | solution.py:360
  10.4 9.2 %collective-permute-start.21 = (bf16[6,64,256]{2,1,0:T(8,128)(2,1)}, bf16[6,64,256]{2,1,0:T(8,128)(2,1)S(1)}, u32[]{:S(2)}, u32[]{:S(2)}) collective-permute-start(bf16[6,64,256]{2,1,0:T(8,128)(2,1)} %get-tuple-element.24), channel_id=1, source_target_pairs={{0,16},{4,68},{8,24},{12,76},{16,0},{20,84},{24,8},{28,92},{32,48}... | collective-permute-start | bytes 589832 | tf_op jit(solution)/shard_map/ppermute | solution.py:360
  14.2 10.3 %collective-permute-start.3 = (bf16[3,32,2048]{2,1,0:T(8,128)(2,1)}, bf16[3,32,2048]{2,1,0:T(8,128)(2,1)S(1)}, u32[]{:S(2)}, u32[]{:S(2)}) collective-permute-start(bf16[3,32,2048]{2,1,0:T(8,128)(2,1)} %get-tuple-element.21), channel_id=1, source_target_pairs={{0,4},{4,0},{8,12},{12,8},{16,20},{20,16},{24,28},{28,24},{32,36},... | collective-permute-start | bytes 1179656 | tf_op jit(solution)/shard_map/ppermute | solution.py:49
  19.7 10.4 %collective-permute-start = (bf16[3,32,2048]{2,1,0:T(8,128)(2,1)}, bf16[3,32,2048]{2,1,0:T(8,128)(2,1)S(1)}, u32[]{:S(2)}, u32[]{:S(2)}) collective-permute-start(bf16[3,32,2048]{2,1,0:T(8,128)(2,1)} %get-tuple-element.20.refs_0_), channel_id=1, source_target_pairs={{0,1},{1,2},{2,3},{3,0},{4,5},{5,6},{6,7},{7,4},{8,9},{9,10},{10,1... | collective-permute-start | bytes 1179656 | tf_op jit(solution)/shard_map/ppermute | solution.py:53
  20.0 15.7 %collective-permute-start.1 = (bf16[3,32,2048]{2,1,0:T(8,128)(2,1)}, bf16[3,32,2048]{2,1,0:T(8,128)(2,1)S(1)}, u32[]{:S(2)}, u32[]{:S(2)}) collective-permute-start(bf16[3,32,2048]{2,1,0:T(8,128)(2,1)} %get-tuple-element.20.refs_0_), channel_id=1, source_target_pairs={{0,2},{1,3},{2,0},{3,1},{4,6},{5,7},{6,4},{7,5},{8,10},{9,11},{10,... | collective-permute-start | bytes 1179656 | tf_op jit(solution)/shard_map/ppermute | solution.py:53
  23.3 19.2 %collective-permute-start.2 = (bf16[3,32,2048]{2,1,0:T(8,128)(2,1)}, bf16[3,32,2048]{2,1,0:T(8,128)(2,1)S(1)}, u32[]{:S(2)}, u32[]{:S(2)}) collective-permute-start(bf16[3,32,2048]{2,1,0:T(8,128)(2,1)} %get-tuple-element.20.refs_0_), channel_id=1, source_target_pairs={{0,3},{1,0},{2,1},{3,2},{4,7},{5,4},{6,5},{7,6},{8,11},{9,8},{10,9... | collective-permute-start | bytes 1179656 | tf_op jit(solution)/shard_map/ppermute | solution.py:53
  24.5 22.4 %collective-permute-start.4 = (bf16[3,32,2048]{2,1,0:T(8,128)(2,1)S(1)}, bf16[3,32,2048]{2,1,0:T(8,128)(2,1)S(1)}, u32[]{:S(2)}, u32[]{:S(2)}) collective-permute-start(bf16[3,32,2048]{2,1,0:T(8,128)(2,1)S(1)} %collective-permute-done.3.refs_4_), channel_id=1, source_target_pairs={{0,1},{1,2},{2,3},{3,0},{4,5},{5,6},{6,7},{7,4},{8,9},{9,10},{10,1... | collective-permute-start | bytes 1179656 | tf_op jit(solution)/shard_map/ppermute | solution.py:53
  26.0 26.5 %collective-permute-start.5 = (bf16[3,32,2048]{2,1,0:T(8,128)(2,1)S(1)}, bf16[3,32,2048]{2,1,0:T(8,128)(2,1)S(1)}, u32[]{:S(2)}, u32[]{:S(2)}) collective-permute-start(bf16[3,32,2048]{2,1,0:T(8,128)(2,1)S(1)} %collective-permute-done.3.refs_4_), channel_id=1, source_target_pairs={{0,2},{1,3},{2,0},{3,1},{4,6},{5,7},{6,4},{7,5},{8,10},{9,11},{10,... | collective-permute-start | bytes 1179656 | tf_op jit(solution)/shard_map/ppermute | solution.py:53
  30.1 29.5 %collective-permute-start.23 = (bf16[4,6,64,256]{3,2,1,0:T(8,128)(2,1)S(1)}, bf16[4,6,64,256]{3,2,1,0:T(8,128)(2,1)S(1)}, u32[]{:S(2)}, u32[]{:S(2)}) collective-permute-start(bf16[4,6,64,256]{3,2,1,0:T(8,128)(2,1)S(1)} %pad_maximum_fusion.1.refs_8_), channel_id=1, source_target_pairs={{0,32},{4,12},{8,40},{12,20},{16,48},{20,28},{24,56},{28,4},{32,64... | collective-permute-start | bytes 2359304 | tf_op jit(solution)/shard_map/ppermute | solution.py:362
  35.6 26.5 %collective-permute-start.24 = (bf16[4,6,64,256]{3,2,1,0:T(8,128)(2,1)S(1)}, bf16[4,6,64,256]{3,2,1,0:T(8,128)(2,1)S(1)}, u32[]{:S(2)}, u32[]{:S(2)}) collective-permute-start(bf16[4,6,64,256]{3,2,1,0:T(8,128)(2,1)S(1)} %pad_maximum_fusion.1.refs_8_), channel_id=1, source_target_pairs={{0,64},{4,20},{8,72},{12,28},{16,80},{20,4},{24,88},{28,12},{32,96... | collective-permute-start | bytes 2359304 | tf_op jit(solution)/shard_map/ppermute | solution.py:362
  42.5 15.7 %collective-permute-start.6 = (bf16[3,32,2048]{2,1,0:T(8,128)(2,1)S(1)}, bf16[3,32,2048]{2,1,0:T(8,128)(2,1)S(1)}, u32[]{:S(2)}, u32[]{:S(2)}) collective-permute-start(bf16[3,32,2048]{2,1,0:T(8,128)(2,1)S(1)} %collective-permute-done.3.refs_4_), channel_id=1, source_target_pairs={{0,3},{1,0},{2,1},{3,2},{4,7},{5,4},{6,5},{7,6},{8,11},{9,8},{10,9... | collective-permute-start | bytes 1179656 | tf_op jit(solution)/shard_map/ppermute | solution.py:53
  46.9 16.4 %collective-permute-start.25 = (bf16[4,6,64,256]{3,2,1,0:T(8,128)(2,1)S(1)}, bf16[4,6,64,256]{3,2,1,0:T(8,128)(2,1)S(1)}, u32[]{:S(2)}, u32[]{:S(2)}) collective-permute-start(bf16[4,6,64,256]{3,2,1,0:T(8,128)(2,1)S(1)} %pad_maximum_fusion.1.refs_8_), channel_id=1, source_target_pairs={{0,96},{4,28},{8,104},{12,4},{16,112},{20,12},{24,120},{28,20},{32... | collective-permute-start | bytes 2359304 | tf_op jit(solution)/shard_map/ppermute | solution.py:362
  52.5 28.4 %collective-permute-start.26 = (bf16[4,6,64,256]{3,2,1,0:T(8,128)(2,1)S(1)}, bf16[4,6,64,256]{3,2,1,0:T(8,128)(2,1)S(1)}, u32[]{:S(2)}, u32[]{:S(2)}) collective-permute-start(bf16[4,6,64,256]{3,2,1,0:T(8,128)(2,1)S(1)} %pad_maximum_fusion.1.refs_8_), channel_id=1, source_target_pairs={{0,4},{4,0},{8,12},{12,8},{16,20},{20,16},{24,28},{28,24},{32,36},... | collective-permute-start | bytes 2359304 | tf_op jit(solution)/shard_map/ppermute | solution.py:49
  58.2 22.9 %collective-permute-start.13 = (bf16[4,7,64,256]{3,2,1,0:T(8,128)(2,1)S(1)}, bf16[4,7,64,256]{3,2,1,0:T(8,128)(2,1)}, u32[]{:S(2)}, u32[]{:S(2)}) collective-permute-start(bf16[4,7,64,256]{3,2,1,0:T(8,128)(2,1)S(1)} %pad_maximum_fusion.refs_8_), channel_id=1, source_target_pairs={{0,32},{4,12},{8,40},{12,20},{16,48},{20,28},{24,56},{28,4},{32,64... | collective-permute-start | bytes 2752520 | tf_op jit(solution)/shard_map/ppermute | solution.py:362
  59.5 23.3 %collective-permute-start.14 = (bf16[4,7,64,256]{3,2,1,0:T(8,128)(2,1)S(1)}, bf16[4,7,64,256]{3,2,1,0:T(8,128)(2,1)}, u32[]{:S(2)}, u32[]{:S(2)}) collective-permute-start(bf16[4,7,64,256]{3,2,1,0:T(8,128)(2,1)S(1)} %pad_maximum_fusion.refs_8_), channel_id=1, source_target_pairs={{0,64},{4,20},{8,72},{12,28},{16,80},{20,4},{24,88},{28,12},{32,96... | collective-permute-start | bytes 2752520 | tf_op jit(solution)/shard_map/ppermute | solution.py:362
  62.2 20.7 %collective-permute-start.15 = (bf16[4,7,64,256]{3,2,1,0:T(8,128)(2,1)S(1)}, bf16[4,7,64,256]{3,2,1,0:T(8,128)(2,1)}, u32[]{:S(2)}, u32[]{:S(2)}) collective-permute-start(bf16[4,7,64,256]{3,2,1,0:T(8,128)(2,1)S(1)} %pad_maximum_fusion.refs_8_), channel_id=1, source_target_pairs={{0,96},{4,28},{8,104},{12,4},{16,112},{20,12},{24,120},{28,20},{32... | collective-permute-start | bytes 2752520 | tf_op jit(solution)/shard_map/ppermute | solution.py:362
  63.2 27.6 %collective-permute-start.27 = (bf16[4,6,64,256]{3,2,1,0:T(8,128)(2,1)S(1)}, bf16[4,6,64,256]{3,2,1,0:T(8,128)(2,1)S(1)}, u32[]{:S(2)}, u32[]{:S(2)}) collective-permute-start(bf16[4,6,64,256]{3,2,1,0:T(8,128)(2,1)S(1)} %collective-permute-done.23.refs_9_), channel_id=1, source_target_pairs={{0,4},{4,0},{8,12},{12,8},{16,20},{20,16},{24,28},{28,24},{32,36},... | collective-permute-start | bytes 2359304 | tf_op jit(solution)/shard_map/ppermute | solution.py:49
  80.9 10.0 %collective-permute-start.28 = (bf16[4,6,64,256]{3,2,1,0:T(8,128)(2,1)S(1)}, bf16[4,6,64,256]{3,2,1,0:T(8,128)(2,1)S(1)}, u32[]{:S(2)}, u32[]{:S(2)}) collective-permute-start(bf16[4,6,64,256]{3,2,1,0:T(8,128)(2,1)S(1)} %collective-permute-done.24.refs_10_), channel_id=1, source_target_pairs={{0,4},{4,0},{8,12},{12,8},{16,20},{20,16},{24,28},{28,24},{32,36},... | collective-permute-start | bytes 2359304 | tf_op jit(solution)/shard_map/ppermute | solution.py:49
  81.0 11.6 %collective-permute-start.29 = (bf16[4,6,64,256]{3,2,1,0:T(8,128)(2,1)S(1)}, bf16[4,6,64,256]{3,2,1,0:T(8,128)(2,1)}, u32[]{:S(2)}, u32[]{:S(2)}) collective-permute-start(bf16[4,6,64,256]{3,2,1,0:T(8,128)(2,1)S(1)} %collective-permute-done.25.refs_11_), channel_id=1, source_target_pairs={{0,4},{4,0},{8,12},{12,8},{16,20},{20,16},{24,28},{28,24},{32,36},... | collective-permute-start | bytes 2359304 | tf_op jit(solution)/shard_map/ppermute | solution.py:49
  82.9 27.6 %collective-permute-start.16 = (bf16[4,7,64,256]{3,2,1,0:T(8,128)(2,1)S(1)}, bf16[4,7,64,256]{3,2,1,0:T(8,128)(2,1)}, u32[]{:S(2)}, u32[]{:S(2)}) collective-permute-start(bf16[4,7,64,256]{3,2,1,0:T(8,128)(2,1)S(1)} %pad_maximum_fusion.refs_8_), channel_id=1, source_target_pairs={{0,4},{4,0},{8,12},{12,8},{16,20},{20,16},{24,28},{28,24},{32,36},... | collective-permute-start | bytes 2752520 | tf_op jit(solution)/shard_map/ppermute | solution.py:49
  82.9 30.8 %collective-permute-start.17 = (bf16[4,7,64,256]{3,2,1,0:T(8,128)(2,1)}, bf16[4,7,64,256]{3,2,1,0:T(8,128)(2,1)}, u32[]{:S(2)}, u32[]{:S(2)}) collective-permute-start(bf16[4,7,64,256]{3,2,1,0:T(8,128)(2,1)} %collective-permute-done.13.refs_9_), channel_id=1, source_target_pairs={{0,4},{4,0},{8,12},{12,8},{16,20},{20,16},{24,28},{28,24},{32,36},... | collective-permute-start | bytes 2752520 | tf_op jit(solution)/shard_map/ppermute | solution.py:49
  90.9 26.1 %collective-permute-start.18 = (bf16[4,7,64,256]{3,2,1,0:T(8,128)(2,1)}, bf16[4,7,64,256]{3,2,1,0:T(8,128)(2,1)}, u32[]{:S(2)}, u32[]{:S(2)}) collective-permute-start(bf16[4,7,64,256]{3,2,1,0:T(8,128)(2,1)} %collective-permute-done.14.refs_10_), channel_id=1, source_target_pairs={{0,4},{4,0},{8,12},{12,8},{16,20},{20,16},{24,28},{28,24},{32,36},... | collective-permute-start | bytes 2752520 | tf_op jit(solution)/shard_map/ppermute | solution.py:49
  91.8 25.2 %collective-permute-start.19 = (bf16[4,7,64,256]{3,2,1,0:T(8,128)(2,1)}, bf16[4,7,64,256]{3,2,1,0:T(8,128)(2,1)}, u32[]{:S(2)}, u32[]{:S(2)}) collective-permute-start(bf16[4,7,64,256]{3,2,1,0:T(8,128)(2,1)} %collective-permute-done.15.refs_11_), channel_id=1, source_target_pairs={{0,4},{4,0},{8,12},{12,8},{16,20},{20,16},{24,28},{28,24},{32,36},... | collective-permute-start | bytes 2752520 | tf_op jit(solution)/shard_map/ppermute | solution.py:49
  98.7 49.8 %collective-permute-start.30 = (bf16[2,3,256,256]{3,2,1,0:T(8,128)(2,1)}, bf16[2,3,256,256]{3,2,1,0:T(8,128)(2,1)S(1)}, u32[]{:S(2)}, u32[]{:S(2)}) collective-permute-start(bf16[2,3,256,256]{3,2,1,0:T(8,128)(2,1)} %get-tuple-element.25.wide), channel_id=1, source_target_pairs={{0,8},{4,12},{8,16},{12,20},{16,24},{20,28},{24,32},{28,36},{32,40... | collective-permute-start | bytes 2359304 | tf_op jit(solution)/shard_map/ppermute | solution.py:57
  110.5 28.5 %collective-permute-start.32 = (bf16[2,3,128,256]{3,2,1,0:T(8,128)(2,1)}, bf16[2,3,128,256]{3,2,1,0:T(8,128)(2,1)S(1)}, u32[]{:S(2)}, u32[]{:S(2)}) collective-permute-start(bf16[2,3,128,256]{3,2,1,0:T(8,128)(2,1)} %get-tuple-element.28), channel_id=1, source_target_pairs={{0,8},{4,12},{8,16},{12,20},{16,24},{20,28},{24,32},{28,36},{32,40... | collective-permute-start | bytes 1179656 | tf_op jit(solution)/shard_map/ppermute | solution.py:57
  113.7 34.7 %collective-permute-start.31 = (bf16[2,3,128,256]{3,2,1,0:T(8,128)(2,1)S(1)}, bf16[2,3,128,256]{3,2,1,0:T(8,128)(2,1)S(1)}, u32[]{:S(2)}, u32[]{:S(2)}) collective-permute-start(bf16[2,3,128,256]{3,2,1,0:T(8,128)(2,1)S(1)} %copy-done.25), channel_id=1, source_target_pairs={{0,16},{4,20},{8,24},{12,28},{16,32},{20,36},{24,40},{28,44},{32,4... | collective-permute-start | bytes 1179656 | tf_op jit(solution)/shard_map/ppermute | solution.py:57
  159.1 7.9 %collective-permute-start.33 = (bf16[2,3,32,256]{3,2,1,0:T(8,128)(2,1)}, bf16[2,3,32,256]{3,2,1,0:T(8,128)(2,1)S(1)}, u32[]{:S(2)}, u32[]{:S(2)}) collective-permute-start(bf16[2,3,32,256]{3,2,1,0:T(8,128)(2,1)} %get-tuple-element.32), channel_id=1, source_target_pairs={{0,1},{1,2},{2,3},{3,0},{4,5},{5,6},{6,7},{7,4},{8,9},{9,10},{10,1... | collective-permute-start | bytes 294920 | tf_op jit(solution)/shard_map/ppermute | solution.py:53
  159.2 8.7 %collective-permute-start.34 = (bf16[2,3,32,256]{3,2,1,0:T(8,128)(2,1)}, bf16[2,3,32,256]{3,2,1,0:T(8,128)(2,1)S(1)}, u32[]{:S(2)}, u32[]{:S(2)}) collective-permute-start(bf16[2,3,32,256]{3,2,1,0:T(8,128)(2,1)} %get-tuple-element.33), channel_id=1, source_target_pairs={{0,2},{1,3},{2,0},{3,1},{4,6},{5,7},{6,4},{7,5},{8,10},{9,11},{10,... | collective-permute-start | bytes 294920 | tf_op jit(solution)/shard_map/ppermute | solution.py:53
  159.7 8.4 %collective-permute-start.35 = (bf16[2,3,32,256]{3,2,1,0:T(8,128)(2,1)}, bf16[2,3,32,256]{3,2,1,0:T(8,128)(2,1)S(1)}, u32[]{:S(2)}, u32[]{:S(2)}) collective-permute-start(bf16[2,3,32,256]{3,2,1,0:T(8,128)(2,1)} %get-tuple-element.34), channel_id=1, source_target_pairs={{0,3},{1,0},{2,1},{3,2},{4,7},{5,4},{6,5},{7,6},{8,11},{9,8},{10,9... | collective-permute-start | bytes 294920 | tf_op jit(solution)/shard_map/ppermute | solution.py:53
  (35 other events, 596.5 us)
where the time goes:
time: 176 us; the launch traced here: 175 us
  starting transfers between devices  83.6 us (48%)
  Pallas kernels  49.1 us (28%)
  waiting for transfers between devices  32.2 us (18%)
  local copies, waits for them, and re-layouts  7.19 us (4%)
  other arithmetic  1.84 us (1%)
    ppermute x14, starting transfers between devices, swapped(): return lax.ppermute(a, 'sp', SWAP)  37.5 us
    ppermute x12, starting transfers between devices, turned(): return lax.ppermute(a, 'tp', [(i, (i + shift) % RING) for i in range(RING)])  15.9 us
    ppermute x6, starting transfers between devices, spread(): far = {d: lax.ppermute(line, 'sp', second_leg(d)) for d in (1, 3, 2)}  15.2 us
    ppermute x3, waiting for transfers between devices, from_behind(): lax.ppermute(a, 'sp', [(i, i + 2 * blocks) for i in range(32 - 2 * blocks)])  13.5 us
    ppermute x12, waiting for transfers between devices, turned(): return lax.ppermute(a, 'tp', [(i, (i + shift) % RING) for i in range(RING)])  11.7 us
    ppermute x3, starting transfers between devices, from_behind(): lax.ppermute(a, 'sp', [(i, i + 2 * blocks) for i in range(32 - 2 * blocks)])  9.78 us
    pallas_call x1, Pallas kernels, attend_wide(): pl.pallas_call(wide_body, out_shape=(piece,) * 4 + (line,) * 2, in_specs=...  9.67 us
    pallas_call x1, Pallas kernels, attend_near(): pl.pallas_call(near_body, out_shape=(shape, shape), in_specs=[VMEM, ANY,...  8.72 us
  transfers between devices with their start and end apart: 41, of which 12 were waited for; matrix products, arithmetic and copies ran while one was open for 3% of the time, Pallas kernels for 20%

commit v1 on v0

v1 whole, which is shorter than its diff:
```python
import math

import jax
import jax.numpy as jnp
from jax import lax
from jax.experimental import pallas as pl
from jax.experimental.pallas import tpu as pltpu
from jax.sharding import PartitionSpec as P


GROUPS = 3
STEPS = 24
DILATIONS = (1, 4, 16)
HALOS = (32, 96, 384)
RING = 4
BATCHES = 3
PIECE = 32
SPAN = 256
HEAD_WIDTH = 128
COLS = 256
ROWS = 64
WIDTH = 2048
BLOCK = 128

epsilon = 1e-06


def chip(z, y, core):
    return (z % RING) * 8 + (y % RING) * 2 + core


def chips():
    return [(z, y, core) for z in range(RING) for y in range(RING) for core in range(2)]


def first_leg(shift, kind):
    def way(k):
        return k if kind == 0 else 0

    return [(chip(z, y, k), chip(z + shift * way(k), y + shift * (1 - way(k)), k)) for z, y, k in chips()]


def second_leg(shift, kind):
    def way(k):
        return k if kind == 0 else 0

    return [(chip(z, y, k), chip(z + shift * (1 - way(k)), y + shift * way(k), k)) for z, y, k in chips()]


SWAP = [(i, i ^ 1) for i in range(32)]


def swapped(a):
    return lax.ppermute(a, "sp", SWAP)


def turned(a, shift):
    return lax.ppermute(a, "tp", [(i, (i + shift) % RING) for i in range(RING)])


def from_behind(a, blocks):
    return lax.ppermute(a, "sp", [(i, i + 2 * blocks) for i in range(32 - 2 * blocks)])


def place_of(core, first, second, kind):
    s = lax.axis_index("sp")
    z, y = s // 8, (s // 2) % RING
    if kind == 0:
        up = jnp.where(core == 0, second, first)
        along = jnp.where(core == 0, first, second)
    else:
        up, along = second, first
    return ((z + RING - up) % RING) * 8 + ((y + RING - along) % RING) * 2 + core


ANY = pl.BlockSpec(memory_space=pl.ANY)
VMEM = pl.BlockSpec(memory_space=pltpu.VMEM)
PARAMS = pltpu.CompilerParams(vmem_limit_bytes=56 * 1024 * 1024)
HALF = SPAN // 2
NEAR = 4


def bf(*dims):
    return jax.ShapeDtypeStruct(dims, jnp.bfloat16)


def pack_body(w_query, w_key, w_value, wide, rest):
    wide[0] = w_key[2]
    wide[1] = w_value[2]
    for g in range(2):
        rest[2 * g] = w_key[g]
        rest[2 * g + 1] = w_value[g]
    rest[NEAR:] = w_query[...]


def pack(w_query, w_key, w_value):
    return pl.pallas_call(
        pack_body, out_shape=(bf(2, ROWS, COLS), bf(NEAR + GROUPS, ROWS, COLS)),
        in_specs=[VMEM] * 3, out_specs=(VMEM,) * 2, compiler_params=PARAMS, name="pack",
    )(w_query, w_key, w_value)


def norm_body(tokens, other, gain, late, early):
    core = lax.axis_index("sp") % 2
    widened_gain = gain[...]

    def normed(v):
        v = v.astype(jnp.float32)
        v = v * lax.rsqrt(jnp.mean(v * v, axis=-1, keepdims=True) + epsilon)
        return (v * widened_gain).astype(jnp.bfloat16)

    for b in range(BATCHES):
        mine = normed(tokens[core * BATCHES + b])
        theirs = normed(other[b])

        @pl.when(core == 1)
        def _():
            late[b] = mine
            early[b] = theirs

        @pl.when(core == 0)
        def _():
            late[b] = theirs
            early[b] = mine


def norm_rows(tokens, other, gain):
    shape = bf(BATCHES, PIECE, WIDTH)
    return pl.pallas_call(
        norm_body, out_shape=(shape, shape), in_specs=[VMEM] * 3, out_specs=(VMEM,) * 2,
        compiler_params=PARAMS, name="norm_rows",
    )(tokens, other, gain.reshape(1, WIDTH))


def row_copies(pieces, base, x_all, sems):
    t = lax.axis_index("tp")
    copies = []
    for d, piece in enumerate(pieces):
        at = pl.multiple_of(base + ((t + RING - d) % RING) * PIECE, PIECE)
        copies.append(pltpu.make_async_copy(piece, x_all.at[:, pl.ds(at, PIECE), :], sems.at[base // HALF, d]))
    return copies


def shard_copies(lines, first, count, w_all, sems, kind):
    core = lax.axis_index("sp") % 2
    copies = []
    for n, line in enumerate(lines):
        whose = core if n < RING else 1 - core
        for j in range(RING):
            at = pl.multiple_of(place_of(whose, j, n % RING, kind) * ROWS, ROWS)
            copies.append(
                pltpu.make_async_copy(
                    line.at[j, pl.ds(first, count)], w_all.at[pl.ds(first, count), pl.ds(at, ROWS), :],
                    sems.at[n * RING + j],
                )
            )
    return copies


def wide_pair_body(*refs):
    pieces, lines = refs[:4], refs[4:12]
    out, x_all, w_all, x_sems, k_sems, v_sems = refs[12:]
    groups = [row_copies(pieces, 0, x_all, x_sems)]
    groups += [shard_copies(lines, 0, 1, w_all, k_sems, 0), shard_copies(lines, 1, 1, w_all, v_sems, 0)]
    for group in groups:
        for c in group:
            c.start()
    for c in groups[0]:
        c.wait()
    for role in range(2):
        for c in groups[1 + role]:
            c.wait()
        x = x_all[...].reshape(BATCHES * HALF, WIDTH)
        y = jnp.dot(x, w_all[role], preferred_element_type=jnp.float32)
        out[role] = y.astype(jnp.bfloat16).reshape(BATCHES, HALF, COLS)


def project_wide(pieces, lines):
    return pl.pallas_call(
        wide_pair_body, out_shape=bf(2, BATCHES, HALF, COLS), in_specs=[ANY] * 12, out_specs=VMEM,
        scratch_shapes=[
            pltpu.VMEM((BATCHES, HALF, WIDTH), jnp.bfloat16), pltpu.VMEM((2, WIDTH, COLS), jnp.bfloat16),
            pltpu.SemaphoreType.DMA((1, RING)), pltpu.SemaphoreType.DMA((32,)), pltpu.SemaphoreType.DMA((32,)),
        ],
        compiler_params=PARAMS, name="project_wide",
    )(*pieces, *lines)


def rest_body(*refs):
    early, late, lines = refs[:4], refs[4:8], refs[8:16]
    near, near_tail, queries, x_all, w_all, x_sems, a_sems, b_sems, c_sems = refs[16:]
    rows = row_copies(early, 0, x_all, x_sems) + row_copies(late, HALF, x_all, x_sems)
    groups = {
        0: rows + shard_copies(lines, 0, 1, w_all, a_sems, 0),
        1: shard_copies(lines, 1, 3, w_all, b_sems, 0),
        4: shard_copies(lines, 4, 3, w_all, c_sems, 0),
    }
    for group in groups.values():
        for c in group:
            c.start()
    for m in range(NEAR + GROUPS):
        for c in groups.get(m, ()):
            c.wait()
        x = x_all[...].reshape(BATCHES * SPAN, WIDTH)
        y = jnp.dot(x, w_all[m], preferred_element_type=jnp.float32)
        y = y.astype(jnp.bfloat16).reshape(BATCHES, SPAN, COLS)
        if m >= NEAR:
            queries[m - NEAR] = y
        else:
            near[m // 2, m % 2] = y
            if m < 2:
                near_tail[m % 2, :, : HALOS[0]] = y[:, SPAN - HALOS[0] :]
            else:
                near_tail[m % 2, :, HALOS[0] :] = y[:, SPAN - HALOS[1] :]


def project_rest(early, late, lines):
    return pl.pallas_call(
        rest_body,
        out_shape=(
            bf(2, 2, BATCHES, SPAN, COLS), bf(2, BATCHES, HALOS[0] + HALOS[1], COLS), bf(GROUPS, BATCHES, SPAN, COLS)
        ),
        in_specs=[ANY] * 16, out_specs=(VMEM,) * 3,
        scratch_shapes=[
            pltpu.VMEM((BATCHES, SPAN, WIDTH), jnp.bfloat16), pltpu.VMEM((NEAR + GROUPS, WIDTH, COLS), jnp.bfloat16),
            pltpu.SemaphoreType.DMA((2, RING)), pltpu.SemaphoreType.DMA((32,)), pltpu.SemaphoreType.DMA((32,)),
            pltpu.SemaphoreType.DMA((32,)),
        ],
        compiler_params=PARAMS, name="project_rest",
    )(*early, *late, *lines)


def bias_of(group, block):
    halo, dilation = HALOS[group], DILATIONS[group]
    dims = (BLOCK, BLOCK + halo)
    q = lax.broadcasted_iota(jnp.int32, dims, 0)
    k = lax.broadcasted_iota(jnp.int32, dims, 1)
    lag = q + halo - k
    start = (lax.axis_index("sp") // 2) * SPAN + block * BLOCK - halo
    seen = (lag >= 0) & (lag <= STEPS * dilation) & ((lag & (dilation - 1)) == 0) & (k + start >= 0)
    return jnp.where(seen, 0.0, -1e30).astype(jnp.float32)


def attend(items):
    scores = [
        lax.dot_general(q, k, (((1,), (1,)), ((), ())), preferred_element_type=jnp.float32) for q, k, _, _ in items
    ]
    lifts = []
    for s, (_, _, _, bias) in zip(scores, items):
        s = s * (1.0 / math.sqrt(HEAD_WIDTH)) + bias
        peak = jnp.max(s, axis=-1, keepdims=True)
        lifted = jnp.exp(s - peak)
        lifts.append((lifted.astype(jnp.bfloat16), peak, jnp.sum(lifted, axis=-1, keepdims=True)))
    outs = [jnp.dot(p, v, preferred_element_type=jnp.float32) for (p, _, _), (_, _, v, _) in zip(lifts, items)]
    return [(o / total, peak + jnp.log(total)) for o, (_, peak, total) in zip(outs, lifts)]


def joined(o1, l1, o2, l2):
    top = jnp.maximum(l1, l2)
    a, c = jnp.exp(l1 - top), jnp.exp(l2 - top)
    total = a + c
    return (a * o1 + c * o2) / total, top + jnp.log(total)


PLACES = [
    (b, h, slice(h * HEAD_WIDTH, (h + 1) * HEAD_WIDTH)) for b in range(BATCHES) for h in range(COLS // HEAD_WIDTH)
]


def wide_body(q, early, late, back_early, back_late, far_late, out, logs, held, sems):
    copies = [
        pltpu.make_async_copy(part, held.at[:, :, pl.ds(n * HALF, HALF)], sems.at[n])
        for n, part in enumerate((far_late, back_early, back_late, early, late))
    ]
    for c in copies:
        c.start()
    for c in copies:
        c.wait()
    for i in range(SPAN // BLOCK):
        rows = slice(i * BLOCK, (i + 1) * BLOCK)
        keys = slice(i * BLOCK, (i + 1) * BLOCK + HALOS[2])
        bias = bias_of(2, i)
        found = attend([(q[b, rows, cols], held[0, b, keys, cols], held[1, b, keys, cols], bias) for b, _, cols in PLACES])
        for (b, _, cols), (o, l) in zip(PLACES, found):
            out[b, rows, cols] = o
            logs[b, rows, cols] = jnp.broadcast_to(l, (BLOCK, HEAD_WIDTH))


def attend_wide(q, early, late, back_early, back_late, far_late):
    shape = jax.ShapeDtypeStruct((BATCHES, SPAN, COLS), jnp.float32)
    return pl.pallas_call(
        wide_body, out_shape=(shape, shape),
        in_specs=[pl.BlockSpec((pl.squeezed, BATCHES, SPAN, COLS), lambda i: (2, 0, 0, 0))] + [ANY] * 5,
        out_specs=(VMEM,) * 2, grid=(1,),
        scratch_shapes=[
            pltpu.VMEM((2, BATCHES, HALOS[2] + SPAN, COLS), jnp.bfloat16), pltpu.SemaphoreType.DMA((5,)),
        ],
        compiler_params=PARAMS, name="attend_wide",
    )(q, early, late, back_early, back_late, far_late)


def near_body(q, near, tail, other, logs, c0, c1, c2, c3, kept, sent, k0, k1, mixed, weights, sems):
    copies = [
        pltpu.make_async_copy(tail.at[:, :, pl.ds(0, HALOS[0])], k0.at[:, :, pl.ds(0, HALOS[0])], sems.at[0]),
        pltpu.make_async_copy(tail.at[:, :, pl.ds(HALOS[0], HALOS[1])], k1.at[:, :, pl.ds(0, HALOS[1])], sems.at[1]),
        pltpu.make_async_copy(near.at[0], k0.at[:, :, pl.ds(HALOS[0], SPAN)], sems.at[2]),
        pltpu.make_async_copy(near.at[1], k1.at[:, :, pl.ds(HALOS[1], SPAN)], sems.at[3]),
    ]
    for c in copies:
        c.start()
    for c in copies:
        c.wait()
    core, t = lax.axis_index("sp") % 2, lax.axis_index("tp")
    for i in range(SPAN // BLOCK):
        rows = slice(i * BLOCK, (i + 1) * BLOCK)
        biases = [bias_of(g, i) for g in range(2)]
        for some in (PLACES[:3], PLACES[3:]):
            items = []
            for g, held in enumerate((k0, k1)):
                keys = slice(i * BLOCK, (i + 1) * BLOCK + HALOS[g])
                items += [
                    (q[g, b, rows, cols], held[0, b, keys, cols], held[1, b, keys, cols], biases[g]) for b, _, cols in some
                ]
            found = attend(items)
            for n, (b, h, cols) in enumerate(some):
                o, l = joined(*found[n], *found[n + 3])
                o, l = joined(o, l, other[b, rows, cols], logs[b, rows, cols])
                mixed[b, rows, cols] = o.astype(jnp.bfloat16)
                weights[i, 2 * b + h : 2 * b + h + 1, :] = jnp.transpose(l)[0:1]
    kept[...] = weights[core]
    sent[...] = weights[1 - core]
    for d, out in enumerate((c0, c1, c2, c3)):
        for far in range(2):
            whose = core if far == 0 else 1 - core
            at = pl.multiple_of(whose * HALF + ((t + d) % RING) * PIECE, PIECE)
            out[far] = mixed[:, pl.ds(at, PIECE), :]


def attend_near(q, near, tail, other, logs):
    piece = bf(2, BATCHES, PIECE, COLS)
    line = jax.ShapeDtypeStruct((2 * BATCHES, BLOCK), jnp.float32)
    return pl.pallas_call(
        near_body, out_shape=(piece,) * 4 + (line,) * 2, grid=(1,),
        in_specs=[pl.BlockSpec((2, BATCHES, SPAN, COLS), lambda i: (0, 0, 0, 0)), ANY, ANY, VMEM, VMEM],
        out_specs=(VMEM,) * 6,
        scratch_shapes=[
            pltpu.VMEM((2, BATCHES, HALOS[0] + SPAN, COLS), jnp.bfloat16),
            pltpu.VMEM((2, BATCHES, HALOS[1] + SPAN, COLS), jnp.bfloat16),
            pltpu.VMEM((BATCHES, SPAN, COLS), jnp.bfloat16),
            pltpu.VMEM((2, 2 * BATCHES, BLOCK), jnp.float32),
            pltpu.SemaphoreType.DMA((4,)),
        ],
        compiler_params=PARAMS, name="attend_near",
    )(q, near, tail, other, logs)


def lay_body(*refs):
    lines, out, sems = refs[:8], refs[8], refs[9]
    copies = shard_copies(lines, 0, RING, out, sems, 1)
    for c in copies:
        c.start()
    for c in copies:
        c.wait()


def lay_out(lines):
    return pl.pallas_call(
        lay_body, out_shape=bf(RING, WIDTH, COLS), in_specs=[ANY] * 8, out_specs=VMEM,
        scratch_shapes=[pltpu.SemaphoreType.DMA((32,))], compiler_params=PARAMS, name="lay_out",
    )(*lines)


def final_body(r0, r1, r2, r3, s0, s1, s2, s3, w, out, held, w_all, sems):
    core = lax.axis_index("sp") % 2
    part = WIDTH // RING
    copies = [
        pltpu.make_async_copy(w.at[:, pl.ds(n * part, part)], w_all.at[n], sems.at[n]) for n in range(RING)
    ]
    for c in copies:
        c.start()
    for d, (r, s) in enumerate(((r0, s0), (r1, s1), (r2, s2), (r3, s3))):
        held[d, core] = r[0].reshape(BATCHES * PIECE, COLS)
        held[d, 1 - core] = s[...].reshape(BATCHES * PIECE, COLS)
    for n in range(RING):
        cols = slice(n * part, (n + 1) * part)
        copies[n].wait()
        acc = None
        for d in range(RING):
            a = held[d].reshape(2 * BATCHES * PIECE, COLS)
            y = lax.dot_general(a, w_all[n, d], (((1,), (1,)), ((), ())), preferred_element_type=jnp.float32)
            acc = y if acc is None else acc + y
        out[:, :, cols] = acc.astype(jnp.bfloat16).reshape(2 * BATCHES, PIECE, part)


def finish(received, crossed, w):
    mixed = pl.pallas_call(
        final_body, out_shape=bf(2 * BATCHES, PIECE, WIDTH),
        in_specs=[VMEM] * 8 + [ANY], out_specs=VMEM,
        scratch_shapes=[
            pltpu.VMEM((RING, 2, BATCHES * PIECE, COLS), jnp.bfloat16),
            pltpu.VMEM((RING, RING, WIDTH // RING, COLS), jnp.bfloat16),
            pltpu.SemaphoreType.DMA((RING,)),
        ],
        compiler_params=PARAMS, name="finish",
    )(*received, *crossed, w)
    return jnp.transpose(mixed, (1, 0, 2))


def ring_of(a):
    came = {d: turned(a, d) for d in (1, 3, 2)}
    return [a, came[1], came[2], came[3]]


def spread(own, kind):
    near = {d: lax.ppermute(own, "sp", first_leg(d, kind)) for d in (1, 3, 2)}
    line = jnp.stack((own, near[1], near[2], near[3]))
    far = {d: lax.ppermute(line, "sp", second_leg(d, kind)) for d in (1, 3, 2)}
    lines = [line, far[1], far[2], far[3]]
    return lines + [swapped(a) for a in lines]


def layer(tokens, norm_gain, w_query, w_key, w_value, w_out):
    core = lax.axis_index("sp") % 2
    tokens = jnp.transpose(tokens, (1, 0, 2))
    send = lax.dynamic_slice_in_dim(tokens, (1 - core) * BATCHES, BATCHES, 0)
    other = swapped(send)
    wide_own, rest_own = pack(w_query, w_key, w_value)
    wide_lines = spread(wide_own, 0)
    late, early = norm_rows(tokens, other, norm_gain)
    late, early = ring_of(late), ring_of(early)
    rest_lines = spread(rest_own, 0)
    out_lines = spread(jnp.stack(ring_of(jnp.transpose(w_out))), 1)

    wide_late = project_wide(late, wide_lines)
    far_late = from_behind(wide_late, 2)
    back_late = from_behind(wide_late, 1)
    wide_early = project_wide(early, wide_lines)
    back_early = from_behind(wide_early, 1)
    near, near_tail, queries = project_rest(early, late, rest_lines)
    near_tail = from_behind(near_tail, 1)
    laid = lay_out(out_lines)
    wide_out, wide_logs = attend_wide(queries, wide_early, wide_late, back_early, back_late, far_late)
    *combined, kept, sent = attend_near(queries, near, near_tail, wide_out, wide_logs)

    received = [combined[0]] + [turned(combined[d], d) for d in (1, 2, 3)]
    crossed = [swapped(a[1]) for a in received]
    mixed = finish(received, crossed, laid)

    came = swapped(sent)
    low = jnp.where(core == 0, kept, came)
    high = jnp.where(core == 0, came, kept)
    log_weight = jnp.concatenate((low, high), 0).reshape(2 * BATCHES, 2, BLOCK)
    return (mixed, jnp.transpose(log_weight, (2, 0, 1)))


def solution(mesh):
    in_specs = (
        P(("sp", "tp"), None, None),
        P(),
        P(None, "sp", "tp"),
        P(None, "sp", "tp"),
        P(None, "sp", "tp"),
        P("tp", "sp"),
    )
    out_specs = (P(("sp", "tp"), None, None), P("sp", None, "tp"))
    return jax.shard_map(layer, mesh=mesh, in_specs=in_specs, out_specs=out_specs, check_vma=False)
```

time: 176 us -> 196 us (1.11)
  the two profiles are of different devices: /device:TPU:97 before, /device:TPU:1 now
where the time goes in v1:
time: 196 us; the launch traced here: 193 us
  starting transfers between devices  87.1 us (44%)
  Pallas kernels  51.5 us (26%)
  waiting for transfers between devices  43.8 us (22%)
  local copies, waits for them, and re-layouts  6.72 us (3%)
  other arithmetic  2.54 us (1%)
    ppermute x18, starting transfers between devices, swapped(): return lax.ppermute(a, 'sp', SWAP)  29.9 us
    ppermute x12, starting transfers between devices, turned(): return lax.ppermute(a, 'tp', [(i, (i + shift) % RING) for i in range(RING)])  22.2 us
    ppermute x9, waiting for transfers between devices, spread(): far = {d: lax.ppermute(line, 'sp', second_leg(d, kind)) for d in (1, 3, 2)}  17.7 us
    ppermute x12, waiting for transfers between devices, turned(): return lax.ppermute(a, 'tp', [(i, (i + shift) % RING) for i in range(RING)])  14.3 us
    pallas_call x1, Pallas kernels, project_rest(): pl.pallas_call(rest_body, out_shape=(bf(2, 2, BATCHES, SPAN, COLS), bf(2,...  14.1 us
    ppermute x4, starting transfers between devices, from_behind(): lax.ppermute(a, 'sp', [(i, i + 2 * blocks) for i in range(32 - 2 * blocks)])  13.4 us
    ppermute x9, starting transfers between devices, spread(): near = {d: lax.ppermute(own, 'sp', first_leg(d, kind)) for d in (1, 3, 2)}  12.1 us
    pallas_call x2, Pallas kernels, project_wide(): pl.pallas_call(wide_pair_body, out_shape=bf(2, BATCHES, HALF, COLS), in_s...  11.2 us
  transfers between devices with their start and end apart: 52, of which 13 were waited for; matrix products, arithmetic and copies ran while one was open for 3% of the time, Pallas kernels for 21%

profile of v1, /device:TPU:1, one launch (start us, length us, event | category | flops | bytes accessed | tf_op | source)
XLA Modules:
  0.0 193.0 jit_solution(4906956287509493069)
XLA Ops:
  0.6 3.4 %collective-permute-start.40 = (bf16[64,256]{1,0:T(8,128)(2,1)}, bf16[64,256]{1,0:T(8,128)(2,1)S(1)}, u32[]{:S(2)}, u32[]{:S(2)}) collective-permute-start(bf16[64,256]{1,0:T(8,128)(2,1)} %bitcast.46), channel_id=1, source_target_pairs={{0,3},{1,0},{2,1},{3,2},{4,7},{5,4},{6,5},{7,6},{8,11},{9,8},{10,9... | collective-permute-start | bytes 98312 | tf_op jit(solution)/shard_map/ppermute | solution.py:58
  6.8 3.8 %collective-permute-start.20 = (bf16[2,64,256]{2,1,0:T(8,128)(2,1)}, bf16[2,64,256]{2,1,0:T(8,128)(2,1)S(1)}, u32[]{:S(2)}, u32[]{:S(2)}) collective-permute-start(bf16[2,64,256]{2,1,0:T(8,128)(2,1)} %get-tuple-element.23), channel_id=1, source_target_pairs={{0,24},{4,100},{8,0},{12,108},{16,8},{20,116},{24,16},{28,124},{32... | collective-permute-start | bytes 196616 | tf_op jit(solution)/shard_map/ppermute | solution.py:415
  12.1 2.8 %collective-permute-start.43 = (bf16[4,64,256]{2,1,0:T(8,128)(2,1)S(1)}, bf16[4,64,256]{2,1,0:T(8,128)(2,1)S(1)}, u32[]{:S(2)}, u32[]{:S(2)}) collective-permute-start(bf16[4,64,256]{2,1,0:T(8,128)(2,1)S(1)} %get-tuple-element.33), channel_id=1, source_target_pairs={{0,24},{4,28},{8,0},{12,4},{16,8},{20,12},{24,16},{28,20},{32,56},... | collective-permute-start | bytes 393224 | tf_op jit(solution)/shard_map/ppermute | solution.py:415
  23.3 5.2 %collective-permute-done.41 = bf16[4,64,256]{2,1,0:T(8,128)(2,1)S(1)} collective-permute-done((bf16[4,64,256]{2,1,0:T(8,128)(2,1)S(1)}, bf16[4,64,256]{2,1,0:T(8,128)(2,1)S(1)}, u32[]{:S(2)}, u32[]{:S(2)}) %collective-permute-start.41) | collective-permute-done | bytes 131104 | tf_op jit(solution)/shard_map/ppermute | solution.py:415
  28.5 5.7 %collective-permute-start = (bf16[3,32,2048]{2,1,0:T(8,128)(2,1)S(1)}, bf16[3,32,2048]{2,1,0:T(8,128)(2,1)S(1)}, u32[]{:S(2)}, u32[]{:S(2)}) collective-permute-start(bf16[3,32,2048]{2,1,0:T(8,128)(2,1)S(1)} %dynamic-slice_bitcast_fusion), channel_id=1, source_target_pairs={{0,4},{4,0},{8,12},{12,8},{16,20},{20,16},{24,28},{28,24},{32,36},... | collective-permute-start | bytes 1179656 | tf_op jit(solution)/shard_map/ppermute | solution.py:54
  36.2 2.4 %collective-permute-start.24 = (bf16[4,2,64,256]{3,2,1,0:T(8,128)(2,1)S(1)}, bf16[4,2,64,256]{3,2,1,0:T(8,128)(2,1)S(1)}, u32[]{:S(2)}, u32[]{:S(2)}) collective-permute-start(bf16[4,2,64,256]{3,2,1,0:T(8,128)(2,1)S(1)} %pad_maximum_fusion.2.refs_4_), channel_id=1, source_target_pairs={{0,4},{4,0},{8,12},{12,8},{16,20},{20,16},{24,28},{28,24},{32,36},... | collective-permute-start | bytes 786440 | tf_op jit(solution)/shard_map/ppermute | solution.py:54
  38.7 2.5 %collective-permute-done.22.refs_6_ = bf16[4,2,64,256]{3,2,1,0:T(8,128)(2,1)S(1)} collective-permute-done((bf16[4,2,64,256]{3,2,1,0:T(8,128)(2,1)S(1)}, bf16[4,2,64,256]{3,2,1,0:T(8,128)(2,1)S(1)}, u32[]{:S(2)}, u32[]{:S(2)}) %collective-permute-start.22) | collective-permute-done | bytes 262176 | tf_op jit(solution)/shard_map/ppermute | solution.py:417
  42.3 3.5 %collective-permute-start.26 = (bf16[4,2,64,256]{3,2,1,0:T(8,128)(2,1)S(1)}, bf16[4,2,64,256]{3,2,1,0:T(8,128)(2,1)S(1)}, u32[]{:S(2)}, u32[]{:S(2)}) collective-permute-start(bf16[4,2,64,256]{3,2,1,0:T(8,128)(2,1)S(1)} %collective-permute-done.22.refs_6_), channel_id=1, source_target_pairs={{0,4},{4,0},{8,12},{12,8},{16,20},{20,16},{24,28},{28,24},{32,36},... | collective-permute-start | bytes 786440 | tf_op jit(solution)/shard_map/ppermute | solution.py:54
  49.6 3.0 %norm_rows.1 = (bf16[3,32,2048]{2,1,0:T(8,128)(2,1)}, bf16[3,32,2048]{2,1,0:T(8,128)(2,1)}) custom-call(bf16[6,32,2048]{2,1,0:T(8,128)(2,1)} %bitcast.33, bf16[3,32,2048]{2,1,0:T(8,128)(2,1)} %copy-done.29, f32[1,2048]{1,0:T(1,128)} %bitcast.53), custom_call_target="tpu_custom_call" | custom-call | tf_op jit(solution)/shard_map/norm_rows/pallas_call | solution.py:129
  57.8 10.2 %collective-permute-done.45.refs_2_ = bf16[4,4,64,256]{3,2,1,0:T(8,128)(2,1)S(1)} collective-permute-done((bf16[4,4,64,256]{3,2,1,0:T(8,128)(2,1)S(1)}, bf16[4,4,64,256]{3,2,1,0:T(8,128)(2,1)S(1)}, u32[]{:S(2)}, u32[]{:S(2)}) %collective-permute-start.45) | collective-permute-done | bytes 524320 | tf_op jit(solution)/shard_map/ppermute | solution.py:417
  69.4 2.5 %collective-permute-done.46.refs_3_ = bf16[4,4,64,256]{3,2,1,0:T(8,128)(2,1)S(1)} collective-permute-done((bf16[4,4,64,256]{3,2,1,0:T(8,128)(2,1)S(1)}, bf16[4,4,64,256]{3,2,1,0:T(8,128)(2,1)S(1)}, u32[]{:S(2)}, u32[]{:S(2)}) %collective-permute-start.46) | collective-permute-done | bytes 524320 | tf_op jit(solution)/shard_map/ppermute | solution.py:417
  74.5 5.8 %collective-permute-done.3.refs_3_ = bf16[3,32,2048]{2,1,0:T(8,128)(2,1)S(1)} collective-permute-done((bf16[3,32,2048]{2,1,0:T(8,128)(2,1)}, bf16[3,32,2048]{2,1,0:T(8,128)(2,1)S(1)}, u32[]{:S(2)}, u32[]{:S(2)}) %collective-permute-start.3) | collective-permute-done | bytes 393248 | tf_op jit(solution)/shard_map/ppermute | solution.py:58
  80.3 3.9 %collective-permute-start.13 = (bf16[4,7,64,256]{3,2,1,0:T(8,128)(2,1)S(1)}, bf16[4,7,64,256]{3,2,1,0:T(8,128)(2,1)S(1)}, u32[]{:S(2)}, u32[]{:S(2)}) collective-permute-start(bf16[4,7,64,256]{3,2,1,0:T(8,128)(2,1)S(1)} %pad_maximum_fusion.refs_8_), channel_id=1, source_target_pairs={{0,4},{4,0},{8,12},{12,8},{16,20},{20,16},{24,28},{28,24},{32,36},... | collective-permute-start | bytes 2752520 | tf_op jit(solution)/shard_map/ppermute | solution.py:54
  86.1 3.4 %collective-permute-start.15 = (bf16[4,7,64,256]{3,2,1,0:T(8,128)(2,1)S(1)}, bf16[4,7,64,256]{3,2,1,0:T(8,128)(2,1)S(1)}, u32[]{:S(2)}, u32[]{:S(2)}) collective-permute-start(bf16[4,7,64,256]{3,2,1,0:T(8,128)(2,1)S(1)} %collective-permute-done.11.refs_10_), channel_id=1, source_target_pairs={{0,4},{4,0},{8,12},{12,8},{16,20},{20,16},{24,28},{28,24},{32,36},... | collective-permute-start | bytes 2752520 | tf_op jit(solution)/shard_map/ppermute | solution.py:54
  90.2 2.5 %collective-permute-start.16 = (bf16[4,7,64,256]{3,2,1,0:T(8,128)(2,1)}, bf16[4,7,64,256]{3,2,1,0:T(8,128)(2,1)}, u32[]{:S(2)}, u32[]{:S(2)}) collective-permute-start(bf16[4,7,64,256]{3,2,1,0:T(8,128)(2,1)} %collective-permute-done.12.refs_11_), channel_id=1, source_target_pairs={{0,4},{4,0},{8,12},{12,8},{16,20},{20,16},{24,28},{28,24},{32,36},... | collective-permute-start | bytes 2752520 | tf_op jit(solution)/shard_map/ppermute | solution.py:54
  93.6 5.9 %collective-permute-start.6 = (bf16[3,32,2048]{2,1,0:T(8,128)(2,1)}, bf16[3,32,2048]{2,1,0:T(8,128)(2,1)S(1)}, u32[]{:S(2)}, u32[]{:S(2)}) collective-permute-start(bf16[3,32,2048]{2,1,0:T(8,128)(2,1)} %get-tuple-element.18.refs_4_.refs_0_), channel_id=1, source_target_pairs={{0,3},{1,0},{2,1},{3,2},{4,7},{5,4},{6,5},{7,6},{8,11},{9,8},{10,9... | collective-permute-start | bytes 1179656 | tf_op jit(solution)/shard_map/ppermute | solution.py:58
  99.6 7.5 %collective-permute-done.6.refs_7_.refs_3_ = bf16[3,32,2048]{2,1,0:T(8,128)(2,1)S(1)} collective-permute-done((bf16[3,32,2048]{2,1,0:T(8,128)(2,1)}, bf16[3,32,2048]{2,1,0:T(8,128)(2,1)S(1)}, u32[]{:S(2)}, u32[]{:S(2)}) %collective-permute-start.6) | collective-permute-done | bytes 393248 | tf_op jit(solution)/shard_map/ppermute | solution.py:58
  107.1 2.1 %collective-permute-start.47 = (bf16[4,4,64,256]{3,2,1,0:T(8,128)(2,1)S(1)}, bf16[4,4,64,256]{3,2,1,0:T(8,128)(2,1)}, u32[]{:S(2)}, u32[]{:S(2)}) collective-permute-start(bf16[4,4,64,256]{3,2,1,0:T(8,128)(2,1)S(1)} %pad_maximum_fusion.1.refs_0_), channel_id=1, source_target_pairs={{0,4},{4,0},{8,12},{12,8},{16,20},{20,16},{24,28},{28,24},{32,36},... | collective-permute-start | bytes 1572872 | tf_op jit(solution)/shard_map/ppermute | solution.py:54
  111.7 5.6 %project_wide.2.early = bf16[2,3,128,256]{3,2,1,0:T(8,128)(2,1)} custom-call(bf16[3,32,2048]{2,1,0:T(8,128)(2,1)} %get-tuple-element.17.refs_0_, bf16[3,32,2048]{2,1,0:T(8,128)(2,1)} %copy-done.3, bf16[3,32,2048]{2,1,0:T(8,128)(2,1)} %copy-done.4, bf16[3,32,2048]{2,1,0:T(8,128)(2,1)} %copy-done.5, bf16[4,2,64,256]{3,2,1,0:T(8,128)(2,1)} %copy-done.1, ...), custom_call_target="tpu_custom_call" | custom-call | tf_op jit(solution)/shard_map/project_wide/pallas_call | solution.py:179
  117.3 5.6 %project_wide.3.late = bf16[2,3,128,256]{3,2,1,0:T(8,128)(2,1)} custom-call(bf16[3,32,2048]{2,1,0:T(8,128)(2,1)} %get-tuple-element.18.refs_4_.refs_0_, bf16[3,32,2048]{2,1,0:T(8,128)(2,1)} %copy-done.6, bf16[3,32,2048]{2,1,0:T(8,128)(2,1)} %copy-done.7, bf16[3,32,2048]{2,1,0:T(8,128)(2,1)} %copy-done.8, bf16[4,2,64,256]{3,2,1,0:T(8,128)(2,1)} %copy-done.1, ...), custom_call_target="tpu_custom_call" | custom-call | tf_op jit(solution)/shard_map/project_wide/pallas_call | solution.py:179
  122.9 3.1 %collective-permute-start.28 = (bf16[2,3,128,256]{3,2,1,0:T(8,128)(2,1)S(1)}, bf16[2,3,128,256]{3,2,1,0:T(8,128)(2,1)S(1)}, u32[]{:S(2)}, u32[]{:S(2)}) collective-permute-start(bf16[2,3,128,256]{3,2,1,0:T(8,128)(2,1)S(1)} %copy-done.9), channel_id=1, source_target_pairs={{0,8},{4,12},{8,16},{12,20},{16,24},{20,28},{24,32},{28,36},{32,40... | collective-permute-start | bytes 1179656 | tf_op jit(solution)/shard_map/ppermute | solution.py:62
  126.0 14.1 %project_rest.1 = (bf16[2,2,3,256,256]{4,3,2,1,0:T(8,128)(2,1)}, bf16[2,3,128,256]{3,2,1,0:T(8,128)(2,1)}, bf16[3,3,256,256]{3,2,1,0:T(8,128)(2,1)}) custom-call(bf16[3,32,2048]{2,1,0:T(8,128)(2,1)} %get-tuple-element.17.refs_0_, bf16[3,32,2048]{2,1,0:T(8,128)(2,1)} %copy-done.3, bf16[3,32,2048]{2,1,0:T(8,128)(2,1)} %copy-done.4, ...), custom_call_target="tpu_custom_call" | custom-call | tf_op jit(solution)/shard_map/project_rest/pallas_call | solution.py:218
  142.1 5.0 %collective-permute-start.30 = (bf16[2,3,128,256]{3,2,1,0:T(8,128)(2,1)S(1)}, bf16[2,3,128,256]{3,2,1,0:T(8,128)(2,1)S(1)}, u32[]{:S(2)}, u32[]{:S(2)}) collective-permute-start(bf16[2,3,128,256]{3,2,1,0:T(8,128)(2,1)S(1)} %copy-done.10), channel_id=1, source_target_pairs={{0,16},{4,20},{8,24},{12,28},{16,32},{20,36},{24,40},{28,44},{32,4... | collective-permute-start | bytes 1179656 | tf_op jit(solution)/shard_map/ppermute | solution.py:62
  147.1 3.4 %collective-permute-start.17 = (bf16[2,3,128,256]{3,2,1,0:T(8,128)(2,1)}, bf16[2,3,128,256]{3,2,1,0:T(8,128)(2,1)S(1)}, u32[]{:S(2)}, u32[]{:S(2)}) collective-permute-start(bf16[2,3,128,256]{3,2,1,0:T(8,128)(2,1)} %get-tuple-element.22), channel_id=1, source_target_pairs={{0,8},{4,12},{8,16},{12,20},{16,24},{20,28},{24,32},{28,36},{32,40... | collective-permute-start | bytes 1179656 | tf_op jit(solution)/shard_map/ppermute | solution.py:62
  150.6 4.6 %lay_out.1.w = bf16[4,2048,256]{2,1,0:T(8,128)(2,1)} custom-call(bf16[4,4,64,256]{3,2,1,0:T(8,128)(2,1)} %copy-done.2, bf16[4,4,64,256]{3,2,1,0:T(8,128)(2,1)} %collective-permute-done.44.refs_1_, bf16[4,4,64,256]{3,2,1,0:T(8,128)(2,1)} %copy-done.23, bf16[4,4,64,256]{3,2,1,0:T(8,128)(2,1)} %copy-done.24, ...), custom_call_target="tpu_custom_call" | custom-call | tf_op jit(solution)/shard_map/lay_out/pallas_call | solution.py:367
  155.2 3.5 %collective-permute-done.30.far_late = bf16[2,3,128,256]{3,2,1,0:T(8,128)(2,1)S(1)} collective-permute-done((bf16[2,3,128,256]{3,2,1,0:T(8,128)(2,1)S(1)}, bf16[2,3,128,256]{3,2,1,0:T(8,128)(2,1)S(1)}, u32[]{:S(2)}, u32[]{:S(2)}) %collective-permute-start.30) | collective-permute-done | bytes 393248 | tf_op jit(solution)/shard_map/ppermute | solution.py:62
  159.4 5.2 %attend_wide.1 = (f32[3,256,256]{2,1,0:T(8,128)}, f32[3,256,256]{2,1,0:T(8,128)}) custom-call(bf16[3,3,256,256]{3,2,1,0:T(8,128)(2,1)} %get-tuple-element.20.q, bf16[2,3,128,256]{3,2,1,0:T(8,128)(2,1)} %project_wide.2.early, bf16[2,3,128,256]{3,2,1,0:T(8,128)(2,1)} %project_wide.3.late, bf16[2,3,128,256]{3,2,1,0:T(8,128)(2,1)} %copy-done.25, ...), custom_call_target="tpu_custom_call" | custom-call | tf_op jit(solution)/shard_map/attend_wide/pallas_call | solution.py:291
  164.6 2.6 %collective-permute-done.17.tail = bf16[2,3,128,256]{3,2,1,0:T(8,128)(2,1)S(1)} collective-permute-done((bf16[2,3,128,256]{3,2,1,0:T(8,128)(2,1)}, bf16[2,3,128,256]{3,2,1,0:T(8,128)(2,1)S(1)}, u32[]{:S(2)}, u32[]{:S(2)}) %collective-permute-start.17) | collective-permute-done | bytes 393248 | tf_op jit(solution)/shard_map/ppermute | solution.py:62
  168.0 6.6 %attend_near.1 = (bf16[2,3,32,256]{3,2,1,0:T(8,128)(2,1)}, bf16[2,3,32,256]{3,2,1,0:T(8,128)(2,1)}, bf16[2,3,32,256]{3,2,1,0:T(8,128)(2,1)}, bf16[2,3,32,256]{3,...) custom-call(bf16[3,3,256,256]{3,2,1,0:T(8,128)(2,1)} %get-tuple-element.20.q, ...), custom_call_target="tpu_custom_call" | custom-call | tf_op jit(solution)/shard_map/attend_near/pallas_call | solution.py:342
  174.9 4.2 %collective-permute-start.32 = (bf16[2,3,32,256]{3,2,1,0:T(8,128)(2,1)}, bf16[2,3,32,256]{3,2,1,0:T(8,128)(2,1)S(1)}, u32[]{:S(2)}, u32[]{:S(2)}) collective-permute-start(bf16[2,3,32,256]{3,2,1,0:T(8,128)(2,1)} %get-tuple-element.28), channel_id=1, source_target_pairs={{0,2},{1,3},{2,0},{3,1},{4,6},{5,7},{6,4},{7,5},{8,10},{9,11},{10,... | collective-permute-start | bytes 294920 | tf_op jit(solution)/shard_map/ppermute | solution.py:58
  183.0 2.2 %collective-permute-start.36 = (bf16[3,32,256]{2,1,0:T(8,128)(2,1)S(1)}, bf16[3,32,256]{2,1,0:T(8,128)(2,1)S(1)}, u32[]{:S(2)}, u32[]{:S(2)}) collective-permute-start(bf16[3,32,256]{2,1,0:T(8,128)(2,1)S(1)} %slice_bitcast_fusion.1), channel_id=1, source_target_pairs={{0,4},{4,0},{8,12},{12,8},{16,20},{20,16},{24,28},{28,24},{32,36},... | collective-permute-start | bytes 147464 | tf_op jit(solution)/shard_map/ppermute | solution.py:54
  187.6 5.2 %finish.1 = bf16[6,32,2048]{2,1,0:T(8,128)(2,1)} custom-call(bf16[2,3,32,256]{3,2,1,0:T(8,128)(2,1)} %get-tuple-element.26.r0, bf16[2,3,32,256]{3,2,1,0:T(8,128)(2,1)} %copy-done.31, bf16[2,3,32,256]{3,2,1,0:T(8,128)(2,1)} %copy-done.32, bf16[2,3,32,256]{3,2,1,0:T(8,128)(2,1)} %copy-done.33, bf16[3,32,256]{2,1,0:T(8,128)(2,1)} %copy-done.34, ...), custom_call_target="tpu_custom_call" | custom-call | tf_op jit(solution)/shard_map/finish/pallas_call | solution.py:396
  (169 shorter events, 44.7 us)
Async XLA Ops:
  0.6 10.0 %collective-permute-start.40 = (bf16[64,256]{1,0:T(8,128)(2,1)}, bf16[64,256]{1,0:T(8,128)(2,1)S(1)}, u32[]{:S(2)}, u32[]{:S(2)}) collective-permute-start(bf16[64,256]{1,0:T(8,128)(2,1)} %bitcast.46), channel_id=1, source_target_pairs={{0,3},{1,0},{2,1},{3,2},{4,7},{5,4},{6,5},{7,6},{8,11},{9,8},{10,9... | collective-permute-start | bytes 98312 | tf_op jit(solution)/shard_map/ppermute | solution.py:58
  15.2 18.9 %collective-permute-start.9 = (bf16[7,64,256]{2,1,0:T(8,128)(2,1)}, bf16[7,64,256]{2,1,0:T(8,128)(2,1)S(1)}, u32[]{:S(2)}, u32[]{:S(2)}) collective-permute-start(bf16[7,64,256]{2,1,0:T(8,128)(2,1)} %get-tuple-element.19), channel_id=1, source_target_pairs={{0,24},{4,100},{8,0},{12,108},{16,8},{20,116},{24,16},{28,124},{32... | collective-permute-start | bytes 688136 | tf_op jit(solution)/shard_map/ppermute | solution.py:415
  17.2 17.8 %collective-permute-start.8 = (bf16[7,64,256]{2,1,0:T(8,128)(2,1)}, bf16[7,64,256]{2,1,0:T(8,128)(2,1)S(1)}, u32[]{:S(2)}, u32[]{:S(2)}) collective-permute-start(bf16[7,64,256]{2,1,0:T(8,128)(2,1)} %get-tuple-element.19), channel_id=1, source_target_pairs={{0,16},{4,68},{8,24},{12,76},{16,0},{20,84},{24,8},{28,92},{32,48}... | collective-permute-start | bytes 688136 | tf_op jit(solution)/shard_map/ppermute | solution.py:415
  19.0 17.2 %collective-permute-start.7 = (bf16[7,64,256]{2,1,0:T(8,128)(2,1)}, bf16[7,64,256]{2,1,0:T(8,128)(2,1)S(1)}, u32[]{:S(2)}, u32[]{:S(2)}) collective-permute-start(bf16[7,64,256]{2,1,0:T(8,128)(2,1)} %get-tuple-element.19), channel_id=1, source_target_pairs={{0,8},{4,36},{8,16},{12,44},{16,24},{20,52},{24,0},{28,60},{32,40}... | collective-permute-start | bytes 688136 | tf_op jit(solution)/shard_map/ppermute | solution.py:415
  19.9 8.6 %collective-permute-start.41 = (bf16[4,64,256]{2,1,0:T(8,128)(2,1)S(1)}, bf16[4,64,256]{2,1,0:T(8,128)(2,1)S(1)}, u32[]{:S(2)}, u32[]{:S(2)}) collective-permute-start(bf16[4,64,256]{2,1,0:T(8,128)(2,1)S(1)} %get-tuple-element.33), channel_id=1, source_target_pairs={{0,8},{4,12},{8,16},{12,20},{16,24},{20,28},{24,0},{28,4},{32,40},... | collective-permute-start | bytes 393224 | tf_op jit(solution)/shard_map/ppermute | solution.py:415
  20.7 17.9 %collective-permute-start.21 = (bf16[4,2,64,256]{3,2,1,0:T(8,128)(2,1)S(1)}, bf16[4,2,64,256]{3,2,1,0:T(8,128)(2,1)S(1)}, u32[]{:S(2)}, u32[]{:S(2)}) collective-permute-start(bf16[4,2,64,256]{3,2,1,0:T(8,128)(2,1)S(1)} %pad_maximum_fusion.2.refs_4_), channel_id=1, source_target_pairs={{0,32},{4,12},{8,40},{12,20},{16,48},{20,28},{24,56},{28,4},{32,64... | collective-permute-start | bytes 786440 | tf_op jit(solution)/shard_map/ppermute | solution.py:417
  28.5 18.4 %collective-permute-start = (bf16[3,32,2048]{2,1,0:T(8,128)(2,1)S(1)}, bf16[3,32,2048]{2,1,0:T(8,128)(2,1)S(1)}, u32[]{:S(2)}, u32[]{:S(2)}) collective-permute-start(bf16[3,32,2048]{2,1,0:T(8,128)(2,1)S(1)} %dynamic-slice_bitcast_fusion), channel_id=1, source_target_pairs={{0,4},{4,0},{8,12},{12,8},{16,20},{20,16},{24,28},{28,24},{32,36},... | collective-permute-start | bytes 1179656 | tf_op jit(solution)/shard_map/ppermute | solution.py:54
  36.2 9.7 %collective-permute-start.24 = (bf16[4,2,64,256]{3,2,1,0:T(8,128)(2,1)S(1)}, bf16[4,2,64,256]{3,2,1,0:T(8,128)(2,1)S(1)}, u32[]{:S(2)}, u32[]{:S(2)}) collective-permute-start(bf16[4,2,64,256]{3,2,1,0:T(8,128)(2,1)S(1)} %pad_maximum_fusion.2.refs_4_), channel_id=1, source_target_pairs={{0,4},{4,0},{8,12},{12,8},{16,20},{20,16},{24,28},{28,24},{32,36},... | collective-permute-start | bytes 786440 | tf_op jit(solution)/shard_map/ppermute | solution.py:54
  38.5 10.1 %collective-permute-start.25 = (bf16[4,2,64,256]{3,2,1,0:T(8,128)(2,1)S(1)}, bf16[4,2,64,256]{3,2,1,0:T(8,128)(2,1)S(1)}, u32[]{:S(2)}, u32[]{:S(2)}) collective-permute-start(bf16[4,2,64,256]{3,2,1,0:T(8,128)(2,1)S(1)} %collective-permute-done.21.refs_5_), channel_id=1, source_target_pairs={{0,4},{4,0},{8,12},{12,8},{16,20},{20,16},{24,28},{28,24},{32,36},... | collective-permute-start | bytes 786440 | tf_op jit(solution)/shard_map/ppermute | solution.py:54
  41.2 14.7 %collective-permute-start.44 = (bf16[4,4,64,256]{3,2,1,0:T(8,128)(2,1)S(1)}, bf16[4,4,64,256]{3,2,1,0:T(8,128)(2,1)}, u32[]{:S(2)}, u32[]{:S(2)}) collective-permute-start(bf16[4,4,64,256]{3,2,1,0:T(8,128)(2,1)S(1)} %pad_maximum_fusion.1.refs_0_), channel_id=1, source_target_pairs={{0,32},{4,36},{8,40},{12,44},{16,48},{20,52},{24,56},{28,60},{32,6... | collective-permute-start | bytes 1572872 | tf_op jit(solution)/shard_map/ppermute | solution.py:417
  45.8 22.2 %collective-permute-start.45 = (bf16[4,4,64,256]{3,2,1,0:T(8,128)(2,1)S(1)}, bf16[4,4,64,256]{3,2,1,0:T(8,128)(2,1)S(1)}, u32[]{:S(2)}, u32[]{:S(2)}) collective-permute-start(bf16[4,4,64,256]{3,2,1,0:T(8,128)(2,1)S(1)} %pad_maximum_fusion.1.refs_0_), channel_id=1, source_target_pairs={{0,64},{4,68},{8,72},{12,76},{16,80},{20,84},{24,88},{28,92},{32,9... | collective-permute-start | bytes 1572872 | tf_op jit(solution)/shard_map/ppermute | solution.py:417
  46.9 25.0 %collective-permute-start.46 = (bf16[4,4,64,256]{3,2,1,0:T(8,128)(2,1)S(1)}, bf16[4,4,64,256]{3,2,1,0:T(8,128)(2,1)S(1)}, u32[]{:S(2)}, u32[]{:S(2)}) collective-permute-start(bf16[4,4,64,256]{3,2,1,0:T(8,128)(2,1)S(1)} %pad_maximum_fusion.1.refs_0_), channel_id=1, source_target_pairs={{0,96},{4,100},{8,104},{12,108},{16,112},{20,116},{24,120},{28,124... | collective-permute-start | bytes 1572872 | tf_op jit(solution)/shard_map/ppermute | solution.py:417
  49.5 34.8 %collective-permute-start.10 = (bf16[4,7,64,256]{3,2,1,0:T(8,128)(2,1)S(1)}, bf16[4,7,64,256]{3,2,1,0:T(8,128)(2,1)S(1)}, u32[]{:S(2)}, u32[]{:S(2)}) collective-permute-start(bf16[4,7,64,256]{3,2,1,0:T(8,128)(2,1)S(1)} %pad_maximum_fusion.refs_8_), channel_id=1, source_target_pairs={{0,32},{4,12},{8,40},{12,20},{16,48},{20,28},{24,56},{28,4},{32,64... | collective-permute-start | bytes 2752520 | tf_op jit(solution)/shard_map/ppermute | solution.py:417
  52.6 19.8 %collective-permute-start.1 = (bf16[3,32,2048]{2,1,0:T(8,128)(2,1)}, bf16[3,32,2048]{2,1,0:T(8,128)(2,1)S(1)}, u32[]{:S(2)}, u32[]{:S(2)}) collective-permute-start(bf16[3,32,2048]{2,1,0:T(8,128)(2,1)} %get-tuple-element.17.refs_0_), channel_id=1, source_target_pairs={{0,1},{1,2},{2,3},{3,0},{4,5},{5,6},{6,7},{7,4},{8,9},{9,10},{10,1... | collective-permute-start | bytes 1179656 | tf_op jit(solution)/shard_map/ppermute | solution.py:58
  56.0 18.6 %collective-permute-start.2 = (bf16[3,32,2048]{2,1,0:T(8,128)(2,1)}, bf16[3,32,2048]{2,1,0:T(8,128)(2,1)S(1)}, u32[]{:S(2)}, u32[]{:S(2)}) collective-permute-start(bf16[3,32,2048]{2,1,0:T(8,128)(2,1)} %get-tuple-element.17.refs_0_), channel_id=1, source_target_pairs={{0,2},{1,3},{2,0},{3,1},{4,6},{5,7},{6,4},{7,5},{8,10},{9,11},{10,... | collective-permute-start | bytes 1179656 | tf_op jit(solution)/shard_map/ppermute | solution.py:58
  68.0 18.1 %collective-permute-start.11 = (bf16[4,7,64,256]{3,2,1,0:T(8,128)(2,1)S(1)}, bf16[4,7,64,256]{3,2,1,0:T(8,128)(2,1)S(1)}, u32[]{:S(2)}, u32[]{:S(2)}) collective-permute-start(bf16[4,7,64,256]{3,2,1,0:T(8,128)(2,1)S(1)} %pad_maximum_fusion.refs_8_), channel_id=1, source_target_pairs={{0,64},{4,20},{8,72},{12,28},{16,80},{20,4},{24,88},{28,12},{32,96... | collective-permute-start | bytes 2752520 | tf_op jit(solution)/shard_map/ppermute | solution.py:417
  72.0 18.2 %collective-permute-start.12 = (bf16[4,7,64,256]{3,2,1,0:T(8,128)(2,1)S(1)}, bf16[4,7,64,256]{3,2,1,0:T(8,128)(2,1)}, u32[]{:S(2)}, u32[]{:S(2)}) collective-permute-start(bf16[4,7,64,256]{3,2,1,0:T(8,128)(2,1)S(1)} %pad_maximum_fusion.refs_8_), channel_id=1, source_target_pairs={{0,96},{4,28},{8,104},{12,4},{16,112},{20,12},{24,120},{28,20},{32... | collective-permute-start | bytes 2752520 | tf_op jit(solution)/shard_map/ppermute | solution.py:417
  74.5 9.8 %collective-permute-start.4 = (bf16[3,32,2048]{2,1,0:T(8,128)(2,1)}, bf16[3,32,2048]{2,1,0:T(8,128)(2,1)S(1)}, u32[]{:S(2)}, u32[]{:S(2)}) collective-permute-start(bf16[3,32,2048]{2,1,0:T(8,128)(2,1)} %get-tuple-element.18.refs_4_.refs_0_), channel_id=1, source_target_pairs={{0,1},{1,2},{2,3},{3,0},{4,5},{5,6},{6,7},{7,4},{8,9},{9,10},{10,1... | collective-permute-start | bytes 1179656 | tf_op jit(solution)/shard_map/ppermute | solution.py:58
  80.3 28.9 %collective-permute-start.13 = (bf16[4,7,64,256]{3,2,1,0:T(8,128)(2,1)S(1)}, bf16[4,7,64,256]{3,2,1,0:T(8,128)(2,1)S(1)}, u32[]{:S(2)}, u32[]{:S(2)}) collective-permute-start(bf16[4,7,64,256]{3,2,1,0:T(8,128)(2,1)S(1)} %pad_maximum_fusion.refs_8_), channel_id=1, source_target_pairs={{0,4},{4,0},{8,12},{12,8},{16,20},{20,16},{24,28},{28,24},{32,36},... | collective-permute-start | bytes 2752520 | tf_op jit(solution)/shard_map/ppermute | solution.py:54
  84.3 25.0 %collective-permute-start.14 = (bf16[4,7,64,256]{3,2,1,0:T(8,128)(2,1)S(1)}, bf16[4,7,64,256]{3,2,1,0:T(8,128)(2,1)S(1)}, u32[]{:S(2)}, u32[]{:S(2)}) collective-permute-start(bf16[4,7,64,256]{3,2,1,0:T(8,128)(2,1)S(1)} %collective-permute-done.10.refs_9_), channel_id=1, source_target_pairs={{0,4},{4,0},{8,12},{12,8},{16,20},{20,16},{24,28},{28,24},{32,36},... | collective-permute-start | bytes 2752520 | tf_op jit(solution)/shard_map/ppermute | solution.py:54
  84.4 9.3 %collective-permute-start.5 = (bf16[3,32,2048]{2,1,0:T(8,128)(2,1)}, bf16[3,32,2048]{2,1,0:T(8,128)(2,1)S(1)}, u32[]{:S(2)}, u32[]{:S(2)}) collective-permute-start(bf16[3,32,2048]{2,1,0:T(8,128)(2,1)} %get-tuple-element.18.refs_4_.refs_0_), channel_id=1, source_target_pairs={{0,2},{1,3},{2,0},{3,1},{4,6},{5,7},{6,4},{7,5},{8,10},{9,11},{10,... | collective-permute-start | bytes 1179656 | tf_op jit(solution)/shard_map/ppermute | solution.py:58
  86.1 23.6 %collective-permute-start.15 = (bf16[4,7,64,256]{3,2,1,0:T(8,128)(2,1)S(1)}, bf16[4,7,64,256]{3,2,1,0:T(8,128)(2,1)S(1)}, u32[]{:S(2)}, u32[]{:S(2)}) collective-permute-start(bf16[4,7,64,256]{3,2,1,0:T(8,128)(2,1)S(1)} %collective-permute-done.11.refs_10_), channel_id=1, source_target_pairs={{0,4},{4,0},{8,12},{12,8},{16,20},{20,16},{24,28},{28,24},{32,36},... | collective-permute-start | bytes 2752520 | tf_op jit(solution)/shard_map/ppermute | solution.py:54
  90.2 32.7 %collective-permute-start.16 = (bf16[4,7,64,256]{3,2,1,0:T(8,128)(2,1)}, bf16[4,7,64,256]{3,2,1,0:T(8,128)(2,1)}, u32[]{:S(2)}, u32[]{:S(2)}) collective-permute-start(bf16[4,7,64,256]{3,2,1,0:T(8,128)(2,1)} %collective-permute-done.12.refs_11_), channel_id=1, source_target_pairs={{0,4},{4,0},{8,12},{12,8},{16,20},{20,16},{24,28},{28,24},{32,36},... | collective-permute-start | bytes 2752520 | tf_op jit(solution)/shard_map/ppermute | solution.py:54
  93.6 13.4 %collective-permute-start.6 = (bf16[3,32,2048]{2,1,0:T(8,128)(2,1)}, bf16[3,32,2048]{2,1,0:T(8,128)(2,1)S(1)}, u32[]{:S(2)}, u32[]{:S(2)}) collective-permute-start(bf16[3,32,2048]{2,1,0:T(8,128)(2,1)} %get-tuple-element.18.refs_4_.refs_0_), channel_id=1, source_target_pairs={{0,3},{1,0},{2,1},{3,2},{4,7},{5,4},{6,5},{7,6},{8,11},{9,8},{10,9... | collective-permute-start | bytes 1179656 | tf_op jit(solution)/shard_map/ppermute | solution.py:58
  107.1 33.0 %collective-permute-start.47 = (bf16[4,4,64,256]{3,2,1,0:T(8,128)(2,1)S(1)}, bf16[4,4,64,256]{3,2,1,0:T(8,128)(2,1)}, u32[]{:S(2)}, u32[]{:S(2)}) collective-permute-start(bf16[4,4,64,256]{3,2,1,0:T(8,128)(2,1)S(1)} %pad_maximum_fusion.1.refs_0_), channel_id=1, source_target_pairs={{0,4},{4,0},{8,12},{12,8},{16,20},{20,16},{24,28},{28,24},{32,36},... | collective-permute-start | bytes 1572872 | tf_op jit(solution)/shard_map/ppermute | solution.py:54
  109.2 32.9 %collective-permute-start.48 = (bf16[4,4,64,256]{3,2,1,0:T(8,128)(2,1)}, bf16[4,4,64,256]{3,2,1,0:T(8,128)(2,1)}, u32[]{:S(2)}, u32[]{:S(2)}) collective-permute-start(bf16[4,4,64,256]{3,2,1,0:T(8,128)(2,1)} %collective-permute-done.44.refs_1_), channel_id=1, source_target_pairs={{0,4},{4,0},{8,12},{12,8},{16,20},{20,16},{24,28},{28,24},{32,36},... | collective-permute-start | bytes 1572872 | tf_op jit(solution)/shard_map/ppermute | solution.py:54
  109.3 37.8 %collective-permute-start.49 = (bf16[4,4,64,256]{3,2,1,0:T(8,128)(2,1)S(1)}, bf16[4,4,64,256]{3,2,1,0:T(8,128)(2,1)}, u32[]{:S(2)}, u32[]{:S(2)}) collective-permute-start(bf16[4,4,64,256]{3,2,1,0:T(8,128)(2,1)S(1)} %collective-permute-done.45.refs_2_), channel_id=1, source_target_pairs={{0,4},{4,0},{8,12},{12,8},{16,20},{20,16},{24,28},{28,24},{32,36},... | collective-permute-start | bytes 1572872 | tf_op jit(solution)/shard_map/ppermute | solution.py:54
  111.4 39.2 %collective-permute-start.50 = (bf16[4,4,64,256]{3,2,1,0:T(8,128)(2,1)S(1)}, bf16[4,4,64,256]{3,2,1,0:T(8,128)(2,1)}, u32[]{:S(2)}, u32[]{:S(2)}) collective-permute-start(bf16[4,4,64,256]{3,2,1,0:T(8,128)(2,1)S(1)} %collective-permute-done.46.refs_3_), channel_id=1, source_target_pairs={{0,4},{4,0},{8,12},{12,8},{16,20},{20,16},{24,28},{28,24},{32,36},... | collective-permute-start | bytes 1572872 | tf_op jit(solution)/shard_map/ppermute | solution.py:54
  122.9 32.2 %collective-permute-start.28 = (bf16[2,3,128,256]{3,2,1,0:T(8,128)(2,1)S(1)}, bf16[2,3,128,256]{3,2,1,0:T(8,128)(2,1)S(1)}, u32[]{:S(2)}, u32[]{:S(2)}) collective-permute-start(bf16[2,3,128,256]{3,2,1,0:T(8,128)(2,1)S(1)} %copy-done.9), channel_id=1, source_target_pairs={{0,8},{4,12},{8,16},{12,20},{16,24},{20,28},{24,32},{28,36},{32,40... | collective-permute-start | bytes 1179656 | tf_op jit(solution)/shard_map/ppermute | solution.py:62
  140.1 15.0 %collective-permute-start.29 = (bf16[2,3,128,256]{3,2,1,0:T(8,128)(2,1)S(1)}, bf16[2,3,128,256]{3,2,1,0:T(8,128)(2,1)S(1)}, u32[]{:S(2)}, u32[]{:S(2)}) collective-permute-start(bf16[2,3,128,256]{3,2,1,0:T(8,128)(2,1)S(1)} %copy-done.10), channel_id=1, source_target_pairs={{0,8},{4,12},{8,16},{12,20},{16,24},{20,28},{24,32},{28,36},{32,40... | collective-permute-start | bytes 1179656 | tf_op jit(solution)/shard_map/ppermute | solution.py:62
  142.1 16.6 %collective-permute-start.30 = (bf16[2,3,128,256]{3,2,1,0:T(8,128)(2,1)S(1)}, bf16[2,3,128,256]{3,2,1,0:T(8,128)(2,1)S(1)}, u32[]{:S(2)}, u32[]{:S(2)}) collective-permute-start(bf16[2,3,128,256]{3,2,1,0:T(8,128)(2,1)S(1)} %copy-done.10), channel_id=1, source_target_pairs={{0,16},{4,20},{8,24},{12,28},{16,32},{20,36},{24,40},{28,44},{32,4... | collective-permute-start | bytes 1179656 | tf_op jit(solution)/shard_map/ppermute | solution.py:62
  147.1 20.1 %collective-permute-start.17 = (bf16[2,3,128,256]{3,2,1,0:T(8,128)(2,1)}, bf16[2,3,128,256]{3,2,1,0:T(8,128)(2,1)S(1)}, u32[]{:S(2)}, u32[]{:S(2)}) collective-permute-start(bf16[2,3,128,256]{3,2,1,0:T(8,128)(2,1)} %get-tuple-element.22), channel_id=1, source_target_pairs={{0,8},{4,12},{8,16},{12,20},{16,24},{20,28},{24,32},{28,36},{32,40... | collective-permute-start | bytes 1179656 | tf_op jit(solution)/shard_map/ppermute | solution.py:62
  (58 other events, 1171.4 us)

commit v2 on v1

--- a/solution.py
+++ b/solution.py
@@ -159,17 +159,13 @@
 
 def wide_pair_body(*refs):
     pieces, lines = refs[:4], refs[4:12]
-    out, x_all, w_all, x_sems, k_sems, v_sems = refs[12:]
-    groups = [row_copies(pieces, 0, x_all, x_sems)]
-    groups += [shard_copies(lines, 0, 1, w_all, k_sems, 0), shard_copies(lines, 1, 1, w_all, v_sems, 0)]
-    for group in groups:
-        for c in group:
-            c.start()
-    for c in groups[0]:
+    out, x_all, w_all, x_sems, w_sems = refs[12:]
+    copies = row_copies(pieces, 0, x_all, x_sems) + shard_copies(lines, 0, 2, w_all, w_sems, 0)
+    for c in copies:
+        c.start()
+    for c in copies:
         c.wait()
     for role in range(2):
-        for c in groups[1 + role]:
-            c.wait()
         x = x_all[...].reshape(BATCHES * HALF, WIDTH)
         y = jnp.dot(x, w_all[role], preferred_element_type=jnp.float32)
         out[role] = y.astype(jnp.bfloat16).reshape(BATCHES, HALF, COLS)
@@ -180,7 +176,7 @@
         wide_pair_body, out_shape=bf(2, BATCHES, HALF, COLS), in_specs=[ANY] * 12, out_specs=VMEM,
         scratch_shapes=[
             pltpu.VMEM((BATCHES, HALF, WIDTH), jnp.bfloat16), pltpu.VMEM((2, WIDTH, COLS), jnp.bfloat16),
-            pltpu.SemaphoreType.DMA((1, RING)), pltpu.SemaphoreType.DMA((32,)), pltpu.SemaphoreType.DMA((32,)),
+            pltpu.SemaphoreType.DMA((1, RING)), pltpu.SemaphoreType.DMA((32,)),
         ],
         compiler_params=PARAMS, name="project_wide",
     )(*pieces, *lines)
@@ -188,19 +184,22 @@
 
 def rest_body(*refs):
     early, late, lines = refs[:4], refs[4:8], refs[8:16]
-    near, near_tail, queries, x_all, w_all, x_sems, a_sems, b_sems, c_sems = refs[16:]
+    near, near_tail, queries, x_all, w_all, x_sems, a_sems, b_sems, c_sems, d_sems = refs[16:]
     rows = row_copies(early, 0, x_all, x_sems) + row_copies(late, HALF, x_all, x_sems)
     groups = {
         0: rows + shard_copies(lines, 0, 1, w_all, a_sems, 0),
-        1: shard_copies(lines, 1, 3, w_all, b_sems, 0),
-        4: shard_copies(lines, 4, 3, w_all, c_sems, 0),
+        1: shard_copies(lines, 1, 2, w_all, b_sems, 0),
+        3: shard_copies(lines, 3, 2, w_all, c_sems, 0),
+        5: shard_copies(lines, 5, 2, w_all, d_sems, 0),
     }
-    for group in groups.values():
-        for c in group:
-            c.start()
+    following = {0: 1, 1: 3, 3: 5}
+    for c in groups[0]:
+        c.start()
     for m in range(NEAR + GROUPS):
         for c in groups.get(m, ()):
             c.wait()
+        for c in groups.get(following.get(m), ()):
+            c.start()
         x = x_all[...].reshape(BATCHES * SPAN, WIDTH)
         y = jnp.dot(x, w_all[m], preferred_element_type=jnp.float32)
         y = y.astype(jnp.bfloat16).reshape(BATCHES, SPAN, COLS)
@@ -224,7 +223,7 @@
         scratch_shapes=[
             pltpu.VMEM((BATCHES, SPAN, WIDTH), jnp.bfloat16), pltpu.VMEM((NEAR + GROUPS, WIDTH, COLS), jnp.bfloat16),
             pltpu.SemaphoreType.DMA((2, RING)), pltpu.SemaphoreType.DMA((32,)), pltpu.SemaphoreType.DMA((32,)),
-            pltpu.SemaphoreType.DMA((32,)),
+            pltpu.SemaphoreType.DMA((32,)), pltpu.SemaphoreType.DMA((32,)),
         ],
         compiler_params=PARAMS, name="project_rest",
     )(*early, *late, *lines)
@@ -370,40 +369,41 @@
     )(*lines)
 
 
-def final_body(r0, r1, r2, r3, s0, s1, s2, s3, w, out, held, w_all, sems):
-    core = lax.axis_index("sp") % 2
+def final_body(r0, r1, r2, r3, w, keep, send, w_all, sems):
     part = WIDTH // RING
+    half = BATCHES * PIECE
     copies = [
         pltpu.make_async_copy(w.at[:, pl.ds(n * part, part)], w_all.at[n], sems.at[n]) for n in range(RING)
     ]
     for c in copies:
         c.start()
-    for d, (r, s) in enumerate(((r0, s0), (r1, s1), (r2, s2), (r3, s3))):
-        held[d, core] = r[0].reshape(BATCHES * PIECE, COLS)
-        held[d, 1 - core] = s[...].reshape(BATCHES * PIECE, COLS)
+    rows = [r[...].reshape(2 * half, COLS) for r in (r0, r1, r2, r3)]
     for n in range(RING):
         cols = slice(n * part, (n + 1) * part)
         copies[n].wait()
         acc = None
         for d in range(RING):
-            a = held[d].reshape(2 * BATCHES * PIECE, COLS)
-            y = lax.dot_general(a, w_all[n, d], (((1,), (1,)), ((), ())), preferred_element_type=jnp.float32)
+            y = lax.dot_general(rows[d], w_all[n, d], (((1,), (1,)), ((), ())), preferred_element_type=jnp.float32)
             acc = y if acc is None else acc + y
-        out[:, :, cols] = acc.astype(jnp.bfloat16).reshape(2 * BATCHES, PIECE, part)
-
-
-def finish(received, crossed, w):
-    mixed = pl.pallas_call(
-        final_body, out_shape=bf(2 * BATCHES, PIECE, WIDTH),
-        in_specs=[VMEM] * 8 + [ANY], out_specs=VMEM,
+        acc = acc.astype(jnp.bfloat16)
+        keep[:, :, cols] = acc[:half].reshape(BATCHES, PIECE, part)
+        send[:, :, cols] = acc[half:].reshape(BATCHES, PIECE, part)
+
+
+def finish(received, w):
+    shape = bf(BATCHES, PIECE, WIDTH)
+    return pl.pallas_call(
+        final_body, out_shape=(shape, shape), in_specs=[VMEM] * 4 + [ANY], out_specs=(VMEM,) * 2,
         scratch_shapes=[
-            pltpu.VMEM((RING, 2, BATCHES * PIECE, COLS), jnp.bfloat16),
-            pltpu.VMEM((RING, RING, WIDTH // RING, COLS), jnp.bfloat16),
-            pltpu.SemaphoreType.DMA((RING,)),
+            pltpu.VMEM((RING, RING, WIDTH // RING, COLS), jnp.bfloat16), pltpu.SemaphoreType.DMA((RING,)),
         ],
         compiler_params=PARAMS, name="finish",
-    )(*received, *crossed, w)
-    return jnp.transpose(mixed, (1, 0, 2))
+    )(*received, w)
+
+
+def joined_cores(mine, theirs):
+    core = lax.axis_index("sp") % 2
+    return jnp.where(core == 0, jnp.concatenate((mine, theirs), 0), jnp.concatenate((theirs, mine), 0))
 
 
 def ring_of(a):
@@ -443,14 +443,11 @@
     *combined, kept, sent = attend_near(queries, near, near_tail, wide_out, wide_logs)
 
     received = [combined[0]] + [turned(combined[d], d) for d in (1, 2, 3)]
-    crossed = [swapped(a[1]) for a in received]
-    mixed = finish(received, crossed, laid)
-
-    came = swapped(sent)
-    low = jnp.where(core == 0, kept, came)
-    high = jnp.where(core == 0, came, kept)
-    log_weight = jnp.concatenate((low, high), 0).reshape(2 * BATCHES, 2, BLOCK)
-    return (mixed, jnp.transpose(log_weight, (2, 0, 1)))
+    mixed_mine, mixed_sent = finish(received, laid)
+    mixed = joined_cores(mixed_mine, swapped(mixed_sent))
+
+    log_weight = joined_cores(kept, swapped(sent)).reshape(2 * BATCHES, 2, BLOCK)
+    return (jnp.transpose(mixed, (1, 0, 2)), jnp.transpose(log_weight, (2, 0, 1)))
 
 
 def solution(mesh):

time: 196 us -> 187 us (0.954)
  the two profiles are of different devices: /device:TPU:1 before, /device:TPU:97 now
where the time goes in v2:
time: 187 us; the launch traced here: 186 us
  starting transfers between devices  70.9 us (38%)
  waiting for transfers between devices  58.6 us (31%)
  Pallas kernels  46 us (25%)
  local copies, waits for them, and re-layouts  5.39 us (3%)
  other arithmetic  3.97 us (2%)
    ppermute x15, starting transfers between devices, swapped(): return lax.ppermute(a, 'sp', SWAP)  23.6 us
    ppermute x12, waiting for transfers between devices, turned(): return lax.ppermute(a, 'tp', [(i, (i + shift) % RING) for i in range(RING)])  19.4 us
    ppermute x9, waiting for transfers between devices, spread(): far = {d: lax.ppermute(line, 'sp', second_leg(d, kind)) for d in (1, 3, 2)}  18.9 us
    ppermute x4, waiting for transfers between devices, from_behind(): lax.ppermute(a, 'sp', [(i, i + 2 * blocks) for i in range(32 - 2 * blocks)])  18.8 us
    ppermute x12, starting transfers between devices, turned(): return lax.ppermute(a, 'tp', [(i, (i + shift) % RING) for i in range(RING)])  16 us
    pallas_call x1, Pallas kernels, project_rest(): pl.pallas_call(rest_body, out_shape=(bf(2, 2, BATCHES, SPAN, COLS), bf(2,...  11.7 us
    ppermute x4, starting transfers between devices, from_behind(): lax.ppermute(a, 'sp', [(i, i + 2 * blocks) for i in range(32 - 2 * blocks)])  11.3 us
    ppermute x9, starting transfers between devices, spread(): near = {d: lax.ppermute(own, 'sp', first_leg(d, kind)) for d in (1, 3, 2)}  11 us
  transfers between devices with their start and end apart: 49, of which 11 were waited for; matrix products, arithmetic and copies ran while one was open for 2% of the time, Pallas kernels for 22%

profile of v2, /device:TPU:97, one launch (start us, length us, event | category | flops | bytes accessed | tf_op | source)
XLA Modules:
  0.0 186.1 jit_solution(18307922410730465080)
XLA Ops:
  0.6 2.5 %collective-permute-start.36 = (bf16[64,256]{1,0:T(8,128)(2,1)}, bf16[64,256]{1,0:T(8,128)(2,1)S(1)}, u32[]{:S(2)}, u32[]{:S(2)}) collective-permute-start(bf16[64,256]{1,0:T(8,128)(2,1)} %bitcast.38), channel_id=1, source_target_pairs={{0,3},{1,0},{2,1},{3,2},{4,7},{5,4},{6,5},{7,6},{8,11},{9,8},{10,9... | collective-permute-start | bytes 98312 | tf_op jit(solution)/shard_map/ppermute | solution.py:58
  6.3 2.4 %collective-permute-start.18 = (bf16[2,64,256]{2,1,0:T(8,128)(2,1)}, bf16[2,64,256]{2,1,0:T(8,128)(2,1)S(1)}, u32[]{:S(2)}, u32[]{:S(2)}) collective-permute-start(bf16[2,64,256]{2,1,0:T(8,128)(2,1)} %get-tuple-element.25), channel_id=1, source_target_pairs={{0,8},{4,36},{8,16},{12,44},{16,24},{20,52},{24,0},{28,60},{32,40}... | collective-permute-start | bytes 196616 | tf_op jit(solution)/shard_map/ppermute | solution.py:415
  9.5 2.8 %collective-permute-start.39 = (bf16[4,64,256]{2,1,0:T(8,128)(2,1)S(1)}, bf16[4,64,256]{2,1,0:T(8,128)(2,1)S(1)}, u32[]{:S(2)}, u32[]{:S(2)}) collective-permute-start(bf16[4,64,256]{2,1,0:T(8,128)(2,1)S(1)} %get-tuple-element.37), channel_id=1, source_target_pairs={{0,24},{4,28},{8,0},{12,4},{16,8},{20,12},{24,16},{28,20},{32,56},... | collective-permute-start | bytes 393224 | tf_op jit(solution)/shard_map/ppermute | solution.py:415
  23.0 6.4 %collective-permute-start = (bf16[3,32,2048]{2,1,0:T(8,128)(2,1)S(1)}, bf16[3,32,2048]{2,1,0:T(8,128)(2,1)S(1)}, u32[]{:S(2)}, u32[]{:S(2)}) collective-permute-start(bf16[3,32,2048]{2,1,0:T(8,128)(2,1)S(1)} %dynamic-slice_bitcast_fusion), channel_id=1, source_target_pairs={{0,4},{4,0},{8,12},{12,8},{16,20},{20,16},{24,28},{28,24},{32,36},... | collective-permute-start | bytes 1179656 | tf_op jit(solution)/shard_map/ppermute | solution.py:54
  29.3 3.3 %collective-permute-start.23 = (bf16[4,2,64,256]{3,2,1,0:T(8,128)(2,1)S(1)}, bf16[4,2,64,256]{3,2,1,0:T(8,128)(2,1)S(1)}, u32[]{:S(2)}, u32[]{:S(2)}) collective-permute-start(bf16[4,2,64,256]{3,2,1,0:T(8,128)(2,1)S(1)} %pad_maximum_fusion.2.refs_4_), channel_id=1, source_target_pairs={{0,96},{4,28},{8,104},{12,4},{16,112},{20,12},{24,120},{28,20},{32... | collective-permute-start | bytes 786440 | tf_op jit(solution)/shard_map/ppermute | solution.py:417
  36.0 2.1 %collective-permute-start.26 = (bf16[4,2,64,256]{3,2,1,0:T(8,128)(2,1)S(1)}, bf16[4,2,64,256]{3,2,1,0:T(8,128)(2,1)S(1)}, u32[]{:S(2)}, u32[]{:S(2)}) collective-permute-start(bf16[4,2,64,256]{3,2,1,0:T(8,128)(2,1)S(1)} %collective-permute-done.22.refs_6_), channel_id=1, source_target_pairs={{0,4},{4,0},{8,12},{12,8},{16,20},{20,16},{24,28},{28,24},{32,36},... | collective-permute-start | bytes 786440 | tf_op jit(solution)/shard_map/ppermute | solution.py:54
  38.9 2.7 %norm_rows.1 = (bf16[3,32,2048]{2,1,0:T(8,128)(2,1)}, bf16[3,32,2048]{2,1,0:T(8,128)(2,1)}) custom-call(bf16[6,32,2048]{2,1,0:T(8,128)(2,1)} %bitcast.26, bf16[3,32,2048]{2,1,0:T(8,128)(2,1)} %copy-done.33, f32[1,2048]{1,0:T(1,128)} %bitcast.45), custom_call_target="tpu_custom_call" | custom-call | tf_op jit(solution)/shard_map/norm_rows/pallas_call | solution.py:129
  45.0 2.2 %collective-permute-done.40.refs_1_ = bf16[4,4,64,256]{3,2,1,0:T(8,128)(2,1)S(1)} collective-permute-done((bf16[4,4,64,256]{3,2,1,0:T(8,128)(2,1)S(1)}, bf16[4,4,64,256]{3,2,1,0:T(8,128)(2,1)S(1)}, u32[]{:S(2)}, u32[]{:S(2)}) %collective-permute-start.40) | collective-permute-done | bytes 524320 | tf_op jit(solution)/shard_map/ppermute | solution.py:417
  47.2 2.1 %collective-permute-start.3 = (bf16[3,32,2048]{2,1,0:T(8,128)(2,1)}, bf16[3,32,2048]{2,1,0:T(8,128)(2,1)S(1)}, u32[]{:S(2)}, u32[]{:S(2)}) collective-permute-start(bf16[3,32,2048]{2,1,0:T(8,128)(2,1)} %get-tuple-element.19.refs_0_), channel_id=1, source_target_pairs={{0,3},{1,0},{2,1},{3,2},{4,7},{5,4},{6,5},{7,6},{8,11},{9,8},{10,9... | collective-permute-start | bytes 1179656 | tf_op jit(solution)/shard_map/ppermute | solution.py:58
  49.4 3.4 %collective-permute-done.41.refs_2_ = bf16[4,4,64,256]{3,2,1,0:T(8,128)(2,1)S(1)} collective-permute-done((bf16[4,4,64,256]{3,2,1,0:T(8,128)(2,1)S(1)}, bf16[4,4,64,256]{3,2,1,0:T(8,128)(2,1)S(1)}, u32[]{:S(2)}, u32[]{:S(2)}) %collective-permute-start.41) | collective-permute-done | bytes 524320 | tf_op jit(solution)/shard_map/ppermute | solution.py:417
  52.8 11.6 %collective-permute-done.42.refs_3_ = bf16[4,4,64,256]{3,2,1,0:T(8,128)(2,1)S(1)} collective-permute-done((bf16[4,4,64,256]{3,2,1,0:T(8,128)(2,1)S(1)}, bf16[4,4,64,256]{3,2,1,0:T(8,128)(2,1)S(1)}, u32[]{:S(2)}, u32[]{:S(2)}) %collective-permute-start.42) | collective-permute-done | bytes 524320 | tf_op jit(solution)/shard_map/ppermute | solution.py:417
  70.1 8.5 %collective-permute-done.4.refs_5_.refs_1_ = bf16[3,32,2048]{2,1,0:T(8,128)(2,1)S(1)} collective-permute-done((bf16[3,32,2048]{2,1,0:T(8,128)(2,1)S(1)}, bf16[3,32,2048]{2,1,0:T(8,128)(2,1)S(1)}, u32[]{:S(2)}, u32[]{:S(2)}) %collective-permute-start.4) | collective-permute-done | bytes 393248 | tf_op jit(solution)/shard_map/ppermute | solution.py:58
  79.5 8.0 %collective-permute-done.5.refs_6_.refs_2_ = bf16[3,32,2048]{2,1,0:T(8,128)(2,1)S(1)} collective-permute-done((bf16[3,32,2048]{2,1,0:T(8,128)(2,1)S(1)}, bf16[3,32,2048]{2,1,0:T(8,128)(2,1)S(1)}, u32[]{:S(2)}, u32[]{:S(2)}) %collective-permute-start.5) | collective-permute-done | bytes 393248 | tf_op jit(solution)/shard_map/ppermute | solution.py:58
  90.0 4.3 %project_wide.2.early = bf16[2,3,128,256]{3,2,1,0:T(8,128)(2,1)} custom-call(bf16[3,32,2048]{2,1,0:T(8,128)(2,1)} %get-tuple-element.19.refs_0_, bf16[3,32,2048]{2,1,0:T(8,128)(2,1)} %copy-done.4, bf16[3,32,2048]{2,1,0:T(8,128)(2,1)} %copy-done.5, bf16[3,32,2048]{2,1,0:T(8,128)(2,1)} %copy-done.6, bf16[4,2,64,256]{3,2,1,0:T(8,128)(2,1)} %copy-done.1, ...), custom_call_target="tpu_custom_call" | custom-call | tf_op jit(solution)/shard_map/project_wide/pallas_call | solution.py:175
  94.4 2.8 %collective-permute-done.6.refs_7_.refs_3_ = bf16[3,32,2048]{2,1,0:T(8,128)(2,1)S(1)} collective-permute-done((bf16[3,32,2048]{2,1,0:T(8,128)(2,1)S(1)}, bf16[3,32,2048]{2,1,0:T(8,128)(2,1)S(1)}, u32[]{:S(2)}, u32[]{:S(2)}) %collective-permute-start.6) | collective-permute-done | bytes 393248 | tf_op jit(solution)/shard_map/ppermute | solution.py:58
  97.2 3.0 %collective-permute-start.28 = (bf16[2,3,128,256]{3,2,1,0:T(8,128)(2,1)}, bf16[2,3,128,256]{3,2,1,0:T(8,128)(2,1)S(1)}, u32[]{:S(2)}, u32[]{:S(2)}) collective-permute-start(bf16[2,3,128,256]{3,2,1,0:T(8,128)(2,1)} %project_wide.2.early), channel_id=1, source_target_pairs={{0,8},{4,12},{8,16},{12,20},{16,24},{20,28},{24,32},{28,36},{32,40... | collective-permute-start | bytes 1179656 | tf_op jit(solution)/shard_map/ppermute | solution.py:62
  100.2 4.3 %project_wide.3.late = bf16[2,3,128,256]{3,2,1,0:T(8,128)(2,1)} custom-call(bf16[3,32,2048]{2,1,0:T(8,128)(2,1)} %get-tuple-element.20.refs_4_.refs_0_, bf16[3,32,2048]{2,1,0:T(8,128)(2,1)} %copy-done.7, bf16[3,32,2048]{2,1,0:T(8,128)(2,1)} %copy-done.8, bf16[3,32,2048]{2,1,0:T(8,128)(2,1)} %copy-done.9, bf16[4,2,64,256]{3,2,1,0:T(8,128)(2,1)} %copy-done.1, ...), custom_call_target="tpu_custom_call" | custom-call | tf_op jit(solution)/shard_map/project_wide/pallas_call | solution.py:175
  104.5 2.7 %collective-permute-start.29 = (bf16[2,3,128,256]{3,2,1,0:T(8,128)(2,1)}, bf16[2,3,128,256]{3,2,1,0:T(8,128)(2,1)S(1)}, u32[]{:S(2)}, u32[]{:S(2)}) collective-permute-start(bf16[2,3,128,256]{3,2,1,0:T(8,128)(2,1)} %project_wide.3.late), channel_id=1, source_target_pairs={{0,8},{4,12},{8,16},{12,20},{16,24},{20,28},{24,32},{28,36},{32,40... | collective-permute-start | bytes 1179656 | tf_op jit(solution)/shard_map/ppermute | solution.py:62
  107.2 3.0 %collective-permute-done.28.back_early = bf16[2,3,128,256]{3,2,1,0:T(8,128)(2,1)S(1)} collective-permute-done((bf16[2,3,128,256]{3,2,1,0:T(8,128)(2,1)}, bf16[2,3,128,256]{3,2,1,0:T(8,128)(2,1)S(1)}, u32[]{:S(2)}, u32[]{:S(2)}) %collective-permute-start.28) | collective-permute-done | bytes 393248 | tf_op jit(solution)/shard_map/ppermute | solution.py:62
  110.2 3.4 %collective-permute-start.30 = (bf16[2,3,128,256]{3,2,1,0:T(8,128)(2,1)}, bf16[2,3,128,256]{3,2,1,0:T(8,128)(2,1)S(1)}, u32[]{:S(2)}, u32[]{:S(2)}) collective-permute-start(bf16[2,3,128,256]{3,2,1,0:T(8,128)(2,1)} %project_wide.3.late), channel_id=1, source_target_pairs={{0,16},{4,20},{8,24},{12,28},{16,32},{20,36},{24,40},{28,44},{32,4... | collective-permute-start | bytes 1179656 | tf_op jit(solution)/shard_map/ppermute | solution.py:62
  113.7 8.6 %collective-permute-done.29.back_late = bf16[2,3,128,256]{3,2,1,0:T(8,128)(2,1)S(1)} collective-permute-done((bf16[2,3,128,256]{3,2,1,0:T(8,128)(2,1)}, bf16[2,3,128,256]{3,2,1,0:T(8,128)(2,1)S(1)}, u32[]{:S(2)}, u32[]{:S(2)}) %collective-permute-start.29) | collective-permute-done | bytes 393248 | tf_op jit(solution)/shard_map/ppermute | solution.py:62
  122.3 7.5 %collective-permute-start.43 = (bf16[4,4,64,256]{3,2,1,0:T(8,128)(2,1)S(1)}, bf16[4,4,64,256]{3,2,1,0:T(8,128)(2,1)S(1)}, u32[]{:S(2)}, u32[]{:S(2)}) collective-permute-start(bf16[4,4,64,256]{3,2,1,0:T(8,128)(2,1)S(1)} %pad_maximum_fusion.1.refs_0_), channel_id=1, source_target_pairs={{0,4},{4,0},{8,12},{12,8},{16,20},{20,16},{24,28},{28,24},{32,36},... | collective-permute-start | bytes 1572872 | tf_op jit(solution)/shard_map/ppermute | solution.py:54
  130.4 11.7 %project_rest.1 = (bf16[2,2,3,256,256]{4,3,2,1,0:T(8,128)(2,1)}, bf16[2,3,128,256]{3,2,1,0:T(8,128)(2,1)}, bf16[3,3,256,256]{3,2,1,0:T(8,128)(2,1)}) custom-call(bf16[3,32,2048]{2,1,0:T(8,128)(2,1)} %get-tuple-element.19.refs_0_, bf16[3,32,2048]{2,1,0:T(8,128)(2,1)} %copy-done.4, bf16[3,32,2048]{2,1,0:T(8,128)(2,1)} %copy-done.5, ...), custom_call_target="tpu_custom_call" | custom-call | tf_op jit(solution)/shard_map/project_rest/pallas_call | solution.py:217
  142.1 2.1 %collective-permute-start.17 = (bf16[2,3,128,256]{3,2,1,0:T(8,128)(2,1)}, bf16[2,3,128,256]{3,2,1,0:T(8,128)(2,1)S(1)}, u32[]{:S(2)}, u32[]{:S(2)}) collective-permute-start(bf16[2,3,128,256]{3,2,1,0:T(8,128)(2,1)} %get-tuple-element.24), channel_id=1, source_target_pairs={{0,8},{4,12},{8,16},{12,20},{16,24},{20,28},{24,32},{28,36},{32,40... | collective-permute-start | bytes 1179656 | tf_op jit(solution)/shard_map/ppermute | solution.py:62
  144.3 5.1 %attend_wide.1 = (f32[3,256,256]{2,1,0:T(8,128)}, f32[3,256,256]{2,1,0:T(8,128)}) custom-call(bf16[3,3,256,256]{3,2,1,0:T(8,128)(2,1)} %get-tuple-element.22.q, bf16[2,3,128,256]{3,2,1,0:T(8,128)(2,1)} %project_wide.2.early, bf16[2,3,128,256]{3,2,1,0:T(8,128)(2,1)} %project_wide.3.late, bf16[2,3,128,256]{3,2,1,0:T(8,128)(2,1)} %copy-done.29, ...), custom_call_target="tpu_custom_call" | custom-call | tf_op jit(solution)/shard_map/attend_wide/pallas_call | solution.py:290
  149.4 7.2 %collective-permute-done.17.tail = bf16[2,3,128,256]{3,2,1,0:T(8,128)(2,1)S(1)} collective-permute-done((bf16[2,3,128,256]{3,2,1,0:T(8,128)(2,1)}, bf16[2,3,128,256]{3,2,1,0:T(8,128)(2,1)S(1)}, u32[]{:S(2)}, u32[]{:S(2)}) %collective-permute-start.17) | collective-permute-done | bytes 393248 | tf_op jit(solution)/shard_map/ppermute | solution.py:62
  157.4 6.6 %attend_near.1 = (bf16[2,3,32,256]{3,2,1,0:T(8,128)(2,1)}, bf16[2,3,32,256]{3,2,1,0:T(8,128)(2,1)}, bf16[2,3,32,256]{3,2,1,0:T(8,128)(2,1)}, bf16[2,3,32,256]{3,...) custom-call(bf16[3,3,256,256]{3,2,1,0:T(8,128)(2,1)} %get-tuple-element.22.q, ...), custom_call_target="tpu_custom_call" | custom-call | tf_op jit(solution)/shard_map/attend_near/pallas_call | solution.py:341
  164.1 2.6 %collective-permute-start.32 = (bf16[2,3,32,256]{3,2,1,0:T(8,128)(2,1)}, bf16[2,3,32,256]{3,2,1,0:T(8,128)(2,1)S(1)}, u32[]{:S(2)}, u32[]{:S(2)}) collective-permute-start(bf16[2,3,32,256]{3,2,1,0:T(8,128)(2,1)} %get-tuple-element.30), channel_id=1, source_target_pairs={{0,2},{1,3},{2,0},{3,1},{4,6},{5,7},{6,4},{7,5},{8,10},{9,11},{10,... | collective-permute-start | bytes 294920 | tf_op jit(solution)/shard_map/ppermute | solution.py:58
  169.2 4.5 %lay_out.1.w = bf16[4,2048,256]{2,1,0:T(8,128)(2,1)} custom-call(bf16[4,4,64,256]{3,2,1,0:T(8,128)(2,1)} %copy-done.2, bf16[4,4,64,256]{3,2,1,0:T(8,128)(2,1)} %copy-done.19, bf16[4,4,64,256]{3,2,1,0:T(8,128)(2,1)} %copy-done.21, bf16[4,4,64,256]{3,2,1,0:T(8,128)(2,1)} %copy-done.23, bf16[4,4,64,256]{3,2,1,0:T(8,128)(2,1)} %copy-done.25, ...), custom_call_target="tpu_custom_call" | custom-call | tf_op jit(solution)/shard_map/lay_out/pallas_call | solution.py:366
  174.4 5.2 %finish.1 = (bf16[3,32,2048]{2,1,0:T(8,128)(2,1)}, bf16[3,32,2048]{2,1,0:T(8,128)(2,1)}) custom-call(bf16[2,3,32,256]{3,2,1,0:T(8,128)(2,1)} %get-tuple-element.28.r0, bf16[2,3,32,256]{3,2,1,0:T(8,128)(2,1)} %copy-done.35, bf16[2,3,32,256]{3,2,1,0:T(8,128)(2,1)} %copy-done.36, bf16[2,3,32,256]{3,2,1,0:T(8,128)(2,1)} %copy-done.37, ...), custom_call_target="tpu_custom_call" | custom-call | tf_op jit(solution)/shard_map/finish/pallas_call | solution.py:395
  179.6 2.2 %collective-permute-start.47 = (bf16[3,32,2048]{2,1,0:T(8,128)(2,1)}, bf16[3,32,2048]{2,1,0:T(8,128)(2,1)S(1)}, u32[]{:S(2)}, u32[]{:S(2)}) collective-permute-start(bf16[3,32,2048]{2,1,0:T(8,128)(2,1)} %get-tuple-element.33), channel_id=1, source_target_pairs={{0,4},{4,0},{8,12},{12,8},{16,20},{20,16},{24,28},{28,24},{32,36},... | collective-permute-start | bytes 1179656 | tf_op jit(solution)/shard_map/ppermute | solution.py:54
  184.0 2.1 %fusion = bf16[32,6,2048]{2,0,1:T(8,128)(2,1)} fusion(bf16[3,32,2048]{2,1,0:T(8,128)(2,1)S(1)} %collective-permute-done.47, bf16[3,32,2048]{2,1,0:T(8,128)(2,1)} %get-tuple-element.32, pred[]{:T(512)S(6)} %eq.8), kind=kLoop, calls=%fused_computation.2 | loop fusion | flops 1179648 | bytes 1572865 | tf_op jit(solution)/shard_map/transpose | solution.py:450
  (163 shorter events, 37.9 us)
Async XLA Ops:
  13.3 9.6 %collective-permute-start.9 = (bf16[7,64,256]{2,1,0:T(8,128)(2,1)}, bf16[7,64,256]{2,1,0:T(8,128)(2,1)S(1)}, u32[]{:S(2)}, u32[]{:S(2)}) collective-permute-start(bf16[7,64,256]{2,1,0:T(8,128)(2,1)} %get-tuple-element.21), channel_id=1, source_target_pairs={{0,24},{4,100},{8,0},{12,108},{16,8},{20,116},{24,16},{28,124},{32... | collective-permute-start | bytes 688136 | tf_op jit(solution)/shard_map/ppermute | solution.py:415
  13.9 15.4 %collective-permute-start.8 = (bf16[7,64,256]{2,1,0:T(8,128)(2,1)}, bf16[7,64,256]{2,1,0:T(8,128)(2,1)S(1)}, u32[]{:S(2)}, u32[]{:S(2)}) collective-permute-start(bf16[7,64,256]{2,1,0:T(8,128)(2,1)} %get-tuple-element.21), channel_id=1, source_target_pairs={{0,16},{4,68},{8,24},{12,76},{16,0},{20,84},{24,8},{28,92},{32,48}... | collective-permute-start | bytes 688136 | tf_op jit(solution)/shard_map/ppermute | solution.py:415
  16.7 15.9 %collective-permute-start.7 = (bf16[7,64,256]{2,1,0:T(8,128)(2,1)}, bf16[7,64,256]{2,1,0:T(8,128)(2,1)S(1)}, u32[]{:S(2)}, u32[]{:S(2)}) collective-permute-start(bf16[7,64,256]{2,1,0:T(8,128)(2,1)} %get-tuple-element.21), channel_id=1, source_target_pairs={{0,8},{4,36},{8,16},{12,44},{16,24},{20,52},{24,0},{28,60},{32,40}... | collective-permute-start | bytes 688136 | tf_op jit(solution)/shard_map/ppermute | solution.py:415
  18.8 15.1 %collective-permute-start.21 = (bf16[4,2,64,256]{3,2,1,0:T(8,128)(2,1)S(1)}, bf16[4,2,64,256]{3,2,1,0:T(8,128)(2,1)S(1)}, u32[]{:S(2)}, u32[]{:S(2)}) collective-permute-start(bf16[4,2,64,256]{3,2,1,0:T(8,128)(2,1)S(1)} %pad_maximum_fusion.2.refs_4_), channel_id=1, source_target_pairs={{0,32},{4,12},{8,40},{12,20},{16,48},{20,28},{24,56},{28,4},{32,64... | collective-permute-start | bytes 786440 | tf_op jit(solution)/shard_map/ppermute | solution.py:417
  20.4 13.7 %collective-permute-start.22 = (bf16[4,2,64,256]{3,2,1,0:T(8,128)(2,1)S(1)}, bf16[4,2,64,256]{3,2,1,0:T(8,128)(2,1)S(1)}, u32[]{:S(2)}, u32[]{:S(2)}) collective-permute-start(bf16[4,2,64,256]{3,2,1,0:T(8,128)(2,1)S(1)} %pad_maximum_fusion.2.refs_4_), channel_id=1, source_target_pairs={{0,64},{4,20},{8,72},{12,28},{16,80},{20,4},{24,88},{28,12},{32,96... | collective-permute-start | bytes 786440 | tf_op jit(solution)/shard_map/ppermute | solution.py:417
  23.0 15.2 %collective-permute-start = (bf16[3,32,2048]{2,1,0:T(8,128)(2,1)S(1)}, bf16[3,32,2048]{2,1,0:T(8,128)(2,1)S(1)}, u32[]{:S(2)}, u32[]{:S(2)}) collective-permute-start(bf16[3,32,2048]{2,1,0:T(8,128)(2,1)S(1)} %dynamic-slice_bitcast_fusion), channel_id=1, source_target_pairs={{0,4},{4,0},{8,12},{12,8},{16,20},{20,16},{24,28},{28,24},{32,36},... | collective-permute-start | bytes 1179656 | tf_op jit(solution)/shard_map/ppermute | solution.py:54
  34.1 13.1 %collective-permute-start.40 = (bf16[4,4,64,256]{3,2,1,0:T(8,128)(2,1)S(1)}, bf16[4,4,64,256]{3,2,1,0:T(8,128)(2,1)S(1)}, u32[]{:S(2)}, u32[]{:S(2)}) collective-permute-start(bf16[4,4,64,256]{3,2,1,0:T(8,128)(2,1)S(1)} %pad_maximum_fusion.1.refs_0_), channel_id=1, source_target_pairs={{0,32},{4,36},{8,40},{12,44},{16,48},{20,52},{24,56},{28,60},{32,6... | collective-permute-start | bytes 1572872 | tf_op jit(solution)/shard_map/ppermute | solution.py:417
  38.2 14.6 %collective-permute-start.41 = (bf16[4,4,64,256]{3,2,1,0:T(8,128)(2,1)S(1)}, bf16[4,4,64,256]{3,2,1,0:T(8,128)(2,1)S(1)}, u32[]{:S(2)}, u32[]{:S(2)}) collective-permute-start(bf16[4,4,64,256]{3,2,1,0:T(8,128)(2,1)S(1)} %pad_maximum_fusion.1.refs_0_), channel_id=1, source_target_pairs={{0,64},{4,68},{8,72},{12,76},{16,80},{20,84},{24,88},{28,92},{32,9... | collective-permute-start | bytes 1572872 | tf_op jit(solution)/shard_map/ppermute | solution.py:417
  38.2 26.2 %collective-permute-start.42 = (bf16[4,4,64,256]{3,2,1,0:T(8,128)(2,1)S(1)}, bf16[4,4,64,256]{3,2,1,0:T(8,128)(2,1)S(1)}, u32[]{:S(2)}, u32[]{:S(2)}) collective-permute-start(bf16[4,4,64,256]{3,2,1,0:T(8,128)(2,1)S(1)} %pad_maximum_fusion.1.refs_0_), channel_id=1, source_target_pairs={{0,96},{4,100},{8,104},{12,108},{16,112},{20,116},{24,120},{28,124... | collective-permute-start | bytes 1572872 | tf_op jit(solution)/shard_map/ppermute | solution.py:417
  41.6 23.1 %collective-permute-start.1 = (bf16[3,32,2048]{2,1,0:T(8,128)(2,1)}, bf16[3,32,2048]{2,1,0:T(8,128)(2,1)S(1)}, u32[]{:S(2)}, u32[]{:S(2)}) collective-permute-start(bf16[3,32,2048]{2,1,0:T(8,128)(2,1)} %get-tuple-element.19.refs_0_), channel_id=1, source_target_pairs={{0,1},{1,2},{2,3},{3,0},{4,5},{5,6},{6,7},{7,4},{8,9},{9,10},{10,1... | collective-permute-start | bytes 1179656 | tf_op jit(solution)/shard_map/ppermute | solution.py:58
  43.2 23.4 %collective-permute-start.2 = (bf16[3,32,2048]{2,1,0:T(8,128)(2,1)}, bf16[3,32,2048]{2,1,0:T(8,128)(2,1)S(1)}, u32[]{:S(2)}, u32[]{:S(2)}) collective-permute-start(bf16[3,32,2048]{2,1,0:T(8,128)(2,1)} %get-tuple-element.19.refs_0_), channel_id=1, source_target_pairs={{0,2},{1,3},{2,0},{3,1},{4,6},{5,7},{6,4},{7,5},{8,10},{9,11},{10,... | collective-permute-start | bytes 1179656 | tf_op jit(solution)/shard_map/ppermute | solution.py:58
  47.2 21.1 %collective-permute-start.3 = (bf16[3,32,2048]{2,1,0:T(8,128)(2,1)}, bf16[3,32,2048]{2,1,0:T(8,128)(2,1)S(1)}, u32[]{:S(2)}, u32[]{:S(2)}) collective-permute-start(bf16[3,32,2048]{2,1,0:T(8,128)(2,1)} %get-tuple-element.19.refs_0_), channel_id=1, source_target_pairs={{0,3},{1,0},{2,1},{3,2},{4,7},{5,4},{6,5},{7,6},{8,11},{9,8},{10,9... | collective-permute-start | bytes 1179656 | tf_op jit(solution)/shard_map/ppermute | solution.py:58
  52.8 34.7 %collective-permute-start.10 = (bf16[4,7,64,256]{3,2,1,0:T(8,128)(2,1)S(1)}, bf16[4,7,64,256]{3,2,1,0:T(8,128)(2,1)S(1)}, u32[]{:S(2)}, u32[]{:S(2)}) collective-permute-start(bf16[4,7,64,256]{3,2,1,0:T(8,128)(2,1)S(1)} %pad_maximum_fusion.refs_8_), channel_id=1, source_target_pairs={{0,32},{4,12},{8,40},{12,20},{16,48},{20,28},{24,56},{28,4},{32,64... | collective-permute-start | bytes 2752520 | tf_op jit(solution)/shard_map/ppermute | solution.py:417
  64.4 24.2 %collective-permute-start.11 = (bf16[4,7,64,256]{3,2,1,0:T(8,128)(2,1)S(1)}, bf16[4,7,64,256]{3,2,1,0:T(8,128)(2,1)S(1)}, u32[]{:S(2)}, u32[]{:S(2)}) collective-permute-start(bf16[4,7,64,256]{3,2,1,0:T(8,128)(2,1)S(1)} %pad_maximum_fusion.refs_8_), channel_id=1, source_target_pairs={{0,64},{4,20},{8,72},{12,28},{16,80},{20,4},{24,88},{28,12},{32,96... | collective-permute-start | bytes 2752520 | tf_op jit(solution)/shard_map/ppermute | solution.py:417
  64.8 23.9 %collective-permute-start.12 = (bf16[4,7,64,256]{3,2,1,0:T(8,128)(2,1)S(1)}, bf16[4,7,64,256]{3,2,1,0:T(8,128)(2,1)}, u32[]{:S(2)}, u32[]{:S(2)}) collective-permute-start(bf16[4,7,64,256]{3,2,1,0:T(8,128)(2,1)S(1)} %pad_maximum_fusion.refs_8_), channel_id=1, source_target_pairs={{0,96},{4,28},{8,104},{12,4},{16,112},{20,12},{24,120},{28,20},{32... | collective-permute-start | bytes 2752520 | tf_op jit(solution)/shard_map/ppermute | solution.py:417
  66.6 11.9 %collective-permute-start.4 = (bf16[3,32,2048]{2,1,0:T(8,128)(2,1)S(1)}, bf16[3,32,2048]{2,1,0:T(8,128)(2,1)S(1)}, u32[]{:S(2)}, u32[]{:S(2)}) collective-permute-start(bf16[3,32,2048]{2,1,0:T(8,128)(2,1)S(1)} %copy-done.3), channel_id=1, source_target_pairs={{0,1},{1,2},{2,3},{3,0},{4,5},{5,6},{6,7},{7,4},{8,9},{9,10},{10,1... | collective-permute-start | bytes 1179656 | tf_op jit(solution)/shard_map/ppermute | solution.py:58
  68.2 19.2 %collective-permute-start.5 = (bf16[3,32,2048]{2,1,0:T(8,128)(2,1)S(1)}, bf16[3,32,2048]{2,1,0:T(8,128)(2,1)S(1)}, u32[]{:S(2)}, u32[]{:S(2)}) collective-permute-start(bf16[3,32,2048]{2,1,0:T(8,128)(2,1)S(1)} %copy-done.3), channel_id=1, source_target_pairs={{0,2},{1,3},{2,0},{3,1},{4,6},{5,7},{6,4},{7,5},{8,10},{9,11},{10,... | collective-permute-start | bytes 1179656 | tf_op jit(solution)/shard_map/ppermute | solution.py:58
  78.6 25.9 %collective-permute-start.13 = (bf16[4,7,64,256]{3,2,1,0:T(8,128)(2,1)S(1)}, bf16[4,7,64,256]{3,2,1,0:T(8,128)(2,1)}, u32[]{:S(2)}, u32[]{:S(2)}) collective-permute-start(bf16[4,7,64,256]{3,2,1,0:T(8,128)(2,1)S(1)} %pad_maximum_fusion.refs_8_), channel_id=1, source_target_pairs={{0,4},{4,0},{8,12},{12,8},{16,20},{20,16},{24,28},{28,24},{32,36},... | collective-permute-start | bytes 2752520 | tf_op jit(solution)/shard_map/ppermute | solution.py:54
  87.5 9.7 %collective-permute-start.6 = (bf16[3,32,2048]{2,1,0:T(8,128)(2,1)S(1)}, bf16[3,32,2048]{2,1,0:T(8,128)(2,1)S(1)}, u32[]{:S(2)}, u32[]{:S(2)}) collective-permute-start(bf16[3,32,2048]{2,1,0:T(8,128)(2,1)S(1)} %copy-done.3), channel_id=1, source_target_pairs={{0,3},{1,0},{2,1},{3,2},{4,7},{5,4},{6,5},{7,6},{8,11},{9,8},{10,9... | collective-permute-start | bytes 1179656 | tf_op jit(solution)/shard_map/ppermute | solution.py:58
  87.5 42.3 %collective-permute-start.14 = (bf16[4,7,64,256]{3,2,1,0:T(8,128)(2,1)S(1)}, bf16[4,7,64,256]{3,2,1,0:T(8,128)(2,1)}, u32[]{:S(2)}, u32[]{:S(2)}) collective-permute-start(bf16[4,7,64,256]{3,2,1,0:T(8,128)(2,1)S(1)} %collective-permute-done.10.refs_9_), channel_id=1, source_target_pairs={{0,4},{4,0},{8,12},{12,8},{16,20},{20,16},{24,28},{28,24},{32,36},... | collective-permute-start | bytes 2752520 | tf_op jit(solution)/shard_map/ppermute | solution.py:54
  88.6 41.3 %collective-permute-start.15 = (bf16[4,7,64,256]{3,2,1,0:T(8,128)(2,1)S(1)}, bf16[4,7,64,256]{3,2,1,0:T(8,128)(2,1)}, u32[]{:S(2)}, u32[]{:S(2)}) collective-permute-start(bf16[4,7,64,256]{3,2,1,0:T(8,128)(2,1)S(1)} %collective-permute-done.11.refs_10_), channel_id=1, source_target_pairs={{0,4},{4,0},{8,12},{12,8},{16,20},{20,16},{24,28},{28,24},{32,36},... | collective-permute-start | bytes 2752520 | tf_op jit(solution)/shard_map/ppermute | solution.py:54
  88.7 41.6 %collective-permute-start.16 = (bf16[4,7,64,256]{3,2,1,0:T(8,128)(2,1)}, bf16[4,7,64,256]{3,2,1,0:T(8,128)(2,1)}, u32[]{:S(2)}, u32[]{:S(2)}) collective-permute-start(bf16[4,7,64,256]{3,2,1,0:T(8,128)(2,1)} %collective-permute-done.12.refs_11_), channel_id=1, source_target_pairs={{0,4},{4,0},{8,12},{12,8},{16,20},{20,16},{24,28},{28,24},{32,36},... | collective-permute-start | bytes 2752520 | tf_op jit(solution)/shard_map/ppermute | solution.py:54
  97.2 13.0 %collective-permute-start.28 = (bf16[2,3,128,256]{3,2,1,0:T(8,128)(2,1)}, bf16[2,3,128,256]{3,2,1,0:T(8,128)(2,1)S(1)}, u32[]{:S(2)}, u32[]{:S(2)}) collective-permute-start(bf16[2,3,128,256]{3,2,1,0:T(8,128)(2,1)} %project_wide.2.early), channel_id=1, source_target_pairs={{0,8},{4,12},{8,16},{12,20},{16,24},{20,28},{24,32},{28,36},{32,40... | collective-permute-start | bytes 1179656 | tf_op jit(solution)/shard_map/ppermute | solution.py:62
  104.5 17.8 %collective-permute-start.29 = (bf16[2,3,128,256]{3,2,1,0:T(8,128)(2,1)}, bf16[2,3,128,256]{3,2,1,0:T(8,128)(2,1)S(1)}, u32[]{:S(2)}, u32[]{:S(2)}) collective-permute-start(bf16[2,3,128,256]{3,2,1,0:T(8,128)(2,1)} %project_wide.3.late), channel_id=1, source_target_pairs={{0,8},{4,12},{8,16},{12,20},{16,24},{20,28},{24,32},{28,36},{32,40... | collective-permute-start | bytes 1179656 | tf_op jit(solution)/shard_map/ppermute | solution.py:62
  110.2 31.9 %collective-permute-start.30 = (bf16[2,3,128,256]{3,2,1,0:T(8,128)(2,1)}, bf16[2,3,128,256]{3,2,1,0:T(8,128)(2,1)S(1)}, u32[]{:S(2)}, u32[]{:S(2)}) collective-permute-start(bf16[2,3,128,256]{3,2,1,0:T(8,128)(2,1)} %project_wide.3.late), channel_id=1, source_target_pairs={{0,16},{4,20},{8,24},{12,28},{16,32},{20,36},{24,40},{28,44},{32,4... | collective-permute-start | bytes 1179656 | tf_op jit(solution)/shard_map/ppermute | solution.py:62
  122.3 41.8 %collective-permute-start.43 = (bf16[4,4,64,256]{3,2,1,0:T(8,128)(2,1)S(1)}, bf16[4,4,64,256]{3,2,1,0:T(8,128)(2,1)S(1)}, u32[]{:S(2)}, u32[]{:S(2)}) collective-permute-start(bf16[4,4,64,256]{3,2,1,0:T(8,128)(2,1)S(1)} %pad_maximum_fusion.1.refs_0_), channel_id=1, source_target_pairs={{0,4},{4,0},{8,12},{12,8},{16,20},{20,16},{24,28},{28,24},{32,36},... | collective-permute-start | bytes 1572872 | tf_op jit(solution)/shard_map/ppermute | solution.py:54
  129.8 36.9 %collective-permute-start.44 = (bf16[4,4,64,256]{3,2,1,0:T(8,128)(2,1)S(1)}, bf16[4,4,64,256]{3,2,1,0:T(8,128)(2,1)S(1)}, u32[]{:S(2)}, u32[]{:S(2)}) collective-permute-start(bf16[4,4,64,256]{3,2,1,0:T(8,128)(2,1)S(1)} %copy-done.20), channel_id=1, source_target_pairs={{0,4},{4,0},{8,12},{12,8},{16,20},{20,16},{24,28},{28,24},{32,36},... | collective-permute-start | bytes 1572872 | tf_op jit(solution)/shard_map/ppermute | solution.py:54
  129.9 37.7 %collective-permute-start.45 = (bf16[4,4,64,256]{3,2,1,0:T(8,128)(2,1)S(1)}, bf16[4,4,64,256]{3,2,1,0:T(8,128)(2,1)S(1)}, u32[]{:S(2)}, u32[]{:S(2)}) collective-permute-start(bf16[4,4,64,256]{3,2,1,0:T(8,128)(2,1)S(1)} %copy-done.22), channel_id=1, source_target_pairs={{0,4},{4,0},{8,12},{12,8},{16,20},{20,16},{24,28},{28,24},{32,36},... | collective-permute-start | bytes 1572872 | tf_op jit(solution)/shard_map/ppermute | solution.py:54
  130.3 37.3 %collective-permute-start.46 = (bf16[4,4,64,256]{3,2,1,0:T(8,128)(2,1)S(1)}, bf16[4,4,64,256]{3,2,1,0:T(8,128)(2,1)S(1)}, u32[]{:S(2)}, u32[]{:S(2)}) collective-permute-start(bf16[4,4,64,256]{3,2,1,0:T(8,128)(2,1)S(1)} %copy-done.24), channel_id=1, source_target_pairs={{0,4},{4,0},{8,12},{12,8},{16,20},{20,16},{24,28},{28,24},{32,36},... | collective-permute-start | bytes 1572872 | tf_op jit(solution)/shard_map/ppermute | solution.py:54
  142.1 14.5 %collective-permute-start.17 = (bf16[2,3,128,256]{3,2,1,0:T(8,128)(2,1)}, bf16[2,3,128,256]{3,2,1,0:T(8,128)(2,1)S(1)}, u32[]{:S(2)}, u32[]{:S(2)}) collective-permute-start(bf16[2,3,128,256]{3,2,1,0:T(8,128)(2,1)} %get-tuple-element.24), channel_id=1, source_target_pairs={{0,8},{4,12},{8,16},{12,20},{16,24},{20,28},{24,32},{28,36},{32,40... | collective-permute-start | bytes 1179656 | tf_op jit(solution)/shard_map/ppermute | solution.py:62
  164.0 9.8 %collective-permute-start.31 = (bf16[2,3,32,256]{3,2,1,0:T(8,128)(2,1)}, bf16[2,3,32,256]{3,2,1,0:T(8,128)(2,1)S(1)}, u32[]{:S(2)}, u32[]{:S(2)}) collective-permute-start(bf16[2,3,32,256]{3,2,1,0:T(8,128)(2,1)} %get-tuple-element.29), channel_id=1, source_target_pairs={{0,1},{1,2},{2,3},{3,0},{4,5},{5,6},{6,7},{7,4},{8,9},{9,10},{10,1... | collective-permute-start | bytes 294920 | tf_op jit(solution)/shard_map/ppermute | solution.py:58
  164.1 9.7 %collective-permute-start.32 = (bf16[2,3,32,256]{3,2,1,0:T(8,128)(2,1)}, bf16[2,3,32,256]{3,2,1,0:T(8,128)(2,1)S(1)}, u32[]{:S(2)}, u32[]{:S(2)}) collective-permute-start(bf16[2,3,32,256]{3,2,1,0:T(8,128)(2,1)} %get-tuple-element.30), channel_id=1, source_target_pairs={{0,2},{1,3},{2,0},{3,1},{4,6},{5,7},{6,4},{7,5},{8,10},{9,11},{10,... | collective-permute-start | bytes 294920 | tf_op jit(solution)/shard_map/ppermute | solution.py:58
  (57 other events, 961.3 us)

commit v3 on v2

--- a/solution.py
+++ b/solution.py
@@ -182,51 +182,78 @@
     )(*pieces, *lines)
 
 
-def rest_body(*refs):
-    early, late, lines = refs[:4], refs[4:8], refs[8:16]
-    near, near_tail, queries, x_all, w_all, x_sems, a_sems, b_sems, c_sems, d_sems = refs[16:]
+def matrix_copies(shards_of, first, count, w_all, sems):
+    return [
+        pltpu.make_async_copy(shards_of.at[:, first + m], w_all.at[m], sems.at[m]) for m in range(count)
+    ]
+
+
+def project(x_all, w_all, m):
+    x = x_all[...].reshape(BATCHES * SPAN, WIDTH)
+    y = jnp.dot(x, w_all[m].reshape(WIDTH, COLS), preferred_element_type=jnp.float32)
+    return y.astype(jnp.bfloat16).reshape(BATCHES, SPAN, COLS)
+
+
+def staged(early, late, rest, first, count, x_all, w_all, x_sems, w_sems, work):
     rows = row_copies(early, 0, x_all, x_sems) + row_copies(late, HALF, x_all, x_sems)
-    groups = {
-        0: rows + shard_copies(lines, 0, 1, w_all, a_sems, 0),
-        1: shard_copies(lines, 1, 2, w_all, b_sems, 0),
-        3: shard_copies(lines, 3, 2, w_all, c_sems, 0),
-        5: shard_copies(lines, 5, 2, w_all, d_sems, 0),
-    }
-    following = {0: 1, 1: 3, 3: 5}
-    for c in groups[0]:
+    weights = matrix_copies(rest, first, count, w_all, w_sems)
+    for c in rows + weights[:1]:
         c.start()
-    for m in range(NEAR + GROUPS):
-        for c in groups.get(m, ()):
-            c.wait()
-        for c in groups.get(following.get(m), ()):
-            c.start()
-        x = x_all[...].reshape(BATCHES * SPAN, WIDTH)
-        y = jnp.dot(x, w_all[m], preferred_element_type=jnp.float32)
-        y = y.astype(jnp.bfloat16).reshape(BATCHES, SPAN, COLS)
-        if m >= NEAR:
-            queries[m - NEAR] = y
+    for c in rows:
+        c.wait()
+    for m in range(count):
+        weights[m].wait()
+        if m + 1 < count:
+            weights[m + 1].start()
+        work(m, project(x_all, w_all, m))
+
+
+def near_pair_body(*refs):
+    early, late, rest = refs[:4], refs[4:8], refs[8]
+    near, near_tail, *scratch = refs[9:]
+
+    def work(m, y):
+        near[m // 2, m % 2] = y
+        if m < 2:
+            near_tail[m % 2, :, : HALOS[0]] = y[:, SPAN - HALOS[0] :]
         else:
-            near[m // 2, m % 2] = y
-            if m < 2:
-                near_tail[m % 2, :, : HALOS[0]] = y[:, SPAN - HALOS[0] :]
-            else:
-                near_tail[m % 2, :, HALOS[0] :] = y[:, SPAN - HALOS[1] :]
-
-
-def project_rest(early, late, lines):
-    return pl.pallas_call(
-        rest_body,
-        out_shape=(
-            bf(2, 2, BATCHES, SPAN, COLS), bf(2, BATCHES, HALOS[0] + HALOS[1], COLS), bf(GROUPS, BATCHES, SPAN, COLS)
-        ),
-        in_specs=[ANY] * 16, out_specs=(VMEM,) * 3,
-        scratch_shapes=[
-            pltpu.VMEM((BATCHES, SPAN, WIDTH), jnp.bfloat16), pltpu.VMEM((NEAR + GROUPS, WIDTH, COLS), jnp.bfloat16),
-            pltpu.SemaphoreType.DMA((2, RING)), pltpu.SemaphoreType.DMA((32,)), pltpu.SemaphoreType.DMA((32,)),
-            pltpu.SemaphoreType.DMA((32,)), pltpu.SemaphoreType.DMA((32,)),
-        ],
-        compiler_params=PARAMS, name="project_rest",
-    )(*early, *late, *lines)
+            near_tail[m % 2, :, HALOS[0] :] = y[:, SPAN - HALOS[1] :]
+
+    staged(early, late, rest, 0, NEAR, *scratch, work)
+
+
+def query_body(*refs):
+    early, late, rest = refs[:4], refs[4:8], refs[8]
+    queries, *scratch = refs[9:]
+
+    def work(m, y):
+        queries[m] = y
+
+    staged(early, late, rest, NEAR, GROUPS, *scratch, work)
+
+
+def rest_scratch(count):
+    return [
+        pltpu.VMEM((BATCHES, SPAN, WIDTH), jnp.bfloat16), pltpu.VMEM((count, 32, ROWS, COLS), jnp.bfloat16),
+        pltpu.SemaphoreType.DMA((2, RING)), pltpu.SemaphoreType.DMA((count,)),
+    ]
+
+
+def project_near(early, late, rest):
+    return pl.pallas_call(
+        near_pair_body,
+        out_shape=(bf(2, 2, BATCHES, SPAN, COLS), bf(2, BATCHES, HALOS[0] + HALOS[1], COLS)),
+        in_specs=[ANY] * 9, out_specs=(VMEM,) * 2, scratch_shapes=rest_scratch(NEAR),
+        compiler_params=PARAMS, name="project_near",
+    )(*early, *late, rest)
+
+
+def project_queries(early, late, rest):
+    return pl.pallas_call(
+        query_body, out_shape=bf(GROUPS, BATCHES, SPAN, COLS),
+        in_specs=[ANY] * 9, out_specs=VMEM, scratch_shapes=rest_scratch(GROUPS),
+        compiler_params=PARAMS, name="project_queries",
+    )(*early, *late, rest)
 
 
 def bias_of(group, block):
@@ -353,37 +380,32 @@
     )(q, near, tail, other, logs)
 
 
-def lay_body(*refs):
-    lines, out, sems = refs[:8], refs[8], refs[9]
-    copies = shard_copies(lines, 0, RING, out, sems, 1)
-    for c in copies:
-        c.start()
-    for c in copies:
-        c.wait()
-
-
-def lay_out(lines):
-    return pl.pallas_call(
-        lay_body, out_shape=bf(RING, WIDTH, COLS), in_specs=[ANY] * 8, out_specs=VMEM,
-        scratch_shapes=[pltpu.SemaphoreType.DMA((32,))], compiler_params=PARAMS, name="lay_out",
-    )(*lines)
-
-
 def final_body(r0, r1, r2, r3, w, keep, send, w_all, sems):
+    t = lax.axis_index("tp")
     part = WIDTH // RING
     half = BATCHES * PIECE
+    count = part // ROWS
     copies = [
-        pltpu.make_async_copy(w.at[:, pl.ds(n * part, part)], w_all.at[n], sems.at[n]) for n in range(RING)
-    ]
-    for c in copies:
-        c.start()
+        [
+            pltpu.make_async_copy(
+                w.at[pl.ds(n * count, count), (t + RING - d) % RING], w_all.at[n, d], sems.at[n, d]
+            )
+            for d in range(RING)
+        ]
+        for n in range(RING)
+    ]
+    for group in copies:
+        for c in group:
+            c.start()
     rows = [r[...].reshape(2 * half, COLS) for r in (r0, r1, r2, r3)]
     for n in range(RING):
         cols = slice(n * part, (n + 1) * part)
-        copies[n].wait()
+        for c in copies[n]:
+            c.wait()
         acc = None
         for d in range(RING):
-            y = lax.dot_general(rows[d], w_all[n, d], (((1,), (1,)), ((), ())), preferred_element_type=jnp.float32)
+            block = w_all[n, d].reshape(part, COLS)
+            y = lax.dot_general(rows[d], block, (((1,), (1,)), ((), ())), preferred_element_type=jnp.float32)
             acc = y if acc is None else acc + y
         acc = acc.astype(jnp.bfloat16)
         keep[:, :, cols] = acc[:half].reshape(BATCHES, PIECE, part)
@@ -395,7 +417,8 @@
     return pl.pallas_call(
         final_body, out_shape=(shape, shape), in_specs=[VMEM] * 4 + [ANY], out_specs=(VMEM,) * 2,
         scratch_shapes=[
-            pltpu.VMEM((RING, RING, WIDTH // RING, COLS), jnp.bfloat16), pltpu.SemaphoreType.DMA((RING,)),
+            pltpu.VMEM((RING, RING, WIDTH // RING // ROWS, ROWS, COLS), jnp.bfloat16),
+            pltpu.SemaphoreType.DMA((RING, RING)),
         ],
         compiler_params=PARAMS, name="finish",
     )(*received, w)
@@ -404,6 +427,25 @@
 def joined_cores(mine, theirs):
     core = lax.axis_index("sp") % 2
     return jnp.where(core == 0, jnp.concatenate((mine, theirs), 0), jnp.concatenate((theirs, mine), 0))
+
+
+def merge_body(mine, theirs, out, sems):
+    core = lax.axis_index("sp") % 2
+    copies = [
+        pltpu.make_async_copy(mine, out.at[pl.ds(core * BATCHES, BATCHES)], sems.at[0]),
+        pltpu.make_async_copy(theirs, out.at[pl.ds((1 - core) * BATCHES, BATCHES)], sems.at[1]),
+    ]
+    for c in copies:
+        c.start()
+    for c in copies:
+        c.wait()
+
+
+def merged(mine, theirs):
+    return pl.pallas_call(
+        merge_body, out_shape=bf(2 * BATCHES, PIECE, WIDTH), in_specs=[ANY] * 2, out_specs=ANY,
+        scratch_shapes=[pltpu.SemaphoreType.DMA((2,))], compiler_params=PARAMS, name="merge",
+    )(mine, theirs)
 
 
 def ring_of(a):
@@ -420,31 +462,33 @@
 
 
 def layer(tokens, norm_gain, w_query, w_key, w_value, w_out):
+    wide_own, rest_own = pack(w_query, w_key, w_value)
+    rest = lax.all_gather(rest_own, "sp")
+    outs = lax.all_gather(jnp.transpose(w_out), ("sp", "tp"))
+    outs = outs.reshape(32, RING, ROWS, COLS)
+
     core = lax.axis_index("sp") % 2
     tokens = jnp.transpose(tokens, (1, 0, 2))
     send = lax.dynamic_slice_in_dim(tokens, (1 - core) * BATCHES, BATCHES, 0)
     other = swapped(send)
-    wide_own, rest_own = pack(w_query, w_key, w_value)
     wide_lines = spread(wide_own, 0)
     late, early = norm_rows(tokens, other, norm_gain)
     late, early = ring_of(late), ring_of(early)
-    rest_lines = spread(rest_own, 0)
-    out_lines = spread(jnp.stack(ring_of(jnp.transpose(w_out))), 1)
 
     wide_late = project_wide(late, wide_lines)
     far_late = from_behind(wide_late, 2)
     back_late = from_behind(wide_late, 1)
     wide_early = project_wide(early, wide_lines)
     back_early = from_behind(wide_early, 1)
-    near, near_tail, queries = project_rest(early, late, rest_lines)
+    near, near_tail = project_near(early, late, rest)
     near_tail = from_behind(near_tail, 1)
-    laid = lay_out(out_lines)
+    queries = project_queries(early, late, rest)
     wide_out, wide_logs = attend_wide(queries, wide_early, wide_late, back_early, back_late, far_late)
     *combined, kept, sent = attend_near(queries, near, near_tail, wide_out, wide_logs)
 
     received = [combined[0]] + [turned(combined[d], d) for d in (1, 2, 3)]
-    mixed_mine, mixed_sent = finish(received, laid)
-    mixed = joined_cores(mixed_mine, swapped(mixed_sent))
+    mixed_mine, mixed_sent = finish(received, outs)
+    mixed = merged(mixed_mine, swapped(mixed_sent))
 
     log_weight = joined_cores(kept, swapped(sent)).reshape(2 * BATCHES, 2, BLOCK)
     return (jnp.transpose(mixed, (1, 0, 2)), jnp.transpose(log_weight, (2, 0, 1)))

time: 187 us -> 182 us (0.973)
  the two profiles are of different devices: /device:TPU:97 before, /device:TPU:1 now
where the time goes in v3:
time: 182 us; the launch traced here: 181 us
  Pallas kernels  73.7 us (40%)
  waiting for transfers between devices  44.2 us (24%)
  starting transfers between devices  40.4 us (22%)
  between operations  14.4 us (8%)
  local copies, waits for them, and re-layouts  7.78 us (4%)
    pallas_call x1, Pallas kernels, merged(): pl.pallas_call(merge_body, out_shape=bf(2 * BATCHES, PIECE, WIDTH), in_sp...  24.9 us
    ppermute x9, waiting for transfers between devices, turned(): return lax.ppermute(a, 'tp', [(i, (i + shift) % RING) for i in range(RING)])  18.9 us
    all_gather x1, waiting for transfers between devices, layer(): outs = lax.all_gather(jnp.transpose(w_out), ('sp', 'tp'))  16.8 us
    ppermute x9, starting transfers between devices, turned(): return lax.ppermute(a, 'tp', [(i, (i + shift) % RING) for i in range(RING)])  12.5 us
    ppermute x4, starting transfers between devices, from_behind(): lax.ppermute(a, 'sp', [(i, i + 2 * blocks) for i in range(32 - 2 * blocks)])  12.4 us
    pallas_call x1, Pallas kernels, project_near(): pl.pallas_call(near_pair_body, out_shape=(bf(2, 2, BATCHES, SPAN, COLS),...  10.7 us
    pallas_call x2, Pallas kernels, project_wide(): pl.pallas_call(wide_pair_body, out_shape=bf(2, BATCHES, HALF, COLS), in_s...  8.64 us
    pallas_call x1, Pallas kernels, project_queries(): pl.pallas_call(query_body, out_shape=bf(GROUPS, BATCHES, SPAN, COLS), in_...  8.04 us
  transfers between devices with their start and end apart: 28, of which 9 were waited for; matrix products, arithmetic and copies ran while one was open for 1% of the time, Pallas kernels for 23%

profile of v3, /device:TPU:1, one launch (start us, length us, event | category | flops | bytes accessed | tf_op | source)
XLA Modules:
  0.0 181.4 jit_solution(3542072497576779376)
XLA Ops:
  7.2 1.7 pack.1
  10.8 1.5 collective-permute-start
  12.2 3.9 %collective-permute-start.10 = (bf16[2,64,256]{2,1,0:T(8,128)(2,1)}, bf16[2,64,256]{2,1,0:T(8,128)(2,1)S(1)}, u32[]{:S(2)}, u32[]{:S(2)}) collective-permute-start(bf16[2,64,256]{2,1,0:T(8,128)(2,1)} %get-tuple-element.23), channel_id=1, source_target_pairs={{0,24},{4,100},{8,0},{12,108},{16,8},{20,116},{24,16},{28,124},{32... | collective-permute-start | bytes 196616 | tf_op jit(solution)/shard_map/ppermute | solution.py:457
  16.8 1.6 collective-permute-done.10
  18.3 2.7 %collective-permute-done.9 = bf16[2,64,256]{2,1,0:T(8,128)(2,1)S(1)} collective-permute-done((bf16[2,64,256]{2,1,0:T(8,128)(2,1)}, bf16[2,64,256]{2,1,0:T(8,128)(2,1)S(1)}, u32[]{:S(2)}, u32[]{:S(2)}) %collective-permute-start.9) | collective-permute-done | bytes 65568 | tf_op jit(solution)/shard_map/ppermute | solution.py:457
  23.6 2.6 %collective-permute-start.12 = (bf16[4,2,64,256]{3,2,1,0:T(8,128)(2,1)S(1)}, bf16[4,2,64,256]{3,2,1,0:T(8,128)(2,1)S(1)}, u32[]{:S(2)}, u32[]{:S(2)}) collective-permute-start(bf16[4,2,64,256]{3,2,1,0:T(8,128)(2,1)S(1)} %pad_maximum_fusion.refs_4_), channel_id=1, source_target_pairs={{0,64},{4,20},{8,72},{12,28},{16,80},{20,4},{24,88},{28,12},{32,96... | collective-permute-start | bytes 786440 | tf_op jit(solution)/shard_map/ppermute | solution.py:459
  28.0 2.7 %norm_rows.1 = (bf16[3,32,2048]{2,1,0:T(8,128)(2,1)}, bf16[3,32,2048]{2,1,0:T(8,128)(2,1)}) custom-call(bf16[6,32,2048]{2,1,0:T(8,128)(2,1)} %bitcast.16, bf16[3,32,2048]{2,1,0:T(8,128)(2,1)} %copy-done.18, f32[1,2048]{1,0:T(1,128)} %bitcast.23), custom_call_target="tpu_custom_call" | custom-call | tf_op jit(solution)/shard_map/norm_rows/pallas_call | solution.py:129
  30.7 1.2 collective-permute-start.4
  31.9 2.6 %collective-permute-start.14 = (bf16[4,2,64,256]{3,2,1,0:T(8,128)(2,1)S(1)}, bf16[4,2,64,256]{3,2,1,0:T(8,128)(2,1)S(1)}, u32[]{:S(2)}, u32[]{:S(2)}) collective-permute-start(bf16[4,2,64,256]{3,2,1,0:T(8,128)(2,1)S(1)} %pad_maximum_fusion.refs_4_), channel_id=1, source_target_pairs={{0,4},{4,0},{8,12},{12,8},{16,20},{20,16},{24,28},{28,24},{32,36},... | collective-permute-start | bytes 786440 | tf_op jit(solution)/shard_map/ppermute | solution.py:54
  34.6 1.5 collective-permute-done.12.refs_6_
  36.1 1.3 collective-permute-start.16
  37.5 2.8 %collective-permute-start.5 = (bf16[3,32,2048]{2,1,0:T(8,128)(2,1)}, bf16[3,32,2048]{2,1,0:T(8,128)(2,1)S(1)}, u32[]{:S(2)}, u32[]{:S(2)}) collective-permute-start(bf16[3,32,2048]{2,1,0:T(8,128)(2,1)} %get-tuple-element.19.refs_4_.refs_0_), channel_id=1, source_target_pairs={{0,2},{1,3},{2,0},{3,1},{4,6},{5,7},{6,4},{7,5},{8,10},{9,11},{10,... | collective-permute-start | bytes 1179656 | tf_op jit(solution)/shard_map/ppermute | solution.py:58
  42.5 2.0 %collective-permute-start.3 = (bf16[3,32,2048]{2,1,0:T(8,128)(2,1)}, bf16[3,32,2048]{2,1,0:T(8,128)(2,1)S(1)}, u32[]{:S(2)}, u32[]{:S(2)}) collective-permute-start(bf16[3,32,2048]{2,1,0:T(8,128)(2,1)} %get-tuple-element.18.refs_0_), channel_id=1, source_target_pairs={{0,3},{1,0},{2,1},{3,2},{4,7},{5,4},{6,5},{7,6},{8,11},{9,8},{10,9... | collective-permute-start | bytes 1179656 | tf_op jit(solution)/shard_map/ppermute | solution.py:58
  44.5 6.0 %collective-permute-done.5.refs_6_.refs_2_ = bf16[3,32,2048]{2,1,0:T(8,128)(2,1)S(1)} collective-permute-done((bf16[3,32,2048]{2,1,0:T(8,128)(2,1)}, bf16[3,32,2048]{2,1,0:T(8,128)(2,1)S(1)}, u32[]{:S(2)}, u32[]{:S(2)}) %collective-permute-start.5) | collective-permute-done | bytes 393248 | tf_op jit(solution)/shard_map/ppermute | solution.py:58
  50.4 7.7 %collective-permute-done.6.refs_7_.refs_3_ = bf16[3,32,2048]{2,1,0:T(8,128)(2,1)S(1)} collective-permute-done((bf16[3,32,2048]{2,1,0:T(8,128)(2,1)}, bf16[3,32,2048]{2,1,0:T(8,128)(2,1)S(1)}, u32[]{:S(2)}, u32[]{:S(2)}) %collective-permute-start.6) | collective-permute-done | bytes 393248 | tf_op jit(solution)/shard_map/ppermute | solution.py:58
  59.0 4.4 %project_wide.3.late = bf16[2,3,128,256]{3,2,1,0:T(8,128)(2,1)} custom-call(bf16[3,32,2048]{2,1,0:T(8,128)(2,1)} %get-tuple-element.19.refs_4_.refs_0_, bf16[3,32,2048]{2,1,0:T(8,128)(2,1)} %copy-done, bf16[3,32,2048]{2,1,0:T(8,128)(2,1)} %copy-done.1, bf16[3,32,2048]{2,1,0:T(8,128)(2,1)} %copy-done.2, bf16[4,2,64,256]{3,2,1,0:T(8,128)(2,1)} %copy-done.6, ...), custom_call_target="tpu_custom_call" | custom-call | tf_op jit(solution)/shard_map/project_wide/pallas_call | solution.py:175
  63.4 1.3 collective-permute-start.19
  64.7 5.0 %collective-permute-start.20 = (bf16[2,3,128,256]{3,2,1,0:T(8,128)(2,1)}, bf16[2,3,128,256]{3,2,1,0:T(8,128)(2,1)S(1)}, u32[]{:S(2)}, u32[]{:S(2)}) collective-permute-start(bf16[2,3,128,256]{3,2,1,0:T(8,128)(2,1)} %project_wide.3.late), channel_id=1, source_target_pairs={{0,16},{4,20},{8,24},{12,28},{16,32},{20,36},{24,40},{28,44},{32,4... | collective-permute-start | bytes 1179656 | tf_op jit(solution)/shard_map/ppermute | solution.py:62
  69.8 5.2 %collective-permute-done.3.refs_3_ = bf16[3,32,2048]{2,1,0:T(8,128)(2,1)S(1)} collective-permute-done((bf16[3,32,2048]{2,1,0:T(8,128)(2,1)}, bf16[3,32,2048]{2,1,0:T(8,128)(2,1)S(1)}, u32[]{:S(2)}, u32[]{:S(2)}) %collective-permute-start.3) | collective-permute-done | bytes 393248 | tf_op jit(solution)/shard_map/ppermute | solution.py:58
  75.7 4.2 %project_wide.2.early = bf16[2,3,128,256]{3,2,1,0:T(8,128)(2,1)} custom-call(bf16[3,32,2048]{2,1,0:T(8,128)(2,1)} %get-tuple-element.18.refs_0_, bf16[3,32,2048]{2,1,0:T(8,128)(2,1)} %copy-done.3, bf16[3,32,2048]{2,1,0:T(8,128)(2,1)} %copy-done.4, bf16[3,32,2048]{2,1,0:T(8,128)(2,1)} %copy-done.5, bf16[4,2,64,256]{3,2,1,0:T(8,128)(2,1)} %copy-done.6, ...), custom_call_target="tpu_custom_call" | custom-call | tf_op jit(solution)/shard_map/project_wide/pallas_call | solution.py:175
  80.0 1.5 collective-permute-start.18
  81.5 10.7 %project_near.1 = (bf16[2,2,3,256,256]{4,3,2,1,0:T(8,128)(2,1)}, bf16[2,3,128,256]{3,2,1,0:T(8,128)(2,1)}) custom-call(bf16[3,32,2048]{2,1,0:T(8,128)(2,1)} %get-tuple-element.18.refs_0_, bf16[3,32,2048]{2,1,0:T(8,128)(2,1)} %copy-done.3, bf16[3,32,2048]{2,1,0:T(8,128)(2,1)} %copy-done.4, bf16[3,32,2048]{2,1,0:T(8,128)(2,1)} %copy-done.5, ...), custom_call_target="tpu_custom_call" | custom-call | tf_op jit(solution)/shard_map/project_near/pallas_call | solution.py:243
  92.2 4.6 %collective-permute-start.7 = (bf16[2,3,128,256]{3,2,1,0:T(8,128)(2,1)}, bf16[2,3,128,256]{3,2,1,0:T(8,128)(2,1)S(1)}, u32[]{:S(2)}, u32[]{:S(2)}) collective-permute-start(bf16[2,3,128,256]{3,2,1,0:T(8,128)(2,1)} %get-tuple-element.22), channel_id=1, source_target_pairs={{0,8},{4,12},{8,16},{12,20},{16,24},{20,28},{24,32},{28,36},{32,40... | collective-permute-start | bytes 1179656 | tf_op jit(solution)/shard_map/ppermute | solution.py:62
  96.8 8.0 %project_queries.1.q = bf16[3,3,256,256]{3,2,1,0:T(8,128)(2,1)} custom-call(bf16[3,32,2048]{2,1,0:T(8,128)(2,1)} %get-tuple-element.18.refs_0_, bf16[3,32,2048]{2,1,0:T(8,128)(2,1)} %copy-done.3, bf16[3,32,2048]{2,1,0:T(8,128)(2,1)} %copy-done.4, bf16[3,32,2048]{2,1,0:T(8,128)(2,1)} %copy-done.5, bf16[3,32,2048]{2,1,0:T(8,128)(2,1)} %get-tuple-element.19.refs_4_.refs_0_, ...), custom_call_target="tpu_custom_call" | custom-call | tf_op jit(solution)/shard_map/project_queries/pallas_call | solution.py:252
  106.5 5.2 %attend_wide.1 = (f32[3,256,256]{2,1,0:T(8,128)}, f32[3,256,256]{2,1,0:T(8,128)}) custom-call(bf16[3,3,256,256]{3,2,1,0:T(8,128)(2,1)} %project_queries.1.q, bf16[2,3,128,256]{3,2,1,0:T(8,128)(2,1)} %project_wide.2.early, bf16[2,3,128,256]{3,2,1,0:T(8,128)(2,1)} %project_wide.3.late, bf16[2,3,128,256]{3,2,1,0:T(8,128)(2,1)} %copy-done.17, ...), custom_call_target="tpu_custom_call" | custom-call | tf_op jit(solution)/shard_map/attend_wide/pallas_call | solution.py:317
  112.5 6.6 %attend_near.1 = (bf16[2,3,32,256]{3,2,1,0:T(8,128)(2,1)}, bf16[2,3,32,256]{3,2,1,0:T(8,128)(2,1)}, bf16[2,3,32,256]{3,2,1,0:T(8,128)(2,1)}, bf16[2,3,32,256]{3,...) custom-call(bf16[3,3,256,256]{3,2,1,0:T(8,128)(2,1)} %project_queries.1.q, ...), custom_call_target="tpu_custom_call" | custom-call | tf_op jit(solution)/shard_map/attend_near/pallas_call | solution.py:368
  119.1 1.9 %collective-permute-start.21 = (bf16[2,3,32,256]{3,2,1,0:T(8,128)(2,1)}, bf16[2,3,32,256]{3,2,1,0:T(8,128)(2,1)S(1)}, u32[]{:S(2)}, u32[]{:S(2)}) collective-permute-start(bf16[2,3,32,256]{3,2,1,0:T(8,128)(2,1)} %get-tuple-element.27), channel_id=1, source_target_pairs={{0,1},{1,2},{2,3},{3,0},{4,5},{5,6},{6,7},{7,4},{8,9},{9,10},{10,1... | collective-permute-start | bytes 294920 | tf_op jit(solution)/shard_map/ppermute | solution.py:58
  120.9 2.5 %collective-permute-start.22 = (bf16[2,3,32,256]{3,2,1,0:T(8,128)(2,1)}, bf16[2,3,32,256]{3,2,1,0:T(8,128)(2,1)S(1)}, u32[]{:S(2)}, u32[]{:S(2)}) collective-permute-start(bf16[2,3,32,256]{3,2,1,0:T(8,128)(2,1)} %get-tuple-element.28), channel_id=1, source_target_pairs={{0,2},{1,3},{2,0},{3,1},{4,6},{5,7},{6,4},{7,5},{8,10},{9,11},{10,... | collective-permute-start | bytes 294920 | tf_op jit(solution)/shard_map/ppermute | solution.py:58
  123.4 16.8 %all-gather.7.cloned.1.call-done = bf16[8192,256]{1,0:T(8,128)(2,1)} async-done(((bf16[64,256]{1,0:T(8,128)(2,1)}), bf16[8192,256]{1,0:T(8,128)(2,1)}) %all-gather.7.cloned.1.call-update) | async-done | bytes 4194320 | tf_op jit(solution)/shard_map/all_gather | solution.py:467
  140.9 5.2 %finish.1 = (bf16[3,32,2048]{2,1,0:T(8,128)(2,1)}, bf16[3,32,2048]{2,1,0:T(8,128)(2,1)}) custom-call(bf16[2,3,32,256]{3,2,1,0:T(8,128)(2,1)} %get-tuple-element.26.r0, bf16[2,3,32,256]{3,2,1,0:T(8,128)(2,1)} %copy-done.20, bf16[2,3,32,256]{3,2,1,0:T(8,128)(2,1)} %copy-done.21, bf16[2,3,32,256]{3,2,1,0:T(8,128)(2,1)} %copy-done.22, ...), custom_call_target="tpu_custom_call" | custom-call | tf_op jit(solution)/shard_map/finish/pallas_call | solution.py:417
  146.8 1.4 collective-permute-done.25
  149.6 24.9 %merge.1 = bf16[6,32,2048]{2,1,0:T(8,128)(2,1)} custom-call(bf16[3,32,2048]{2,1,0:T(8,128)(2,1)} %get-tuple-element.30.mine, bf16[3,32,2048]{2,1,0:T(8,128)(2,1)} %copy-done.19), custom_call_target="tpu_custom_call" | custom-call | tf_op jit(solution)/shard_map/merge/pallas_call | solution.py:445
  (90 shorter events, 16.0 us)
Async XLA Ops:
  7.2 74.4 %all-gather.5.cloned.1.call-start = ((), (), s32[]{:S(2)}) async-start(), calls=%async_computation | async-start | bytes 7569408 | tf_op jit(solution)/shard_map/all_gather | solution.py:466
  9.0 131.3 %all-gather.7.cloned.1.call-start = ((), (), s32[]{:S(2)}) async-start(), calls=%async_computation.1 | async-start | bytes 4227072 | tf_op jit(solution)/shard_map/all_gather | solution.py:467
  10.8 16.5 %collective-permute-start = (bf16[3,32,2048]{2,1,0:T(8,128)(2,1)S(1)}, bf16[3,32,2048]{2,1,0:T(8,128)(2,1)S(1)}, u32[]{:S(2)}, u32[]{:S(2)}) collective-permute-start(bf16[3,32,2048]{2,1,0:T(8,128)(2,1)S(1)} %dynamic-slice_bitcast_fusion), channel_id=1, source_target_pairs={{0,4},{4,0},{8,12},{12,8},{16,20},{20,16},{24,28},{28,24},{32,36},... | collective-permute-start | bytes 1179656 | tf_op jit(solution)/shard_map/ppermute | solution.py:54
  12.2 6.1 %collective-permute-start.10 = (bf16[2,64,256]{2,1,0:T(8,128)(2,1)}, bf16[2,64,256]{2,1,0:T(8,128)(2,1)S(1)}, u32[]{:S(2)}, u32[]{:S(2)}) collective-permute-start(bf16[2,64,256]{2,1,0:T(8,128)(2,1)} %get-tuple-element.23), channel_id=1, source_target_pairs={{0,24},{4,100},{8,0},{12,108},{16,8},{20,116},{24,16},{28,124},{32... | collective-permute-start | bytes 196616 | tf_op jit(solution)/shard_map/ppermute | solution.py:457
  16.1 4.9 %collective-permute-start.9 = (bf16[2,64,256]{2,1,0:T(8,128)(2,1)}, bf16[2,64,256]{2,1,0:T(8,128)(2,1)S(1)}, u32[]{:S(2)}, u32[]{:S(2)}) collective-permute-start(bf16[2,64,256]{2,1,0:T(8,128)(2,1)} %get-tuple-element.23), channel_id=1, source_target_pairs={{0,16},{4,68},{8,24},{12,76},{16,0},{20,84},{24,8},{28,92},{32,48}... | collective-permute-start | bytes 196616 | tf_op jit(solution)/shard_map/ppermute | solution.py:457
  16.1 5.5 %collective-permute-start.8 = (bf16[2,64,256]{2,1,0:T(8,128)(2,1)}, bf16[2,64,256]{2,1,0:T(8,128)(2,1)S(1)}, u32[]{:S(2)}, u32[]{:S(2)}) collective-permute-start(bf16[2,64,256]{2,1,0:T(8,128)(2,1)} %get-tuple-element.23), channel_id=1, source_target_pairs={{0,8},{4,36},{8,16},{12,44},{16,24},{20,52},{24,0},{28,60},{32,40}... | collective-permute-start | bytes 196616 | tf_op jit(solution)/shard_map/ppermute | solution.py:457
  22.5 35.7 %copy-start.6 = (bf16[4,2,64,256]{3,2,1,0:T(8,128)(2,1)}, bf16[4,2,64,256]{3,2,1,0:T(8,128)(2,1)S(1)}, u32[]{:S(2)}) copy-start(bf16[4,2,64,256]{3,2,1,0:T(8,128)(2,1)S(1)} %pad_maximum_fusion.refs_4_) | copy-start | bytes 786436
  22.5 12.0 %collective-permute-start.11 = (bf16[4,2,64,256]{3,2,1,0:T(8,128)(2,1)S(1)}, bf16[4,2,64,256]{3,2,1,0:T(8,128)(2,1)S(1)}, u32[]{:S(2)}, u32[]{:S(2)}) collective-permute-start(bf16[4,2,64,256]{3,2,1,0:T(8,128)(2,1)S(1)} %pad_maximum_fusion.refs_4_), channel_id=1, source_target_pairs={{0,32},{4,12},{8,40},{12,20},{16,48},{20,28},{24,56},{28,4},{32,64... | collective-permute-start | bytes 786440 | tf_op jit(solution)/shard_map/ppermute | solution.py:459
  23.6 12.6 %collective-permute-start.12 = (bf16[4,2,64,256]{3,2,1,0:T(8,128)(2,1)S(1)}, bf16[4,2,64,256]{3,2,1,0:T(8,128)(2,1)S(1)}, u32[]{:S(2)}, u32[]{:S(2)}) collective-permute-start(bf16[4,2,64,256]{3,2,1,0:T(8,128)(2,1)S(1)} %pad_maximum_fusion.refs_4_), channel_id=1, source_target_pairs={{0,64},{4,20},{8,72},{12,28},{16,80},{20,4},{24,88},{28,12},{32,96... | collective-permute-start | bytes 786440 | tf_op jit(solution)/shard_map/ppermute | solution.py:459
  26.2 11.2 %collective-permute-start.13 = (bf16[4,2,64,256]{3,2,1,0:T(8,128)(2,1)S(1)}, bf16[4,2,64,256]{3,2,1,0:T(8,128)(2,1)S(1)}, u32[]{:S(2)}, u32[]{:S(2)}) collective-permute-start(bf16[4,2,64,256]{3,2,1,0:T(8,128)(2,1)S(1)} %pad_maximum_fusion.refs_4_), channel_id=1, source_target_pairs={{0,96},{4,28},{8,104},{12,4},{16,112},{20,12},{24,120},{28,20},{32... | collective-permute-start | bytes 786440 | tf_op jit(solution)/shard_map/ppermute | solution.py:459
  30.7 11.8 %collective-permute-start.4 = (bf16[3,32,2048]{2,1,0:T(8,128)(2,1)}, bf16[3,32,2048]{2,1,0:T(8,128)(2,1)S(1)}, u32[]{:S(2)}, u32[]{:S(2)}) collective-permute-start(bf16[3,32,2048]{2,1,0:T(8,128)(2,1)} %get-tuple-element.19.refs_4_.refs_0_), channel_id=1, source_target_pairs={{0,1},{1,2},{2,3},{3,0},{4,5},{5,6},{6,7},{7,4},{8,9},{9,10},{10,1... | collective-permute-start | bytes 1179656 | tf_op jit(solution)/shard_map/ppermute | solution.py:58
  31.9 5.6 %collective-permute-start.14 = (bf16[4,2,64,256]{3,2,1,0:T(8,128)(2,1)S(1)}, bf16[4,2,64,256]{3,2,1,0:T(8,128)(2,1)S(1)}, u32[]{:S(2)}, u32[]{:S(2)}) collective-permute-start(bf16[4,2,64,256]{3,2,1,0:T(8,128)(2,1)S(1)} %pad_maximum_fusion.refs_4_), channel_id=1, source_target_pairs={{0,4},{4,0},{8,12},{12,8},{16,20},{20,16},{24,28},{28,24},{32,36},... | collective-permute-start | bytes 786440 | tf_op jit(solution)/shard_map/ppermute | solution.py:54
  34.5 23.6 %copy-start.7 = (bf16[4,2,64,256]{3,2,1,0:T(8,128)(2,1)}, bf16[4,2,64,256]{3,2,1,0:T(8,128)(2,1)S(1)}, u32[]{:S(2)}) copy-start(bf16[4,2,64,256]{3,2,1,0:T(8,128)(2,1)S(1)} %collective-permute-done.11.refs_5_) | copy-start | bytes 786436
  34.5 5.7 %collective-permute-start.15 = (bf16[4,2,64,256]{3,2,1,0:T(8,128)(2,1)S(1)}, bf16[4,2,64,256]{3,2,1,0:T(8,128)(2,1)S(1)}, u32[]{:S(2)}, u32[]{:S(2)}) collective-permute-start(bf16[4,2,64,256]{3,2,1,0:T(8,128)(2,1)S(1)} %collective-permute-done.11.refs_5_), channel_id=1, source_target_pairs={{0,4},{4,0},{8,12},{12,8},{16,20},{20,16},{24,28},{28,24},{32,36},... | collective-permute-start | bytes 786440 | tf_op jit(solution)/shard_map/ppermute | solution.py:54
  36.1 5.0 %collective-permute-start.16 = (bf16[4,2,64,256]{3,2,1,0:T(8,128)(2,1)S(1)}, bf16[4,2,64,256]{3,2,1,0:T(8,128)(2,1)S(1)}, u32[]{:S(2)}, u32[]{:S(2)}) collective-permute-start(bf16[4,2,64,256]{3,2,1,0:T(8,128)(2,1)S(1)} %collective-permute-done.12.refs_6_), channel_id=1, source_target_pairs={{0,4},{4,0},{8,12},{12,8},{16,20},{20,16},{24,28},{28,24},{32,36},... | collective-permute-start | bytes 786440 | tf_op jit(solution)/shard_map/ppermute | solution.py:54
  37.4 4.3 %collective-permute-start.17 = (bf16[4,2,64,256]{3,2,1,0:T(8,128)(2,1)S(1)}, bf16[4,2,64,256]{3,2,1,0:T(8,128)(2,1)S(1)}, u32[]{:S(2)}, u32[]{:S(2)}) collective-permute-start(bf16[4,2,64,256]{3,2,1,0:T(8,128)(2,1)S(1)} %collective-permute-done.13.refs_7_), channel_id=1, source_target_pairs={{0,4},{4,0},{8,12},{12,8},{16,20},{20,16},{24,28},{28,24},{32,36},... | collective-permute-start | bytes 786440 | tf_op jit(solution)/shard_map/ppermute | solution.py:54
  37.5 12.9 %collective-permute-start.5 = (bf16[3,32,2048]{2,1,0:T(8,128)(2,1)}, bf16[3,32,2048]{2,1,0:T(8,128)(2,1)S(1)}, u32[]{:S(2)}, u32[]{:S(2)}) collective-permute-start(bf16[3,32,2048]{2,1,0:T(8,128)(2,1)} %get-tuple-element.19.refs_4_.refs_0_), channel_id=1, source_target_pairs={{0,2},{1,3},{2,0},{3,1},{4,6},{5,7},{6,4},{7,5},{8,10},{9,11},{10,... | collective-permute-start | bytes 1179656 | tf_op jit(solution)/shard_map/ppermute | solution.py:58
  40.3 17.9 %collective-permute-start.6 = (bf16[3,32,2048]{2,1,0:T(8,128)(2,1)}, bf16[3,32,2048]{2,1,0:T(8,128)(2,1)S(1)}, u32[]{:S(2)}, u32[]{:S(2)}) collective-permute-start(bf16[3,32,2048]{2,1,0:T(8,128)(2,1)} %get-tuple-element.19.refs_4_.refs_0_), channel_id=1, source_target_pairs={{0,3},{1,0},{2,1},{3,2},{4,7},{5,4},{6,5},{7,6},{8,11},{9,8},{10,9... | collective-permute-start | bytes 1179656 | tf_op jit(solution)/shard_map/ppermute | solution.py:58
  41.1 28.6 %collective-permute-start.1 = (bf16[3,32,2048]{2,1,0:T(8,128)(2,1)}, bf16[3,32,2048]{2,1,0:T(8,128)(2,1)S(1)}, u32[]{:S(2)}, u32[]{:S(2)}) collective-permute-start(bf16[3,32,2048]{2,1,0:T(8,128)(2,1)} %get-tuple-element.18.refs_0_), channel_id=1, source_target_pairs={{0,1},{1,2},{2,3},{3,0},{4,5},{5,6},{6,7},{7,4},{8,9},{9,10},{10,1... | collective-permute-start | bytes 1179656 | tf_op jit(solution)/shard_map/ppermute | solution.py:58
  41.7 28.0 %collective-permute-start.2 = (bf16[3,32,2048]{2,1,0:T(8,128)(2,1)}, bf16[3,32,2048]{2,1,0:T(8,128)(2,1)S(1)}, u32[]{:S(2)}, u32[]{:S(2)}) collective-permute-start(bf16[3,32,2048]{2,1,0:T(8,128)(2,1)} %get-tuple-element.18.refs_0_), channel_id=1, source_target_pairs={{0,2},{1,3},{2,0},{3,1},{4,6},{5,7},{6,4},{7,5},{8,10},{9,11},{10,... | collective-permute-start | bytes 1179656 | tf_op jit(solution)/shard_map/ppermute | solution.py:58
  42.5 32.5 %collective-permute-start.3 = (bf16[3,32,2048]{2,1,0:T(8,128)(2,1)}, bf16[3,32,2048]{2,1,0:T(8,128)(2,1)S(1)}, u32[]{:S(2)}, u32[]{:S(2)}) collective-permute-start(bf16[3,32,2048]{2,1,0:T(8,128)(2,1)} %get-tuple-element.18.refs_0_), channel_id=1, source_target_pairs={{0,3},{1,0},{2,1},{3,2},{4,7},{5,4},{6,5},{7,6},{8,11},{9,8},{10,9... | collective-permute-start | bytes 1179656 | tf_op jit(solution)/shard_map/ppermute | solution.py:58
  63.4 41.4 %collective-permute-start.19 = (bf16[2,3,128,256]{3,2,1,0:T(8,128)(2,1)}, bf16[2,3,128,256]{3,2,1,0:T(8,128)(2,1)S(1)}, u32[]{:S(2)}, u32[]{:S(2)}) collective-permute-start(bf16[2,3,128,256]{3,2,1,0:T(8,128)(2,1)} %project_wide.3.late), channel_id=1, source_target_pairs={{0,8},{4,12},{8,16},{12,20},{16,24},{20,28},{24,32},{28,36},{32,40... | collective-permute-start | bytes 1179656 | tf_op jit(solution)/shard_map/ppermute | solution.py:62
  64.7 40.1 %collective-permute-start.20 = (bf16[2,3,128,256]{3,2,1,0:T(8,128)(2,1)}, bf16[2,3,128,256]{3,2,1,0:T(8,128)(2,1)S(1)}, u32[]{:S(2)}, u32[]{:S(2)}) collective-permute-start(bf16[2,3,128,256]{3,2,1,0:T(8,128)(2,1)} %project_wide.3.late), channel_id=1, source_target_pairs={{0,16},{4,20},{8,24},{12,28},{16,32},{20,36},{24,40},{28,44},{32,4... | collective-permute-start | bytes 1179656 | tf_op jit(solution)/shard_map/ppermute | solution.py:62
  80.0 24.9 %collective-permute-start.18 = (bf16[2,3,128,256]{3,2,1,0:T(8,128)(2,1)}, bf16[2,3,128,256]{3,2,1,0:T(8,128)(2,1)S(1)}, u32[]{:S(2)}, u32[]{:S(2)}) collective-permute-start(bf16[2,3,128,256]{3,2,1,0:T(8,128)(2,1)} %project_wide.2.early), channel_id=1, source_target_pairs={{0,8},{4,12},{8,16},{12,20},{16,24},{20,28},{24,32},{28,36},{32,40... | collective-permute-start | bytes 1179656 | tf_op jit(solution)/shard_map/ppermute | solution.py:62
  92.2 19.5 %collective-permute-start.7 = (bf16[2,3,128,256]{3,2,1,0:T(8,128)(2,1)}, bf16[2,3,128,256]{3,2,1,0:T(8,128)(2,1)S(1)}, u32[]{:S(2)}, u32[]{:S(2)}) collective-permute-start(bf16[2,3,128,256]{3,2,1,0:T(8,128)(2,1)} %get-tuple-element.22), channel_id=1, source_target_pairs={{0,8},{4,12},{8,16},{12,20},{16,24},{20,28},{24,32},{28,36},{32,40... | collective-permute-start | bytes 1179656 | tf_op jit(solution)/shard_map/ppermute | solution.py:62
  119.0 27.5 %copy-start.24 = (f32[6,128]{1,0:T(8,128)S(1)}, f32[6,128]{1,0:T(8,128)}, u32[]{:S(2)}) copy-start(f32[6,128]{1,0:T(8,128)} %get-tuple-element.33) | copy-start | bytes 9220
  119.1 29.1 %copy-start.23 = (f32[6,128]{1,0:T(8,128)S(1)}, f32[6,128]{1,0:T(8,128)}, u32[]{:S(2)}) copy-start(f32[6,128]{1,0:T(8,128)} %get-tuple-element.32) | copy-start | bytes 9220
  119.1 21.1 %collective-permute-start.21 = (bf16[2,3,32,256]{3,2,1,0:T(8,128)(2,1)}, bf16[2,3,32,256]{3,2,1,0:T(8,128)(2,1)S(1)}, u32[]{:S(2)}, u32[]{:S(2)}) collective-permute-start(bf16[2,3,32,256]{3,2,1,0:T(8,128)(2,1)} %get-tuple-element.27), channel_id=1, source_target_pairs={{0,1},{1,2},{2,3},{3,0},{4,5},{5,6},{6,7},{7,4},{8,9},{9,10},{10,1... | collective-permute-start | bytes 294920 | tf_op jit(solution)/shard_map/ppermute | solution.py:58
  120.9 19.3 %collective-permute-start.22 = (bf16[2,3,32,256]{3,2,1,0:T(8,128)(2,1)}, bf16[2,3,32,256]{3,2,1,0:T(8,128)(2,1)S(1)}, u32[]{:S(2)}, u32[]{:S(2)}) collective-permute-start(bf16[2,3,32,256]{3,2,1,0:T(8,128)(2,1)} %get-tuple-element.28), channel_id=1, source_target_pairs={{0,2},{1,3},{2,0},{3,1},{4,6},{5,7},{6,4},{7,5},{8,10},{9,11},{10,... | collective-permute-start | bytes 294920 | tf_op jit(solution)/shard_map/ppermute | solution.py:58
  123.4 16.8 %collective-permute-start.23 = (bf16[2,3,32,256]{3,2,1,0:T(8,128)(2,1)}, bf16[2,3,32,256]{3,2,1,0:T(8,128)(2,1)S(1)}, u32[]{:S(2)}, u32[]{:S(2)}) collective-permute-start(bf16[2,3,32,256]{3,2,1,0:T(8,128)(2,1)} %get-tuple-element.29), channel_id=1, source_target_pairs={{0,3},{1,0},{2,1},{3,2},{4,7},{5,4},{6,5},{7,6},{8,11},{9,8},{10,9... | collective-permute-start | bytes 294920 | tf_op jit(solution)/shard_map/ppermute | solution.py:58
  146.2 2.6 %collective-permute-start.24 = (bf16[3,32,2048]{2,1,0:T(8,128)(2,1)}, bf16[3,32,2048]{2,1,0:T(8,128)(2,1)S(1)}, u32[]{:S(2)}, u32[]{:S(2)}) collective-permute-start(bf16[3,32,2048]{2,1,0:T(8,128)(2,1)} %get-tuple-element.31), channel_id=1, source_target_pairs={{0,4},{4,0},{8,12},{12,8},{16,20},{20,16},{24,28},{28,24},{32,36},... | collective-permute-start | bytes 1179656 | tf_op jit(solution)/shard_map/ppermute | solution.py:54
  146.5 1.7 collective-permute-start.25
  (21 other events, 157.1 us)
Sparse Core Ops, SparseCore 0:
  10.2 56.9 all-gather.4
  70.3 69.8 all-gather.6

commit v4 on v3

--- a/solution.py
+++ b/solution.py
@@ -78,26 +78,28 @@
 PARAMS = pltpu.CompilerParams(vmem_limit_bytes=56 * 1024 * 1024)
 HALF = SPAN // 2
 NEAR = 4
+LAST = NEAR + GROUPS
 
 
 def bf(*dims):
     return jax.ShapeDtypeStruct(dims, jnp.bfloat16)
 
 
-def pack_body(w_query, w_key, w_value, wide, rest):
+def pack_body(w_query, w_key, w_value, w_out, wide, rest):
     wide[0] = w_key[2]
     wide[1] = w_value[2]
     for g in range(2):
         rest[2 * g] = w_key[g]
         rest[2 * g + 1] = w_value[g]
-    rest[NEAR:] = w_query[...]
-
-
-def pack(w_query, w_key, w_value):
-    return pl.pallas_call(
-        pack_body, out_shape=(bf(2, ROWS, COLS), bf(NEAR + GROUPS, ROWS, COLS)),
-        in_specs=[VMEM] * 3, out_specs=(VMEM,) * 2, compiler_params=PARAMS, name="pack",
-    )(w_query, w_key, w_value)
+    rest[NEAR:LAST] = w_query[...]
+    rest[LAST] = w_out[...]
+
+
+def pack(w_query, w_key, w_value, w_out):
+    return pl.pallas_call(
+        pack_body, out_shape=(bf(2, ROWS, COLS), bf(LAST + 1, ROWS, COLS)),
+        in_specs=[VMEM] * 4, out_specs=(VMEM,) * 2, compiler_params=PARAMS, name="pack",
+    )(w_query, w_key, w_value, jnp.transpose(w_out))
 
 
 def norm_body(tokens, other, gain, late, early):
@@ -197,14 +199,14 @@
 def staged(early, late, rest, first, count, x_all, w_all, x_sems, w_sems, work):
     rows = row_copies(early, 0, x_all, x_sems) + row_copies(late, HALF, x_all, x_sems)
     weights = matrix_copies(rest, first, count, w_all, w_sems)
-    for c in rows + weights[:1]:
+    for c in rows + weights[:2]:
         c.start()
     for c in rows:
         c.wait()
     for m in range(count):
         weights[m].wait()
-        if m + 1 < count:
-            weights[m + 1].start()
+        if m + 2 < count:
+            weights[m + 2].start()
         work(m, project(x_all, w_all, m))
 
 
@@ -380,28 +382,26 @@
     )(q, near, tail, other, logs)
 
 
-def final_body(r0, r1, r2, r3, w, keep, send, w_all, sems):
-    t = lax.axis_index("tp")
+def final_body(r0, r1, r2, r3, rest, p1, p2, p3, q1, q2, q3, keep, send, w_all, sems):
+    core = lax.axis_index("sp") % 2
     part = WIDTH // RING
     half = BATCHES * PIECE
     count = part // ROWS
-    copies = [
-        [
-            pltpu.make_async_copy(
-                w.at[pl.ds(n * count, count), (t + RING - d) % RING], w_all.at[n, d], sems.at[n, d]
-            )
-            for d in range(RING)
-        ]
-        for n in range(RING)
-    ]
-    for group in copies:
-        for c in group:
-            c.start()
+
+    def copy(source, n, d):
+        return pltpu.make_async_copy(source, w_all.at[n, d], sems.at[n, d])
+
+    for m in range(2):
+        for n in (m, m + 2):
+            copy(rest.at[pl.ds(n * count, count), LAST], n, 0).start()
+        for d, (p, q) in enumerate(((p1, q1), (p2, q2), (p3, q3)), 1):
+            copy(p.at[pl.ds(m * count, count)], 2 * core + m, d).start()
+            copy(q.at[pl.ds(m * count, count)], 2 * (1 - core) + m, d).start()
     rows = [r[...].reshape(2 * half, COLS) for r in (r0, r1, r2, r3)]
-    for n in range(RING):
+    for n in (0, 2, 1, 3):
         cols = slice(n * part, (n + 1) * part)
-        for c in copies[n]:
-            c.wait()
+        for d in range(RING):
+            copy(p1.at[pl.ds(0, count)], n, d).wait()
         acc = None
         for d in range(RING):
             block = w_all[n, d].reshape(part, COLS)
@@ -412,16 +412,16 @@
         send[:, :, cols] = acc[half:].reshape(BATCHES, PIECE, part)
 
 
-def finish(received, w):
+def finish(received, rest, pieces, crossed):
     shape = bf(BATCHES, PIECE, WIDTH)
     return pl.pallas_call(
-        final_body, out_shape=(shape, shape), in_specs=[VMEM] * 4 + [ANY], out_specs=(VMEM,) * 2,
+        final_body, out_shape=(shape, shape), in_specs=[VMEM] * 4 + [ANY] * 7, out_specs=(VMEM,) * 2,
         scratch_shapes=[
             pltpu.VMEM((RING, RING, WIDTH // RING // ROWS, ROWS, COLS), jnp.bfloat16),
             pltpu.SemaphoreType.DMA((RING, RING)),
         ],
         compiler_params=PARAMS, name="finish",
-    )(*received, w)
+    )(*received, rest, *pieces, *crossed)
 
 
 def joined_cores(mine, theirs):
@@ -429,22 +429,16 @@
     return jnp.where(core == 0, jnp.concatenate((mine, theirs), 0), jnp.concatenate((theirs, mine), 0))
 
 
-def merge_body(mine, theirs, out, sems):
+def merge_body(mine, theirs, out):
     core = lax.axis_index("sp") % 2
-    copies = [
-        pltpu.make_async_copy(mine, out.at[pl.ds(core * BATCHES, BATCHES)], sems.at[0]),
-        pltpu.make_async_copy(theirs, out.at[pl.ds((1 - core) * BATCHES, BATCHES)], sems.at[1]),
-    ]
-    for c in copies:
-        c.start()
-    for c in copies:
-        c.wait()
+    out[pl.ds(core * BATCHES, BATCHES)] = mine[...]
+    out[pl.ds((1 - core) * BATCHES, BATCHES)] = theirs[...]
 
 
 def merged(mine, theirs):
     return pl.pallas_call(
-        merge_body, out_shape=bf(2 * BATCHES, PIECE, WIDTH), in_specs=[ANY] * 2, out_specs=ANY,
-        scratch_shapes=[pltpu.SemaphoreType.DMA((2,))], compiler_params=PARAMS, name="merge",
+        merge_body, out_shape=bf(2 * BATCHES, PIECE, WIDTH), in_specs=[VMEM] * 2, out_specs=VMEM,
+        compiler_params=PARAMS, name="merge",
     )(mine, theirs)
 
 
@@ -462,10 +456,8 @@
 
 
 def layer(tokens, norm_gain, w_query, w_key, w_value, w_out):
-    wide_own, rest_own = pack(w_query, w_key, w_value)
+    wide_own, rest_own = pack(w_query, w_key, w_value, w_out)
     rest = lax.all_gather(rest_own, "sp")
-    outs = lax.all_gather(jnp.transpose(w_out), ("sp", "tp"))
-    outs = outs.reshape(32, RING, ROWS, COLS)
 
     core = lax.axis_index("sp") % 2
     tokens = jnp.transpose(tokens, (1, 0, 2))
@@ -482,12 +474,14 @@
     back_early = from_behind(wide_early, 1)
     near, near_tail = project_near(early, late, rest)
     near_tail = from_behind(near_tail, 1)
+    outs = lax.dynamic_slice(rest, (16 * core, LAST, 0, 0), (16, 1, ROWS, COLS))[:, 0]
+    outs = ring_of(outs)[1:]
     queries = project_queries(early, late, rest)
     wide_out, wide_logs = attend_wide(queries, wide_early, wide_late, back_early, back_late, far_late)
     *combined, kept, sent = attend_near(queries, near, near_tail, wide_out, wide_logs)
 
     received = [combined[0]] + [turned(combined[d], d) for d in (1, 2, 3)]
-    mixed_mine, mixed_sent = finish(received, outs)
+    mixed_mine, mixed_sent = finish(received, rest, outs, [swapped(a) for a in outs])
     mixed = merged(mixed_mine, swapped(mixed_sent))
 
     log_weight = joined_cores(kept, swapped(sent)).reshape(2 * BATCHES, 2, BLOCK)

time: 182 us -> 165 us (0.907)
  Pallas kernels: 73.7 us -> 50.8 us
  starting transfers between devices: 40.4 us -> 48.5 us
  waiting for transfers between devices: 44.2 us -> 41.2 us
    all_gather x1, waiting for transfers between devices: 0.02 us -> 25 us  [layer(): rest = lax.all_gather(rest_own, 'sp')]
    pallas_call x1, Pallas kernels: 24.9 us -> 2.06 us  [merged(): pl.pallas_call(merge_body, out_shape=bf(2 * BATCHES, PIECE, WIDTH), in_sp...]
    all_gather x1 -> x0, waiting for transfers between devices: 16.8 us -> none  [layer(): outs = lax.all_gather(jnp.transpose(w_out), ('sp', 'tp'))]
    ppermute x9 -> x12, waiting for transfers between devices: 18.9 us -> 10.4 us  [turned(): return lax.ppermute(a, 'tp', [(i, (i + shift) % RING) for i in range(RING)])]
    ppermute x7 -> x10, starting transfers between devices: 6.1 us -> 12 us  [swapped(): return lax.ppermute(a, 'sp', SWAP)]
    ppermute x3, waiting for transfers between devices: 4.84 us -> 2.89 us  [spread(): near = {d: lax.ppermute(own, 'sp', first_leg(d, kind)) for d in (1, 3, 2)}]
    ppermute x9 -> x12, starting transfers between devices: 12.5 us -> 14.1 us  [turned(): return lax.ppermute(a, 'tp', [(i, (i + shift) % RING) for i in range(RING)])]
    unnamed x50 -> x58, local copies, waits for them, and re-layouts: 6.15 us -> 4.91 us
  transfers between devices with their start and end apart: 28 -> 33, of which waited for: 9 -> 7; matrix products, arithmetic and copies ran while one was open for 1% -> 2% of each run, Pallas kernels for 23% -> 25%
where the time goes in v4:
time: 165 us; the launch traced here: 164 us
  Pallas kernels  50.8 us (31%)
  starting transfers between devices  48.5 us (29%)
  waiting for transfers between devices  41.2 us (25%)
  between operations  14.5 us (9%)
  local copies, waits for them, and re-layouts  7.62 us (5%)
    all_gather x1, waiting for transfers between devices, layer(): rest = lax.all_gather(rest_own, 'sp')  25 us
    ppermute x12, starting transfers between devices, turned(): return lax.ppermute(a, 'tp', [(i, (i + shift) % RING) for i in range(RING)])  14.1 us
    ppermute x10, starting transfers between devices, swapped(): return lax.ppermute(a, 'sp', SWAP)  12 us
    ppermute x4, starting transfers between devices, from_behind(): lax.ppermute(a, 'sp', [(i, i + 2 * blocks) for i in range(32 - 2 * blocks)])  11.7 us
    pallas_call x1, Pallas kernels, project_near(): pl.pallas_call(near_pair_body, out_shape=(bf(2, 2, BATCHES, SPAN, COLS),...  10.7 us
    ppermute x12, waiting for transfers between devices, turned(): return lax.ppermute(a, 'tp', [(i, (i + shift) % RING) for i in range(RING)])  10.4 us
    pallas_call x2, Pallas kernels, project_wide(): pl.pallas_call(wide_pair_body, out_shape=bf(2, BATCHES, HALF, COLS), in_s...  8.58 us
    pallas_call x1, Pallas kernels, project_queries(): pl.pallas_call(query_body, out_shape=bf(GROUPS, BATCHES, SPAN, COLS), in_...  7.79 us
  transfers between devices with their start and end apart: 33, of which 7 were waited for; matrix products, arithmetic and copies ran while one was open for 2% of the time, Pallas kernels for 25%

profile of v4, /device:TPU:1, one launch (start us, length us, event | category | flops | bytes accessed | tf_op | source)
XLA Modules:
  0.0 163.6 jit_solution(6045374394214179863)
XLA Ops:
  7.2 1.7 %pack.1 = (bf16[2,64,256]{2,1,0:T(8,128)(2,1)}, bf16[8,64,256]{2,1,0:T(8,128)(2,1)}) custom-call(bf16[3,64,256]{2,1,0:T(8,128)(2,1)} %w_query.1, bf16[3,64,256]{2,1,0:T(8,128)(2,1)} %w_key.1, bf16[3,64,256]{2,1,0:T(8,128)(2,1)} %w_value.1, bf16[64,256]{1,0:T(8,128)(2,1)} %bitcast.24), custom_call_target="tpu_custom_call" | custom-call | tf_op jit(solution)/shard_map/pack/pallas_call | solution.py:99
  10.0 1.5 collective-permute-start
  11.5 1.7 %collective-permute-start.8 = (bf16[2,64,256]{2,1,0:T(8,128)(2,1)}, bf16[2,64,256]{2,1,0:T(8,128)(2,1)S(1)}, u32[]{:S(2)}, u32[]{:S(2)}) collective-permute-start(bf16[2,64,256]{2,1,0:T(8,128)(2,1)} %get-tuple-element.23), channel_id=1, source_target_pairs={{0,8},{4,36},{8,16},{12,44},{16,24},{20,52},{24,0},{28,60},{32,40}... | collective-permute-start | bytes 196616 | tf_op jit(solution)/shard_map/ppermute | solution.py:451
  13.2 3.3 %collective-permute-start.9 = (bf16[2,64,256]{2,1,0:T(8,128)(2,1)}, bf16[2,64,256]{2,1,0:T(8,128)(2,1)S(1)}, u32[]{:S(2)}, u32[]{:S(2)}) collective-permute-start(bf16[2,64,256]{2,1,0:T(8,128)(2,1)} %get-tuple-element.23), channel_id=1, source_target_pairs={{0,16},{4,68},{8,24},{12,76},{16,0},{20,84},{24,8},{28,92},{32,48}... | collective-permute-start | bytes 196616 | tf_op jit(solution)/shard_map/ppermute | solution.py:451
  17.3 1.8 %collective-permute-done.9 = bf16[2,64,256]{2,1,0:T(8,128)(2,1)S(1)} collective-permute-done((bf16[2,64,256]{2,1,0:T(8,128)(2,1)}, bf16[2,64,256]{2,1,0:T(8,128)(2,1)S(1)}, u32[]{:S(2)}, u32[]{:S(2)}) %collective-permute-start.9) | collective-permute-done | bytes 65568 | tf_op jit(solution)/shard_map/ppermute | solution.py:451
  22.1 2.6 %collective-permute-start.12 = (bf16[4,2,64,256]{3,2,1,0:T(8,128)(2,1)S(1)}, bf16[4,2,64,256]{3,2,1,0:T(8,128)(2,1)S(1)}, u32[]{:S(2)}, u32[]{:S(2)}) collective-permute-start(bf16[4,2,64,256]{3,2,1,0:T(8,128)(2,1)S(1)} %pad_maximum_fusion.refs_4_), channel_id=1, source_target_pairs={{0,64},{4,20},{8,72},{12,28},{16,80},{20,4},{24,88},{28,12},{32,96... | collective-permute-start | bytes 786440 | tf_op jit(solution)/shard_map/ppermute | solution.py:453
  26.5 2.7 %norm_rows.1 = (bf16[3,32,2048]{2,1,0:T(8,128)(2,1)}, bf16[3,32,2048]{2,1,0:T(8,128)(2,1)}) custom-call(bf16[6,32,2048]{2,1,0:T(8,128)(2,1)} %bitcast.18, bf16[3,32,2048]{2,1,0:T(8,128)(2,1)} %copy-done.22, f32[1,2048]{1,0:T(1,128)} %bitcast.25), custom_call_target="tpu_custom_call" | custom-call | tf_op jit(solution)/shard_map/norm_rows/pallas_call | solution.py:131
  30.5 2.6 %collective-permute-start.14 = (bf16[4,2,64,256]{3,2,1,0:T(8,128)(2,1)S(1)}, bf16[4,2,64,256]{3,2,1,0:T(8,128)(2,1)}, u32[]{:S(2)}, u32[]{:S(2)}) collective-permute-start(bf16[4,2,64,256]{3,2,1,0:T(8,128)(2,1)S(1)} %pad_maximum_fusion.refs_4_), channel_id=1, source_target_pairs={{0,4},{4,0},{8,12},{12,8},{16,20},{20,16},{24,28},{28,24},{32,36},... | collective-permute-start | bytes 786440 | tf_op jit(solution)/shard_map/ppermute | solution.py:54
  33.1 1.4 collective-permute-done.12.refs_6_
  34.5 3.0 %collective-permute-start.16 = (bf16[4,2,64,256]{3,2,1,0:T(8,128)(2,1)S(1)}, bf16[4,2,64,256]{3,2,1,0:T(8,128)(2,1)S(1)}, u32[]{:S(2)}, u32[]{:S(2)}) collective-permute-start(bf16[4,2,64,256]{3,2,1,0:T(8,128)(2,1)S(1)} %collective-permute-done.12.refs_6_), channel_id=1, source_target_pairs={{0,4},{4,0},{8,12},{12,8},{16,20},{20,16},{24,28},{28,24},{32,36},... | collective-permute-start | bytes 786440 | tf_op jit(solution)/shard_map/ppermute | solution.py:54
  37.6 2.7 %collective-permute-start.5 = (bf16[3,32,2048]{2,1,0:T(8,128)(2,1)}, bf16[3,32,2048]{2,1,0:T(8,128)(2,1)S(1)}, u32[]{:S(2)}, u32[]{:S(2)}) collective-permute-start(bf16[3,32,2048]{2,1,0:T(8,128)(2,1)} %get-tuple-element.19.refs_4_.refs_0_), channel_id=1, source_target_pairs={{0,2},{1,3},{2,0},{3,1},{4,6},{5,7},{6,4},{7,5},{8,10},{9,11},{10,... | collective-permute-start | bytes 1179656 | tf_op jit(solution)/shard_map/ppermute | solution.py:58
  43.1 2.1 %collective-permute-start.3 = (bf16[3,32,2048]{2,1,0:T(8,128)(2,1)}, bf16[3,32,2048]{2,1,0:T(8,128)(2,1)S(1)}, u32[]{:S(2)}, u32[]{:S(2)}) collective-permute-start(bf16[3,32,2048]{2,1,0:T(8,128)(2,1)} %get-tuple-element.18.refs_0_), channel_id=1, source_target_pairs={{0,3},{1,0},{2,1},{3,2},{4,7},{5,4},{6,5},{7,6},{8,11},{9,8},{10,9... | collective-permute-start | bytes 1179656 | tf_op jit(solution)/shard_map/ppermute | solution.py:58
  45.2 25.0 %all-gather.3.cloned.1.call-done = bf16[256,64,256]{2,1,0:T(8,128)(2,1)} async-done(((bf16[8,64,256]{2,1,0:T(8,128)(2,1)}), bf16[256,64,256]{2,1,0:T(8,128)(2,1)}) %all-gather.3.cloned.1.call-update) | async-done | bytes 8388624 | tf_op jit(solution)/shard_map/all_gather | solution.py:460
  71.3 1.3 collective-permute-start.24
  72.5 2.4 %collective-permute-start.25 = (bf16[16,64,256]{2,1,0:T(8,128)(2,1)S(1)}, bf16[16,64,256]{2,1,0:T(8,128)(2,1)S(1)}, u32[]{:S(2)}, u32[]{:S(2)}) collective-permute-start(bf16[16,64,256]{2,1,0:T(8,128)(2,1)S(1)} %dynamic-slice_bitcast_fusion), channel_id=1, source_target_pairs={{0,2},{1,3},{2,0},{3,1},{4,6},{5,7},{6,4},{7,5},{8,10},{9,11},{10,... | collective-permute-start | bytes 1572872 | tf_op jit(solution)/shard_map/ppermute | solution.py:58
  76.2 4.3 %project_wide.3.late = bf16[2,3,128,256]{3,2,1,0:T(8,128)(2,1)} custom-call(bf16[3,32,2048]{2,1,0:T(8,128)(2,1)} %get-tuple-element.19.refs_4_.refs_0_, bf16[3,32,2048]{2,1,0:T(8,128)(2,1)} %copy-done, bf16[3,32,2048]{2,1,0:T(8,128)(2,1)} %copy-done.1, bf16[3,32,2048]{2,1,0:T(8,128)(2,1)} %copy-done.2, bf16[4,2,64,256]{3,2,1,0:T(8,128)(2,1)} %copy-done.6, ...), custom_call_target="tpu_custom_call" | custom-call | tf_op jit(solution)/shard_map/project_wide/pallas_call | solution.py:177
  80.5 3.1 %collective-permute-start.19 = (bf16[2,3,128,256]{3,2,1,0:T(8,128)(2,1)}, bf16[2,3,128,256]{3,2,1,0:T(8,128)(2,1)S(1)}, u32[]{:S(2)}, u32[]{:S(2)}) collective-permute-start(bf16[2,3,128,256]{3,2,1,0:T(8,128)(2,1)} %project_wide.3.late), channel_id=1, source_target_pairs={{0,8},{4,12},{8,16},{12,20},{16,24},{20,28},{24,32},{28,36},{32,40... | collective-permute-start | bytes 1179656 | tf_op jit(solution)/shard_map/ppermute | solution.py:62
  83.7 4.5 %collective-permute-start.20 = (bf16[2,3,128,256]{3,2,1,0:T(8,128)(2,1)}, bf16[2,3,128,256]{3,2,1,0:T(8,128)(2,1)S(1)}, u32[]{:S(2)}, u32[]{:S(2)}) collective-permute-start(bf16[2,3,128,256]{3,2,1,0:T(8,128)(2,1)} %project_wide.3.late), channel_id=1, source_target_pairs={{0,16},{4,20},{8,24},{12,28},{16,32},{20,36},{24,40},{28,44},{32,4... | collective-permute-start | bytes 1179656 | tf_op jit(solution)/shard_map/ppermute | solution.py:62
  88.2 4.3 %project_wide.2.early = bf16[2,3,128,256]{3,2,1,0:T(8,128)(2,1)} custom-call(bf16[3,32,2048]{2,1,0:T(8,128)(2,1)} %get-tuple-element.18.refs_0_, bf16[3,32,2048]{2,1,0:T(8,128)(2,1)} %copy-done.3, bf16[3,32,2048]{2,1,0:T(8,128)(2,1)} %copy-done.4, bf16[3,32,2048]{2,1,0:T(8,128)(2,1)} %copy-done.5, bf16[4,2,64,256]{3,2,1,0:T(8,128)(2,1)} %copy-done.6, ...), custom_call_target="tpu_custom_call" | custom-call | tf_op jit(solution)/shard_map/project_wide/pallas_call | solution.py:177
  92.5 10.7 %project_near.1 = (bf16[2,2,3,256,256]{4,3,2,1,0:T(8,128)(2,1)}, bf16[2,3,128,256]{3,2,1,0:T(8,128)(2,1)}) custom-call(bf16[3,32,2048]{2,1,0:T(8,128)(2,1)} %get-tuple-element.18.refs_0_, bf16[3,32,2048]{2,1,0:T(8,128)(2,1)} %copy-done.3, bf16[3,32,2048]{2,1,0:T(8,128)(2,1)} %copy-done.4, bf16[3,32,2048]{2,1,0:T(8,128)(2,1)} %copy-done.5, ...), custom_call_target="tpu_custom_call" | custom-call | tf_op jit(solution)/shard_map/project_near/pallas_call | solution.py:245
  103.3 2.2 %collective-permute-start.18 = (bf16[2,3,128,256]{3,2,1,0:T(8,128)(2,1)S(1)}, bf16[2,3,128,256]{3,2,1,0:T(8,128)(2,1)S(1)}, u32[]{:S(2)}, u32[]{:S(2)}) collective-permute-start(bf16[2,3,128,256]{3,2,1,0:T(8,128)(2,1)S(1)} %copy-done.7), channel_id=1, source_target_pairs={{0,8},{4,12},{8,16},{12,20},{16,24},{20,28},{24,32},{28,36},{32,40... | collective-permute-start | bytes 1179656 | tf_op jit(solution)/shard_map/ppermute | solution.py:62
  105.5 1.9 %collective-permute-start.7 = (bf16[2,3,128,256]{3,2,1,0:T(8,128)(2,1)}, bf16[2,3,128,256]{3,2,1,0:T(8,128)(2,1)S(1)}, u32[]{:S(2)}, u32[]{:S(2)}) collective-permute-start(bf16[2,3,128,256]{3,2,1,0:T(8,128)(2,1)} %get-tuple-element.22), channel_id=1, source_target_pairs={{0,8},{4,12},{8,16},{12,20},{16,24},{20,28},{24,32},{28,36},{32,40... | collective-permute-start | bytes 1179656 | tf_op jit(solution)/shard_map/ppermute | solution.py:62
  107.4 2.0 %collective-permute-start.27 = (bf16[16,64,256]{2,1,0:T(8,128)(2,1)S(1)}, bf16[16,64,256]{2,1,0:T(8,128)(2,1)S(1)}, u32[]{:S(2)}, u32[]{:S(2)}) collective-permute-start(bf16[16,64,256]{2,1,0:T(8,128)(2,1)S(1)} %collective-permute-done.24.p1), channel_id=1, source_target_pairs={{0,4},{4,0},{8,12},{12,8},{16,20},{20,16},{24,28},{28,24},{32,36},... | collective-permute-start | bytes 1572872 | tf_op jit(solution)/shard_map/ppermute | solution.py:54
  110.0 7.8 %project_queries.1.q = bf16[3,3,256,256]{3,2,1,0:T(8,128)(2,1)} custom-call(bf16[3,32,2048]{2,1,0:T(8,128)(2,1)} %get-tuple-element.18.refs_0_, bf16[3,32,2048]{2,1,0:T(8,128)(2,1)} %copy-done.3, bf16[3,32,2048]{2,1,0:T(8,128)(2,1)} %copy-done.4, bf16[3,32,2048]{2,1,0:T(8,128)(2,1)} %copy-done.5, bf16[3,32,2048]{2,1,0:T(8,128)(2,1)} %get-tuple-element.19.refs_4_.refs_0_, ...), custom_call_target="tpu_custom_call" | custom-call | tf_op jit(solution)/shard_map/project_queries/pallas_call | solution.py:254
  118.6 5.1 %attend_wide.1 = (f32[3,256,256]{2,1,0:T(8,128)}, f32[3,256,256]{2,1,0:T(8,128)}) custom-call(bf16[3,3,256,256]{3,2,1,0:T(8,128)(2,1)} %project_queries.1.q, bf16[2,3,128,256]{3,2,1,0:T(8,128)(2,1)} %project_wide.2.early, bf16[2,3,128,256]{3,2,1,0:T(8,128)(2,1)} %project_wide.3.late, bf16[2,3,128,256]{3,2,1,0:T(8,128)(2,1)} %copy-done.21, ...), custom_call_target="tpu_custom_call" | custom-call | tf_op jit(solution)/shard_map/attend_wide/pallas_call | solution.py:319
  124.5 6.6 %attend_near.1 = (bf16[2,3,32,256]{3,2,1,0:T(8,128)(2,1)}, bf16[2,3,32,256]{3,2,1,0:T(8,128)(2,1)}, bf16[2,3,32,256]{3,2,1,0:T(8,128)(2,1)}, bf16[2,3,32,256]{3,...) custom-call(bf16[3,3,256,256]{3,2,1,0:T(8,128)(2,1)} %project_queries.1.q, ...), custom_call_target="tpu_custom_call" | custom-call | tf_op jit(solution)/shard_map/attend_near/pallas_call | solution.py:370
  132.4 6.7 %collective-permute-done.21.r1 = bf16[2,3,32,256]{3,2,1,0:T(8,128)(2,1)S(1)} collective-permute-done((bf16[2,3,32,256]{3,2,1,0:T(8,128)(2,1)}, bf16[2,3,32,256]{3,2,1,0:T(8,128)(2,1)S(1)}, u32[]{:S(2)}, u32[]{:S(2)}) %collective-permute-start.21) | collective-permute-done | bytes 98336 | tf_op jit(solution)/shard_map/ppermute | solution.py:58
  139.1 3.7 %collective-permute-done.23.r3 = bf16[2,3,32,256]{3,2,1,0:T(8,128)(2,1)S(1)} collective-permute-done((bf16[2,3,32,256]{3,2,1,0:T(8,128)(2,1)}, bf16[2,3,32,256]{3,2,1,0:T(8,128)(2,1)S(1)}, u32[]{:S(2)}, u32[]{:S(2)}) %collective-permute-start.23) | collective-permute-done | bytes 98336 | tf_op jit(solution)/shard_map/ppermute | solution.py:58
  143.9 5.5 %finish.1 = (bf16[3,32,2048]{2,1,0:T(8,128)(2,1)}, bf16[3,32,2048]{2,1,0:T(8,128)(2,1)}) custom-call(bf16[2,3,32,256]{3,2,1,0:T(8,128)(2,1)} %get-tuple-element.26.r0, bf16[2,3,32,256]{3,2,1,0:T(8,128)(2,1)} %copy-done.24, bf16[2,3,32,256]{3,2,1,0:T(8,128)(2,1)} %copy-done.25, bf16[2,3,32,256]{3,2,1,0:T(8,128)(2,1)} %copy-done.26, ...), custom_call_target="tpu_custom_call" | custom-call | tf_op jit(solution)/shard_map/finish/pallas_call | solution.py:417
  149.5 2.2 %collective-permute-start.30 = (bf16[3,32,2048]{2,1,0:T(8,128)(2,1)}, bf16[3,32,2048]{2,1,0:T(8,128)(2,1)S(1)}, u32[]{:S(2)}, u32[]{:S(2)}) collective-permute-start(bf16[3,32,2048]{2,1,0:T(8,128)(2,1)} %get-tuple-element.31), channel_id=1, source_target_pairs={{0,4},{4,0},{8,12},{12,8},{16,20},{20,16},{24,28},{28,24},{32,36},... | collective-permute-start | bytes 1179656 | tf_op jit(solution)/shard_map/ppermute | solution.py:54
  151.8 1.5 collective-permute-done.31
  154.7 2.1 %merge.1 = bf16[6,32,2048]{2,1,0:T(8,128)(2,1)} custom-call(bf16[3,32,2048]{2,1,0:T(8,128)(2,1)} %get-tuple-element.30.mine, bf16[3,32,2048]{2,1,0:T(8,128)(2,1)} %copy-done.23), custom_call_target="tpu_custom_call" | custom-call | tf_op jit(solution)/shard_map/merge/pallas_call | solution.py:439
  (108 shorter events, 19.1 us)
Async XLA Ops:
  7.2 63.0 %all-gather.3.cloned.1.call-start = ((), (), s32[]{:S(2)}) async-start(), calls=%async_computation | async-start | bytes 8650752 | tf_op jit(solution)/shard_map/all_gather | solution.py:460
  10.0 15.8 %collective-permute-start = (bf16[3,32,2048]{2,1,0:T(8,128)(2,1)S(1)}, bf16[3,32,2048]{2,1,0:T(8,128)(2,1)S(1)}, u32[]{:S(2)}, u32[]{:S(2)}) collective-permute-start(bf16[3,32,2048]{2,1,0:T(8,128)(2,1)S(1)} %dynamic-slice_bitcast_fusion.1), channel_id=1, source_target_pairs={{0,4},{4,0},{8,12},{12,8},{16,20},{20,16},{24,28},{28,24},{32,36},... | collective-permute-start | bytes 1179656 | tf_op jit(solution)/shard_map/ppermute | solution.py:54
  11.5 5.8 %collective-permute-start.8 = (bf16[2,64,256]{2,1,0:T(8,128)(2,1)}, bf16[2,64,256]{2,1,0:T(8,128)(2,1)S(1)}, u32[]{:S(2)}, u32[]{:S(2)}) collective-permute-start(bf16[2,64,256]{2,1,0:T(8,128)(2,1)} %get-tuple-element.23), channel_id=1, source_target_pairs={{0,8},{4,36},{8,16},{12,44},{16,24},{20,52},{24,0},{28,60},{32,40}... | collective-permute-start | bytes 196616 | tf_op jit(solution)/shard_map/ppermute | solution.py:451
  13.2 5.9 %collective-permute-start.9 = (bf16[2,64,256]{2,1,0:T(8,128)(2,1)}, bf16[2,64,256]{2,1,0:T(8,128)(2,1)S(1)}, u32[]{:S(2)}, u32[]{:S(2)}) collective-permute-start(bf16[2,64,256]{2,1,0:T(8,128)(2,1)} %get-tuple-element.23), channel_id=1, source_target_pairs={{0,16},{4,68},{8,24},{12,76},{16,0},{20,84},{24,8},{28,92},{32,48}... | collective-permute-start | bytes 196616 | tf_op jit(solution)/shard_map/ppermute | solution.py:451
  16.5 3.6 %collective-permute-start.10 = (bf16[2,64,256]{2,1,0:T(8,128)(2,1)}, bf16[2,64,256]{2,1,0:T(8,128)(2,1)S(1)}, u32[]{:S(2)}, u32[]{:S(2)}) collective-permute-start(bf16[2,64,256]{2,1,0:T(8,128)(2,1)} %get-tuple-element.23), channel_id=1, source_target_pairs={{0,24},{4,100},{8,0},{12,108},{16,8},{20,116},{24,16},{28,124},{32... | collective-permute-start | bytes 196616 | tf_op jit(solution)/shard_map/ppermute | solution.py:451
  21.0 12.0 %collective-permute-start.11 = (bf16[4,2,64,256]{3,2,1,0:T(8,128)(2,1)S(1)}, bf16[4,2,64,256]{3,2,1,0:T(8,128)(2,1)S(1)}, u32[]{:S(2)}, u32[]{:S(2)}) collective-permute-start(bf16[4,2,64,256]{3,2,1,0:T(8,128)(2,1)S(1)} %pad_maximum_fusion.refs_4_), channel_id=1, source_target_pairs={{0,32},{4,12},{8,40},{12,20},{16,48},{20,28},{24,56},{28,4},{32,64... | collective-permute-start | bytes 786440 | tf_op jit(solution)/shard_map/ppermute | solution.py:453
  22.1 12.4 %collective-permute-start.12 = (bf16[4,2,64,256]{3,2,1,0:T(8,128)(2,1)S(1)}, bf16[4,2,64,256]{3,2,1,0:T(8,128)(2,1)S(1)}, u32[]{:S(2)}, u32[]{:S(2)}) collective-permute-start(bf16[4,2,64,256]{3,2,1,0:T(8,128)(2,1)S(1)} %pad_maximum_fusion.refs_4_), channel_id=1, source_target_pairs={{0,64},{4,20},{8,72},{12,28},{16,80},{20,4},{24,88},{28,12},{32,96... | collective-permute-start | bytes 786440 | tf_op jit(solution)/shard_map/ppermute | solution.py:453
  24.7 12.8 %collective-permute-start.13 = (bf16[4,2,64,256]{3,2,1,0:T(8,128)(2,1)S(1)}, bf16[4,2,64,256]{3,2,1,0:T(8,128)(2,1)S(1)}, u32[]{:S(2)}, u32[]{:S(2)}) collective-permute-start(bf16[4,2,64,256]{3,2,1,0:T(8,128)(2,1)S(1)} %pad_maximum_fusion.refs_4_), channel_id=1, source_target_pairs={{0,96},{4,28},{8,104},{12,4},{16,112},{20,12},{24,120},{28,20},{32... | collective-permute-start | bytes 786440 | tf_op jit(solution)/shard_map/ppermute | solution.py:453
  29.2 13.8 %collective-permute-start.4 = (bf16[3,32,2048]{2,1,0:T(8,128)(2,1)}, bf16[3,32,2048]{2,1,0:T(8,128)(2,1)S(1)}, u32[]{:S(2)}, u32[]{:S(2)}) collective-permute-start(bf16[3,32,2048]{2,1,0:T(8,128)(2,1)} %get-tuple-element.19.refs_4_.refs_0_), channel_id=1, source_target_pairs={{0,1},{1,2},{2,3},{3,0},{4,5},{5,6},{6,7},{7,4},{8,9},{9,10},{10,1... | collective-permute-start | bytes 1179656 | tf_op jit(solution)/shard_map/ppermute | solution.py:58
  30.5 7.1 %collective-permute-start.14 = (bf16[4,2,64,256]{3,2,1,0:T(8,128)(2,1)S(1)}, bf16[4,2,64,256]{3,2,1,0:T(8,128)(2,1)}, u32[]{:S(2)}, u32[]{:S(2)}) collective-permute-start(bf16[4,2,64,256]{3,2,1,0:T(8,128)(2,1)S(1)} %pad_maximum_fusion.refs_4_), channel_id=1, source_target_pairs={{0,4},{4,0},{8,12},{12,8},{16,20},{20,16},{24,28},{28,24},{32,36},... | collective-permute-start | bytes 786440 | tf_op jit(solution)/shard_map/ppermute | solution.py:54
  33.0 7.2 %collective-permute-start.15 = (bf16[4,2,64,256]{3,2,1,0:T(8,128)(2,1)S(1)}, bf16[4,2,64,256]{3,2,1,0:T(8,128)(2,1)}, u32[]{:S(2)}, u32[]{:S(2)}) collective-permute-start(bf16[4,2,64,256]{3,2,1,0:T(8,128)(2,1)S(1)} %collective-permute-done.11.refs_5_), channel_id=1, source_target_pairs={{0,4},{4,0},{8,12},{12,8},{16,20},{20,16},{24,28},{28,24},{32,36},... | collective-permute-start | bytes 786440 | tf_op jit(solution)/shard_map/ppermute | solution.py:54
  34.5 6.7 %collective-permute-start.16 = (bf16[4,2,64,256]{3,2,1,0:T(8,128)(2,1)S(1)}, bf16[4,2,64,256]{3,2,1,0:T(8,128)(2,1)S(1)}, u32[]{:S(2)}, u32[]{:S(2)}) collective-permute-start(bf16[4,2,64,256]{3,2,1,0:T(8,128)(2,1)S(1)} %collective-permute-done.12.refs_6_), channel_id=1, source_target_pairs={{0,4},{4,0},{8,12},{12,8},{16,20},{20,16},{24,28},{28,24},{32,36},... | collective-permute-start | bytes 786440 | tf_op jit(solution)/shard_map/ppermute | solution.py:54
  37.5 5.0 %collective-permute-start.17 = (bf16[4,2,64,256]{3,2,1,0:T(8,128)(2,1)S(1)}, bf16[4,2,64,256]{3,2,1,0:T(8,128)(2,1)}, u32[]{:S(2)}, u32[]{:S(2)}) collective-permute-start(bf16[4,2,64,256]{3,2,1,0:T(8,128)(2,1)S(1)} %collective-permute-done.13.refs_7_), channel_id=1, source_target_pairs={{0,4},{4,0},{8,12},{12,8},{16,20},{20,16},{24,28},{28,24},{32,36},... | collective-permute-start | bytes 786440 | tf_op jit(solution)/shard_map/ppermute | solution.py:54
  37.6 33.7 %collective-permute-start.5 = (bf16[3,32,2048]{2,1,0:T(8,128)(2,1)}, bf16[3,32,2048]{2,1,0:T(8,128)(2,1)S(1)}, u32[]{:S(2)}, u32[]{:S(2)}) collective-permute-start(bf16[3,32,2048]{2,1,0:T(8,128)(2,1)} %get-tuple-element.19.refs_4_.refs_0_), channel_id=1, source_target_pairs={{0,2},{1,3},{2,0},{3,1},{4,6},{5,7},{6,4},{7,5},{8,10},{9,11},{10,... | collective-permute-start | bytes 1179656 | tf_op jit(solution)/shard_map/ppermute | solution.py:58
  40.3 32.2 %collective-permute-start.6 = (bf16[3,32,2048]{2,1,0:T(8,128)(2,1)}, bf16[3,32,2048]{2,1,0:T(8,128)(2,1)S(1)}, u32[]{:S(2)}, u32[]{:S(2)}) collective-permute-start(bf16[3,32,2048]{2,1,0:T(8,128)(2,1)} %get-tuple-element.19.refs_4_.refs_0_), channel_id=1, source_target_pairs={{0,3},{1,0},{2,1},{3,2},{4,7},{5,4},{6,5},{7,6},{8,11},{9,8},{10,9... | collective-permute-start | bytes 1179656 | tf_op jit(solution)/shard_map/ppermute | solution.py:58
  41.9 33.1 %collective-permute-start.1 = (bf16[3,32,2048]{2,1,0:T(8,128)(2,1)}, bf16[3,32,2048]{2,1,0:T(8,128)(2,1)S(1)}, u32[]{:S(2)}, u32[]{:S(2)}) collective-permute-start(bf16[3,32,2048]{2,1,0:T(8,128)(2,1)} %get-tuple-element.18.refs_0_), channel_id=1, source_target_pairs={{0,1},{1,2},{2,3},{3,0},{4,5},{5,6},{6,7},{7,4},{8,9},{9,10},{10,1... | collective-permute-start | bytes 1179656 | tf_op jit(solution)/shard_map/ppermute | solution.py:58
  42.5 38.0 %collective-permute-start.2 = (bf16[3,32,2048]{2,1,0:T(8,128)(2,1)}, bf16[3,32,2048]{2,1,0:T(8,128)(2,1)S(1)}, u32[]{:S(2)}, u32[]{:S(2)}) collective-permute-start(bf16[3,32,2048]{2,1,0:T(8,128)(2,1)} %get-tuple-element.18.refs_0_), channel_id=1, source_target_pairs={{0,2},{1,3},{2,0},{3,1},{4,6},{5,7},{6,4},{7,5},{8,10},{9,11},{10,... | collective-permute-start | bytes 1179656 | tf_op jit(solution)/shard_map/ppermute | solution.py:58
  43.1 40.6 %collective-permute-start.3 = (bf16[3,32,2048]{2,1,0:T(8,128)(2,1)}, bf16[3,32,2048]{2,1,0:T(8,128)(2,1)S(1)}, u32[]{:S(2)}, u32[]{:S(2)}) collective-permute-start(bf16[3,32,2048]{2,1,0:T(8,128)(2,1)} %get-tuple-element.18.refs_0_), channel_id=1, source_target_pairs={{0,3},{1,0},{2,1},{3,2},{4,7},{5,4},{6,5},{7,6},{8,11},{9,8},{10,9... | collective-permute-start | bytes 1179656 | tf_op jit(solution)/shard_map/ppermute | solution.py:58
  71.3 36.1 %collective-permute-start.24 = (bf16[16,64,256]{2,1,0:T(8,128)(2,1)S(1)}, bf16[16,64,256]{2,1,0:T(8,128)(2,1)S(1)}, u32[]{:S(2)}, u32[]{:S(2)}) collective-permute-start(bf16[16,64,256]{2,1,0:T(8,128)(2,1)S(1)} %dynamic-slice_bitcast_fusion), channel_id=1, source_target_pairs={{0,1},{1,2},{2,3},{3,0},{4,5},{5,6},{6,7},{7,4},{8,9},{9,10},{10,1... | collective-permute-start | bytes 1572872 | tf_op jit(solution)/shard_map/ppermute | solution.py:58
  72.5 36.9 %collective-permute-start.25 = (bf16[16,64,256]{2,1,0:T(8,128)(2,1)S(1)}, bf16[16,64,256]{2,1,0:T(8,128)(2,1)S(1)}, u32[]{:S(2)}, u32[]{:S(2)}) collective-permute-start(bf16[16,64,256]{2,1,0:T(8,128)(2,1)S(1)} %dynamic-slice_bitcast_fusion), channel_id=1, source_target_pairs={{0,2},{1,3},{2,0},{3,1},{4,6},{5,7},{6,4},{7,5},{8,10},{9,11},{10,... | collective-permute-start | bytes 1572872 | tf_op jit(solution)/shard_map/ppermute | solution.py:58
  75.0 34.6 %collective-permute-start.26 = (bf16[16,64,256]{2,1,0:T(8,128)(2,1)S(1)}, bf16[16,64,256]{2,1,0:T(8,128)(2,1)S(1)}, u32[]{:S(2)}, u32[]{:S(2)}) collective-permute-start(bf16[16,64,256]{2,1,0:T(8,128)(2,1)S(1)} %dynamic-slice_bitcast_fusion), channel_id=1, source_target_pairs={{0,3},{1,0},{2,1},{3,2},{4,7},{5,4},{6,5},{7,6},{8,11},{9,8},{10,9... | collective-permute-start | bytes 1572872 | tf_op jit(solution)/shard_map/ppermute | solution.py:58
  80.5 22.7 %collective-permute-start.19 = (bf16[2,3,128,256]{3,2,1,0:T(8,128)(2,1)}, bf16[2,3,128,256]{3,2,1,0:T(8,128)(2,1)S(1)}, u32[]{:S(2)}, u32[]{:S(2)}) collective-permute-start(bf16[2,3,128,256]{3,2,1,0:T(8,128)(2,1)} %project_wide.3.late), channel_id=1, source_target_pairs={{0,8},{4,12},{8,16},{12,20},{16,24},{20,28},{24,32},{28,36},{32,40... | collective-permute-start | bytes 1179656 | tf_op jit(solution)/shard_map/ppermute | solution.py:62
  83.7 21.8 %collective-permute-start.20 = (bf16[2,3,128,256]{3,2,1,0:T(8,128)(2,1)}, bf16[2,3,128,256]{3,2,1,0:T(8,128)(2,1)S(1)}, u32[]{:S(2)}, u32[]{:S(2)}) collective-permute-start(bf16[2,3,128,256]{3,2,1,0:T(8,128)(2,1)} %project_wide.3.late), channel_id=1, source_target_pairs={{0,16},{4,20},{8,24},{12,28},{16,32},{20,36},{24,40},{28,44},{32,4... | collective-permute-start | bytes 1179656 | tf_op jit(solution)/shard_map/ppermute | solution.py:62
  103.3 14.5 %collective-permute-start.18 = (bf16[2,3,128,256]{3,2,1,0:T(8,128)(2,1)S(1)}, bf16[2,3,128,256]{3,2,1,0:T(8,128)(2,1)S(1)}, u32[]{:S(2)}, u32[]{:S(2)}) collective-permute-start(bf16[2,3,128,256]{3,2,1,0:T(8,128)(2,1)S(1)} %copy-done.7), channel_id=1, source_target_pairs={{0,8},{4,12},{8,16},{12,20},{16,24},{20,28},{24,32},{28,36},{32,40... | collective-permute-start | bytes 1179656 | tf_op jit(solution)/shard_map/ppermute | solution.py:62
  105.5 18.3 %collective-permute-start.7 = (bf16[2,3,128,256]{3,2,1,0:T(8,128)(2,1)}, bf16[2,3,128,256]{3,2,1,0:T(8,128)(2,1)S(1)}, u32[]{:S(2)}, u32[]{:S(2)}) collective-permute-start(bf16[2,3,128,256]{3,2,1,0:T(8,128)(2,1)} %get-tuple-element.22), channel_id=1, source_target_pairs={{0,8},{4,12},{8,16},{12,20},{16,24},{20,28},{24,32},{28,36},{32,40... | collective-permute-start | bytes 1179656 | tf_op jit(solution)/shard_map/ppermute | solution.py:62
  107.4 35.4 %collective-permute-start.27 = (bf16[16,64,256]{2,1,0:T(8,128)(2,1)S(1)}, bf16[16,64,256]{2,1,0:T(8,128)(2,1)S(1)}, u32[]{:S(2)}, u32[]{:S(2)}) collective-permute-start(bf16[16,64,256]{2,1,0:T(8,128)(2,1)S(1)} %collective-permute-done.24.p1), channel_id=1, source_target_pairs={{0,4},{4,0},{8,12},{12,8},{16,20},{20,16},{24,28},{28,24},{32,36},... | collective-permute-start | bytes 1572872 | tf_op jit(solution)/shard_map/ppermute | solution.py:54
  109.4 33.3 %collective-permute-start.28 = (bf16[16,64,256]{2,1,0:T(8,128)(2,1)S(1)}, bf16[16,64,256]{2,1,0:T(8,128)(2,1)S(1)}, u32[]{:S(2)}, u32[]{:S(2)}) collective-permute-start(bf16[16,64,256]{2,1,0:T(8,128)(2,1)S(1)} %collective-permute-done.25.p2), channel_id=1, source_target_pairs={{0,4},{4,0},{8,12},{12,8},{16,20},{20,16},{24,28},{28,24},{32,36},... | collective-permute-start | bytes 1572872 | tf_op jit(solution)/shard_map/ppermute | solution.py:54
  109.6 33.2 %collective-permute-start.29 = (bf16[16,64,256]{2,1,0:T(8,128)(2,1)S(1)}, bf16[16,64,256]{2,1,0:T(8,128)(2,1)S(1)}, u32[]{:S(2)}, u32[]{:S(2)}) collective-permute-start(bf16[16,64,256]{2,1,0:T(8,128)(2,1)S(1)} %collective-permute-done.26.p3), channel_id=1, source_target_pairs={{0,4},{4,0},{8,12},{12,8},{16,20},{20,16},{24,28},{28,24},{32,36},... | collective-permute-start | bytes 1572872 | tf_op jit(solution)/shard_map/ppermute | solution.py:54
  131.1 8.0 %collective-permute-start.21 = (bf16[2,3,32,256]{3,2,1,0:T(8,128)(2,1)}, bf16[2,3,32,256]{3,2,1,0:T(8,128)(2,1)S(1)}, u32[]{:S(2)}, u32[]{:S(2)}) collective-permute-start(bf16[2,3,32,256]{3,2,1,0:T(8,128)(2,1)} %get-tuple-element.27), channel_id=1, source_target_pairs={{0,1},{1,2},{2,3},{3,0},{4,5},{5,6},{6,7},{7,4},{8,9},{9,10},{10,1... | collective-permute-start | bytes 294920 | tf_op jit(solution)/shard_map/ppermute | solution.py:58
  131.7 7.4 %collective-permute-start.22 = (bf16[2,3,32,256]{3,2,1,0:T(8,128)(2,1)}, bf16[2,3,32,256]{3,2,1,0:T(8,128)(2,1)S(1)}, u32[]{:S(2)}, u32[]{:S(2)}) collective-permute-start(bf16[2,3,32,256]{3,2,1,0:T(8,128)(2,1)} %get-tuple-element.28), channel_id=1, source_target_pairs={{0,2},{1,3},{2,0},{3,1},{4,6},{5,7},{6,4},{7,5},{8,10},{9,11},{10,... | collective-permute-start | bytes 294920 | tf_op jit(solution)/shard_map/ppermute | solution.py:58
  139.1 3.7 %collective-permute-start.23 = (bf16[2,3,32,256]{3,2,1,0:T(8,128)(2,1)}, bf16[2,3,32,256]{3,2,1,0:T(8,128)(2,1)S(1)}, u32[]{:S(2)}, u32[]{:S(2)}) collective-permute-start(bf16[2,3,32,256]{3,2,1,0:T(8,128)(2,1)} %get-tuple-element.29), channel_id=1, source_target_pairs={{0,3},{1,0},{2,1},{3,2},{4,7},{5,4},{6,5},{7,6},{8,11},{9,8},{10,9... | collective-permute-start | bytes 294920 | tf_op jit(solution)/shard_map/ppermute | solution.py:58
  149.5 4.4 %collective-permute-start.30 = (bf16[3,32,2048]{2,1,0:T(8,128)(2,1)}, bf16[3,32,2048]{2,1,0:T(8,128)(2,1)S(1)}, u32[]{:S(2)}, u32[]{:S(2)}) collective-permute-start(bf16[3,32,2048]{2,1,0:T(8,128)(2,1)} %get-tuple-element.31), channel_id=1, source_target_pairs={{0,4},{4,0},{8,12},{12,8},{16,20},{20,16},{24,28},{28,24},{32,36},... | collective-permute-start | bytes 1179656 | tf_op jit(solution)/shard_map/ppermute | solution.py:54
  (30 other events, 409.1 us)
Sparse Core Ops, SparseCore 0:
  10.2 59.8 all-gather.2

commit v5 on v4

--- a/solution.py
+++ b/solution.py
@@ -184,35 +184,47 @@
     )(*pieces, *lines)
 
 
-def matrix_copies(shards_of, first, count, w_all, sems):
-    return [
-        pltpu.make_async_copy(shards_of.at[:, first + m], w_all.at[m], sems.at[m]) for m in range(count)
-    ]
+def matrix_copies(lines, first, count, w_all, sems):
+    core = lax.axis_index("sp") % 2
+    groups = [[] for _ in range(count)]
+    for n, line in enumerate(lines):
+        whose = core if n < RING else 1 - core
+        for j in range(RING):
+            at = pl.multiple_of(place_of(whose, j, n % RING, 0) * ROWS, ROWS)
+            for m in range(count):
+                groups[m].append(
+                    pltpu.make_async_copy(
+                        line.at[j, first + m], w_all.at[m, pl.ds(at, ROWS), :], sems.at[m, n * RING + j]
+                    )
+                )
+    return groups
 
 
 def project(x_all, w_all, m):
     x = x_all[...].reshape(BATCHES * SPAN, WIDTH)
-    y = jnp.dot(x, w_all[m].reshape(WIDTH, COLS), preferred_element_type=jnp.float32)
+    y = jnp.dot(x, w_all[m], preferred_element_type=jnp.float32)
     return y.astype(jnp.bfloat16).reshape(BATCHES, SPAN, COLS)
 
 
 def staged(early, late, rest, first, count, x_all, w_all, x_sems, w_sems, work):
     rows = row_copies(early, 0, x_all, x_sems) + row_copies(late, HALF, x_all, x_sems)
     weights = matrix_copies(rest, first, count, w_all, w_sems)
-    for c in rows + weights[:2]:
+    for c in rows + weights[0] + weights[1]:
         c.start()
     for c in rows:
         c.wait()
     for m in range(count):
-        weights[m].wait()
+        for c in weights[m]:
+            c.wait()
         if m + 2 < count:
-            weights[m + 2].start()
+            for c in weights[m + 2]:
+                c.start()
         work(m, project(x_all, w_all, m))
 
 
 def near_pair_body(*refs):
-    early, late, rest = refs[:4], refs[4:8], refs[8]
-    near, near_tail, *scratch = refs[9:]
+    early, late, rest = refs[:4], refs[4:8], refs[8:16]
+    near, near_tail, *scratch = refs[16:]
 
     def work(m, y):
         near[m // 2, m % 2] = y
@@ -225,8 +237,8 @@
 
 
 def query_body(*refs):
-    early, late, rest = refs[:4], refs[4:8], refs[8]
-    queries, *scratch = refs[9:]
+    early, late, rest = refs[:4], refs[4:8], refs[8:16]
+    queries, *scratch = refs[16:]
 
     def work(m, y):
         queries[m] = y
@@ -236,8 +248,8 @@
 
 def rest_scratch(count):
     return [
-        pltpu.VMEM((BATCHES, SPAN, WIDTH), jnp.bfloat16), pltpu.VMEM((count, 32, ROWS, COLS), jnp.bfloat16),
-        pltpu.SemaphoreType.DMA((2, RING)), pltpu.SemaphoreType.DMA((count,)),
+        pltpu.VMEM((BATCHES, SPAN, WIDTH), jnp.bfloat16), pltpu.VMEM((count, WIDTH, COLS), jnp.bfloat16),
+        pltpu.SemaphoreType.DMA((2, RING)), pltpu.SemaphoreType.DMA((count, 32)),
     ]
 
 
@@ -245,17 +257,17 @@
     return pl.pallas_call(
         near_pair_body,
         out_shape=(bf(2, 2, BATCHES, SPAN, COLS), bf(2, BATCHES, HALOS[0] + HALOS[1], COLS)),
-        in_specs=[ANY] * 9, out_specs=(VMEM,) * 2, scratch_shapes=rest_scratch(NEAR),
+        in_specs=[ANY] * 16, out_specs=(VMEM,) * 2, scratch_shapes=rest_scratch(NEAR),
         compiler_params=PARAMS, name="project_near",
-    )(*early, *late, rest)
+    )(*early, *late, *rest)
 
 
 def project_queries(early, late, rest):
     return pl.pallas_call(
         query_body, out_shape=bf(GROUPS, BATCHES, SPAN, COLS),
-        in_specs=[ANY] * 9, out_specs=VMEM, scratch_shapes=rest_scratch(GROUPS),
+        in_specs=[ANY] * 16, out_specs=VMEM, scratch_shapes=rest_scratch(GROUPS),
         compiler_params=PARAMS, name="project_queries",
-    )(*early, *late, rest)
+    )(*early, *late, *rest)
 
 
 def bias_of(group, block):
@@ -382,29 +394,52 @@
     )(q, near, tail, other, logs)
 
 
-def final_body(r0, r1, r2, r3, rest, p1, p2, p3, q1, q2, q3, keep, send, w_all, sems):
+def pick_body(a0, a1, a2, a3, out, sems):
+    copies = [
+        pltpu.make_async_copy(a.at[:, LAST], out.at[pl.ds(RING * e, RING)], sems.at[e])
+        for e, a in enumerate((a0, a1, a2, a3))
+    ]
+    for c in copies:
+        c.start()
+    for c in copies:
+        c.wait()
+
+
+def pick(lines):
+    return pl.pallas_call(
+        pick_body, out_shape=bf(16, ROWS, COLS), in_specs=[ANY] * 4, out_specs=VMEM,
+        scratch_shapes=[pltpu.SemaphoreType.DMA((4,))], compiler_params=PARAMS, name="pick",
+    )(*lines)
+
+
+def final_body(*refs):
+    received, lines, ours, crossed = refs[:4], refs[4:12], refs[12:15], refs[15:18]
+    keep, send, w_all, sems = refs[18:]
     core = lax.axis_index("sp") % 2
     part = WIDTH // RING
     half = BATCHES * PIECE
     count = part // ROWS
-
-    def copy(source, n, d):
-        return pltpu.make_async_copy(source, w_all.at[n, d], sems.at[n, d])
-
-    for m in range(2):
-        for n in (m, m + 2):
-            copy(rest.at[pl.ds(n * count, count), LAST], n, 0).start()
-        for d, (p, q) in enumerate(((p1, q1), (p2, q2), (p3, q3)), 1):
-            copy(p.at[pl.ds(m * count, count)], 2 * core + m, d).start()
-            copy(q.at[pl.ds(m * count, count)], 2 * (1 - core) + m, d).start()
-    rows = [r[...].reshape(2 * half, COLS) for r in (r0, r1, r2, r3)]
-    for n in (0, 2, 1, 3):
+    copies = []
+    for n in range(2 * RING):
+        whose = core if n < RING else 1 - core
+        others = ours if n < RING else crossed
+        for j in range(RING):
+            k = place_of(whose, j, n % RING, 0)
+            at = n * RING + j
+            copies.append(pltpu.make_async_copy(lines[n].at[j, LAST], w_all.at[0, k], sems.at[0, at]))
+            for d, piece in enumerate(others, 1):
+                source = piece.at[(n % RING) * RING + j]
+                copies.append(pltpu.make_async_copy(source, w_all.at[d, k], sems.at[d, at]))
+    for c in copies:
+        c.start()
+    for c in copies:
+        c.wait()
+    rows = [r[...].reshape(2 * half, COLS) for r in received]
+    for n in range(RING):
         cols = slice(n * part, (n + 1) * part)
-        for d in range(RING):
-            copy(p1.at[pl.ds(0, count)], n, d).wait()
         acc = None
         for d in range(RING):
-            block = w_all[n, d].reshape(part, COLS)
+            block = w_all[d, n * count : (n + 1) * count].reshape(part, COLS)
             y = lax.dot_general(rows[d], block, (((1,), (1,)), ((), ())), preferred_element_type=jnp.float32)
             acc = y if acc is None else acc + y
         acc = acc.astype(jnp.bfloat16)
@@ -412,16 +447,15 @@
         send[:, :, cols] = acc[half:].reshape(BATCHES, PIECE, part)
 
 
-def finish(received, rest, pieces, crossed):
+def finish(received, lines, pieces, crossed):
     shape = bf(BATCHES, PIECE, WIDTH)
     return pl.pallas_call(
-        final_body, out_shape=(shape, shape), in_specs=[VMEM] * 4 + [ANY] * 7, out_specs=(VMEM,) * 2,
+        final_body, out_shape=(shape, shape), in_specs=[VMEM] * 4 + [ANY] * 14, out_specs=(VMEM,) * 2,
         scratch_shapes=[
-            pltpu.VMEM((RING, RING, WIDTH // RING // ROWS, ROWS, COLS), jnp.bfloat16),
-            pltpu.SemaphoreType.DMA((RING, RING)),
+            pltpu.VMEM((RING, WIDTH // ROWS, ROWS, COLS), jnp.bfloat16), pltpu.SemaphoreType.DMA((RING, 32)),
         ],
         compiler_params=PARAMS, name="finish",
-    )(*received, rest, *pieces, *crossed)
+    )(*received, *lines, *pieces, *crossed)
 
 
 def joined_cores(mine, theirs):
@@ -457,7 +491,6 @@
 
 def layer(tokens, norm_gain, w_query, w_key, w_value, w_out):
     wide_own, rest_own = pack(w_query, w_key, w_value, w_out)
-    rest = lax.all_gather(rest_own, "sp")
 
     core = lax.axis_index("sp") % 2
     tokens = jnp.transpose(tokens, (1, 0, 2))
@@ -466,6 +499,7 @@
     wide_lines = spread(wide_own, 0)
     late, early = norm_rows(tokens, other, norm_gain)
     late, early = ring_of(late), ring_of(early)
+    rest = spread(rest_own, 0)
 
     wide_late = project_wide(late, wide_lines)
     far_late = from_behind(wide_late, 2)
@@ -474,8 +508,7 @@
     back_early = from_behind(wide_early, 1)
     near, near_tail = project_near(early, late, rest)
     near_tail = from_behind(near_tail, 1)
-    outs = lax.dynamic_slice(rest, (16 * core, LAST, 0, 0), (16, 1, ROWS, COLS))[:, 0]
-    outs = ring_of(outs)[1:]
+    outs = ring_of(pick(rest[:RING]))[1:]
     queries = project_queries(early, late, rest)
     wide_out, wide_logs = attend_wide(queries, wide_early, wide_late, back_early, back_late, far_late)
     *combined, kept, sent = attend_near(queries, near, near_tail, wide_out, wide_logs)

time: 165 us -> 191 us (1.16)
  starting transfers between devices: 48.5 us -> 74.9 us
  between operations: 14.5 us -> 1.12 us
  waiting for transfers between devices: 41.2 us -> 50 us
  Pallas kernels: 50.8 us -> 57.4 us
  local copies, waits for them, and re-layouts: 7.62 us -> 4.65 us
    ppermute x12, waiting for transfers between devices: 10.4 us -> 48.4 us  [turned(): return lax.ppermute(a, 'tp', [(i, (i + shift) % RING) for i in range(RING)])]
    all_gather x1 -> x0, waiting for transfers between devices: 25 us -> none  [layer(): rest = lax.all_gather(rest_own, 'sp')]
    ppermute x10 -> x14, starting transfers between devices: 12 us -> 34.8 us  [swapped(): return lax.ppermute(a, 'sp', SWAP)]
    ppermute x3 -> x6, starting transfers between devices: 5.78 us -> 9.5 us  [spread(): near = {d: lax.ppermute(own, 'sp', first_leg(d, kind)) for d in (1, 3, 2)}]
    ppermute x3 -> x6, waiting for transfers between devices: 2.89 us -> 0.02 us  [spread(): near = {d: lax.ppermute(own, 'sp', first_leg(d, kind)) for d in (1, 3, 2)}]
    ppermute x12, starting transfers between devices: 14.1 us -> 12 us  [turned(): return lax.ppermute(a, 'tp', [(i, (i + shift) % RING) for i in range(RING)])]
    ppermute x3 -> x6, starting transfers between devices: 4.76 us -> 6.8 us  [spread(): far = {d: lax.ppermute(line, 'sp', second_leg(d, kind)) for d in (1, 3, 2)}]
    pallas_call x0 -> x1, Pallas kernels: none -> 1.92 us  [pick(): pl.pallas_call(pick_body, out_shape=bf(16, ROWS, COLS), in_specs=[ANY] *...]
  transfers between devices with their start and end apart: 33 -> 42, of which waited for: 7 -> 12; matrix products, arithmetic and copies ran while one was open for 2% -> 2% of each run, Pallas kernels for 25% -> 25%
where the time goes in v5:
time: 191 us; the launch traced here: 190 us
  starting transfers between devices  74.9 us (39%)
  Pallas kernels  57.4 us (30%)
  waiting for transfers between devices  50 us (26%)
  local copies, waits for them, and re-layouts  4.65 us (2%)
  other arithmetic  1.96 us (1%)
    ppermute x12, waiting for transfers between devices, turned(): return lax.ppermute(a, 'tp', [(i, (i + shift) % RING) for i in range(RING)])  48.4 us
    ppermute x14, starting transfers between devices, swapped(): return lax.ppermute(a, 'sp', SWAP)  34.8 us
    pallas_call x1, Pallas kernels, project_near(): pl.pallas_call(near_pair_body, out_shape=(bf(2, 2, BATCHES, SPAN, COLS),...  12.6 us
    ppermute x12, starting transfers between devices, turned(): return lax.ppermute(a, 'tp', [(i, (i + shift) % RING) for i in range(RING)])  12 us
    ppermute x4, starting transfers between devices, from_behind(): lax.ppermute(a, 'sp', [(i, i + 2 * blocks) for i in range(32 - 2 * blocks)])  11.8 us
    ppermute x6, starting transfers between devices, spread(): near = {d: lax.ppermute(own, 'sp', first_leg(d, kind)) for d in (1, 3, 2)}  9.5 us
    pallas_call x1, Pallas kernels, project_queries(): pl.pallas_call(query_body, out_shape=bf(GROUPS, BATCHES, SPAN, COLS), in_...  9.33 us
    pallas_call x2, Pallas kernels, project_wide(): pl.pallas_call(wide_pair_body, out_shape=bf(2, BATCHES, HALF, COLS), in_s...  8.67 us
  transfers between devices with their start and end apart: 42, of which 12 were waited for; matrix products, arithmetic and copies ran while one was open for 2% of the time, Pallas kernels for 25%

profile of v5, /device:TPU:1, one launch (start us, length us, event | category | flops | bytes accessed | tf_op | source)
XLA Modules:
  0.0 190.1 jit_solution(8146430294750380045)
XLA Ops:
  2.4 4.4 %collective-permute-start.19 = (bf16[2,64,256]{2,1,0:T(8,128)(2,1)}, bf16[2,64,256]{2,1,0:T(8,128)(2,1)S(1)}, u32[]{:S(2)}, u32[]{:S(2)}) collective-permute-start(bf16[2,64,256]{2,1,0:T(8,128)(2,1)} %get-tuple-element.23), channel_id=1, source_target_pairs={{0,16},{4,68},{8,24},{12,76},{16,0},{20,84},{24,8},{28,92},{32,48}... | collective-permute-start | bytes 196616 | tf_op jit(solution)/shard_map/ppermute | solution.py:485
  9.0 2.1 %collective-permute-start.8 = (bf16[8,64,256]{2,1,0:T(8,128)(2,1)}, bf16[8,64,256]{2,1,0:T(8,128)(2,1)S(1)}, u32[]{:S(2)}, u32[]{:S(2)}) collective-permute-start(bf16[8,64,256]{2,1,0:T(8,128)(2,1)} %get-tuple-element.20), channel_id=1, source_target_pairs={{0,16},{4,68},{8,24},{12,76},{16,0},{20,84},{24,8},{28,92},{32,48}... | collective-permute-start | bytes 786440 | tf_op jit(solution)/shard_map/ppermute | solution.py:485
  14.1 2.6 %collective-permute-start.22 = (bf16[4,2,64,256]{3,2,1,0:T(8,128)(2,1)S(1)}, bf16[4,2,64,256]{3,2,1,0:T(8,128)(2,1)S(1)}, u32[]{:S(2)}, u32[]{:S(2)}) collective-permute-start(bf16[4,2,64,256]{3,2,1,0:T(8,128)(2,1)S(1)} %pad_maximum_fusion.1.refs_4_), channel_id=1, source_target_pairs={{0,64},{4,20},{8,72},{12,28},{16,80},{20,4},{24,88},{28,12},{32,96... | collective-permute-start | bytes 786440 | tf_op jit(solution)/shard_map/ppermute | solution.py:487
  17.8 3.6 %collective-permute-start = (bf16[3,32,2048]{2,1,0:T(8,128)(2,1)S(1)}, bf16[3,32,2048]{2,1,0:T(8,128)(2,1)S(1)}, u32[]{:S(2)}, u32[]{:S(2)}) collective-permute-start(bf16[3,32,2048]{2,1,0:T(8,128)(2,1)S(1)} %dynamic-slice_bitcast_fusion), channel_id=1, source_target_pairs={{0,4},{4,0},{8,12},{12,8},{16,20},{20,16},{24,28},{28,24},{32,36},... | collective-permute-start | bytes 1179656 | tf_op jit(solution)/shard_map/ppermute | solution.py:54
  21.4 7.5 %collective-permute-start.24 = (bf16[4,2,64,256]{3,2,1,0:T(8,128)(2,1)S(1)}, bf16[4,2,64,256]{3,2,1,0:T(8,128)(2,1)}, u32[]{:S(2)}, u32[]{:S(2)}) collective-permute-start(bf16[4,2,64,256]{3,2,1,0:T(8,128)(2,1)S(1)} %pad_maximum_fusion.1.refs_4_), channel_id=1, source_target_pairs={{0,4},{4,0},{8,12},{12,8},{16,20},{20,16},{24,28},{28,24},{32,36},... | collective-permute-start | bytes 786440 | tf_op jit(solution)/shard_map/ppermute | solution.py:54
  30.9 2.4 %collective-permute-start.12 = (bf16[4,8,64,256]{3,2,1,0:T(8,128)(2,1)S(1)}, bf16[4,8,64,256]{3,2,1,0:T(8,128)(2,1)S(1)}, u32[]{:S(2)}, u32[]{:S(2)}) collective-permute-start(bf16[4,8,64,256]{3,2,1,0:T(8,128)(2,1)S(1)} %pad_maximum_fusion.refs_8_.a0.refs_4_), channel_id=1, source_target_pairs={{0,96},{4,28},{8,104},{12,4},{16,112},{20,12},{24,120},{28,20},{32... | collective-permute-start | bytes 3145736 | tf_op jit(solution)/shard_map/ppermute | solution.py:487
  33.4 4.7 %collective-permute-start.27 = (bf16[4,2,64,256]{3,2,1,0:T(8,128)(2,1)S(1)}, bf16[4,2,64,256]{3,2,1,0:T(8,128)(2,1)}, u32[]{:S(2)}, u32[]{:S(2)}) collective-permute-start(bf16[4,2,64,256]{3,2,1,0:T(8,128)(2,1)S(1)} %collective-permute-done.23.refs_7_), channel_id=1, source_target_pairs={{0,4},{4,0},{8,12},{12,8},{16,20},{20,16},{24,28},{28,24},{32,36},... | collective-permute-start | bytes 786440 | tf_op jit(solution)/shard_map/ppermute | solution.py:54
  38.0 2.7 %norm_rows.1 = (bf16[3,32,2048]{2,1,0:T(8,128)(2,1)}, bf16[3,32,2048]{2,1,0:T(8,128)(2,1)}) custom-call(bf16[6,32,2048]{2,1,0:T(8,128)(2,1)} %bitcast.15, bf16[3,32,2048]{2,1,0:T(8,128)(2,1)} %copy-done.30, f32[1,2048]{1,0:T(1,128)} %bitcast.26), custom_call_target="tpu_custom_call" | custom-call | tf_op jit(solution)/shard_map/norm_rows/pallas_call | solution.py:131
  42.1 2.5 %collective-permute-start.5 = (bf16[3,32,2048]{2,1,0:T(8,128)(2,1)}, bf16[3,32,2048]{2,1,0:T(8,128)(2,1)S(1)}, u32[]{:S(2)}, u32[]{:S(2)}) collective-permute-start(bf16[3,32,2048]{2,1,0:T(8,128)(2,1)} %get-tuple-element.19.refs_4_.refs_0_), channel_id=1, source_target_pairs={{0,2},{1,3},{2,0},{3,1},{4,6},{5,7},{6,4},{7,5},{8,10},{9,11},{10,... | collective-permute-start | bytes 1179656 | tf_op jit(solution)/shard_map/ppermute | solution.py:58
  44.5 7.8 %collective-permute-done.4.refs_5_.refs_1_ = bf16[3,32,2048]{2,1,0:T(8,128)(2,1)S(1)} collective-permute-done((bf16[3,32,2048]{2,1,0:T(8,128)(2,1)}, bf16[3,32,2048]{2,1,0:T(8,128)(2,1)S(1)}, u32[]{:S(2)}, u32[]{:S(2)}) %collective-permute-start.4) | collective-permute-done | bytes 393248 | tf_op jit(solution)/shard_map/ppermute | solution.py:58
  53.9 7.8 %collective-permute-done.5.refs_6_.refs_2_ = bf16[3,32,2048]{2,1,0:T(8,128)(2,1)S(1)} collective-permute-done((bf16[3,32,2048]{2,1,0:T(8,128)(2,1)}, bf16[3,32,2048]{2,1,0:T(8,128)(2,1)S(1)}, u32[]{:S(2)}, u32[]{:S(2)}) %collective-permute-start.5) | collective-permute-done | bytes 393248 | tf_op jit(solution)/shard_map/ppermute | solution.py:58
  63.7 2.0 %collective-permute-start.3 = (bf16[3,32,2048]{2,1,0:T(8,128)(2,1)}, bf16[3,32,2048]{2,1,0:T(8,128)(2,1)S(1)}, u32[]{:S(2)}, u32[]{:S(2)}) collective-permute-start(bf16[3,32,2048]{2,1,0:T(8,128)(2,1)} %get-tuple-element.18.refs_0_), channel_id=1, source_target_pairs={{0,3},{1,0},{2,1},{3,2},{4,7},{5,4},{6,5},{7,6},{8,11},{9,8},{10,9... | collective-permute-start | bytes 1179656 | tf_op jit(solution)/shard_map/ppermute | solution.py:58
  65.7 1.9 %pick.1 = bf16[16,64,256]{2,1,0:T(8,128)(2,1)} custom-call(bf16[4,8,64,256]{3,2,1,0:T(8,128)(2,1)} %copy-done, bf16[4,8,64,256]{3,2,1,0:T(8,128)(2,1)} %copy-done.1, bf16[4,8,64,256]{3,2,1,0:T(8,128)(2,1)} %copy-done.2, bf16[4,8,64,256]{3,2,1,0:T(8,128)(2,1)} %copy-done.3), custom_call_target="tpu_custom_call" | custom-call | tf_op jit(solution)/shard_map/pick/pallas_call | solution.py:409
  67.6 3.5 %collective-permute-done.6.refs_7_.refs_3_ = bf16[3,32,2048]{2,1,0:T(8,128)(2,1)S(1)} collective-permute-done((bf16[3,32,2048]{2,1,0:T(8,128)(2,1)}, bf16[3,32,2048]{2,1,0:T(8,128)(2,1)S(1)}, u32[]{:S(2)}, u32[]{:S(2)}) %collective-permute-start.6) | collective-permute-done | bytes 393248 | tf_op jit(solution)/shard_map/ppermute | solution.py:58
  71.1 2.4 %collective-permute-done.1.refs_1_ = bf16[3,32,2048]{2,1,0:T(8,128)(2,1)S(1)} collective-permute-done((bf16[3,32,2048]{2,1,0:T(8,128)(2,1)}, bf16[3,32,2048]{2,1,0:T(8,128)(2,1)S(1)}, u32[]{:S(2)}, u32[]{:S(2)}) %collective-permute-start.1) | collective-permute-done | bytes 393248 | tf_op jit(solution)/shard_map/ppermute | solution.py:58
  73.5 10.3 %collective-permute-start.14 = (bf16[4,8,64,256]{3,2,1,0:T(8,128)(2,1)}, bf16[4,8,64,256]{3,2,1,0:T(8,128)(2,1)S(1)}, u32[]{:S(2)}, u32[]{:S(2)}) collective-permute-start(bf16[4,8,64,256]{3,2,1,0:T(8,128)(2,1)} %copy-done.1), channel_id=1, source_target_pairs={{0,4},{4,0},{8,12},{12,8},{16,20},{20,16},{24,28},{28,24},{32,36},... | collective-permute-start | bytes 3145736 | tf_op jit(solution)/shard_map/ppermute | solution.py:54
  84.7 3.3 %collective-permute-done.3.refs_3_ = bf16[3,32,2048]{2,1,0:T(8,128)(2,1)S(1)} collective-permute-done((bf16[3,32,2048]{2,1,0:T(8,128)(2,1)}, bf16[3,32,2048]{2,1,0:T(8,128)(2,1)S(1)}, u32[]{:S(2)}, u32[]{:S(2)}) %collective-permute-start.3) | collective-permute-done | bytes 393248 | tf_op jit(solution)/shard_map/ppermute | solution.py:58
  88.0 2.4 %collective-permute-start.16 = (bf16[4,8,64,256]{3,2,1,0:T(8,128)(2,1)}, bf16[4,8,64,256]{3,2,1,0:T(8,128)(2,1)S(1)}, u32[]{:S(2)}, u32[]{:S(2)}) collective-permute-start(bf16[4,8,64,256]{3,2,1,0:T(8,128)(2,1)} %copy-done.3), channel_id=1, source_target_pairs={{0,4},{4,0},{8,12},{12,8},{16,20},{20,16},{24,28},{28,24},{32,36},... | collective-permute-start | bytes 3145736 | tf_op jit(solution)/shard_map/ppermute | solution.py:54
  92.1 4.3 %project_wide.3.late = bf16[2,3,128,256]{3,2,1,0:T(8,128)(2,1)} custom-call(bf16[3,32,2048]{2,1,0:T(8,128)(2,1)} %get-tuple-element.19.refs_4_.refs_0_, bf16[3,32,2048]{2,1,0:T(8,128)(2,1)} %copy-done.8, bf16[3,32,2048]{2,1,0:T(8,128)(2,1)} %copy-done.9, bf16[3,32,2048]{2,1,0:T(8,128)(2,1)} %copy-done.10, bf16[4,2,64,256]{3,2,1,0:T(8,128)(2,1)} %copy-done.14, ...), custom_call_target="tpu_custom_call" | custom-call | tf_op jit(solution)/shard_map/project_wide/pallas_call | solution.py:177
  96.5 9.0 %collective-permute-done.35.refs_13_ = bf16[16,64,256]{2,1,0:T(8,128)(2,1)S(1)} collective-permute-done((bf16[16,64,256]{2,1,0:T(8,128)(2,1)}, bf16[16,64,256]{2,1,0:T(8,128)(2,1)S(1)}, u32[]{:S(2)}, u32[]{:S(2)}) %collective-permute-start.35) | collective-permute-done | bytes 524320 | tf_op jit(solution)/shard_map/ppermute | solution.py:58
  106.8 8.8 %collective-permute-done.36.refs_14_ = bf16[16,64,256]{2,1,0:T(8,128)(2,1)} collective-permute-done((bf16[16,64,256]{2,1,0:T(8,128)(2,1)}, bf16[16,64,256]{2,1,0:T(8,128)(2,1)}, u32[]{:S(2)}, u32[]{:S(2)}) %collective-permute-start.36) | collective-permute-done | bytes 524320 | tf_op jit(solution)/shard_map/ppermute | solution.py:58
  115.6 2.3 %collective-permute-start.30 = (bf16[2,3,128,256]{3,2,1,0:T(8,128)(2,1)}, bf16[2,3,128,256]{3,2,1,0:T(8,128)(2,1)S(1)}, u32[]{:S(2)}, u32[]{:S(2)}) collective-permute-start(bf16[2,3,128,256]{3,2,1,0:T(8,128)(2,1)} %project_wide.3.late), channel_id=1, source_target_pairs={{0,16},{4,20},{8,24},{12,28},{16,32},{20,36},{24,40},{28,44},{32,4... | collective-permute-start | bytes 1179656 | tf_op jit(solution)/shard_map/ppermute | solution.py:62
  119.8 4.4 %project_wide.2.early = bf16[2,3,128,256]{3,2,1,0:T(8,128)(2,1)} custom-call(bf16[3,32,2048]{2,1,0:T(8,128)(2,1)} %get-tuple-element.18.refs_0_, bf16[3,32,2048]{2,1,0:T(8,128)(2,1)} %copy-done.11, bf16[3,32,2048]{2,1,0:T(8,128)(2,1)} %copy-done.12, bf16[3,32,2048]{2,1,0:T(8,128)(2,1)} %copy-done.13, bf16[4,2,64,256]{3,2,1,0:T(8,128)(2,1)} %copy-done.14, ...), custom_call_target="tpu_custom_call" | custom-call | tf_op jit(solution)/shard_map/project_wide/pallas_call | solution.py:177
  124.3 12.6 %project_near.1 = (bf16[2,2,3,256,256]{4,3,2,1,0:T(8,128)(2,1)}, bf16[2,3,128,256]{3,2,1,0:T(8,128)(2,1)}) custom-call(bf16[3,32,2048]{2,1,0:T(8,128)(2,1)} %get-tuple-element.18.refs_0_, bf16[3,32,2048]{2,1,0:T(8,128)(2,1)} %copy-done.11, bf16[3,32,2048]{2,1,0:T(8,128)(2,1)} %copy-done.12, bf16[3,32,2048]{2,1,0:T(8,128)(2,1)} %copy-done.13, ...), custom_call_target="tpu_custom_call" | custom-call | tf_op jit(solution)/shard_map/project_near/pallas_call | solution.py:257
  138.3 6.8 %collective-permute-start.17 = (bf16[2,3,128,256]{3,2,1,0:T(8,128)(2,1)}, bf16[2,3,128,256]{3,2,1,0:T(8,128)(2,1)S(1)}, u32[]{:S(2)}, u32[]{:S(2)}) collective-permute-start(bf16[2,3,128,256]{3,2,1,0:T(8,128)(2,1)} %get-tuple-element.22), channel_id=1, source_target_pairs={{0,8},{4,12},{8,16},{12,20},{16,24},{20,28},{24,32},{28,36},{32,40... | collective-permute-start | bytes 1179656 | tf_op jit(solution)/shard_map/ppermute | solution.py:62
  145.1 9.3 %project_queries.1.q = bf16[3,3,256,256]{3,2,1,0:T(8,128)(2,1)} custom-call(bf16[3,32,2048]{2,1,0:T(8,128)(2,1)} %get-tuple-element.18.refs_0_, bf16[3,32,2048]{2,1,0:T(8,128)(2,1)} %copy-done.11, bf16[3,32,2048]{2,1,0:T(8,128)(2,1)} %copy-done.12, bf16[3,32,2048]{2,1,0:T(8,128)(2,1)} %copy-done.13, bf16[3,32,2048]{2,1,0:T(8,128)(2,1)} %get-tuple-element.19.refs_4_.refs_0_, ...), custom_call_target="tpu_custom_call" | custom-call | tf_op jit(solution)/shard_map/project_queries/pallas_call | solution.py:266
  155.2 5.2 %attend_wide.1 = (f32[3,256,256]{2,1,0:T(8,128)}, f32[3,256,256]{2,1,0:T(8,128)}) custom-call(bf16[3,3,256,256]{3,2,1,0:T(8,128)(2,1)} %project_queries.1.q, bf16[2,3,128,256]{3,2,1,0:T(8,128)(2,1)} %project_wide.2.early, bf16[2,3,128,256]{3,2,1,0:T(8,128)(2,1)} %project_wide.3.late, bf16[2,3,128,256]{3,2,1,0:T(8,128)(2,1)} %copy-done.29, ...), custom_call_target="tpu_custom_call" | custom-call | tf_op jit(solution)/shard_map/attend_wide/pallas_call | solution.py:331
  161.1 6.6 %attend_near.1 = (bf16[2,3,32,256]{3,2,1,0:T(8,128)(2,1)}, bf16[2,3,32,256]{3,2,1,0:T(8,128)(2,1)}, bf16[2,3,32,256]{3,2,1,0:T(8,128)(2,1)}, bf16[2,3,32,256]{3,...) custom-call(bf16[3,3,256,256]{3,2,1,0:T(8,128)(2,1)} %project_queries.1.q, ...), custom_call_target="tpu_custom_call" | custom-call | tf_op jit(solution)/shard_map/attend_near/pallas_call | solution.py:382
  168.3 3.0 %collective-permute-start.32 = (bf16[2,3,32,256]{3,2,1,0:T(8,128)(2,1)}, bf16[2,3,32,256]{3,2,1,0:T(8,128)(2,1)S(1)}, u32[]{:S(2)}, u32[]{:S(2)}) collective-permute-start(bf16[2,3,32,256]{3,2,1,0:T(8,128)(2,1)} %get-tuple-element.28), channel_id=1, source_target_pairs={{0,2},{1,3},{2,0},{3,1},{4,6},{5,7},{6,4},{7,5},{8,10},{9,11},{10,... | collective-permute-start | bytes 294920 | tf_op jit(solution)/shard_map/ppermute | solution.py:58
  172.7 2.7 %collective-permute-done.32.refs_2_ = bf16[2,3,32,256]{3,2,1,0:T(8,128)(2,1)S(1)} collective-permute-done((bf16[2,3,32,256]{3,2,1,0:T(8,128)(2,1)}, bf16[2,3,32,256]{3,2,1,0:T(8,128)(2,1)S(1)}, u32[]{:S(2)}, u32[]{:S(2)}) %collective-permute-start.32) | collective-permute-done | bytes 98336 | tf_op jit(solution)/shard_map/ppermute | solution.py:58
  176.9 6.7 %finish.1 = (bf16[3,32,2048]{2,1,0:T(8,128)(2,1)}, bf16[3,32,2048]{2,1,0:T(8,128)(2,1)}) custom-call(bf16[2,3,32,256]{3,2,1,0:T(8,128)(2,1)} %get-tuple-element.26.refs_0_, bf16[2,3,32,256]{3,2,1,0:T(8,128)(2,1)} %copy-done.32, bf16[2,3,32,256]{3,2,1,0:T(8,128)(2,1)} %copy-done.33, bf16[2,3,32,256]{3,2,1,0:T(8,128)(2,1)} %copy-done.34, ...), custom_call_target="tpu_custom_call" | custom-call | tf_op jit(solution)/shard_map/finish/pallas_call | solution.py:452
  188.0 2.1 %merge.1 = bf16[6,32,2048]{2,1,0:T(8,128)(2,1)} custom-call(bf16[3,32,2048]{2,1,0:T(8,128)(2,1)} %get-tuple-element.30.mine, bf16[3,32,2048]{2,1,0:T(8,128)(2,1)} %copy-done.31), custom_call_target="tpu_custom_call" | custom-call | tf_op jit(solution)/shard_map/merge/pallas_call | solution.py:473
  (142 shorter events, 31.4 us)
Async XLA Ops:
  8.2 9.5 %collective-permute-start.7 = (bf16[8,64,256]{2,1,0:T(8,128)(2,1)}, bf16[8,64,256]{2,1,0:T(8,128)(2,1)S(1)}, u32[]{:S(2)}, u32[]{:S(2)}) collective-permute-start(bf16[8,64,256]{2,1,0:T(8,128)(2,1)} %get-tuple-element.20), channel_id=1, source_target_pairs={{0,8},{4,36},{8,16},{12,44},{16,24},{20,52},{24,0},{28,60},{32,40}... | collective-permute-start | bytes 786440 | tf_op jit(solution)/shard_map/ppermute | solution.py:485
  9.0 12.4 %collective-permute-start.8 = (bf16[8,64,256]{2,1,0:T(8,128)(2,1)}, bf16[8,64,256]{2,1,0:T(8,128)(2,1)S(1)}, u32[]{:S(2)}, u32[]{:S(2)}) collective-permute-start(bf16[8,64,256]{2,1,0:T(8,128)(2,1)} %get-tuple-element.20), channel_id=1, source_target_pairs={{0,16},{4,68},{8,24},{12,76},{16,0},{20,84},{24,8},{28,92},{32,48}... | collective-permute-start | bytes 786440 | tf_op jit(solution)/shard_map/ppermute | solution.py:485
  11.1 10.3 %collective-permute-start.9 = (bf16[8,64,256]{2,1,0:T(8,128)(2,1)}, bf16[8,64,256]{2,1,0:T(8,128)(2,1)S(1)}, u32[]{:S(2)}, u32[]{:S(2)}) collective-permute-start(bf16[8,64,256]{2,1,0:T(8,128)(2,1)} %get-tuple-element.20), channel_id=1, source_target_pairs={{0,24},{4,100},{8,0},{12,108},{16,8},{20,116},{24,16},{28,124},{32... | collective-permute-start | bytes 786440 | tf_op jit(solution)/shard_map/ppermute | solution.py:485
  12.8 16.1 %collective-permute-start.21 = (bf16[4,2,64,256]{3,2,1,0:T(8,128)(2,1)S(1)}, bf16[4,2,64,256]{3,2,1,0:T(8,128)(2,1)S(1)}, u32[]{:S(2)}, u32[]{:S(2)}) collective-permute-start(bf16[4,2,64,256]{3,2,1,0:T(8,128)(2,1)S(1)} %pad_maximum_fusion.1.refs_4_), channel_id=1, source_target_pairs={{0,32},{4,12},{8,40},{12,20},{16,48},{20,28},{24,56},{28,4},{32,64... | collective-permute-start | bytes 786440 | tf_op jit(solution)/shard_map/ppermute | solution.py:487
  14.1 14.9 %collective-permute-start.22 = (bf16[4,2,64,256]{3,2,1,0:T(8,128)(2,1)S(1)}, bf16[4,2,64,256]{3,2,1,0:T(8,128)(2,1)S(1)}, u32[]{:S(2)}, u32[]{:S(2)}) collective-permute-start(bf16[4,2,64,256]{3,2,1,0:T(8,128)(2,1)S(1)} %pad_maximum_fusion.1.refs_4_), channel_id=1, source_target_pairs={{0,64},{4,20},{8,72},{12,28},{16,80},{20,4},{24,88},{28,12},{32,96... | collective-permute-start | bytes 786440 | tf_op jit(solution)/shard_map/ppermute | solution.py:487
  17.8 13.2 %collective-permute-start = (bf16[3,32,2048]{2,1,0:T(8,128)(2,1)S(1)}, bf16[3,32,2048]{2,1,0:T(8,128)(2,1)S(1)}, u32[]{:S(2)}, u32[]{:S(2)}) collective-permute-start(bf16[3,32,2048]{2,1,0:T(8,128)(2,1)S(1)} %dynamic-slice_bitcast_fusion), channel_id=1, source_target_pairs={{0,4},{4,0},{8,12},{12,8},{16,20},{20,16},{24,28},{28,24},{32,36},... | collective-permute-start | bytes 1179656 | tf_op jit(solution)/shard_map/ppermute | solution.py:54
  21.4 9.1 %collective-permute-start.23 = (bf16[4,2,64,256]{3,2,1,0:T(8,128)(2,1)S(1)}, bf16[4,2,64,256]{3,2,1,0:T(8,128)(2,1)S(1)}, u32[]{:S(2)}, u32[]{:S(2)}) collective-permute-start(bf16[4,2,64,256]{3,2,1,0:T(8,128)(2,1)S(1)} %pad_maximum_fusion.1.refs_4_), channel_id=1, source_target_pairs={{0,96},{4,28},{8,104},{12,4},{16,112},{20,12},{24,120},{28,20},{32... | collective-permute-start | bytes 786440 | tf_op jit(solution)/shard_map/ppermute | solution.py:487
  21.4 9.2 %collective-permute-start.24 = (bf16[4,2,64,256]{3,2,1,0:T(8,128)(2,1)S(1)}, bf16[4,2,64,256]{3,2,1,0:T(8,128)(2,1)}, u32[]{:S(2)}, u32[]{:S(2)}) collective-permute-start(bf16[4,2,64,256]{3,2,1,0:T(8,128)(2,1)S(1)} %pad_maximum_fusion.1.refs_4_), channel_id=1, source_target_pairs={{0,4},{4,0},{8,12},{12,8},{16,20},{20,16},{24,28},{28,24},{32,36},... | collective-permute-start | bytes 786440 | tf_op jit(solution)/shard_map/ppermute | solution.py:54
  29.0 11.8 %collective-permute-start.26 = (bf16[4,2,64,256]{3,2,1,0:T(8,128)(2,1)S(1)}, bf16[4,2,64,256]{3,2,1,0:T(8,128)(2,1)S(1)}, u32[]{:S(2)}, u32[]{:S(2)}) collective-permute-start(bf16[4,2,64,256]{3,2,1,0:T(8,128)(2,1)S(1)} %collective-permute-done.22.refs_6_), channel_id=1, source_target_pairs={{0,4},{4,0},{8,12},{12,8},{16,20},{20,16},{24,28},{28,24},{32,36},... | collective-permute-start | bytes 786440 | tf_op jit(solution)/shard_map/ppermute | solution.py:54
  30.5 31.2 %collective-permute-start.10 = (bf16[4,8,64,256]{3,2,1,0:T(8,128)(2,1)S(1)}, bf16[4,8,64,256]{3,2,1,0:T(8,128)(2,1)S(1)}, u32[]{:S(2)}, u32[]{:S(2)}) collective-permute-start(bf16[4,8,64,256]{3,2,1,0:T(8,128)(2,1)S(1)} %pad_maximum_fusion.refs_8_.a0.refs_4_), channel_id=1, source_target_pairs={{0,32},{4,12},{8,40},{12,20},{16,48},{20,28},{24,56},{28,4},{32,64... | collective-permute-start | bytes 3145736 | tf_op jit(solution)/shard_map/ppermute | solution.py:487
  30.6 32.6 %collective-permute-start.11 = (bf16[4,8,64,256]{3,2,1,0:T(8,128)(2,1)S(1)}, bf16[4,8,64,256]{3,2,1,0:T(8,128)(2,1)S(1)}, u32[]{:S(2)}, u32[]{:S(2)}) collective-permute-start(bf16[4,8,64,256]{3,2,1,0:T(8,128)(2,1)S(1)} %pad_maximum_fusion.refs_8_.a0.refs_4_), channel_id=1, source_target_pairs={{0,64},{4,20},{8,72},{12,28},{16,80},{20,4},{24,88},{28,12},{32,96... | collective-permute-start | bytes 3145736 | tf_op jit(solution)/shard_map/ppermute | solution.py:487
  30.9 32.8 %collective-permute-start.12 = (bf16[4,8,64,256]{3,2,1,0:T(8,128)(2,1)S(1)}, bf16[4,8,64,256]{3,2,1,0:T(8,128)(2,1)S(1)}, u32[]{:S(2)}, u32[]{:S(2)}) collective-permute-start(bf16[4,8,64,256]{3,2,1,0:T(8,128)(2,1)S(1)} %pad_maximum_fusion.refs_8_.a0.refs_4_), channel_id=1, source_target_pairs={{0,96},{4,28},{8,104},{12,4},{16,112},{20,12},{24,120},{28,20},{32... | collective-permute-start | bytes 3145736 | tf_op jit(solution)/shard_map/ppermute | solution.py:487
  40.8 11.5 %collective-permute-start.4 = (bf16[3,32,2048]{2,1,0:T(8,128)(2,1)}, bf16[3,32,2048]{2,1,0:T(8,128)(2,1)S(1)}, u32[]{:S(2)}, u32[]{:S(2)}) collective-permute-start(bf16[3,32,2048]{2,1,0:T(8,128)(2,1)} %get-tuple-element.19.refs_4_.refs_0_), channel_id=1, source_target_pairs={{0,1},{1,2},{2,3},{3,0},{4,5},{5,6},{6,7},{7,4},{8,9},{9,10},{10,1... | collective-permute-start | bytes 1179656 | tf_op jit(solution)/shard_map/ppermute | solution.py:58
  42.1 19.6 %collective-permute-start.5 = (bf16[3,32,2048]{2,1,0:T(8,128)(2,1)}, bf16[3,32,2048]{2,1,0:T(8,128)(2,1)S(1)}, u32[]{:S(2)}, u32[]{:S(2)}) collective-permute-start(bf16[3,32,2048]{2,1,0:T(8,128)(2,1)} %get-tuple-element.19.refs_4_.refs_0_), channel_id=1, source_target_pairs={{0,2},{1,3},{2,0},{3,1},{4,6},{5,7},{6,4},{7,5},{8,10},{9,11},{10,... | collective-permute-start | bytes 1179656 | tf_op jit(solution)/shard_map/ppermute | solution.py:58
  52.3 38.1 %collective-permute-start.13 = (bf16[4,8,64,256]{3,2,1,0:T(8,128)(2,1)S(1)}, bf16[4,8,64,256]{3,2,1,0:T(8,128)(2,1)S(1)}, u32[]{:S(2)}, u32[]{:S(2)}) collective-permute-start(bf16[4,8,64,256]{3,2,1,0:T(8,128)(2,1)S(1)} %pad_maximum_fusion.refs_8_.a0.refs_4_), channel_id=1, source_target_pairs={{0,4},{4,0},{8,12},{12,8},{16,20},{20,16},{24,28},{28,24},{32,36},... | collective-permute-start | bytes 3145736 | tf_op jit(solution)/shard_map/ppermute | solution.py:54
  61.7 9.4 %collective-permute-start.6 = (bf16[3,32,2048]{2,1,0:T(8,128)(2,1)}, bf16[3,32,2048]{2,1,0:T(8,128)(2,1)S(1)}, u32[]{:S(2)}, u32[]{:S(2)}) collective-permute-start(bf16[3,32,2048]{2,1,0:T(8,128)(2,1)} %get-tuple-element.19.refs_4_.refs_0_), channel_id=1, source_target_pairs={{0,3},{1,0},{2,1},{3,2},{4,7},{5,4},{6,5},{7,6},{8,11},{9,8},{10,9... | collective-permute-start | bytes 1179656 | tf_op jit(solution)/shard_map/ppermute | solution.py:58
  61.7 11.7 %collective-permute-start.1 = (bf16[3,32,2048]{2,1,0:T(8,128)(2,1)}, bf16[3,32,2048]{2,1,0:T(8,128)(2,1)S(1)}, u32[]{:S(2)}, u32[]{:S(2)}) collective-permute-start(bf16[3,32,2048]{2,1,0:T(8,128)(2,1)} %get-tuple-element.18.refs_0_), channel_id=1, source_target_pairs={{0,1},{1,2},{2,3},{3,0},{4,5},{5,6},{6,7},{7,4},{8,9},{9,10},{10,1... | collective-permute-start | bytes 1179656 | tf_op jit(solution)/shard_map/ppermute | solution.py:58
  63.2 20.6 %collective-permute-start.2 = (bf16[3,32,2048]{2,1,0:T(8,128)(2,1)}, bf16[3,32,2048]{2,1,0:T(8,128)(2,1)S(1)}, u32[]{:S(2)}, u32[]{:S(2)}) collective-permute-start(bf16[3,32,2048]{2,1,0:T(8,128)(2,1)} %get-tuple-element.18.refs_0_), channel_id=1, source_target_pairs={{0,2},{1,3},{2,0},{3,1},{4,6},{5,7},{6,4},{7,5},{8,10},{9,11},{10,... | collective-permute-start | bytes 1179656 | tf_op jit(solution)/shard_map/ppermute | solution.py:58
  63.7 24.3 %collective-permute-start.3 = (bf16[3,32,2048]{2,1,0:T(8,128)(2,1)}, bf16[3,32,2048]{2,1,0:T(8,128)(2,1)S(1)}, u32[]{:S(2)}, u32[]{:S(2)}) collective-permute-start(bf16[3,32,2048]{2,1,0:T(8,128)(2,1)} %get-tuple-element.18.refs_0_), channel_id=1, source_target_pairs={{0,3},{1,0},{2,1},{3,2},{4,7},{5,4},{6,5},{7,6},{8,11},{9,8},{10,9... | collective-permute-start | bytes 1179656 | tf_op jit(solution)/shard_map/ppermute | solution.py:58
  71.1 20.8 %collective-permute-start.34 = (bf16[16,64,256]{2,1,0:T(8,128)(2,1)}, bf16[16,64,256]{2,1,0:T(8,128)(2,1)S(1)}, u32[]{:S(2)}, u32[]{:S(2)}) collective-permute-start(bf16[16,64,256]{2,1,0:T(8,128)(2,1)} %pick.1), channel_id=1, source_target_pairs={{0,1},{1,2},{2,3},{3,0},{4,5},{5,6},{6,7},{7,4},{8,9},{9,10},{10,1... | collective-permute-start | bytes 1572872 | tf_op jit(solution)/shard_map/ppermute | solution.py:58
  73.5 44.5 %collective-permute-start.14 = (bf16[4,8,64,256]{3,2,1,0:T(8,128)(2,1)}, bf16[4,8,64,256]{3,2,1,0:T(8,128)(2,1)S(1)}, u32[]{:S(2)}, u32[]{:S(2)}) collective-permute-start(bf16[4,8,64,256]{3,2,1,0:T(8,128)(2,1)} %copy-done.1), channel_id=1, source_target_pairs={{0,4},{4,0},{8,12},{12,8},{16,20},{20,16},{24,28},{28,24},{32,36},... | collective-permute-start | bytes 3145736 | tf_op jit(solution)/shard_map/ppermute | solution.py:54
  83.8 35.5 %collective-permute-start.15 = (bf16[4,8,64,256]{3,2,1,0:T(8,128)(2,1)}, bf16[4,8,64,256]{3,2,1,0:T(8,128)(2,1)S(1)}, u32[]{:S(2)}, u32[]{:S(2)}) collective-permute-start(bf16[4,8,64,256]{3,2,1,0:T(8,128)(2,1)} %copy-done.2), channel_id=1, source_target_pairs={{0,4},{4,0},{8,12},{12,8},{16,20},{20,16},{24,28},{28,24},{32,36},... | collective-permute-start | bytes 3145736 | tf_op jit(solution)/shard_map/ppermute | solution.py:54
  88.0 31.4 %collective-permute-start.16 = (bf16[4,8,64,256]{3,2,1,0:T(8,128)(2,1)}, bf16[4,8,64,256]{3,2,1,0:T(8,128)(2,1)S(1)}, u32[]{:S(2)}, u32[]{:S(2)}) collective-permute-start(bf16[4,8,64,256]{3,2,1,0:T(8,128)(2,1)} %copy-done.3), channel_id=1, source_target_pairs={{0,4},{4,0},{8,12},{12,8},{16,20},{20,16},{24,28},{28,24},{32,36},... | collective-permute-start | bytes 3145736 | tf_op jit(solution)/shard_map/ppermute | solution.py:54
  90.4 15.1 %collective-permute-start.35 = (bf16[16,64,256]{2,1,0:T(8,128)(2,1)}, bf16[16,64,256]{2,1,0:T(8,128)(2,1)S(1)}, u32[]{:S(2)}, u32[]{:S(2)}) collective-permute-start(bf16[16,64,256]{2,1,0:T(8,128)(2,1)} %pick.1), channel_id=1, source_target_pairs={{0,2},{1,3},{2,0},{3,1},{4,6},{5,7},{6,4},{7,5},{8,10},{9,11},{10,... | collective-permute-start | bytes 1572872 | tf_op jit(solution)/shard_map/ppermute | solution.py:58
  91.9 23.7 %collective-permute-start.36 = (bf16[16,64,256]{2,1,0:T(8,128)(2,1)}, bf16[16,64,256]{2,1,0:T(8,128)(2,1)}, u32[]{:S(2)}, u32[]{:S(2)}) collective-permute-start(bf16[16,64,256]{2,1,0:T(8,128)(2,1)} %pick.1), channel_id=1, source_target_pairs={{0,3},{1,0},{2,1},{3,2},{4,7},{5,4},{6,5},{7,6},{8,11},{9,8},{10,9... | collective-permute-start | bytes 1572872 | tf_op jit(solution)/shard_map/ppermute | solution.py:58
  105.5 31.4 %collective-permute-start.29 = (bf16[2,3,128,256]{3,2,1,0:T(8,128)(2,1)}, bf16[2,3,128,256]{3,2,1,0:T(8,128)(2,1)S(1)}, u32[]{:S(2)}, u32[]{:S(2)}) collective-permute-start(bf16[2,3,128,256]{3,2,1,0:T(8,128)(2,1)} %project_wide.3.late), channel_id=1, source_target_pairs={{0,8},{4,12},{8,16},{12,20},{16,24},{20,28},{24,32},{28,36},{32,40... | collective-permute-start | bytes 1179656 | tf_op jit(solution)/shard_map/ppermute | solution.py:62
  115.6 22.6 %collective-permute-start.30 = (bf16[2,3,128,256]{3,2,1,0:T(8,128)(2,1)}, bf16[2,3,128,256]{3,2,1,0:T(8,128)(2,1)S(1)}, u32[]{:S(2)}, u32[]{:S(2)}) collective-permute-start(bf16[2,3,128,256]{3,2,1,0:T(8,128)(2,1)} %project_wide.3.late), channel_id=1, source_target_pairs={{0,16},{4,20},{8,24},{12,28},{16,32},{20,36},{24,40},{28,44},{32,4... | collective-permute-start | bytes 1179656 | tf_op jit(solution)/shard_map/ppermute | solution.py:62
  118.0 53.3 %collective-permute-start.37 = (bf16[16,64,256]{2,1,0:T(8,128)(2,1)S(1)}, bf16[16,64,256]{2,1,0:T(8,128)(2,1)S(1)}, u32[]{:S(2)}, u32[]{:S(2)}) collective-permute-start(bf16[16,64,256]{2,1,0:T(8,128)(2,1)S(1)} %collective-permute-done.34.refs_12_), channel_id=1, source_target_pairs={{0,4},{4,0},{8,12},{12,8},{16,20},{20,16},{24,28},{28,24},{32,36},... | collective-permute-start | bytes 1572872 | tf_op jit(solution)/shard_map/ppermute | solution.py:54
  119.3 52.0 %collective-permute-start.38 = (bf16[16,64,256]{2,1,0:T(8,128)(2,1)S(1)}, bf16[16,64,256]{2,1,0:T(8,128)(2,1)S(1)}, u32[]{:S(2)}, u32[]{:S(2)}) collective-permute-start(bf16[16,64,256]{2,1,0:T(8,128)(2,1)S(1)} %collective-permute-done.35.refs_13_), channel_id=1, source_target_pairs={{0,4},{4,0},{8,12},{12,8},{16,20},{20,16},{24,28},{28,24},{32,36},... | collective-permute-start | bytes 1572872 | tf_op jit(solution)/shard_map/ppermute | solution.py:54
  119.4 51.9 %collective-permute-start.39 = (bf16[16,64,256]{2,1,0:T(8,128)(2,1)}, bf16[16,64,256]{2,1,0:T(8,128)(2,1)S(1)}, u32[]{:S(2)}, u32[]{:S(2)}) collective-permute-start(bf16[16,64,256]{2,1,0:T(8,128)(2,1)} %collective-permute-done.36.refs_14_), channel_id=1, source_target_pairs={{0,4},{4,0},{8,12},{12,8},{16,20},{20,16},{24,28},{28,24},{32,36},... | collective-permute-start | bytes 1572872 | tf_op jit(solution)/shard_map/ppermute | solution.py:54
  136.9 17.5 %collective-permute-start.28 = (bf16[2,3,128,256]{3,2,1,0:T(8,128)(2,1)S(1)}, bf16[2,3,128,256]{3,2,1,0:T(8,128)(2,1)S(1)}, u32[]{:S(2)}, u32[]{:S(2)}) collective-permute-start(bf16[2,3,128,256]{3,2,1,0:T(8,128)(2,1)S(1)} %copy-done.15), channel_id=1, source_target_pairs={{0,8},{4,12},{8,16},{12,20},{16,24},{20,28},{24,32},{28,36},{32,40... | collective-permute-start | bytes 1179656 | tf_op jit(solution)/shard_map/ppermute | solution.py:62
  138.3 22.1 %collective-permute-start.17 = (bf16[2,3,128,256]{3,2,1,0:T(8,128)(2,1)}, bf16[2,3,128,256]{3,2,1,0:T(8,128)(2,1)S(1)}, u32[]{:S(2)}, u32[]{:S(2)}) collective-permute-start(bf16[2,3,128,256]{3,2,1,0:T(8,128)(2,1)} %get-tuple-element.22), channel_id=1, source_target_pairs={{0,8},{4,12},{8,16},{12,20},{16,24},{20,28},{24,32},{28,36},{32,40... | collective-permute-start | bytes 1179656 | tf_op jit(solution)/shard_map/ppermute | solution.py:62
  (47 other events, 473.7 us)

commit v6 on v5

--- a/solution.py
+++ b/solution.py
@@ -243,7 +243,7 @@
     def work(m, y):
         queries[m] = y
 
-    staged(early, late, rest, NEAR, GROUPS, *scratch, work)
+    staged(early, late, rest, 0, GROUPS, *scratch, work)
 
 
 def rest_scratch(count):
@@ -396,7 +396,7 @@
 
 def pick_body(a0, a1, a2, a3, out, sems):
     copies = [
-        pltpu.make_async_copy(a.at[:, LAST], out.at[pl.ds(RING * e, RING)], sems.at[e])
+        pltpu.make_async_copy(a.at[:, GROUPS], out.at[pl.ds(RING * e, RING)], sems.at[e])
         for e, a in enumerate((a0, a1, a2, a3))
     ]
     for c in copies:
@@ -426,7 +426,7 @@
         for j in range(RING):
             k = place_of(whose, j, n % RING, 0)
             at = n * RING + j
-            copies.append(pltpu.make_async_copy(lines[n].at[j, LAST], w_all.at[0, k], sems.at[0, at]))
+            copies.append(pltpu.make_async_copy(lines[n].at[j, GROUPS], w_all.at[0, k], sems.at[0, at]))
             for d, piece in enumerate(others, 1):
                 source = piece.at[(n % RING) * RING + j]
                 copies.append(pltpu.make_async_copy(source, w_all.at[d, k], sems.at[d, at]))
@@ -489,6 +489,18 @@
     return lines + [swapped(a) for a in lines]
 
 
+def spread_halves(own):
+    near = {d: lax.ppermute(own, "sp", first_leg(d, 0)) for d in (1, 3, 2)}
+    halves = []
+    for part, way in ((slice(0, NEAR), 1), (slice(NEAR, None), 3)):
+        line = jnp.stack([a[part] for a in (own, near[1], near[2], near[3])])
+        far = {d: lax.ppermute(line, "sp", second_leg(d, 0)) for d in (1, 3)}
+        far[2] = lax.ppermute(far[way], "sp", second_leg(way, 0))
+        lines = [line, far[1], far[2], far[3]]
+        halves.append(lines + [swapped(a) for a in lines])
+    return halves
+
+
 def layer(tokens, norm_gain, w_query, w_key, w_value, w_out):
     wide_own, rest_own = pack(w_query, w_key, w_value, w_out)
 
@@ -499,22 +511,22 @@
     wide_lines = spread(wide_own, 0)
     late, early = norm_rows(tokens, other, norm_gain)
     late, early = ring_of(late), ring_of(early)
-    rest = spread(rest_own, 0)
+    pair_lines, query_lines = spread_halves(rest_own)
 
     wide_late = project_wide(late, wide_lines)
     far_late = from_behind(wide_late, 2)
     back_late = from_behind(wide_late, 1)
     wide_early = project_wide(early, wide_lines)
     back_early = from_behind(wide_early, 1)
-    near, near_tail = project_near(early, late, rest)
+    near, near_tail = project_near(early, late, pair_lines)
     near_tail = from_behind(near_tail, 1)
-    outs = ring_of(pick(rest[:RING]))[1:]
-    queries = project_queries(early, late, rest)
+    outs = ring_of(pick(query_lines[:RING]))[1:]
+    queries = project_queries(early, late, query_lines)
     wide_out, wide_logs = attend_wide(queries, wide_early, wide_late, back_early, back_late, far_late)
     *combined, kept, sent = attend_near(queries, near, near_tail, wide_out, wide_logs)
 
     received = [combined[0]] + [turned(combined[d], d) for d in (1, 2, 3)]
-    mixed_mine, mixed_sent = finish(received, rest, outs, [swapped(a) for a in outs])
+    mixed_mine, mixed_sent = finish(received, query_lines, outs, [swapped(a) for a in outs])
     mixed = merged(mixed_mine, swapped(mixed_sent))
 
     log_weight = joined_cores(kept, swapped(sent)).reshape(2 * BATCHES, 2, BLOCK)

time: 191 us -> 185 us (0.969)
  waiting for transfers between devices: 50 us -> 39.6 us
  starting transfers between devices: 74.9 us -> 77.3 us
    ppermute x12, waiting for transfers between devices: 48.4 us -> 20 us  [turned(): return lax.ppermute(a, 'tp', [(i, (i + shift) % RING) for i in range(RING)])]
    ppermute x0 -> x9, starting transfers between devices: none -> 16.5 us  [the longest x4 7.8 us: spread_halves(): far = {d: lax.ppermute(line, 'sp', second_leg(d, 0)) for d in (1, 3)}]
    ppermute x14 -> x18, starting transfers between devices: 34.8 us -> 19.3 us  [swapped(): return lax.ppermute(a, 'sp', SWAP)]
    ppermute x4, waiting for transfers between devices: 0.01 us -> 10.9 us  [from_behind(): lax.ppermute(a, 'sp', [(i, i + 2 * blocks) for i in range(32 - 2 * blocks)])]
    ppermute x12, starting transfers between devices: 12 us -> 18 us  [turned(): return lax.ppermute(a, 'tp', [(i, (i + shift) % RING) for i in range(RING)])]
    ppermute x6 -> x3, starting transfers between devices: 9.5 us -> 3.83 us  [spread(): near = {d: lax.ppermute(own, 'sp', first_leg(d, kind)) for d in (1, 3, 2)}]
    ppermute x6 -> x3, waiting for transfers between devices: 0.02 us -> 3.03 us  [spread(): far = {d: lax.ppermute(line, 'sp', second_leg(d, kind)) for d in (1, 3, 2)}]
    ppermute x0 -> x9, waiting for transfers between devices: none -> 2.07 us  [the longest x4 2.05 us: spread_halves(): far = {d: lax.ppermute(line, 'sp', second_leg(d, 0)) for d in (1, 3)}]
  transfers between devices with their start and end apart: 42 -> 49, of which waited for: 12 -> 15; matrix products, arithmetic and copies ran while one was open for 2% -> 2% of each run, Pallas kernels for 25% -> 26%
where the time goes in v6:
time: 185 us; the launch traced here: 183 us
  starting transfers between devices  77.3 us (42%)
  Pallas kernels  57.3 us (31%)
  waiting for transfers between devices  39.6 us (21%)
  local copies, waits for them, and re-layouts  6.56 us (4%)
    ppermute x12, waiting for transfers between devices, turned(): return lax.ppermute(a, 'tp', [(i, (i + shift) % RING) for i in range(RING)])  20 us
    ppermute x18, starting transfers between devices, swapped(): return lax.ppermute(a, 'sp', SWAP)  19.3 us
    ppermute x12, starting transfers between devices, turned(): return lax.ppermute(a, 'tp', [(i, (i + shift) % RING) for i in range(RING)])  18 us
    ppermute x4, starting transfers between devices, from_behind(): lax.ppermute(a, 'sp', [(i, i + 2 * blocks) for i in range(32 - 2 * blocks)])  13 us
    pallas_call x1, Pallas kernels, project_near(): pl.pallas_call(near_pair_body, out_shape=(bf(2, 2, BATCHES, SPAN, COLS),...  12.5 us
    ppermute x4, waiting for transfers between devices, from_behind(): lax.ppermute(a, 'sp', [(i, i + 2 * blocks) for i in range(32 - 2 * blocks)])  10.9 us
    pallas_call x1, Pallas kernels, project_queries(): pl.pallas_call(query_body, out_shape=bf(GROUPS, BATCHES, SPAN, COLS), in_...  9.3 us
    pallas_call x2, Pallas kernels, project_wide(): pl.pallas_call(wide_pair_body, out_shape=bf(2, BATCHES, HALF, COLS), in_s...  8.6 us
  transfers between devices with their start and end apart: 49, of which 15 were waited for; matrix products, arithmetic and copies ran while one was open for 2% of the time, Pallas kernels for 26%

profile of v6, /device:TPU:1, one launch (start us, length us, event | category | flops | bytes accessed | tf_op | source)
XLA Modules:
  0.0 183.0 jit_solution(12772420674932958599)
XLA Ops:
  2.4 4.6 %collective-permute-start.9 = (bf16[8,64,256]{2,1,0:T(8,128)(2,1)}, bf16[8,64,256]{2,1,0:T(8,128)(2,1)S(1)}, u32[]{:S(2)}, u32[]{:S(2)}) collective-permute-start(bf16[8,64,256]{2,1,0:T(8,128)(2,1)} %get-tuple-element.20), channel_id=1, source_target_pairs={{0,24},{4,100},{8,0},{12,108},{16,8},{20,116},{24,16},{28,124},{32... | collective-permute-start | bytes 786440 | tf_op jit(solution)/shard_map/ppermute | solution.py:493
  7.2 2.7 %collective-permute-start.26 = (bf16[2,64,256]{2,1,0:T(8,128)(2,1)}, bf16[2,64,256]{2,1,0:T(8,128)(2,1)S(1)}, u32[]{:S(2)}, u32[]{:S(2)}) collective-permute-start(bf16[2,64,256]{2,1,0:T(8,128)(2,1)} %get-tuple-element.23), channel_id=1, source_target_pairs={{0,16},{4,68},{8,24},{12,76},{16,0},{20,84},{24,8},{28,92},{32,48}... | collective-permute-start | bytes 196616 | tf_op jit(solution)/shard_map/ppermute | solution.py:485
  17.9 3.2 %collective-permute-start.29 = (bf16[4,2,64,256]{3,2,1,0:T(8,128)(2,1)S(1)}, bf16[4,2,64,256]{3,2,1,0:T(8,128)(2,1)S(1)}, u32[]{:S(2)}, u32[]{:S(2)}) collective-permute-start(bf16[4,2,64,256]{3,2,1,0:T(8,128)(2,1)S(1)} %pad_maximum_fusion.2.refs_4_), channel_id=1, source_target_pairs={{0,64},{4,20},{8,72},{12,28},{16,80},{20,4},{24,88},{28,12},{32,96... | collective-permute-start | bytes 786440 | tf_op jit(solution)/shard_map/ppermute | solution.py:487
  23.2 2.4 %collective-permute-start.31 = (bf16[4,2,64,256]{3,2,1,0:T(8,128)(2,1)S(1)}, bf16[4,2,64,256]{3,2,1,0:T(8,128)(2,1)S(1)}, u32[]{:S(2)}, u32[]{:S(2)}) collective-permute-start(bf16[4,2,64,256]{3,2,1,0:T(8,128)(2,1)S(1)} %pad_maximum_fusion.2.refs_4_), channel_id=1, source_target_pairs={{0,4},{4,0},{8,12},{12,8},{16,20},{20,16},{24,28},{28,24},{32,36},... | collective-permute-start | bytes 786440 | tf_op jit(solution)/shard_map/ppermute | solution.py:54
  26.8 3.0 %collective-permute-done.29.refs_6_ = bf16[4,2,64,256]{3,2,1,0:T(8,128)(2,1)S(1)} collective-permute-done((bf16[4,2,64,256]{3,2,1,0:T(8,128)(2,1)S(1)}, bf16[4,2,64,256]{3,2,1,0:T(8,128)(2,1)S(1)}, u32[]{:S(2)}, u32[]{:S(2)}) %collective-permute-start.29) | collective-permute-done | bytes 262176 | tf_op jit(solution)/shard_map/ppermute | solution.py:487
  31.4 2.7 %norm_rows.1 = (bf16[3,32,2048]{2,1,0:T(8,128)(2,1)}, bf16[3,32,2048]{2,1,0:T(8,128)(2,1)}) custom-call(bf16[6,32,2048]{2,1,0:T(8,128)(2,1)} %bitcast.27, bf16[3,32,2048]{2,1,0:T(8,128)(2,1)} %copy-done.38, f32[1,2048]{1,0:T(1,128)} %bitcast.34), custom_call_target="tpu_custom_call" | custom-call | tf_op jit(solution)/shard_map/norm_rows/pallas_call | solution.py:131
  35.4 2.5 %collective-permute-start.2 = (bf16[3,32,2048]{2,1,0:T(8,128)(2,1)}, bf16[3,32,2048]{2,1,0:T(8,128)(2,1)S(1)}, u32[]{:S(2)}, u32[]{:S(2)}) collective-permute-start(bf16[3,32,2048]{2,1,0:T(8,128)(2,1)} %get-tuple-element.18.refs_0_), channel_id=1, source_target_pairs={{0,2},{1,3},{2,0},{3,1},{4,6},{5,7},{6,4},{7,5},{8,10},{9,11},{10,... | collective-permute-start | bytes 1179656 | tf_op jit(solution)/shard_map/ppermute | solution.py:58
  41.3 2.7 %collective-permute-start.5 = (bf16[3,32,2048]{2,1,0:T(8,128)(2,1)}, bf16[3,32,2048]{2,1,0:T(8,128)(2,1)S(1)}, u32[]{:S(2)}, u32[]{:S(2)}) collective-permute-start(bf16[3,32,2048]{2,1,0:T(8,128)(2,1)} %get-tuple-element.19.refs_4_.refs_0_), channel_id=1, source_target_pairs={{0,2},{1,3},{2,0},{3,1},{4,6},{5,7},{6,4},{7,5},{8,10},{9,11},{10,... | collective-permute-start | bytes 1179656 | tf_op jit(solution)/shard_map/ppermute | solution.py:58
  44.7 3.0 %collective-permute-start.11 = (bf16[4,4,64,256]{3,2,1,0:T(8,128)(2,1)S(1)}, bf16[4,4,64,256]{3,2,1,0:T(8,128)(2,1)S(1)}, u32[]{:S(2)}, u32[]{:S(2)}) collective-permute-start(bf16[4,4,64,256]{3,2,1,0:T(8,128)(2,1)S(1)} %pad_maximum_fusion.refs_8_.a0.refs_4_), channel_id=1, source_target_pairs={{0,96},{4,28},{8,104},{12,4},{16,112},{20,12},{24,120},{28,20},{32... | collective-permute-start | bytes 1572872 | tf_op jit(solution)/shard_map/ppermute | solution.py:497
  47.7 6.4 %collective-permute-done.2.refs_2_ = bf16[3,32,2048]{2,1,0:T(8,128)(2,1)S(1)} collective-permute-done((bf16[3,32,2048]{2,1,0:T(8,128)(2,1)}, bf16[3,32,2048]{2,1,0:T(8,128)(2,1)S(1)}, u32[]{:S(2)}, u32[]{:S(2)}) %collective-permute-start.2) | collective-permute-done | bytes 393248 | tf_op jit(solution)/shard_map/ppermute | solution.py:58
  54.1 4.5 %collective-permute-start.13 = (bf16[4,4,64,256]{3,2,1,0:T(8,128)(2,1)S(1)}, bf16[4,4,64,256]{3,2,1,0:T(8,128)(2,1)S(1)}, u32[]{:S(2)}, u32[]{:S(2)}) collective-permute-start(bf16[4,4,64,256]{3,2,1,0:T(8,128)(2,1)S(1)} %pad_maximum_fusion.refs_8_.a0.refs_4_), channel_id=1, source_target_pairs={{0,4},{4,0},{8,12},{12,8},{16,20},{20,16},{24,28},{28,24},{32,36},... | collective-permute-start | bytes 1572872 | tf_op jit(solution)/shard_map/ppermute | solution.py:54
  61.5 3.0 %collective-permute-start.19 = (bf16[4,4,64,256]{3,2,1,0:T(8,128)(2,1)S(1)}, bf16[4,4,64,256]{3,2,1,0:T(8,128)(2,1)}, u32[]{:S(2)}, u32[]{:S(2)}) collective-permute-start(bf16[4,4,64,256]{3,2,1,0:T(8,128)(2,1)S(1)} %pad_maximum_fusion.1.refs_8_), channel_id=1, source_target_pairs={{0,96},{4,28},{8,104},{12,4},{16,112},{20,12},{24,120},{28,20},{32... | collective-permute-start | bytes 1572872 | tf_op jit(solution)/shard_map/ppermute | solution.py:497
  64.6 6.4 %collective-permute-done.5.refs_6_.refs_2_ = bf16[3,32,2048]{2,1,0:T(8,128)(2,1)S(1)} collective-permute-done((bf16[3,32,2048]{2,1,0:T(8,128)(2,1)}, bf16[3,32,2048]{2,1,0:T(8,128)(2,1)S(1)}, u32[]{:S(2)}, u32[]{:S(2)}) %collective-permute-start.5) | collective-permute-done | bytes 393248 | tf_op jit(solution)/shard_map/ppermute | solution.py:58
  71.0 2.4 %collective-permute-start.20 = (bf16[4,4,64,256]{3,2,1,0:T(8,128)(2,1)S(1)}, bf16[4,4,64,256]{3,2,1,0:T(8,128)(2,1)}, u32[]{:S(2)}, u32[]{:S(2)}) collective-permute-start(bf16[4,4,64,256]{3,2,1,0:T(8,128)(2,1)S(1)} %pad_maximum_fusion.1.refs_8_), channel_id=1, source_target_pairs={{0,4},{4,0},{8,12},{12,8},{16,20},{20,16},{24,28},{28,24},{32,36},... | collective-permute-start | bytes 1572872 | tf_op jit(solution)/shard_map/ppermute | solution.py:54
  75.0 4.3 %project_wide.2.early = bf16[2,3,128,256]{3,2,1,0:T(8,128)(2,1)} custom-call(bf16[3,32,2048]{2,1,0:T(8,128)(2,1)} %get-tuple-element.18.refs_0_, bf16[3,32,2048]{2,1,0:T(8,128)(2,1)} %copy-done.4, bf16[3,32,2048]{2,1,0:T(8,128)(2,1)} %copy-done.5, bf16[3,32,2048]{2,1,0:T(8,128)(2,1)} %copy-done.6, bf16[4,2,64,256]{3,2,1,0:T(8,128)(2,1)} %copy-done.10, ...), custom_call_target="tpu_custom_call" | custom-call | tf_op jit(solution)/shard_map/project_wide/pallas_call | solution.py:177
  79.4 4.3 %project_wide.3.late = bf16[2,3,128,256]{3,2,1,0:T(8,128)(2,1)} custom-call(bf16[3,32,2048]{2,1,0:T(8,128)(2,1)} %get-tuple-element.19.refs_4_.refs_0_, bf16[3,32,2048]{2,1,0:T(8,128)(2,1)} %copy-done.7, bf16[3,32,2048]{2,1,0:T(8,128)(2,1)} %copy-done.8, bf16[3,32,2048]{2,1,0:T(8,128)(2,1)} %copy-done.9, bf16[4,2,64,256]{3,2,1,0:T(8,128)(2,1)} %copy-done.10, ...), custom_call_target="tpu_custom_call" | custom-call | tf_op jit(solution)/shard_map/project_wide/pallas_call | solution.py:177
  83.7 3.8 %collective-permute-start.35 = (bf16[2,3,128,256]{3,2,1,0:T(8,128)(2,1)S(1)}, bf16[2,3,128,256]{3,2,1,0:T(8,128)(2,1)S(1)}, u32[]{:S(2)}, u32[]{:S(2)}) collective-permute-start(bf16[2,3,128,256]{3,2,1,0:T(8,128)(2,1)S(1)} %copy-done.16), channel_id=1, source_target_pairs={{0,8},{4,12},{8,16},{12,20},{16,24},{20,28},{24,32},{28,36},{32,40... | collective-permute-start | bytes 1179656 | tf_op jit(solution)/shard_map/ppermute | solution.py:62
  87.5 2.7 %collective-permute-start.36 = (bf16[2,3,128,256]{3,2,1,0:T(8,128)(2,1)}, bf16[2,3,128,256]{3,2,1,0:T(8,128)(2,1)}, u32[]{:S(2)}, u32[]{:S(2)}) collective-permute-start(bf16[2,3,128,256]{3,2,1,0:T(8,128)(2,1)} %project_wide.3.late), channel_id=1, source_target_pairs={{0,8},{4,12},{8,16},{12,20},{16,24},{20,28},{24,32},{28,36},{32,40... | collective-permute-start | bytes 1179656 | tf_op jit(solution)/shard_map/ppermute | solution.py:62
  90.2 2.6 %collective-permute-start.12 = (bf16[4,4,64,256]{3,2,1,0:T(8,128)(2,1)S(1)}, bf16[4,4,64,256]{3,2,1,0:T(8,128)(2,1)S(1)}, u32[]{:S(2)}, u32[]{:S(2)}) collective-permute-start(bf16[4,4,64,256]{3,2,1,0:T(8,128)(2,1)S(1)} %collective-permute-done.11.refs_11_.a3.refs_7_), channel_id=1, source_target_pairs={{0,96},{4,28},{8,104},{12,4},{16,112},{20,12},{24,120},{28,20},{32... | collective-permute-start | bytes 1572872 | tf_op jit(solution)/shard_map/ppermute | solution.py:498
  93.6 2.8 %collective-permute-done.35.back_early = bf16[2,3,128,256]{3,2,1,0:T(8,128)(2,1)S(1)} collective-permute-done((bf16[2,3,128,256]{3,2,1,0:T(8,128)(2,1)S(1)}, bf16[2,3,128,256]{3,2,1,0:T(8,128)(2,1)S(1)}, u32[]{:S(2)}, u32[]{:S(2)}) %collective-permute-start.35) | collective-permute-done | bytes 393248 | tf_op jit(solution)/shard_map/ppermute | solution.py:62
  96.8 8.1 %collective-permute-done.36.back_late = bf16[2,3,128,256]{3,2,1,0:T(8,128)(2,1)} collective-permute-done((bf16[2,3,128,256]{3,2,1,0:T(8,128)(2,1)}, bf16[2,3,128,256]{3,2,1,0:T(8,128)(2,1)}, u32[]{:S(2)}, u32[]{:S(2)}) %collective-permute-start.36) | collective-permute-done | bytes 393248 | tf_op jit(solution)/shard_map/ppermute | solution.py:62
  112.0 12.5 %project_near.1 = (bf16[2,2,3,256,256]{4,3,2,1,0:T(8,128)(2,1)}, bf16[2,3,128,256]{3,2,1,0:T(8,128)(2,1)}) custom-call(bf16[3,32,2048]{2,1,0:T(8,128)(2,1)} %get-tuple-element.18.refs_0_, bf16[3,32,2048]{2,1,0:T(8,128)(2,1)} %copy-done.4, bf16[3,32,2048]{2,1,0:T(8,128)(2,1)} %copy-done.5, bf16[3,32,2048]{2,1,0:T(8,128)(2,1)} %copy-done.6, ...), custom_call_target="tpu_custom_call" | custom-call | tf_op jit(solution)/shard_map/project_near/pallas_call | solution.py:257
  124.6 4.5 %collective-permute-start.37 = (bf16[2,3,128,256]{3,2,1,0:T(8,128)(2,1)S(1)}, bf16[2,3,128,256]{3,2,1,0:T(8,128)(2,1)S(1)}, u32[]{:S(2)}, u32[]{:S(2)}) collective-permute-start(bf16[2,3,128,256]{3,2,1,0:T(8,128)(2,1)S(1)} %copy-done.17), channel_id=1, source_target_pairs={{0,16},{4,20},{8,24},{12,28},{16,32},{20,36},{24,40},{28,44},{32,4... | collective-permute-start | bytes 1179656 | tf_op jit(solution)/shard_map/ppermute | solution.py:62
  129.1 2.1 %collective-permute-start.24 = (bf16[2,3,128,256]{3,2,1,0:T(8,128)(2,1)}, bf16[2,3,128,256]{3,2,1,0:T(8,128)(2,1)S(1)}, u32[]{:S(2)}, u32[]{:S(2)}) collective-permute-start(bf16[2,3,128,256]{3,2,1,0:T(8,128)(2,1)} %get-tuple-element.22), channel_id=1, source_target_pairs={{0,8},{4,12},{8,16},{12,20},{16,24},{20,28},{24,32},{28,36},{32,40... | collective-permute-start | bytes 1179656 | tf_op jit(solution)/shard_map/ppermute | solution.py:62
  135.9 9.3 %project_queries.1.q = bf16[3,3,256,256]{3,2,1,0:T(8,128)(2,1)} custom-call(bf16[3,32,2048]{2,1,0:T(8,128)(2,1)} %get-tuple-element.18.refs_0_, bf16[3,32,2048]{2,1,0:T(8,128)(2,1)} %copy-done.4, bf16[3,32,2048]{2,1,0:T(8,128)(2,1)} %copy-done.5, bf16[3,32,2048]{2,1,0:T(8,128)(2,1)} %copy-done.6, bf16[3,32,2048]{2,1,0:T(8,128)(2,1)} %get-tuple-element.19.refs_4_.refs_0_, ...), custom_call_target="tpu_custom_call" | custom-call | tf_op jit(solution)/shard_map/project_queries/pallas_call | solution.py:266
  146.0 5.1 %attend_wide.1 = (f32[3,256,256]{2,1,0:T(8,128)}, f32[3,256,256]{2,1,0:T(8,128)}) custom-call(bf16[3,3,256,256]{3,2,1,0:T(8,128)(2,1)} %project_queries.1.q, bf16[2,3,128,256]{3,2,1,0:T(8,128)(2,1)} %project_wide.2.early, bf16[2,3,128,256]{3,2,1,0:T(8,128)(2,1)} %project_wide.3.late, bf16[2,3,128,256]{3,2,1,0:T(8,128)(2,1)} %copy-done.35, ...), custom_call_target="tpu_custom_call" | custom-call | tf_op jit(solution)/shard_map/attend_wide/pallas_call | solution.py:331
  151.9 6.6 %attend_near.1 = (bf16[2,3,32,256]{3,2,1,0:T(8,128)(2,1)}, bf16[2,3,32,256]{3,2,1,0:T(8,128)(2,1)}, bf16[2,3,32,256]{3,2,1,0:T(8,128)(2,1)}, bf16[2,3,32,256]{3,...) custom-call(bf16[3,3,256,256]{3,2,1,0:T(8,128)(2,1)} %project_queries.1.q, ...), custom_call_target="tpu_custom_call" | custom-call | tf_op jit(solution)/shard_map/attend_near/pallas_call | solution.py:382
  159.6 2.6 %collective-permute-start.39 = (bf16[2,3,32,256]{3,2,1,0:T(8,128)(2,1)}, bf16[2,3,32,256]{3,2,1,0:T(8,128)(2,1)S(1)}, u32[]{:S(2)}, u32[]{:S(2)}) collective-permute-start(bf16[2,3,32,256]{3,2,1,0:T(8,128)(2,1)} %get-tuple-element.28), channel_id=1, source_target_pairs={{0,2},{1,3},{2,0},{3,1},{4,6},{5,7},{6,4},{7,5},{8,10},{9,11},{10,... | collective-permute-start | bytes 294920 | tf_op jit(solution)/shard_map/ppermute | solution.py:58
  162.1 2.1 %collective-permute-done.38.refs_1_ = bf16[2,3,32,256]{3,2,1,0:T(8,128)(2,1)S(1)} collective-permute-done((bf16[2,3,32,256]{3,2,1,0:T(8,128)(2,1)}, bf16[2,3,32,256]{3,2,1,0:T(8,128)(2,1)S(1)}, u32[]{:S(2)}, u32[]{:S(2)}) %collective-permute-start.38) | collective-permute-done | bytes 98336 | tf_op jit(solution)/shard_map/ppermute | solution.py:58
  169.0 6.7 %finish.1 = (bf16[3,32,2048]{2,1,0:T(8,128)(2,1)}, bf16[3,32,2048]{2,1,0:T(8,128)(2,1)}) custom-call(bf16[2,3,32,256]{3,2,1,0:T(8,128)(2,1)} %get-tuple-element.26.refs_0_, bf16[2,3,32,256]{3,2,1,0:T(8,128)(2,1)} %copy-done.40, bf16[2,3,32,256]{3,2,1,0:T(8,128)(2,1)} %copy-done.41, bf16[2,3,32,256]{3,2,1,0:T(8,128)(2,1)} %copy-done.42, ...), custom_call_target="tpu_custom_call" | custom-call | tf_op jit(solution)/shard_map/finish/pallas_call | solution.py:452
  175.7 2.3 %collective-permute-start.47 = (bf16[3,32,2048]{2,1,0:T(8,128)(2,1)}, bf16[3,32,2048]{2,1,0:T(8,128)(2,1)S(1)}, u32[]{:S(2)}, u32[]{:S(2)}) collective-permute-start(bf16[3,32,2048]{2,1,0:T(8,128)(2,1)} %get-tuple-element.31), channel_id=1, source_target_pairs={{0,4},{4,0},{8,12},{12,8},{16,20},{20,16},{24,28},{28,24},{32,36},... | collective-permute-start | bytes 1179656 | tf_op jit(solution)/shard_map/ppermute | solution.py:54
  181.0 2.1 %merge.1 = bf16[6,32,2048]{2,1,0:T(8,128)(2,1)} custom-call(bf16[3,32,2048]{2,1,0:T(8,128)(2,1)} %get-tuple-element.30.mine, bf16[3,32,2048]{2,1,0:T(8,128)(2,1)} %copy-done.39), custom_call_target="tpu_custom_call" | custom-call | tf_op jit(solution)/shard_map/merge/pallas_call | solution.py:473
  (177 shorter events, 47.8 us)
Async XLA Ops:
  2.4 15.6 %collective-permute-start.9 = (bf16[8,64,256]{2,1,0:T(8,128)(2,1)}, bf16[8,64,256]{2,1,0:T(8,128)(2,1)S(1)}, u32[]{:S(2)}, u32[]{:S(2)}) collective-permute-start(bf16[8,64,256]{2,1,0:T(8,128)(2,1)} %get-tuple-element.20), channel_id=1, source_target_pairs={{0,24},{4,100},{8,0},{12,108},{16,8},{20,116},{24,16},{28,124},{32... | collective-permute-start | bytes 786440 | tf_op jit(solution)/shard_map/ppermute | solution.py:493
  6.9 14.2 %collective-permute-start.8 = (bf16[8,64,256]{2,1,0:T(8,128)(2,1)}, bf16[8,64,256]{2,1,0:T(8,128)(2,1)S(1)}, u32[]{:S(2)}, u32[]{:S(2)}) collective-permute-start(bf16[8,64,256]{2,1,0:T(8,128)(2,1)} %get-tuple-element.20), channel_id=1, source_target_pairs={{0,16},{4,68},{8,24},{12,76},{16,0},{20,84},{24,8},{28,92},{32,48}... | collective-permute-start | bytes 786440 | tf_op jit(solution)/shard_map/ppermute | solution.py:493
  14.9 15.7 %collective-permute-start = (bf16[3,32,2048]{2,1,0:T(8,128)(2,1)S(1)}, bf16[3,32,2048]{2,1,0:T(8,128)(2,1)S(1)}, u32[]{:S(2)}, u32[]{:S(2)}) collective-permute-start(bf16[3,32,2048]{2,1,0:T(8,128)(2,1)S(1)} %dynamic-slice_bitcast_fusion), channel_id=1, source_target_pairs={{0,4},{4,0},{8,12},{12,8},{16,20},{20,16},{24,28},{28,24},{32,36},... | collective-permute-start | bytes 1179656 | tf_op jit(solution)/shard_map/ppermute | solution.py:54
  17.9 11.9 %collective-permute-start.29 = (bf16[4,2,64,256]{3,2,1,0:T(8,128)(2,1)S(1)}, bf16[4,2,64,256]{3,2,1,0:T(8,128)(2,1)S(1)}, u32[]{:S(2)}, u32[]{:S(2)}) collective-permute-start(bf16[4,2,64,256]{3,2,1,0:T(8,128)(2,1)S(1)} %pad_maximum_fusion.2.refs_4_), channel_id=1, source_target_pairs={{0,64},{4,20},{8,72},{12,28},{16,80},{20,4},{24,88},{28,12},{32,96... | collective-permute-start | bytes 786440 | tf_op jit(solution)/shard_map/ppermute | solution.py:487
  25.8 13.2 %collective-permute-start.10 = (bf16[4,4,64,256]{3,2,1,0:T(8,128)(2,1)S(1)}, bf16[4,4,64,256]{3,2,1,0:T(8,128)(2,1)S(1)}, u32[]{:S(2)}, u32[]{:S(2)}) collective-permute-start(bf16[4,4,64,256]{3,2,1,0:T(8,128)(2,1)S(1)} %pad_maximum_fusion.refs_8_.a0.refs_4_), channel_id=1, source_target_pairs={{0,32},{4,12},{8,40},{12,20},{16,48},{20,28},{24,56},{28,4},{32,64... | collective-permute-start | bytes 1572872 | tf_op jit(solution)/shard_map/ppermute | solution.py:497
  30.6 10.7 %collective-permute-start.17 = (bf16[4,4,64,256]{3,2,1,0:T(8,128)(2,1)S(1)}, bf16[4,4,64,256]{3,2,1,0:T(8,128)(2,1)S(1)}, u32[]{:S(2)}, u32[]{:S(2)}) collective-permute-start(bf16[4,4,64,256]{3,2,1,0:T(8,128)(2,1)S(1)} %pad_maximum_fusion.1.refs_8_), channel_id=1, source_target_pairs={{0,32},{4,12},{8,40},{12,20},{16,48},{20,28},{24,56},{28,4},{32,64... | collective-permute-start | bytes 1572872 | tf_op jit(solution)/shard_map/ppermute | solution.py:497
  34.2 10.5 %collective-permute-start.1 = (bf16[3,32,2048]{2,1,0:T(8,128)(2,1)}, bf16[3,32,2048]{2,1,0:T(8,128)(2,1)S(1)}, u32[]{:S(2)}, u32[]{:S(2)}) collective-permute-start(bf16[3,32,2048]{2,1,0:T(8,128)(2,1)} %get-tuple-element.18.refs_0_), channel_id=1, source_target_pairs={{0,1},{1,2},{2,3},{3,0},{4,5},{5,6},{6,7},{7,4},{8,9},{9,10},{10,1... | collective-permute-start | bytes 1179656 | tf_op jit(solution)/shard_map/ppermute | solution.py:58
  35.4 18.8 %collective-permute-start.2 = (bf16[3,32,2048]{2,1,0:T(8,128)(2,1)}, bf16[3,32,2048]{2,1,0:T(8,128)(2,1)S(1)}, u32[]{:S(2)}, u32[]{:S(2)}) collective-permute-start(bf16[3,32,2048]{2,1,0:T(8,128)(2,1)} %get-tuple-element.18.refs_0_), channel_id=1, source_target_pairs={{0,2},{1,3},{2,0},{3,1},{4,6},{5,7},{6,4},{7,5},{8,10},{9,11},{10,... | collective-permute-start | bytes 1179656 | tf_op jit(solution)/shard_map/ppermute | solution.py:58
  37.8 20.8 %collective-permute-start.3 = (bf16[3,32,2048]{2,1,0:T(8,128)(2,1)}, bf16[3,32,2048]{2,1,0:T(8,128)(2,1)S(1)}, u32[]{:S(2)}, u32[]{:S(2)}) collective-permute-start(bf16[3,32,2048]{2,1,0:T(8,128)(2,1)} %get-tuple-element.18.refs_0_), channel_id=1, source_target_pairs={{0,3},{1,0},{2,1},{3,2},{4,7},{5,4},{6,5},{7,6},{8,11},{9,8},{10,9... | collective-permute-start | bytes 1179656 | tf_op jit(solution)/shard_map/ppermute | solution.py:58
  39.0 22.5 %collective-permute-start.4 = (bf16[3,32,2048]{2,1,0:T(8,128)(2,1)}, bf16[3,32,2048]{2,1,0:T(8,128)(2,1)S(1)}, u32[]{:S(2)}, u32[]{:S(2)}) collective-permute-start(bf16[3,32,2048]{2,1,0:T(8,128)(2,1)} %get-tuple-element.19.refs_4_.refs_0_), channel_id=1, source_target_pairs={{0,1},{1,2},{2,3},{3,0},{4,5},{5,6},{6,7},{7,4},{8,9},{9,10},{10,1... | collective-permute-start | bytes 1179656 | tf_op jit(solution)/shard_map/ppermute | solution.py:58
  41.3 29.6 %collective-permute-start.5 = (bf16[3,32,2048]{2,1,0:T(8,128)(2,1)}, bf16[3,32,2048]{2,1,0:T(8,128)(2,1)S(1)}, u32[]{:S(2)}, u32[]{:S(2)}) collective-permute-start(bf16[3,32,2048]{2,1,0:T(8,128)(2,1)} %get-tuple-element.19.refs_4_.refs_0_), channel_id=1, source_target_pairs={{0,2},{1,3},{2,0},{3,1},{4,6},{5,7},{6,4},{7,5},{8,10},{9,11},{10,... | collective-permute-start | bytes 1179656 | tf_op jit(solution)/shard_map/ppermute | solution.py:58
  44.7 39.0 %collective-permute-start.11 = (bf16[4,4,64,256]{3,2,1,0:T(8,128)(2,1)S(1)}, bf16[4,4,64,256]{3,2,1,0:T(8,128)(2,1)S(1)}, u32[]{:S(2)}, u32[]{:S(2)}) collective-permute-start(bf16[4,4,64,256]{3,2,1,0:T(8,128)(2,1)S(1)} %pad_maximum_fusion.refs_8_.a0.refs_4_), channel_id=1, source_target_pairs={{0,96},{4,28},{8,104},{12,4},{16,112},{20,12},{24,120},{28,20},{32... | collective-permute-start | bytes 1572872 | tf_op jit(solution)/shard_map/ppermute | solution.py:497
  54.1 33.4 %collective-permute-start.13 = (bf16[4,4,64,256]{3,2,1,0:T(8,128)(2,1)S(1)}, bf16[4,4,64,256]{3,2,1,0:T(8,128)(2,1)S(1)}, u32[]{:S(2)}, u32[]{:S(2)}) collective-permute-start(bf16[4,4,64,256]{3,2,1,0:T(8,128)(2,1)S(1)} %pad_maximum_fusion.refs_8_.a0.refs_4_), channel_id=1, source_target_pairs={{0,4},{4,0},{8,12},{12,8},{16,20},{20,16},{24,28},{28,24},{32,36},... | collective-permute-start | bytes 1572872 | tf_op jit(solution)/shard_map/ppermute | solution.py:54
  58.6 14.8 %collective-permute-start.6 = (bf16[3,32,2048]{2,1,0:T(8,128)(2,1)}, bf16[3,32,2048]{2,1,0:T(8,128)(2,1)S(1)}, u32[]{:S(2)}, u32[]{:S(2)}) collective-permute-start(bf16[3,32,2048]{2,1,0:T(8,128)(2,1)} %get-tuple-element.19.refs_4_.refs_0_), channel_id=1, source_target_pairs={{0,3},{1,0},{2,1},{3,2},{4,7},{5,4},{6,5},{7,6},{8,11},{9,8},{10,9... | collective-permute-start | bytes 1179656 | tf_op jit(solution)/shard_map/ppermute | solution.py:58
  61.5 28.7 %collective-permute-start.19 = (bf16[4,4,64,256]{3,2,1,0:T(8,128)(2,1)S(1)}, bf16[4,4,64,256]{3,2,1,0:T(8,128)(2,1)}, u32[]{:S(2)}, u32[]{:S(2)}) collective-permute-start(bf16[4,4,64,256]{3,2,1,0:T(8,128)(2,1)S(1)} %pad_maximum_fusion.1.refs_8_), channel_id=1, source_target_pairs={{0,96},{4,28},{8,104},{12,4},{16,112},{20,12},{24,120},{28,20},{32... | collective-permute-start | bytes 1572872 | tf_op jit(solution)/shard_map/ppermute | solution.py:497
  71.0 21.9 %collective-permute-start.20 = (bf16[4,4,64,256]{3,2,1,0:T(8,128)(2,1)S(1)}, bf16[4,4,64,256]{3,2,1,0:T(8,128)(2,1)}, u32[]{:S(2)}, u32[]{:S(2)}) collective-permute-start(bf16[4,4,64,256]{3,2,1,0:T(8,128)(2,1)S(1)} %pad_maximum_fusion.1.refs_8_), channel_id=1, source_target_pairs={{0,4},{4,0},{8,12},{12,8},{16,20},{20,16},{24,28},{28,24},{32,36},... | collective-permute-start | bytes 1572872 | tf_op jit(solution)/shard_map/ppermute | solution.py:54
  73.4 31.9 %collective-permute-start.18 = (bf16[4,4,64,256]{3,2,1,0:T(8,128)(2,1)S(1)}, bf16[4,4,64,256]{3,2,1,0:T(8,128)(2,1)}, u32[]{:S(2)}, u32[]{:S(2)}) collective-permute-start(bf16[4,4,64,256]{3,2,1,0:T(8,128)(2,1)S(1)} %collective-permute-done.17.refs_9_), channel_id=1, source_target_pairs={{0,32},{4,12},{8,40},{12,20},{16,48},{20,28},{24,56},{28,4},{32,64... | collective-permute-start | bytes 1572872 | tf_op jit(solution)/shard_map/ppermute | solution.py:498
  83.7 12.7 %collective-permute-start.35 = (bf16[2,3,128,256]{3,2,1,0:T(8,128)(2,1)S(1)}, bf16[2,3,128,256]{3,2,1,0:T(8,128)(2,1)S(1)}, u32[]{:S(2)}, u32[]{:S(2)}) collective-permute-start(bf16[2,3,128,256]{3,2,1,0:T(8,128)(2,1)S(1)} %copy-done.16), channel_id=1, source_target_pairs={{0,8},{4,12},{8,16},{12,20},{16,24},{20,28},{24,32},{28,36},{32,40... | collective-permute-start | bytes 1179656 | tf_op jit(solution)/shard_map/ppermute | solution.py:62
  87.5 17.4 %collective-permute-start.36 = (bf16[2,3,128,256]{3,2,1,0:T(8,128)(2,1)}, bf16[2,3,128,256]{3,2,1,0:T(8,128)(2,1)}, u32[]{:S(2)}, u32[]{:S(2)}) collective-permute-start(bf16[2,3,128,256]{3,2,1,0:T(8,128)(2,1)} %project_wide.3.late), channel_id=1, source_target_pairs={{0,8},{4,12},{8,16},{12,20},{16,24},{20,28},{24,32},{28,36},{32,40... | collective-permute-start | bytes 1179656 | tf_op jit(solution)/shard_map/ppermute | solution.py:62
  90.2 15.2 %collective-permute-start.12 = (bf16[4,4,64,256]{3,2,1,0:T(8,128)(2,1)S(1)}, bf16[4,4,64,256]{3,2,1,0:T(8,128)(2,1)S(1)}, u32[]{:S(2)}, u32[]{:S(2)}) collective-permute-start(bf16[4,4,64,256]{3,2,1,0:T(8,128)(2,1)S(1)} %collective-permute-done.11.refs_11_.a3.refs_7_), channel_id=1, source_target_pairs={{0,96},{4,28},{8,104},{12,4},{16,112},{20,12},{24,120},{28,20},{32... | collective-permute-start | bytes 1572872 | tf_op jit(solution)/shard_map/ppermute | solution.py:498
  92.8 13.0 %collective-permute-start.14 = (bf16[4,4,64,256]{3,2,1,0:T(8,128)(2,1)S(1)}, bf16[4,4,64,256]{3,2,1,0:T(8,128)(2,1)S(1)}, u32[]{:S(2)}, u32[]{:S(2)}) collective-permute-start(bf16[4,4,64,256]{3,2,1,0:T(8,128)(2,1)S(1)} %collective-permute-done.10.refs_9_.a1.refs_5_), channel_id=1, source_target_pairs={{0,4},{4,0},{8,12},{12,8},{16,20},{20,16},{24,28},{28,24},{32,36},... | collective-permute-start | bytes 1572872 | tf_op jit(solution)/shard_map/ppermute | solution.py:54
  96.4 11.8 %collective-permute-start.21 = (bf16[4,4,64,256]{3,2,1,0:T(8,128)(2,1)S(1)}, bf16[4,4,64,256]{3,2,1,0:T(8,128)(2,1)S(1)}, u32[]{:S(2)}, u32[]{:S(2)}) collective-permute-start(bf16[4,4,64,256]{3,2,1,0:T(8,128)(2,1)S(1)} %collective-permute-done.17.refs_9_), channel_id=1, source_target_pairs={{0,4},{4,0},{8,12},{12,8},{16,20},{20,16},{24,28},{28,24},{32,36},... | collective-permute-start | bytes 1572872 | tf_op jit(solution)/shard_map/ppermute | solution.py:54
  105.5 19.1 %collective-permute-start.16 = (bf16[4,4,64,256]{3,2,1,0:T(8,128)(2,1)S(1)}, bf16[4,4,64,256]{3,2,1,0:T(8,128)(2,1)S(1)}, u32[]{:S(2)}, u32[]{:S(2)}) collective-permute-start(bf16[4,4,64,256]{3,2,1,0:T(8,128)(2,1)S(1)} %collective-permute-done.11.refs_11_.a3.refs_7_), channel_id=1, source_target_pairs={{0,4},{4,0},{8,12},{12,8},{16,20},{20,16},{24,28},{28,24},{32,36},... | collective-permute-start | bytes 1572872 | tf_op jit(solution)/shard_map/ppermute | solution.py:54
  105.9 23.2 %collective-permute-start.15 = (bf16[4,4,64,256]{3,2,1,0:T(8,128)(2,1)S(1)}, bf16[4,4,64,256]{3,2,1,0:T(8,128)(2,1)S(1)}, u32[]{:S(2)}, u32[]{:S(2)}) collective-permute-start(bf16[4,4,64,256]{3,2,1,0:T(8,128)(2,1)S(1)} %collective-permute-done.12.refs_10_.a2.refs_6_), channel_id=1, source_target_pairs={{0,4},{4,0},{8,12},{12,8},{16,20},{20,16},{24,28},{28,24},{32,36},... | collective-permute-start | bytes 1572872 | tf_op jit(solution)/shard_map/ppermute | solution.py:54
  108.2 23.0 %collective-permute-start.41 = (bf16[16,64,256]{2,1,0:T(8,128)(2,1)}, bf16[16,64,256]{2,1,0:T(8,128)(2,1)S(1)}, u32[]{:S(2)}, u32[]{:S(2)}) collective-permute-start(bf16[16,64,256]{2,1,0:T(8,128)(2,1)} %pick.1), channel_id=1, source_target_pairs={{0,1},{1,2},{2,3},{3,0},{4,5},{5,6},{6,7},{7,4},{8,9},{9,10},{10,1... | collective-permute-start | bytes 1572872 | tf_op jit(solution)/shard_map/ppermute | solution.py:58
  109.5 24.4 %collective-permute-start.42 = (bf16[16,64,256]{2,1,0:T(8,128)(2,1)}, bf16[16,64,256]{2,1,0:T(8,128)(2,1)S(1)}, u32[]{:S(2)}, u32[]{:S(2)}) collective-permute-start(bf16[16,64,256]{2,1,0:T(8,128)(2,1)} %pick.1), channel_id=1, source_target_pairs={{0,2},{1,3},{2,0},{3,1},{4,6},{5,7},{6,4},{7,5},{8,10},{9,11},{10,... | collective-permute-start | bytes 1572872 | tf_op jit(solution)/shard_map/ppermute | solution.py:58
  110.9 24.4 %collective-permute-start.43 = (bf16[16,64,256]{2,1,0:T(8,128)(2,1)}, bf16[16,64,256]{2,1,0:T(8,128)(2,1)S(1)}, u32[]{:S(2)}, u32[]{:S(2)}) collective-permute-start(bf16[16,64,256]{2,1,0:T(8,128)(2,1)} %pick.1), channel_id=1, source_target_pairs={{0,3},{1,0},{2,1},{3,2},{4,7},{5,4},{6,5},{7,6},{8,11},{9,8},{10,9... | collective-permute-start | bytes 1572872 | tf_op jit(solution)/shard_map/ppermute | solution.py:58
  124.6 20.7 %collective-permute-start.37 = (bf16[2,3,128,256]{3,2,1,0:T(8,128)(2,1)S(1)}, bf16[2,3,128,256]{3,2,1,0:T(8,128)(2,1)S(1)}, u32[]{:S(2)}, u32[]{:S(2)}) collective-permute-start(bf16[2,3,128,256]{3,2,1,0:T(8,128)(2,1)S(1)} %copy-done.17), channel_id=1, source_target_pairs={{0,16},{4,20},{8,24},{12,28},{16,32},{20,36},{24,40},{28,44},{32,4... | collective-permute-start | bytes 1179656 | tf_op jit(solution)/shard_map/ppermute | solution.py:62
  129.1 22.0 %collective-permute-start.24 = (bf16[2,3,128,256]{3,2,1,0:T(8,128)(2,1)}, bf16[2,3,128,256]{3,2,1,0:T(8,128)(2,1)S(1)}, u32[]{:S(2)}, u32[]{:S(2)}) collective-permute-start(bf16[2,3,128,256]{3,2,1,0:T(8,128)(2,1)} %get-tuple-element.22), channel_id=1, source_target_pairs={{0,8},{4,12},{8,16},{12,20},{16,24},{20,28},{24,32},{28,36},{32,40... | collective-permute-start | bytes 1179656 | tf_op jit(solution)/shard_map/ppermute | solution.py:62
  131.2 36.6 %collective-permute-start.44 = (bf16[16,64,256]{2,1,0:T(8,128)(2,1)S(1)}, bf16[16,64,256]{2,1,0:T(8,128)(2,1)S(1)}, u32[]{:S(2)}, u32[]{:S(2)}) collective-permute-start(bf16[16,64,256]{2,1,0:T(8,128)(2,1)S(1)} %collective-permute-done.41.refs_12_), channel_id=1, source_target_pairs={{0,4},{4,0},{8,12},{12,8},{16,20},{20,16},{24,28},{28,24},{32,36},... | collective-permute-start | bytes 1572872 | tf_op jit(solution)/shard_map/ppermute | solution.py:54
  133.9 34.0 %collective-permute-start.45 = (bf16[16,64,256]{2,1,0:T(8,128)(2,1)S(1)}, bf16[16,64,256]{2,1,0:T(8,128)(2,1)S(1)}, u32[]{:S(2)}, u32[]{:S(2)}) collective-permute-start(bf16[16,64,256]{2,1,0:T(8,128)(2,1)S(1)} %collective-permute-done.42.refs_13_), channel_id=1, source_target_pairs={{0,4},{4,0},{8,12},{12,8},{16,20},{20,16},{24,28},{28,24},{32,36},... | collective-permute-start | bytes 1572872 | tf_op jit(solution)/shard_map/ppermute | solution.py:54
  135.3 32.6 %collective-permute-start.46 = (bf16[16,64,256]{2,1,0:T(8,128)(2,1)S(1)}, bf16[16,64,256]{2,1,0:T(8,128)(2,1)S(1)}, u32[]{:S(2)}, u32[]{:S(2)}) collective-permute-start(bf16[16,64,256]{2,1,0:T(8,128)(2,1)S(1)} %collective-permute-done.43.refs_14_), channel_id=1, source_target_pairs={{0,4},{4,0},{8,12},{12,8},{16,20},{20,16},{24,28},{28,24},{32,36},... | collective-permute-start | bytes 1572872 | tf_op jit(solution)/shard_map/ppermute | solution.py:54
  (62 other events, 962.6 us)

commit v7 on v6

--- a/solution.py
+++ b/solution.py
@@ -184,42 +184,27 @@
     )(*pieces, *lines)
 
 
-def matrix_copies(lines, first, count, w_all, sems):
-    core = lax.axis_index("sp") % 2
-    groups = [[] for _ in range(count)]
-    for n, line in enumerate(lines):
-        whose = core if n < RING else 1 - core
-        for j in range(RING):
-            at = pl.multiple_of(place_of(whose, j, n % RING, 0) * ROWS, ROWS)
-            for m in range(count):
-                groups[m].append(
-                    pltpu.make_async_copy(
-                        line.at[j, first + m], w_all.at[m, pl.ds(at, ROWS), :], sems.at[m, n * RING + j]
-                    )
-                )
-    return groups
-
-
 def project(x_all, w_all, m):
     x = x_all[...].reshape(BATCHES * SPAN, WIDTH)
     y = jnp.dot(x, w_all[m], preferred_element_type=jnp.float32)
     return y.astype(jnp.bfloat16).reshape(BATCHES, SPAN, COLS)
 
 
-def staged(early, late, rest, first, count, x_all, w_all, x_sems, w_sems, work):
+def staged(early, late, lines, parts, x_all, w_all, x_sems, w_sems, work):
     rows = row_copies(early, 0, x_all, x_sems) + row_copies(late, HALF, x_all, x_sems)
-    weights = matrix_copies(rest, first, count, w_all, w_sems)
-    for c in rows + weights[0] + weights[1]:
+    weights = [shard_copies(lines, first, count, w_all, w_sems.at[n], 0) for n, (first, count) in enumerate(parts)]
+    for c in rows + weights[0]:
         c.start()
     for c in rows:
         c.wait()
-    for m in range(count):
-        for c in weights[m]:
+    for n, (first, count) in enumerate(parts):
+        for c in weights[n]:
             c.wait()
-        if m + 2 < count:
-            for c in weights[m + 2]:
+        if n + 1 < len(parts):
+            for c in weights[n + 1]:
                 c.start()
-        work(m, project(x_all, w_all, m))
+        for m in range(first, first + count):
+            work(m, project(x_all, w_all, m))
 
 
 def near_pair_body(*refs):
@@ -233,7 +218,7 @@
         else:
             near_tail[m % 2, :, HALOS[0] :] = y[:, SPAN - HALOS[1] :]
 
-    staged(early, late, rest, 0, NEAR, *scratch, work)
+    staged(early, late, rest, ((0, 2), (2, 2)), *scratch, work)
 
 
 def query_body(*refs):
@@ -243,13 +228,13 @@
     def work(m, y):
         queries[m] = y
 
-    staged(early, late, rest, 0, GROUPS, *scratch, work)
+    staged(early, late, rest, ((0, 1), (1, 2)), *scratch, work)
 
 
 def rest_scratch(count):
     return [
         pltpu.VMEM((BATCHES, SPAN, WIDTH), jnp.bfloat16), pltpu.VMEM((count, WIDTH, COLS), jnp.bfloat16),
-        pltpu.SemaphoreType.DMA((2, RING)), pltpu.SemaphoreType.DMA((count, 32)),
+        pltpu.SemaphoreType.DMA((2, RING)), pltpu.SemaphoreType.DMA((2, 32)),
     ]
 
 

time: 185 us -> 183 us (0.989)
  Pallas kernels: 57.3 us -> 51.2 us
  waiting for transfers between devices: 39.6 us -> 43.8 us
    pallas_call x1, Pallas kernels: 12.5 us -> 8.32 us  [project_near(): pl.pallas_call(near_pair_body, out_shape=(bf(2, 2, BATCHES, SPAN, COLS),...]
    ppermute x12, waiting for transfers between devices: 20 us -> 24.2 us  [turned(): return lax.ppermute(a, 'tp', [(i, (i + shift) % RING) for i in range(RING)])]
    pallas_call x1, Pallas kernels: 9.3 us -> 7.38 us  [project_queries(): pl.pallas_call(query_body, out_shape=bf(GROUPS, BATCHES, SPAN, COLS), in_...]
  transfers between devices with their start and end apart: 49 -> 49, of which waited for: 15 -> 15; matrix products, arithmetic and copies ran while one was open for 2% -> 2% of each run, Pallas kernels for 26% -> 22%
where the time goes in v7:
time: 183 us; the launch traced here: 181 us
  starting transfers between devices  77.3 us (42%)
  Pallas kernels  51.2 us (28%)
  waiting for transfers between devices  43.8 us (24%)
  local copies, waits for them, and re-layouts  6.56 us (4%)
    ppermute x12, waiting for transfers between devices, turned(): return lax.ppermute(a, 'tp', [(i, (i + shift) % RING) for i in range(RING)])  24.2 us
    ppermute x18, starting transfers between devices, swapped(): return lax.ppermute(a, 'sp', SWAP)  19.3 us
    ppermute x12, starting transfers between devices, turned(): return lax.ppermute(a, 'tp', [(i, (i + shift) % RING) for i in range(RING)])  18 us
    ppermute x4, starting transfers between devices, from_behind(): lax.ppermute(a, 'sp', [(i, i + 2 * blocks) for i in range(32 - 2 * blocks)])  13 us
    ppermute x4, waiting for transfers between devices, from_behind(): lax.ppermute(a, 'sp', [(i, i + 2 * blocks) for i in range(32 - 2 * blocks)])  10.9 us
    pallas_call x2, Pallas kernels, project_wide(): pl.pallas_call(wide_pair_body, out_shape=bf(2, BATCHES, HALF, COLS), in_s...  8.6 us
    pallas_call x1, Pallas kernels, project_near(): pl.pallas_call(near_pair_body, out_shape=(bf(2, 2, BATCHES, SPAN, COLS),...  8.32 us
    ppermute x4, starting transfers between devices, spread_halves(): far = {d: lax.ppermute(line, 'sp', second_leg(d, 0)) for d in (1, 3)}  7.8 us
  transfers between devices with their start and end apart: 49, of which 15 were waited for; matrix products, arithmetic and copies ran while one was open for 2% of the time, Pallas kernels for 22%

profile of v7, /device:TPU:1, one launch (start us, length us, event | category | flops | bytes accessed | tf_op | source)
XLA Modules:
  0.0 181.1 jit_solution(12809643786281139778)
XLA Ops:
  2.4 4.6 %collective-permute-start.9 = (bf16[8,64,256]{2,1,0:T(8,128)(2,1)}, bf16[8,64,256]{2,1,0:T(8,128)(2,1)S(1)}, u32[]{:S(2)}, u32[]{:S(2)}) collective-permute-start(bf16[8,64,256]{2,1,0:T(8,128)(2,1)} %get-tuple-element.20), channel_id=1, source_target_pairs={{0,24},{4,100},{8,0},{12,108},{16,8},{20,116},{24,16},{28,124},{32... | collective-permute-start | bytes 786440 | tf_op jit(solution)/shard_map/ppermute | solution.py:478
  7.2 2.7 %collective-permute-start.26 = (bf16[2,64,256]{2,1,0:T(8,128)(2,1)}, bf16[2,64,256]{2,1,0:T(8,128)(2,1)S(1)}, u32[]{:S(2)}, u32[]{:S(2)}) collective-permute-start(bf16[2,64,256]{2,1,0:T(8,128)(2,1)} %get-tuple-element.23), channel_id=1, source_target_pairs={{0,16},{4,68},{8,24},{12,76},{16,0},{20,84},{24,8},{28,92},{32,48}... | collective-permute-start | bytes 196616 | tf_op jit(solution)/shard_map/ppermute | solution.py:470
  17.9 3.2 %collective-permute-start.29 = (bf16[4,2,64,256]{3,2,1,0:T(8,128)(2,1)S(1)}, bf16[4,2,64,256]{3,2,1,0:T(8,128)(2,1)S(1)}, u32[]{:S(2)}, u32[]{:S(2)}) collective-permute-start(bf16[4,2,64,256]{3,2,1,0:T(8,128)(2,1)S(1)} %pad_maximum_fusion.2.refs_4_), channel_id=1, source_target_pairs={{0,64},{4,20},{8,72},{12,28},{16,80},{20,4},{24,88},{28,12},{32,96... | collective-permute-start | bytes 786440 | tf_op jit(solution)/shard_map/ppermute | solution.py:472
  23.2 2.4 %collective-permute-start.31 = (bf16[4,2,64,256]{3,2,1,0:T(8,128)(2,1)S(1)}, bf16[4,2,64,256]{3,2,1,0:T(8,128)(2,1)S(1)}, u32[]{:S(2)}, u32[]{:S(2)}) collective-permute-start(bf16[4,2,64,256]{3,2,1,0:T(8,128)(2,1)S(1)} %pad_maximum_fusion.2.refs_4_), channel_id=1, source_target_pairs={{0,4},{4,0},{8,12},{12,8},{16,20},{20,16},{24,28},{28,24},{32,36},... | collective-permute-start | bytes 786440 | tf_op jit(solution)/shard_map/ppermute | solution.py:54
  26.8 3.0 %collective-permute-done.29.refs_6_ = bf16[4,2,64,256]{3,2,1,0:T(8,128)(2,1)S(1)} collective-permute-done((bf16[4,2,64,256]{3,2,1,0:T(8,128)(2,1)S(1)}, bf16[4,2,64,256]{3,2,1,0:T(8,128)(2,1)S(1)}, u32[]{:S(2)}, u32[]{:S(2)}) %collective-permute-start.29) | collective-permute-done | bytes 262176 | tf_op jit(solution)/shard_map/ppermute | solution.py:472
  31.4 2.7 %norm_rows.1 = (bf16[3,32,2048]{2,1,0:T(8,128)(2,1)}, bf16[3,32,2048]{2,1,0:T(8,128)(2,1)}) custom-call(bf16[6,32,2048]{2,1,0:T(8,128)(2,1)} %bitcast.27, bf16[3,32,2048]{2,1,0:T(8,128)(2,1)} %copy-done.38, f32[1,2048]{1,0:T(1,128)} %bitcast.34), custom_call_target="tpu_custom_call" | custom-call | tf_op jit(solution)/shard_map/norm_rows/pallas_call | solution.py:131
  35.4 2.5 %collective-permute-start.2 = (bf16[3,32,2048]{2,1,0:T(8,128)(2,1)}, bf16[3,32,2048]{2,1,0:T(8,128)(2,1)S(1)}, u32[]{:S(2)}, u32[]{:S(2)}) collective-permute-start(bf16[3,32,2048]{2,1,0:T(8,128)(2,1)} %get-tuple-element.18.refs_0_), channel_id=1, source_target_pairs={{0,2},{1,3},{2,0},{3,1},{4,6},{5,7},{6,4},{7,5},{8,10},{9,11},{10,... | collective-permute-start | bytes 1179656 | tf_op jit(solution)/shard_map/ppermute | solution.py:58
  41.3 2.7 %collective-permute-start.5 = (bf16[3,32,2048]{2,1,0:T(8,128)(2,1)}, bf16[3,32,2048]{2,1,0:T(8,128)(2,1)S(1)}, u32[]{:S(2)}, u32[]{:S(2)}) collective-permute-start(bf16[3,32,2048]{2,1,0:T(8,128)(2,1)} %get-tuple-element.19.refs_4_.refs_0_), channel_id=1, source_target_pairs={{0,2},{1,3},{2,0},{3,1},{4,6},{5,7},{6,4},{7,5},{8,10},{9,11},{10,... | collective-permute-start | bytes 1179656 | tf_op jit(solution)/shard_map/ppermute | solution.py:58
  44.7 3.0 %collective-permute-start.11 = (bf16[4,4,64,256]{3,2,1,0:T(8,128)(2,1)S(1)}, bf16[4,4,64,256]{3,2,1,0:T(8,128)(2,1)S(1)}, u32[]{:S(2)}, u32[]{:S(2)}) collective-permute-start(bf16[4,4,64,256]{3,2,1,0:T(8,128)(2,1)S(1)} %pad_maximum_fusion.refs_8_.a0.refs_4_), channel_id=1, source_target_pairs={{0,96},{4,28},{8,104},{12,4},{16,112},{20,12},{24,120},{28,20},{32... | collective-permute-start | bytes 1572872 | tf_op jit(solution)/shard_map/ppermute | solution.py:482
  47.7 6.4 %collective-permute-done.2.refs_2_ = bf16[3,32,2048]{2,1,0:T(8,128)(2,1)S(1)} collective-permute-done((bf16[3,32,2048]{2,1,0:T(8,128)(2,1)}, bf16[3,32,2048]{2,1,0:T(8,128)(2,1)S(1)}, u32[]{:S(2)}, u32[]{:S(2)}) %collective-permute-start.2) | collective-permute-done | bytes 393248 | tf_op jit(solution)/shard_map/ppermute | solution.py:58
  54.1 4.5 %collective-permute-start.13 = (bf16[4,4,64,256]{3,2,1,0:T(8,128)(2,1)S(1)}, bf16[4,4,64,256]{3,2,1,0:T(8,128)(2,1)S(1)}, u32[]{:S(2)}, u32[]{:S(2)}) collective-permute-start(bf16[4,4,64,256]{3,2,1,0:T(8,128)(2,1)S(1)} %pad_maximum_fusion.refs_8_.a0.refs_4_), channel_id=1, source_target_pairs={{0,4},{4,0},{8,12},{12,8},{16,20},{20,16},{24,28},{28,24},{32,36},... | collective-permute-start | bytes 1572872 | tf_op jit(solution)/shard_map/ppermute | solution.py:54
  61.5 3.0 %collective-permute-start.19 = (bf16[4,4,64,256]{3,2,1,0:T(8,128)(2,1)S(1)}, bf16[4,4,64,256]{3,2,1,0:T(8,128)(2,1)}, u32[]{:S(2)}, u32[]{:S(2)}) collective-permute-start(bf16[4,4,64,256]{3,2,1,0:T(8,128)(2,1)S(1)} %pad_maximum_fusion.1.refs_8_), channel_id=1, source_target_pairs={{0,96},{4,28},{8,104},{12,4},{16,112},{20,12},{24,120},{28,20},{32... | collective-permute-start | bytes 1572872 | tf_op jit(solution)/shard_map/ppermute | solution.py:482
  64.6 6.4 %collective-permute-done.5.refs_6_.refs_2_ = bf16[3,32,2048]{2,1,0:T(8,128)(2,1)S(1)} collective-permute-done((bf16[3,32,2048]{2,1,0:T(8,128)(2,1)}, bf16[3,32,2048]{2,1,0:T(8,128)(2,1)S(1)}, u32[]{:S(2)}, u32[]{:S(2)}) %collective-permute-start.5) | collective-permute-done | bytes 393248 | tf_op jit(solution)/shard_map/ppermute | solution.py:58
  71.0 2.4 %collective-permute-start.20 = (bf16[4,4,64,256]{3,2,1,0:T(8,128)(2,1)S(1)}, bf16[4,4,64,256]{3,2,1,0:T(8,128)(2,1)}, u32[]{:S(2)}, u32[]{:S(2)}) collective-permute-start(bf16[4,4,64,256]{3,2,1,0:T(8,128)(2,1)S(1)} %pad_maximum_fusion.1.refs_8_), channel_id=1, source_target_pairs={{0,4},{4,0},{8,12},{12,8},{16,20},{20,16},{24,28},{28,24},{32,36},... | collective-permute-start | bytes 1572872 | tf_op jit(solution)/shard_map/ppermute | solution.py:54
  75.0 4.3 %project_wide.2.early = bf16[2,3,128,256]{3,2,1,0:T(8,128)(2,1)} custom-call(bf16[3,32,2048]{2,1,0:T(8,128)(2,1)} %get-tuple-element.18.refs_0_, bf16[3,32,2048]{2,1,0:T(8,128)(2,1)} %copy-done.4, bf16[3,32,2048]{2,1,0:T(8,128)(2,1)} %copy-done.5, bf16[3,32,2048]{2,1,0:T(8,128)(2,1)} %copy-done.6, bf16[4,2,64,256]{3,2,1,0:T(8,128)(2,1)} %copy-done.10, ...), custom_call_target="tpu_custom_call" | custom-call | tf_op jit(solution)/shard_map/project_wide/pallas_call | solution.py:177
  79.4 4.3 %project_wide.3.late = bf16[2,3,128,256]{3,2,1,0:T(8,128)(2,1)} custom-call(bf16[3,32,2048]{2,1,0:T(8,128)(2,1)} %get-tuple-element.19.refs_4_.refs_0_, bf16[3,32,2048]{2,1,0:T(8,128)(2,1)} %copy-done.7, bf16[3,32,2048]{2,1,0:T(8,128)(2,1)} %copy-done.8, bf16[3,32,2048]{2,1,0:T(8,128)(2,1)} %copy-done.9, bf16[4,2,64,256]{3,2,1,0:T(8,128)(2,1)} %copy-done.10, ...), custom_call_target="tpu_custom_call" | custom-call | tf_op jit(solution)/shard_map/project_wide/pallas_call | solution.py:177
  83.7 3.8 %collective-permute-start.35 = (bf16[2,3,128,256]{3,2,1,0:T(8,128)(2,1)S(1)}, bf16[2,3,128,256]{3,2,1,0:T(8,128)(2,1)S(1)}, u32[]{:S(2)}, u32[]{:S(2)}) collective-permute-start(bf16[2,3,128,256]{3,2,1,0:T(8,128)(2,1)S(1)} %copy-done.16), channel_id=1, source_target_pairs={{0,8},{4,12},{8,16},{12,20},{16,24},{20,28},{24,32},{28,36},{32,40... | collective-permute-start | bytes 1179656 | tf_op jit(solution)/shard_map/ppermute | solution.py:62
  87.5 2.7 %collective-permute-start.36 = (bf16[2,3,128,256]{3,2,1,0:T(8,128)(2,1)}, bf16[2,3,128,256]{3,2,1,0:T(8,128)(2,1)}, u32[]{:S(2)}, u32[]{:S(2)}) collective-permute-start(bf16[2,3,128,256]{3,2,1,0:T(8,128)(2,1)} %project_wide.3.late), channel_id=1, source_target_pairs={{0,8},{4,12},{8,16},{12,20},{16,24},{20,28},{24,32},{28,36},{32,40... | collective-permute-start | bytes 1179656 | tf_op jit(solution)/shard_map/ppermute | solution.py:62
  90.2 2.6 %collective-permute-start.12 = (bf16[4,4,64,256]{3,2,1,0:T(8,128)(2,1)S(1)}, bf16[4,4,64,256]{3,2,1,0:T(8,128)(2,1)S(1)}, u32[]{:S(2)}, u32[]{:S(2)}) collective-permute-start(bf16[4,4,64,256]{3,2,1,0:T(8,128)(2,1)S(1)} %collective-permute-done.11.refs_11_.a3.refs_7_), channel_id=1, source_target_pairs={{0,96},{4,28},{8,104},{12,4},{16,112},{20,12},{24,120},{28,20},{32... | collective-permute-start | bytes 1572872 | tf_op jit(solution)/shard_map/ppermute | solution.py:483
  93.6 2.8 %collective-permute-done.35.back_early = bf16[2,3,128,256]{3,2,1,0:T(8,128)(2,1)S(1)} collective-permute-done((bf16[2,3,128,256]{3,2,1,0:T(8,128)(2,1)S(1)}, bf16[2,3,128,256]{3,2,1,0:T(8,128)(2,1)S(1)}, u32[]{:S(2)}, u32[]{:S(2)}) %collective-permute-start.35) | collective-permute-done | bytes 393248 | tf_op jit(solution)/shard_map/ppermute | solution.py:62
  96.8 8.1 %collective-permute-done.36.back_late = bf16[2,3,128,256]{3,2,1,0:T(8,128)(2,1)} collective-permute-done((bf16[2,3,128,256]{3,2,1,0:T(8,128)(2,1)}, bf16[2,3,128,256]{3,2,1,0:T(8,128)(2,1)}, u32[]{:S(2)}, u32[]{:S(2)}) %collective-permute-start.36) | collective-permute-done | bytes 393248 | tf_op jit(solution)/shard_map/ppermute | solution.py:62
  112.0 8.3 %project_near.1 = (bf16[2,2,3,256,256]{4,3,2,1,0:T(8,128)(2,1)}, bf16[2,3,128,256]{3,2,1,0:T(8,128)(2,1)}) custom-call(bf16[3,32,2048]{2,1,0:T(8,128)(2,1)} %get-tuple-element.18.refs_0_, bf16[3,32,2048]{2,1,0:T(8,128)(2,1)} %copy-done.4, bf16[3,32,2048]{2,1,0:T(8,128)(2,1)} %copy-done.5, bf16[3,32,2048]{2,1,0:T(8,128)(2,1)} %copy-done.6, ...), custom_call_target="tpu_custom_call" | custom-call | tf_op jit(solution)/shard_map/project_near/pallas_call | solution.py:242
  120.4 4.5 %collective-permute-start.37 = (bf16[2,3,128,256]{3,2,1,0:T(8,128)(2,1)S(1)}, bf16[2,3,128,256]{3,2,1,0:T(8,128)(2,1)S(1)}, u32[]{:S(2)}, u32[]{:S(2)}) collective-permute-start(bf16[2,3,128,256]{3,2,1,0:T(8,128)(2,1)S(1)} %copy-done.17), channel_id=1, source_target_pairs={{0,16},{4,20},{8,24},{12,28},{16,32},{20,36},{24,40},{28,44},{32,4... | collective-permute-start | bytes 1179656 | tf_op jit(solution)/shard_map/ppermute | solution.py:62
  124.9 2.1 %collective-permute-start.24 = (bf16[2,3,128,256]{3,2,1,0:T(8,128)(2,1)}, bf16[2,3,128,256]{3,2,1,0:T(8,128)(2,1)S(1)}, u32[]{:S(2)}, u32[]{:S(2)}) collective-permute-start(bf16[2,3,128,256]{3,2,1,0:T(8,128)(2,1)} %get-tuple-element.22), channel_id=1, source_target_pairs={{0,8},{4,12},{8,16},{12,20},{16,24},{20,28},{24,32},{28,36},{32,40... | collective-permute-start | bytes 1179656 | tf_op jit(solution)/shard_map/ppermute | solution.py:62
  129.0 4.9 %collective-permute-done.42.refs_13_ = bf16[16,64,256]{2,1,0:T(8,128)(2,1)S(1)} collective-permute-done((bf16[16,64,256]{2,1,0:T(8,128)(2,1)}, bf16[16,64,256]{2,1,0:T(8,128)(2,1)S(1)}, u32[]{:S(2)}, u32[]{:S(2)}) %collective-permute-start.42) | collective-permute-done | bytes 524320 | tf_op jit(solution)/shard_map/ppermute | solution.py:58
  135.9 7.4 %project_queries.1.q = bf16[3,3,256,256]{3,2,1,0:T(8,128)(2,1)} custom-call(bf16[3,32,2048]{2,1,0:T(8,128)(2,1)} %get-tuple-element.18.refs_0_, bf16[3,32,2048]{2,1,0:T(8,128)(2,1)} %copy-done.4, bf16[3,32,2048]{2,1,0:T(8,128)(2,1)} %copy-done.5, bf16[3,32,2048]{2,1,0:T(8,128)(2,1)} %copy-done.6, bf16[3,32,2048]{2,1,0:T(8,128)(2,1)} %get-tuple-element.19.refs_4_.refs_0_, ...), custom_call_target="tpu_custom_call" | custom-call | tf_op jit(solution)/shard_map/project_queries/pallas_call | solution.py:251
  144.1 5.1 %attend_wide.1 = (f32[3,256,256]{2,1,0:T(8,128)}, f32[3,256,256]{2,1,0:T(8,128)}) custom-call(bf16[3,3,256,256]{3,2,1,0:T(8,128)(2,1)} %project_queries.1.q, bf16[2,3,128,256]{3,2,1,0:T(8,128)(2,1)} %project_wide.2.early, bf16[2,3,128,256]{3,2,1,0:T(8,128)(2,1)} %project_wide.3.late, bf16[2,3,128,256]{3,2,1,0:T(8,128)(2,1)} %copy-done.35, ...), custom_call_target="tpu_custom_call" | custom-call | tf_op jit(solution)/shard_map/attend_wide/pallas_call | solution.py:316
  150.0 6.6 %attend_near.1 = (bf16[2,3,32,256]{3,2,1,0:T(8,128)(2,1)}, bf16[2,3,32,256]{3,2,1,0:T(8,128)(2,1)}, bf16[2,3,32,256]{3,2,1,0:T(8,128)(2,1)}, bf16[2,3,32,256]{3,...) custom-call(bf16[3,3,256,256]{3,2,1,0:T(8,128)(2,1)} %project_queries.1.q, ...), custom_call_target="tpu_custom_call" | custom-call | tf_op jit(solution)/shard_map/attend_near/pallas_call | solution.py:367
  157.6 2.6 %collective-permute-start.39 = (bf16[2,3,32,256]{3,2,1,0:T(8,128)(2,1)}, bf16[2,3,32,256]{3,2,1,0:T(8,128)(2,1)S(1)}, u32[]{:S(2)}, u32[]{:S(2)}) collective-permute-start(bf16[2,3,32,256]{3,2,1,0:T(8,128)(2,1)} %get-tuple-element.28), channel_id=1, source_target_pairs={{0,2},{1,3},{2,0},{3,1},{4,6},{5,7},{6,4},{7,5},{8,10},{9,11},{10,... | collective-permute-start | bytes 294920 | tf_op jit(solution)/shard_map/ppermute | solution.py:58
  160.2 2.1 %collective-permute-done.38.refs_1_ = bf16[2,3,32,256]{3,2,1,0:T(8,128)(2,1)S(1)} collective-permute-done((bf16[2,3,32,256]{3,2,1,0:T(8,128)(2,1)}, bf16[2,3,32,256]{3,2,1,0:T(8,128)(2,1)S(1)}, u32[]{:S(2)}, u32[]{:S(2)}) %collective-permute-start.38) | collective-permute-done | bytes 98336 | tf_op jit(solution)/shard_map/ppermute | solution.py:58
  167.1 6.7 %finish.1 = (bf16[3,32,2048]{2,1,0:T(8,128)(2,1)}, bf16[3,32,2048]{2,1,0:T(8,128)(2,1)}) custom-call(bf16[2,3,32,256]{3,2,1,0:T(8,128)(2,1)} %get-tuple-element.26.refs_0_, bf16[2,3,32,256]{3,2,1,0:T(8,128)(2,1)} %copy-done.40, bf16[2,3,32,256]{3,2,1,0:T(8,128)(2,1)} %copy-done.41, bf16[2,3,32,256]{3,2,1,0:T(8,128)(2,1)} %copy-done.42, ...), custom_call_target="tpu_custom_call" | custom-call | tf_op jit(solution)/shard_map/finish/pallas_call | solution.py:437
  173.8 2.3 %collective-permute-start.47 = (bf16[3,32,2048]{2,1,0:T(8,128)(2,1)}, bf16[3,32,2048]{2,1,0:T(8,128)(2,1)S(1)}, u32[]{:S(2)}, u32[]{:S(2)}) collective-permute-start(bf16[3,32,2048]{2,1,0:T(8,128)(2,1)} %get-tuple-element.31), channel_id=1, source_target_pairs={{0,4},{4,0},{8,12},{12,8},{16,20},{20,16},{24,28},{28,24},{32,36},... | collective-permute-start | bytes 1179656 | tf_op jit(solution)/shard_map/ppermute | solution.py:54
  (177 shorter events, 49.1 us)
Async XLA Ops:
  2.4 15.6 %collective-permute-start.9 = (bf16[8,64,256]{2,1,0:T(8,128)(2,1)}, bf16[8,64,256]{2,1,0:T(8,128)(2,1)S(1)}, u32[]{:S(2)}, u32[]{:S(2)}) collective-permute-start(bf16[8,64,256]{2,1,0:T(8,128)(2,1)} %get-tuple-element.20), channel_id=1, source_target_pairs={{0,24},{4,100},{8,0},{12,108},{16,8},{20,116},{24,16},{28,124},{32... | collective-permute-start | bytes 786440 | tf_op jit(solution)/shard_map/ppermute | solution.py:478
  6.9 14.2 %collective-permute-start.8 = (bf16[8,64,256]{2,1,0:T(8,128)(2,1)}, bf16[8,64,256]{2,1,0:T(8,128)(2,1)S(1)}, u32[]{:S(2)}, u32[]{:S(2)}) collective-permute-start(bf16[8,64,256]{2,1,0:T(8,128)(2,1)} %get-tuple-element.20), channel_id=1, source_target_pairs={{0,16},{4,68},{8,24},{12,76},{16,0},{20,84},{24,8},{28,92},{32,48}... | collective-permute-start | bytes 786440 | tf_op jit(solution)/shard_map/ppermute | solution.py:478
  14.9 15.7 %collective-permute-start = (bf16[3,32,2048]{2,1,0:T(8,128)(2,1)S(1)}, bf16[3,32,2048]{2,1,0:T(8,128)(2,1)S(1)}, u32[]{:S(2)}, u32[]{:S(2)}) collective-permute-start(bf16[3,32,2048]{2,1,0:T(8,128)(2,1)S(1)} %dynamic-slice_bitcast_fusion), channel_id=1, source_target_pairs={{0,4},{4,0},{8,12},{12,8},{16,20},{20,16},{24,28},{28,24},{32,36},... | collective-permute-start | bytes 1179656 | tf_op jit(solution)/shard_map/ppermute | solution.py:54
  17.9 11.9 %collective-permute-start.29 = (bf16[4,2,64,256]{3,2,1,0:T(8,128)(2,1)S(1)}, bf16[4,2,64,256]{3,2,1,0:T(8,128)(2,1)S(1)}, u32[]{:S(2)}, u32[]{:S(2)}) collective-permute-start(bf16[4,2,64,256]{3,2,1,0:T(8,128)(2,1)S(1)} %pad_maximum_fusion.2.refs_4_), channel_id=1, source_target_pairs={{0,64},{4,20},{8,72},{12,28},{16,80},{20,4},{24,88},{28,12},{32,96... | collective-permute-start | bytes 786440 | tf_op jit(solution)/shard_map/ppermute | solution.py:472
  25.8 13.2 %collective-permute-start.10 = (bf16[4,4,64,256]{3,2,1,0:T(8,128)(2,1)S(1)}, bf16[4,4,64,256]{3,2,1,0:T(8,128)(2,1)S(1)}, u32[]{:S(2)}, u32[]{:S(2)}) collective-permute-start(bf16[4,4,64,256]{3,2,1,0:T(8,128)(2,1)S(1)} %pad_maximum_fusion.refs_8_.a0.refs_4_), channel_id=1, source_target_pairs={{0,32},{4,12},{8,40},{12,20},{16,48},{20,28},{24,56},{28,4},{32,64... | collective-permute-start | bytes 1572872 | tf_op jit(solution)/shard_map/ppermute | solution.py:482
  30.6 10.7 %collective-permute-start.17 = (bf16[4,4,64,256]{3,2,1,0:T(8,128)(2,1)S(1)}, bf16[4,4,64,256]{3,2,1,0:T(8,128)(2,1)S(1)}, u32[]{:S(2)}, u32[]{:S(2)}) collective-permute-start(bf16[4,4,64,256]{3,2,1,0:T(8,128)(2,1)S(1)} %pad_maximum_fusion.1.refs_8_), channel_id=1, source_target_pairs={{0,32},{4,12},{8,40},{12,20},{16,48},{20,28},{24,56},{28,4},{32,64... | collective-permute-start | bytes 1572872 | tf_op jit(solution)/shard_map/ppermute | solution.py:482
  34.2 10.5 %collective-permute-start.1 = (bf16[3,32,2048]{2,1,0:T(8,128)(2,1)}, bf16[3,32,2048]{2,1,0:T(8,128)(2,1)S(1)}, u32[]{:S(2)}, u32[]{:S(2)}) collective-permute-start(bf16[3,32,2048]{2,1,0:T(8,128)(2,1)} %get-tuple-element.18.refs_0_), channel_id=1, source_target_pairs={{0,1},{1,2},{2,3},{3,0},{4,5},{5,6},{6,7},{7,4},{8,9},{9,10},{10,1... | collective-permute-start | bytes 1179656 | tf_op jit(solution)/shard_map/ppermute | solution.py:58
  35.4 18.8 %collective-permute-start.2 = (bf16[3,32,2048]{2,1,0:T(8,128)(2,1)}, bf16[3,32,2048]{2,1,0:T(8,128)(2,1)S(1)}, u32[]{:S(2)}, u32[]{:S(2)}) collective-permute-start(bf16[3,32,2048]{2,1,0:T(8,128)(2,1)} %get-tuple-element.18.refs_0_), channel_id=1, source_target_pairs={{0,2},{1,3},{2,0},{3,1},{4,6},{5,7},{6,4},{7,5},{8,10},{9,11},{10,... | collective-permute-start | bytes 1179656 | tf_op jit(solution)/shard_map/ppermute | solution.py:58
  37.8 20.8 %collective-permute-start.3 = (bf16[3,32,2048]{2,1,0:T(8,128)(2,1)}, bf16[3,32,2048]{2,1,0:T(8,128)(2,1)S(1)}, u32[]{:S(2)}, u32[]{:S(2)}) collective-permute-start(bf16[3,32,2048]{2,1,0:T(8,128)(2,1)} %get-tuple-element.18.refs_0_), channel_id=1, source_target_pairs={{0,3},{1,0},{2,1},{3,2},{4,7},{5,4},{6,5},{7,6},{8,11},{9,8},{10,9... | collective-permute-start | bytes 1179656 | tf_op jit(solution)/shard_map/ppermute | solution.py:58
  39.0 22.5 %collective-permute-start.4 = (bf16[3,32,2048]{2,1,0:T(8,128)(2,1)}, bf16[3,32,2048]{2,1,0:T(8,128)(2,1)S(1)}, u32[]{:S(2)}, u32[]{:S(2)}) collective-permute-start(bf16[3,32,2048]{2,1,0:T(8,128)(2,1)} %get-tuple-element.19.refs_4_.refs_0_), channel_id=1, source_target_pairs={{0,1},{1,2},{2,3},{3,0},{4,5},{5,6},{6,7},{7,4},{8,9},{9,10},{10,1... | collective-permute-start | bytes 1179656 | tf_op jit(solution)/shard_map/ppermute | solution.py:58
  41.3 29.6 %collective-permute-start.5 = (bf16[3,32,2048]{2,1,0:T(8,128)(2,1)}, bf16[3,32,2048]{2,1,0:T(8,128)(2,1)S(1)}, u32[]{:S(2)}, u32[]{:S(2)}) collective-permute-start(bf16[3,32,2048]{2,1,0:T(8,128)(2,1)} %get-tuple-element.19.refs_4_.refs_0_), channel_id=1, source_target_pairs={{0,2},{1,3},{2,0},{3,1},{4,6},{5,7},{6,4},{7,5},{8,10},{9,11},{10,... | collective-permute-start | bytes 1179656 | tf_op jit(solution)/shard_map/ppermute | solution.py:58
  44.7 39.0 %collective-permute-start.11 = (bf16[4,4,64,256]{3,2,1,0:T(8,128)(2,1)S(1)}, bf16[4,4,64,256]{3,2,1,0:T(8,128)(2,1)S(1)}, u32[]{:S(2)}, u32[]{:S(2)}) collective-permute-start(bf16[4,4,64,256]{3,2,1,0:T(8,128)(2,1)S(1)} %pad_maximum_fusion.refs_8_.a0.refs_4_), channel_id=1, source_target_pairs={{0,96},{4,28},{8,104},{12,4},{16,112},{20,12},{24,120},{28,20},{32... | collective-permute-start | bytes 1572872 | tf_op jit(solution)/shard_map/ppermute | solution.py:482
  54.1 33.4 %collective-permute-start.13 = (bf16[4,4,64,256]{3,2,1,0:T(8,128)(2,1)S(1)}, bf16[4,4,64,256]{3,2,1,0:T(8,128)(2,1)S(1)}, u32[]{:S(2)}, u32[]{:S(2)}) collective-permute-start(bf16[4,4,64,256]{3,2,1,0:T(8,128)(2,1)S(1)} %pad_maximum_fusion.refs_8_.a0.refs_4_), channel_id=1, source_target_pairs={{0,4},{4,0},{8,12},{12,8},{16,20},{20,16},{24,28},{28,24},{32,36},... | collective-permute-start | bytes 1572872 | tf_op jit(solution)/shard_map/ppermute | solution.py:54
  58.6 14.8 %collective-permute-start.6 = (bf16[3,32,2048]{2,1,0:T(8,128)(2,1)}, bf16[3,32,2048]{2,1,0:T(8,128)(2,1)S(1)}, u32[]{:S(2)}, u32[]{:S(2)}) collective-permute-start(bf16[3,32,2048]{2,1,0:T(8,128)(2,1)} %get-tuple-element.19.refs_4_.refs_0_), channel_id=1, source_target_pairs={{0,3},{1,0},{2,1},{3,2},{4,7},{5,4},{6,5},{7,6},{8,11},{9,8},{10,9... | collective-permute-start | bytes 1179656 | tf_op jit(solution)/shard_map/ppermute | solution.py:58
  61.5 28.7 %collective-permute-start.19 = (bf16[4,4,64,256]{3,2,1,0:T(8,128)(2,1)S(1)}, bf16[4,4,64,256]{3,2,1,0:T(8,128)(2,1)}, u32[]{:S(2)}, u32[]{:S(2)}) collective-permute-start(bf16[4,4,64,256]{3,2,1,0:T(8,128)(2,1)S(1)} %pad_maximum_fusion.1.refs_8_), channel_id=1, source_target_pairs={{0,96},{4,28},{8,104},{12,4},{16,112},{20,12},{24,120},{28,20},{32... | collective-permute-start | bytes 1572872 | tf_op jit(solution)/shard_map/ppermute | solution.py:482
  71.0 21.9 %collective-permute-start.20 = (bf16[4,4,64,256]{3,2,1,0:T(8,128)(2,1)S(1)}, bf16[4,4,64,256]{3,2,1,0:T(8,128)(2,1)}, u32[]{:S(2)}, u32[]{:S(2)}) collective-permute-start(bf16[4,4,64,256]{3,2,1,0:T(8,128)(2,1)S(1)} %pad_maximum_fusion.1.refs_8_), channel_id=1, source_target_pairs={{0,4},{4,0},{8,12},{12,8},{16,20},{20,16},{24,28},{28,24},{32,36},... | collective-permute-start | bytes 1572872 | tf_op jit(solution)/shard_map/ppermute | solution.py:54
  73.4 31.9 %collective-permute-start.18 = (bf16[4,4,64,256]{3,2,1,0:T(8,128)(2,1)S(1)}, bf16[4,4,64,256]{3,2,1,0:T(8,128)(2,1)}, u32[]{:S(2)}, u32[]{:S(2)}) collective-permute-start(bf16[4,4,64,256]{3,2,1,0:T(8,128)(2,1)S(1)} %collective-permute-done.17.refs_9_), channel_id=1, source_target_pairs={{0,32},{4,12},{8,40},{12,20},{16,48},{20,28},{24,56},{28,4},{32,64... | collective-permute-start | bytes 1572872 | tf_op jit(solution)/shard_map/ppermute | solution.py:483
  83.7 12.7 %collective-permute-start.35 = (bf16[2,3,128,256]{3,2,1,0:T(8,128)(2,1)S(1)}, bf16[2,3,128,256]{3,2,1,0:T(8,128)(2,1)S(1)}, u32[]{:S(2)}, u32[]{:S(2)}) collective-permute-start(bf16[2,3,128,256]{3,2,1,0:T(8,128)(2,1)S(1)} %copy-done.16), channel_id=1, source_target_pairs={{0,8},{4,12},{8,16},{12,20},{16,24},{20,28},{24,32},{28,36},{32,40... | collective-permute-start | bytes 1179656 | tf_op jit(solution)/shard_map/ppermute | solution.py:62
  87.5 17.4 %collective-permute-start.36 = (bf16[2,3,128,256]{3,2,1,0:T(8,128)(2,1)}, bf16[2,3,128,256]{3,2,1,0:T(8,128)(2,1)}, u32[]{:S(2)}, u32[]{:S(2)}) collective-permute-start(bf16[2,3,128,256]{3,2,1,0:T(8,128)(2,1)} %project_wide.3.late), channel_id=1, source_target_pairs={{0,8},{4,12},{8,16},{12,20},{16,24},{20,28},{24,32},{28,36},{32,40... | collective-permute-start | bytes 1179656 | tf_op jit(solution)/shard_map/ppermute | solution.py:62
  90.2 15.2 %collective-permute-start.12 = (bf16[4,4,64,256]{3,2,1,0:T(8,128)(2,1)S(1)}, bf16[4,4,64,256]{3,2,1,0:T(8,128)(2,1)S(1)}, u32[]{:S(2)}, u32[]{:S(2)}) collective-permute-start(bf16[4,4,64,256]{3,2,1,0:T(8,128)(2,1)S(1)} %collective-permute-done.11.refs_11_.a3.refs_7_), channel_id=1, source_target_pairs={{0,96},{4,28},{8,104},{12,4},{16,112},{20,12},{24,120},{28,20},{32... | collective-permute-start | bytes 1572872 | tf_op jit(solution)/shard_map/ppermute | solution.py:483
  92.8 13.0 %collective-permute-start.14 = (bf16[4,4,64,256]{3,2,1,0:T(8,128)(2,1)S(1)}, bf16[4,4,64,256]{3,2,1,0:T(8,128)(2,1)S(1)}, u32[]{:S(2)}, u32[]{:S(2)}) collective-permute-start(bf16[4,4,64,256]{3,2,1,0:T(8,128)(2,1)S(1)} %collective-permute-done.10.refs_9_.a1.refs_5_), channel_id=1, source_target_pairs={{0,4},{4,0},{8,12},{12,8},{16,20},{20,16},{24,28},{28,24},{32,36},... | collective-permute-start | bytes 1572872 | tf_op jit(solution)/shard_map/ppermute | solution.py:54
  96.4 11.8 %collective-permute-start.21 = (bf16[4,4,64,256]{3,2,1,0:T(8,128)(2,1)S(1)}, bf16[4,4,64,256]{3,2,1,0:T(8,128)(2,1)S(1)}, u32[]{:S(2)}, u32[]{:S(2)}) collective-permute-start(bf16[4,4,64,256]{3,2,1,0:T(8,128)(2,1)S(1)} %collective-permute-done.17.refs_9_), channel_id=1, source_target_pairs={{0,4},{4,0},{8,12},{12,8},{16,20},{20,16},{24,28},{28,24},{32,36},... | collective-permute-start | bytes 1572872 | tf_op jit(solution)/shard_map/ppermute | solution.py:54
  105.5 14.9 %collective-permute-start.16 = (bf16[4,4,64,256]{3,2,1,0:T(8,128)(2,1)S(1)}, bf16[4,4,64,256]{3,2,1,0:T(8,128)(2,1)S(1)}, u32[]{:S(2)}, u32[]{:S(2)}) collective-permute-start(bf16[4,4,64,256]{3,2,1,0:T(8,128)(2,1)S(1)} %collective-permute-done.11.refs_11_.a3.refs_7_), channel_id=1, source_target_pairs={{0,4},{4,0},{8,12},{12,8},{16,20},{20,16},{24,28},{28,24},{32,36},... | collective-permute-start | bytes 1572872 | tf_op jit(solution)/shard_map/ppermute | solution.py:54
  105.9 19.0 %collective-permute-start.15 = (bf16[4,4,64,256]{3,2,1,0:T(8,128)(2,1)S(1)}, bf16[4,4,64,256]{3,2,1,0:T(8,128)(2,1)S(1)}, u32[]{:S(2)}, u32[]{:S(2)}) collective-permute-start(bf16[4,4,64,256]{3,2,1,0:T(8,128)(2,1)S(1)} %collective-permute-done.12.refs_10_.a2.refs_6_), channel_id=1, source_target_pairs={{0,4},{4,0},{8,12},{12,8},{16,20},{20,16},{24,28},{28,24},{32,36},... | collective-permute-start | bytes 1572872 | tf_op jit(solution)/shard_map/ppermute | solution.py:54
  108.2 18.8 %collective-permute-start.41 = (bf16[16,64,256]{2,1,0:T(8,128)(2,1)}, bf16[16,64,256]{2,1,0:T(8,128)(2,1)S(1)}, u32[]{:S(2)}, u32[]{:S(2)}) collective-permute-start(bf16[16,64,256]{2,1,0:T(8,128)(2,1)} %pick.1), channel_id=1, source_target_pairs={{0,1},{1,2},{2,3},{3,0},{4,5},{5,6},{6,7},{7,4},{8,9},{9,10},{10,1... | collective-permute-start | bytes 1572872 | tf_op jit(solution)/shard_map/ppermute | solution.py:58
  109.5 24.4 %collective-permute-start.42 = (bf16[16,64,256]{2,1,0:T(8,128)(2,1)}, bf16[16,64,256]{2,1,0:T(8,128)(2,1)S(1)}, u32[]{:S(2)}, u32[]{:S(2)}) collective-permute-start(bf16[16,64,256]{2,1,0:T(8,128)(2,1)} %pick.1), channel_id=1, source_target_pairs={{0,2},{1,3},{2,0},{3,1},{4,6},{5,7},{6,4},{7,5},{8,10},{9,11},{10,... | collective-permute-start | bytes 1572872 | tf_op jit(solution)/shard_map/ppermute | solution.py:58
  110.9 24.4 %collective-permute-start.43 = (bf16[16,64,256]{2,1,0:T(8,128)(2,1)}, bf16[16,64,256]{2,1,0:T(8,128)(2,1)S(1)}, u32[]{:S(2)}, u32[]{:S(2)}) collective-permute-start(bf16[16,64,256]{2,1,0:T(8,128)(2,1)} %pick.1), channel_id=1, source_target_pairs={{0,3},{1,0},{2,1},{3,2},{4,7},{5,4},{6,5},{7,6},{8,11},{9,8},{10,9... | collective-permute-start | bytes 1572872 | tf_op jit(solution)/shard_map/ppermute | solution.py:58
  120.4 22.9 %collective-permute-start.37 = (bf16[2,3,128,256]{3,2,1,0:T(8,128)(2,1)S(1)}, bf16[2,3,128,256]{3,2,1,0:T(8,128)(2,1)S(1)}, u32[]{:S(2)}, u32[]{:S(2)}) collective-permute-start(bf16[2,3,128,256]{3,2,1,0:T(8,128)(2,1)S(1)} %copy-done.17), channel_id=1, source_target_pairs={{0,16},{4,20},{8,24},{12,28},{16,32},{20,36},{24,40},{28,44},{32,4... | collective-permute-start | bytes 1179656 | tf_op jit(solution)/shard_map/ppermute | solution.py:62
  124.9 24.3 %collective-permute-start.24 = (bf16[2,3,128,256]{3,2,1,0:T(8,128)(2,1)}, bf16[2,3,128,256]{3,2,1,0:T(8,128)(2,1)S(1)}, u32[]{:S(2)}, u32[]{:S(2)}) collective-permute-start(bf16[2,3,128,256]{3,2,1,0:T(8,128)(2,1)} %get-tuple-element.22), channel_id=1, source_target_pairs={{0,8},{4,12},{8,16},{12,20},{16,24},{20,28},{24,32},{28,36},{32,40... | collective-permute-start | bytes 1179656 | tf_op jit(solution)/shard_map/ppermute | solution.py:62
  127.0 38.9 %collective-permute-start.44 = (bf16[16,64,256]{2,1,0:T(8,128)(2,1)S(1)}, bf16[16,64,256]{2,1,0:T(8,128)(2,1)S(1)}, u32[]{:S(2)}, u32[]{:S(2)}) collective-permute-start(bf16[16,64,256]{2,1,0:T(8,128)(2,1)S(1)} %collective-permute-done.41.refs_12_), channel_id=1, source_target_pairs={{0,4},{4,0},{8,12},{12,8},{16,20},{20,16},{24,28},{28,24},{32,36},... | collective-permute-start | bytes 1572872 | tf_op jit(solution)/shard_map/ppermute | solution.py:54
  133.9 32.1 %collective-permute-start.45 = (bf16[16,64,256]{2,1,0:T(8,128)(2,1)S(1)}, bf16[16,64,256]{2,1,0:T(8,128)(2,1)S(1)}, u32[]{:S(2)}, u32[]{:S(2)}) collective-permute-start(bf16[16,64,256]{2,1,0:T(8,128)(2,1)S(1)} %collective-permute-done.42.refs_13_), channel_id=1, source_target_pairs={{0,4},{4,0},{8,12},{12,8},{16,20},{20,16},{24,28},{28,24},{32,36},... | collective-permute-start | bytes 1572872 | tf_op jit(solution)/shard_map/ppermute | solution.py:54
  135.3 30.7 %collective-permute-start.46 = (bf16[16,64,256]{2,1,0:T(8,128)(2,1)S(1)}, bf16[16,64,256]{2,1,0:T(8,128)(2,1)S(1)}, u32[]{:S(2)}, u32[]{:S(2)}) collective-permute-start(bf16[16,64,256]{2,1,0:T(8,128)(2,1)S(1)} %collective-permute-done.43.refs_14_), channel_id=1, source_target_pairs={{0,4},{4,0},{8,12},{12,8},{16,20},{20,16},{24,28},{28,24},{32,36},... | collective-permute-start | bytes 1572872 | tf_op jit(solution)/shard_map/ppermute | solution.py:54
  (62 other events, 952.6 us)
